TPU v7x, 32 devices: a whole 2x2x4 slice. The times are simulated.
32 devices in a mesh: fs: 8 (over z, x), tp: 4 (over y, core).
Axes of the slice: x: 2, y: 2, z: 4, core: 2. Of those that a mesh axis runs over, the one named last changes fastest.
Arguments:
- tokens: bfloat16 [4096, 2048], P(('fs', 'tp')), may hold values from -6 to 6
- norm_gain: float32 [2048], P('fs'), may hold values from 0.1 to 1.9
- gate_proj: float32 [32, 2048, 512], P(None, 'fs', 'tp'), may hold values from -0.125 to 0.125
- up_proj: float32 [32, 2048, 512], P(None, 'fs', 'tp'), may hold values from -0.125 to 0.125
- down_proj: float32 [32, 512, 2048], P(None, 'fs', 'tp'), may hold values from -0.25 to 0.25
- expert_ids: int32 [4096, 2], P(('fs', 'tp')), may hold values from 0 to 31, as said below
- route_weight: float32 [4096, 2], P(('fs', 'tp')), may hold values from 0.05 to 1
Outputs:
- mixed: bfloat16 [4096, 2048], P(('fs', 'tp'))
- new_gate: bfloat16 [32, 2048, 512], P(('fs', 'tp'))
- new_up: bfloat16 [32, 2048, 512], P(('fs', 'tp'))
- new_down: bfloat16 [32, 512, 2048], P(('fs', 'tp'))
Inputs may be any that keep to these rules, and one draw needn't show every extreme that they name: `expert_ids`: the two experts of a row differ and lie in one group of 4 consecutive experts. In each aligned block of 128 rows (the rows of one device) every group is named by exactly 16 rows, no expert by more than 16 rows, and one expert, the same in all blocks, by exactly 16 rows.
All inputs are finite; a program needn't handle non-finite values.
Results may differ from a plain program's by a relative error of at most 0.0087.
Values may be sent and summed in bfloat16 or wider, within the bound.
No kernel may reach another device: no remote copies, remote signals or barrier semaphores. Data moves between devices by JAX's collectives and lax.ppermute only.
A program may use at most 128 MiB of HBM per device.

v0:
```python
import jax
import jax.numpy as jnp
from jax import lax
from jax.sharding import PartitionSpec as P

norm_eps = 1e-06


def shards(tokens, norm_gain, gate_proj, up_proj, down_proj, expert_ids, route_weight):
    row_scale = norm_gain[None, :, None]
    gate_low = (gate_proj * row_scale).astype(jnp.bfloat16)
    up_low = (up_proj * row_scale).astype(jnp.bfloat16)
    down_low = down_proj.astype(jnp.bfloat16)
    width_fs = lax.axis_size("fs")
    width_tp = lax.axis_size("tp")

    def expand(matrix):
        return matrix.reshape((matrix.shape[0], 1) + matrix.shape[1:])

    def assemble(pieces):
        row_count, col_count = (pieces.shape[2], pieces.shape[3])
        tiled = pieces.reshape(width_fs, width_tp, row_count, col_count).transpose(0, 2, 1, 3)
        return tiled.reshape(1, width_fs * row_count, width_tp * col_count)

    arrived = (
        lax.all_to_all(expand(gate_low), ("fs", "tp"), split_axis=0, concat_axis=1, tiled=True),
        lax.all_to_all(expand(up_low), ("fs", "tp"), split_axis=0, concat_axis=1, tiled=True),
        lax.all_to_all(expand(down_low), ("fs", "tp"), split_axis=0, concat_axis=1, tiled=True),
    )
    new_gate, new_up, new_down = (assemble(arrived[0]), assemble(arrived[1]), assemble(arrived[2]))
    tok_count, width = tokens.shape
    experts = gate_proj.shape[0]
    slot_cap = 4 * tok_count // experts
    widened = tokens.astype(jnp.float32)
    normed = (
        widened * lax.rsqrt(jnp.mean(widened * widened, axis=-1, keepdims=True) + norm_eps)
    ).astype(jnp.bfloat16)
    flat_ids = expert_ids.reshape(-1)
    onehot = (flat_ids[:, None] == jnp.arange(experts, dtype=jnp.int32)[None, :]).astype(jnp.int32)
    slot_rank = jnp.sum(jnp.cumsum(onehot, axis=0) * onehot, axis=1) - 1
    slot_index = flat_ids * slot_cap + slot_rank
    source = (
        jnp.zeros((experts * slot_cap,), jnp.int32)
        .at[slot_index]
        .set(jnp.arange(2 * tok_count, dtype=jnp.int32) // 2 + 1)
    )
    filled = source > 0
    outgoing = jnp.where(
        filled[:, None], normed[jnp.maximum(source - 1, 0)], jnp.zeros((), jnp.bfloat16)
    )
    outgoing = outgoing.reshape(experts, slot_cap, width)
    arrived_rows = lax.all_to_all(outgoing, ("fs", "tp"), split_axis=0, concat_axis=0, tiled=True)
    flat_rows = arrived_rows.reshape(-1, width)
    gate_act = jnp.dot(flat_rows, new_gate[0], preferred_element_type=jnp.float32)
    up_act = jnp.dot(flat_rows, new_up[0], preferred_element_type=jnp.float32)
    hidden = (jax.nn.silu(gate_act) * up_act).astype(jnp.bfloat16)
    results = jnp.dot(hidden, new_down[0], preferred_element_type=jnp.float32).astype(jnp.bfloat16)
    returned = lax.all_to_all(
        results.reshape(arrived_rows.shape), ("fs", "tp"), split_axis=0, concat_axis=0, tiled=True
    )
    picked = returned.reshape(experts * slot_cap, width)[slot_index].reshape(tok_count, 2, width)
    mixed = jnp.sum(route_weight[:, :, None] * picked.astype(jnp.float32), axis=1).astype(
        jnp.bfloat16
    )
    return (mixed, new_gate, new_up, new_down)


def solution(mesh):
    in_specs = (
        P(("fs", "tp"), None),
        P("fs"),
        P(None, "fs", "tp"),
        P(None, "fs", "tp"),
        P(None, "fs", "tp"),
        P(("fs", "tp"), None),
        P(("fs", "tp"), None),
    )
    out_specs = (
        P(("fs", "tp"), None),
        P(("fs", "tp"), None, None),
        P(("fs", "tp"), None, None),
        P(("fs", "tp"), None, None),
    )
    return jax.shard_map(shards, mesh=mesh, in_specs=in_specs, out_specs=out_specs, check_vma=False)
```

profile of v0, /device:TPU:0, one launch (start us, length us, event | category | flops | bytes accessed | tf_op | source)
XLA Modules:
  0.0 289.6 jit_solution(2449153422553158705)
XLA Ops:
  0.6 6.0 %fusion = (bf16[32,1,256,128]{3,2,1,0:T(8,128)(2,1)S(1)}, bf16[32,1,256,128]{3,2,1,0:T(8,128)(2,1)}) fusion(f32[32,256,128]{2,1,0:T(8,128)} %param.9, f32[256]{0:T(256)} %param.8, f32[32,256,128]{2,1,0:T(8,128)} %param.10), kind=kLoop, calls=%fused_computation.6 | loop fusion | flops 4194304 | bytes 12583936 | tf_op jit(solution)/shard_map/reshape | solution.py:18
  6.6 55.9 %all_to_all.37 = bf16[32,1,256,128]{3,2,1,0:T(8,128)(2,1)} all-to-all(bf16[32,1,256,128]{3,2,1,0:T(8,128)(2,1)S(1)} %get-tuple-element.6), channel_id=1, replica_groups=mesh['fs'=8,'tp'=4] {'fs','tp'}, dimensions={0} | all-to-all | bytes 4194304 | tf_op jit(solution)/shard_map/all_to_all | solution.py:26
  62.5 3.7 %all-to-all-start.2 = ((bf16[32,1,256,128]{3,2,1,0:T(8,128)(2,1)}), bf16[32,1,256,128]{3,2,1,0:T(8,128)(2,1)S(1)}, u32[]{:S(2)}, u32[]{:S(2)}) async-start(bf16[32,1,256,128]{3,2,1,0:T(8,128)(2,1)} %get-tuple-element.7), calls=%async_computation.2 | async-start | bytes 4194304 | tf_op jit(solution)/shard_map/all_to_all | solution.py:27
  66.2 3.8 %convert_bitcast_fusion = bf16[32,1,64,512]{3,2,1,0:T(8,128)(2,1)} fusion(f32[32,64,512]{2,1,0:T(8,128)} %param.11), kind=kLoop, calls=%fused_computation.9 | loop fusion | flops 1048576 | bytes 6291456 | tf_op jit(solution)/shard_map/reshape | solution.py:18
  70.0 44.9 %all-to-all-done.2 = bf16[32,1,256,128]{3,2,1,0:T(8,128)(2,1)S(1)} async-done(((bf16[32,1,256,128]{3,2,1,0:T(8,128)(2,1)}), bf16[32,1,256,128]{3,2,1,0:T(8,128)(2,1)S(1)}, u32[]{:S(2)}, u32[]{:S(2)}) %all-to-all-start.2) | async-done | bytes 2097184 | tf_op jit(solution)/shard_map/all_to_all | solution.py:27
  114.9 4.1 %all-to-all-start.3 = ((bf16[32,1,64,512]{3,2,1,0:T(8,128)(2,1)}), bf16[32,1,64,512]{3,2,1,0:T(8,128)(2,1)}, u32[]{:S(2)}, u32[]{:S(2)}) async-start(bf16[32,1,64,512]{3,2,1,0:T(8,128)(2,1)} %convert_bitcast_fusion), calls=%async_computation.3 | async-start | bytes 4194304 | tf_op jit(solution)/shard_map/all_to_all | solution.py:28
  119.5 0.6 reduce-window.6
  120.7 1.4 scatter_custom_fusion
  122.6 3.3 %gather_fusion = bf16[512,2048]{1,0:T(8,128)(2,1)} fusion(bf16[128,2048]{1,0:T(8,128)(2,1)S(1)} %fusion.4, s32[1024]{0:T(1024)S(1)} %pad_clamp_fusion.1), kind=kCustom, calls=%fused_computation | custom fusion | bytes 4196352 | tf_op jit(solution)/shard_map/gather | solution.py:49
  125.9 3.1 %broadcast_select_fusion = bf16[32,16,2048]{2,1,0:T(8,128)(2,1)} fusion(bf16[32,16,2048]{2,1,0:T(8,128)(2,1)} %bitcast.66, pred[32,16]{1,0:T(8,128)(4,1)S(1)} %broadcast_in_dim.24), kind=kLoop, calls=%fused_computation.10 | loop fusion | flops 1048576 | bytes 4194816 | tf_op jit(solution)/shard_map/jit(_where)/select_n | solution.py:48
  129.0 38.8 %all-to-all-done.3 = bf16[32,1,64,512]{3,2,1,0:T(8,128)(2,1)} async-done(((bf16[32,1,64,512]{3,2,1,0:T(8,128)(2,1)}), bf16[32,1,64,512]{3,2,1,0:T(8,128)(2,1)}, u32[]{:S(2)}, u32[]{:S(2)}) %all-to-all-start.3) | async-done | bytes 2097184 | tf_op jit(solution)/shard_map/all_to_all | solution.py:28
  167.7 4.3 %all-to-all-start = ((bf16[32,16,2048]{2,1,0:T(8,128)(2,1)}), bf16[32,16,2048]{2,1,0:T(8,128)(2,1)}, u32[]{:S(2)}, u32[]{:S(2)}) async-start(bf16[32,16,2048]{2,1,0:T(8,128)(2,1)} %broadcast_select_fusion), calls=%async_computation | async-start | bytes 4194304 | tf_op jit(solution)/shard_map/all_to_all | solution.py:52
  172.1 4.5 %copy.37 = bf16[8,4,256,128]{2,0,3,1:T(8,128)(2,1)} copy(bf16[8,4,256,128]{3,2,1,0:T(8,128)(2,1)} %bitcast.62) | data formatting | bytes 4194304 | tf_op jit(solution)/shard_map/reshape | solution.py:22
  176.6 3.7 %copy.46 = bf16[64,8,8,256]{3,1,2,0:T(8,128)(2,1)} copy(bf16[64,8,8,256]{3,2,1,0:T(8,128)(2,1)} %bitcast.67) | data formatting | bytes 4194304
  180.2 2.9 copy.39
  183.1 3.6 %copy.47 = bf16[64,8,8,256]{3,1,2,0:T(8,128)(2,1)} copy(bf16[64,8,8,256]{3,2,1,0:T(8,128)(2,1)} %bitcast.68) | data formatting | bytes 4194304
  186.7 3.2 %copy.52 = bf16[8,4,64,512]{3,1,2,0:T(4,128)(2,1)S(1)} copy(bf16[8,4,64,512]{3,2,1,0:T(8,128)(2,1)} %bitcast.13) | data formatting | bytes 4194304 | tf_op jit(solution)/shard_map/reshape | solution.py:22
  190.0 1.3 copy-done.1
  191.3 2.0 copy.48
  193.2 27.3 %all-to-all-done = bf16[32,16,2048]{2,1,0:T(8,128)(2,1)} async-done(((bf16[32,16,2048]{2,1,0:T(8,128)(2,1)}), bf16[32,16,2048]{2,1,0:T(8,128)(2,1)}, u32[]{:S(2)}, u32[]{:S(2)}) %all-to-all-start) | async-done | bytes 2097184 | tf_op jit(solution)/shard_map/all_to_all | solution.py:52
  220.6 2.9 fusion.13
  223.5 6.7 %convolution_convert_fusion = bf16[512,2048]{1,0:T(8,128)(2,1)} fusion(bf16[512,2048]{1,0:T(8,128)(2,1)} %bitcast.72, bf16[512,2048]{1,0:T(8,128)(2,1)} %bitcast.4, bf16[2048,512]{0,1:T(8,128)(2,1)} %bitcast.71, f32[512,512]{1,0:T(8,128)S(1)} %fusion.13), kind=kOutput, calls=%fused_computation.5 | convolution fusion | flops 2150105088 | bytes 9437184 | tf_op jit(solution)/shard_map/dot_general | solution.py:57
  230.2 4.2 %all-to-all-start.4 = ((bf16[32,16,2048]{2,1,0:T(8,128)(2,1)}), bf16[32,16,2048]{2,1,0:T(8,128)(2,1)S(1)}, u32[]{:S(2)}, u32[]{:S(2)}) async-start(bf16[32,16,2048]{2,1,0:T(8,128)(2,1)} %bitcast.69), calls=%async_computation.4 | async-start | bytes 4194304 | tf_op jit(solution)/shard_map/all_to_all | solution.py:58
  234.6 4.5 %copy.41 = bf16[8,256,4,128]{3,2,1,0:T(4,128)(2,1)} copy(bf16[8,256,4,128]{3,1,2,0:T(8,128)(2,1)} %bitcast.63) | data formatting | bytes 4194304 | tf_op jit(solution)/shard_map/transpose | solution.py:22
  239.1 4.1 %reshape.138 = bf16[1,2048,512]{2,1,0:T(8,128)(2,1)} reshape(bf16[8,256,4,128]{3,2,1,0:T(4,128)(2,1)} %copy.41) | data formatting | bytes 4194304 | tf_op jit(solution)/shard_map/reshape | solution.py:23
  243.2 4.5 %copy.42 = bf16[8,256,4,128]{3,2,1,0:T(4,128)(2,1)} copy(bf16[8,256,4,128]{3,1,2,0:T(8,128)(2,1)} %bitcast.61) | data formatting | bytes 4194304 | tf_op jit(solution)/shard_map/transpose | solution.py:22
  247.7 4.1 %reshape.139 = bf16[1,2048,512]{2,1,0:T(8,128)(2,1)} reshape(bf16[8,256,4,128]{3,2,1,0:T(4,128)(2,1)} %copy.42) | data formatting | bytes 4194304 | tf_op jit(solution)/shard_map/reshape | solution.py:23
  251.8 4.4 %reshape.140 = bf16[1,512,2048]{2,1,0:T(8,128)(2,1)} reshape(bf16[8,64,4,512]{3,2,1,0:T(4,128)(2,1)} %bitcast.65) | data formatting | bytes 4194304 | tf_op jit(solution)/shard_map/reshape | solution.py:23
  256.3 26.6 %all-to-all-done.4 = bf16[32,16,2048]{2,1,0:T(8,128)(2,1)S(1)} async-done(((bf16[32,16,2048]{2,1,0:T(8,128)(2,1)}), bf16[32,16,2048]{2,1,0:T(8,128)(2,1)S(1)}, u32[]{:S(2)}, u32[]{:S(2)}) %all-to-all-start.4) | async-done | bytes 2097184 | tf_op jit(solution)/shard_map/all_to_all | solution.py:58
  282.9 1.4 gather_fusion.1
  284.3 1.3 reshape.141
  285.6 3.9 %multiply_reduce_fusion = bf16[128,2048]{1,0:T(8,128)(2,1)} fusion(f32[128,2,2048]{2,1,0:T(2,128)S(1)} %reshape.141, f32[128,2]{1,0:T(8,128)S(1)} %copy.32), kind=kLoop, calls=%fused_computation.8 | loop fusion | flops 786432 | bytes 2622464 | tf_op jit(solution)/shard_map/reduce_sum | solution.py:62
  (34 shorter events, 1.6 us)
Async XLA Ops:
  62.5 52.4 %all-to-all-start.2 = ((bf16[32,1,256,128]{3,2,1,0:T(8,128)(2,1)}), bf16[32,1,256,128]{3,2,1,0:T(8,128)(2,1)S(1)}, u32[]{:S(2)}, u32[]{:S(2)}) async-start(bf16[32,1,256,128]{3,2,1,0:T(8,128)(2,1)} %get-tuple-element.7), calls=%async_computation.2 | async-start | bytes 4194304 | tf_op jit(solution)/shard_map/all_to_all | solution.py:27
  70.0 49.1 %copy-start.4 = (s32[128,2]{0,1:T(2,128)S(1)}, s32[128,2]{0,1:T(2,128)}, u32[]{:S(2)}) copy-start(s32[128,2]{0,1:T(2,128)} %param.12) | copy-start | bytes 3076
  70.0 52.2 %copy-start.3 = (bf16[128,2048]{1,0:T(8,128)(2,1)S(1)}, bf16[128,2048]{1,0:T(8,128)(2,1)}, u32[]{:S(2)}) copy-start(bf16[128,2048]{1,0:T(8,128)(2,1)} %param.7) | copy-start | bytes 1572868
  114.9 65.4 %copy-start = (bf16[32,1,256,128]{3,2,1,0:T(8,128)(2,1)}, bf16[32,1,256,128]{3,2,1,0:T(8,128)(2,1)S(1)}, u32[]{:S(2)}) copy-start(bf16[32,1,256,128]{3,2,1,0:T(8,128)(2,1)S(1)} %all-to-all-done.2) | copy-start | bytes 6291460
  114.9 52.8 %all-to-all-start.3 = ((bf16[32,1,64,512]{3,2,1,0:T(8,128)(2,1)}), bf16[32,1,64,512]{3,2,1,0:T(8,128)(2,1)}, u32[]{:S(2)}, u32[]{:S(2)}) async-start(bf16[32,1,64,512]{3,2,1,0:T(8,128)(2,1)} %convert_bitcast_fusion), calls=%async_computation.3 | async-start | bytes 4194304 | tf_op jit(solution)/shard_map/all_to_all | solution.py:28
  167.7 52.8 %all-to-all-start = ((bf16[32,16,2048]{2,1,0:T(8,128)(2,1)}), bf16[32,16,2048]{2,1,0:T(8,128)(2,1)}, u32[]{:S(2)}, u32[]{:S(2)}) async-start(bf16[32,16,2048]{2,1,0:T(8,128)(2,1)} %broadcast_select_fusion), calls=%async_computation | async-start | bytes 4194304 | tf_op jit(solution)/shard_map/all_to_all | solution.py:52
  189.9 1.3 copy-start.1
  191.3 29.3 %copy-start.2 = (bf16[64,8,8,256]{3,1,2,0:T(8,128)(2,1)S(1)}, bf16[64,8,8,256]{3,1,2,0:T(8,128)(2,1)}, u32[]{:S(2)}) copy-start(bf16[64,8,8,256]{3,1,2,0:T(8,128)(2,1)} %copy.46) | copy-start | bytes 6291460
  230.2 4.3 %copy-start.5 = (f32[128,2]{0,1:T(2,128)S(1)}, f32[128,2]{0,1:T(2,128)}, u32[]{:S(2)}) copy-start(f32[128,2]{0,1:T(2,128)} %param.13) | copy-start | bytes 3076
  230.2 52.7 %all-to-all-start.4 = ((bf16[32,16,2048]{2,1,0:T(8,128)(2,1)}), bf16[32,16,2048]{2,1,0:T(8,128)(2,1)S(1)}, u32[]{:S(2)}, u32[]{:S(2)}) async-start(bf16[32,16,2048]{2,1,0:T(8,128)(2,1)} %bitcast.69), calls=%async_computation.4 | async-start | bytes 4194304 | tf_op jit(solution)/shard_map/all_to_all | solution.py:58
where the time goes:
time: 291 us; the launch traced here: 290 us
  waiting for transfers between devices  138 us (47%)
  blocking collectives  55.9 us (19%)
  local copies, waits for them, and re-layouts  51.3 us (18%)
  other arithmetic  18 us (6%)
  starting transfers between devices  16.4 us (6%)
  matrix products  9.6 us (3%)
    all_to_all x1, blocking collectives, shards(): lax.all_to_all(expand(gate_low), ('fs', 'tp'), split_axis=0, concat_axis=...  55.9 us
    all_to_all x1, waiting for transfers between devices, shards(): lax.all_to_all(expand(up_low), ('fs', 'tp'), split_axis=0, concat_axis=1,...  44.9 us
    all_to_all x1, waiting for transfers between devices, shards(): lax.all_to_all(expand(down_low), ('fs', 'tp'), split_axis=0, concat_axis=...  38.8 us
    all_to_all x1, waiting for transfers between devices, shards(): lax.all_to_all(outgoing, ('fs', 'tp'), split_axis=0, concat_axis=0, tiled...  27.3 us
    all_to_all x1, waiting for transfers between devices, shards(): lax.all_to_all(results.reshape(arrived_rows.shape), ('fs', 'tp'), split_a...  26.6 us
    reshape x3, local copies, waits for them, and re-layouts, assemble(): return tiled.reshape(1, width_fs * row_count, width_tp * col_count)  12.6 us
    unnamed x17, local copies, waits for them, and re-layouts  10.8 us
    reshape x3, local copies, waits for them, and re-layouts, assemble(): pieces.reshape(width_fs, width_tp, row_count, col_count)  10.6 us
  transfers between devices with their start and end apart: 4, of which 4 were waited for; matrix products, arithmetic and copies ran while one was open for 19% of the time, Pallas kernels for 0%

commit v1 on v0

v1 whole, which is shorter than its diff:
```python
import functools

import jax
import jax.numpy as jnp
from jax import lax
from jax.experimental import pallas as pl
from jax.experimental.pallas import tpu as pltpu
from jax.sharding import PartitionSpec as P


norm_eps = 1e-06
lanes = 128
bf16 = jnp.bfloat16
f32 = jnp.float32
grant = 24 * 1024 * 1024


def cost(flops, nbytes):
    return pl.CostEstimate(flops=int(flops), bytes_accessed=int(nbytes), transcendentals=0)


def params():
    return pltpu.CompilerParams(vmem_limit_bytes=grant)


def whole(shape):
    return pl.BlockSpec(shape, lambda *_: (0,) * len(shape))


def square(n):
    return lax.broadcasted_iota(jnp.int32, (n, n), 0), lax.broadcasted_iota(jnp.int32, (n, n), 1)


def to_col(row):
    n = row.shape[1]
    down, across = square(n)
    return jnp.sum(jnp.where(down == across, row, jnp.zeros((), row.dtype)), axis=1, keepdims=True)


def slot_onehot(group_row, per_group):
    down, across = square(group_row.shape[1])
    group_col = to_col(group_row)
    earlier = jnp.where((group_col == group_row) & (across < down), 1.0, 0.0)
    rank = jnp.sum(earlier, axis=1, keepdims=True)
    slot = (group_col * float(per_group) + rank).astype(jnp.int32)
    return jnp.where(slot == across, 1.0, 0.0).astype(bf16)


def group_of(ids, fs, tp):
    group = jnp.zeros(ids.shape, f32)
    for bound in range(1, fs):
        group = group + jnp.where(ids >= bound * tp, 1.0, 0.0)
    return group


def prep_kernel(fs, tp, tok_ref, ids_ref, weight_ref, out_ref):
    count, width = tok_ref.shape
    group = group_of(ids_ref[0:1, :], fs, tp)
    onehot = slot_onehot(group, count // fs)
    wide = tok_ref[...].astype(f32)
    scale = lax.rsqrt(jnp.mean(wide * wide, axis=-1, keepdims=True) + norm_eps)
    normed = (wide * scale).astype(bf16)
    lane = lax.broadcasted_iota(jnp.int32, (count, lanes), 1)
    extra = jnp.zeros((count, lanes), f32)
    for pick in range(2):
        local = ids_ref[pick : pick + 1, :].astype(f32) - group * float(tp)
        local = to_col(local).astype(jnp.int32)
        rest = to_col(weight_ref[pick : pick + 1, :])
        for part in range(3):
            piece = rest.astype(bf16).astype(f32)
            extra = extra + jnp.where(lane == local + part * tp, piece, 0.0)
            rest = rest - piece
    dims = (((0,), (0,)), ((), ()))
    out_ref[:, :width] = lax.dot_general(onehot, normed, dims, preferred_element_type=f32).astype(bf16)
    out_ref[:, width:] = lax.dot_general(
        onehot, extra.astype(bf16), dims, preferred_element_type=f32
    ).astype(bf16)


def cast_kernel(steps, scaled, squeeze, me_ref, in_ref, *refs):
    step = pl.program_id(0)
    value = in_ref[:, 0] if squeeze else in_ref[0]
    if scaled:
        value = value * to_col(refs[0][...])[None]
        refs = refs[1:]
    value = value.astype(bf16)
    for r in range(steps):

        @pl.when(step == r)
        def _(r=r):
            refs[r][...] = value


def cast_along(me, matrix, scale, axis):
    fs, tp, rows, cols = matrix.shape
    steps = (fs, tp)[axis]
    if axis == 0:
        in_spec = pl.BlockSpec((1, tp, rows, cols), lambda r, m: (lax.rem(m[0] + r, fs), 0, 0, 0))
        shape = (tp, rows, cols)
    else:
        in_spec = pl.BlockSpec((fs, 1, rows, cols), lambda r, m: (0, lax.rem(m[1] + r, tp), 0, 0))
        shape = (fs, rows, cols)
    in_specs, args = [in_spec], [matrix]
    if scale is not None:
        in_specs.append(whole(scale.shape))
        args.append(scale)
    return pl.pallas_call(
        functools.partial(cast_kernel, steps, scale is not None, axis == 1),
        grid_spec=pltpu.PrefetchScalarGridSpec(
            num_scalar_prefetch=1, grid=(steps,), in_specs=in_specs, out_specs=[whole(shape)] * steps
        ),
        out_shape=[jax.ShapeDtypeStruct(shape, bf16)] * steps,
        compiler_params=params(),
        cost_estimate=cost(1e9, 6 * matrix.size),
    )(me, *args)


def in_order(me_ref, tp, action):
    for value in range(tp):

        @pl.when(me_ref[1] == value)
        def _(value=value):
            action([(value - j) % tp for j in range(tp)])


def merge_kernel(tp, me_ref, *refs):
    out_ref = refs[tp]

    def store(order):
        out_ref[0] = jnp.concatenate([refs[q][0] for q in order], axis=-1)

    in_order(me_ref, tp, store)


def merge(me, parts):
    tp = len(parts)
    fs, rows, cols = parts[0].shape
    return pl.pallas_call(
        functools.partial(merge_kernel, tp),
        grid_spec=pltpu.PrefetchScalarGridSpec(
            num_scalar_prefetch=1,
            grid=(fs,),
            in_specs=[pl.BlockSpec((1, rows, cols), lambda g, m: (g, 0, 0))] * tp,
            out_specs=pl.BlockSpec((1, rows, tp * cols), lambda g, m: (g, 0, 0)),
        ),
        out_shape=jax.ShapeDtypeStruct((fs, rows, tp * cols), bf16),
        compiler_params=params(),
        cost_estimate=cost(1e9, 4 * tp * parts[0].size),
    )(me, *parts)


def merge_down_kernel(fs, tp, first, me_ref, *refs):
    ins, outs = refs[:tp], refs[tp:]

    def store(order):
        for r in range(fs):
            group = lax.rem(me_ref[0] + r, fs)
            full = jnp.concatenate([ins[q][group] for q in order], axis=-1)
            outs[r][...] = full[:, :first]
            outs[fs][group] = full[:, first:]

    in_order(me_ref, tp, store)


def merge_down(me, parts, first):
    tp = len(parts)
    fs, rows, cols = parts[0].shape
    shapes = [(rows, first)] * fs + [(fs, rows, tp * cols - first)]
    outs = pl.pallas_call(
        functools.partial(merge_down_kernel, fs, tp, first),
        grid_spec=pltpu.PrefetchScalarGridSpec(
            num_scalar_prefetch=1,
            grid=(1,),
            in_specs=[whole(parts[0].shape)] * tp,
            out_specs=[whole(shape) for shape in shapes],
        ),
        out_shape=[jax.ShapeDtypeStruct(shape, bf16) for shape in shapes],
        compiler_params=params(),
        cost_estimate=cost(1e9, 4 * tp * parts[0].size),
    )(me, *parts)
    return outs[:fs], outs[fs]


def regroup_kernel(fs, tp, me_ref, *refs):
    for q in range(tp):
        target = lax.rem(me_ref[1] + q, tp)
        for r in range(fs):
            refs[fs + q][r] = refs[r][target]


def regroup(me, parts):
    fs = len(parts)
    tp, rows, cols = parts[0].shape
    shape = (fs, rows, cols)
    return pl.pallas_call(
        functools.partial(regroup_kernel, fs, tp),
        grid_spec=pltpu.PrefetchScalarGridSpec(
            num_scalar_prefetch=1,
            grid=(1,),
            in_specs=[whole(parts[0].shape)] * fs,
            out_specs=[whole(shape)] * tp,
        ),
        out_shape=[jax.ShapeDtypeStruct(shape, bf16)] * tp,
        compiler_params=params(),
        cost_estimate=cost(1e9, 4 * fs * parts[0].size),
    )(me, *parts)


def product_of(x_refs, matrix_ref, rows_ref):
    width = matrix_ref.shape[0]
    count = x_refs[0].shape[0]
    for q, ref in enumerate(x_refs):
        rows_ref[q * count : (q + 1) * count, :] = ref[:, :width]
    return jnp.dot(rows_ref[...], matrix_ref[...], preferred_element_type=f32)


def gate_kernel(fs, tp, me_ref, *refs):
    x_refs, parts, (matrix_ref, out_ref, rows_ref) = refs[:tp], refs[tp : 2 * tp], refs[2 * tp :]
    height = parts[0].shape[1]

    def store(order):
        for r in range(fs):
            origin = lax.rem(me_ref[0] - r + fs, fs)
            matrix_ref[pl.ds(pl.multiple_of(origin * height, height), height), :] = jnp.concatenate(
                [parts[q][r] for q in order], axis=-1
            )

    in_order(me_ref, tp, store)
    out_ref[...] = product_of(x_refs, matrix_ref, rows_ref)


def gate_rows(me, rows, parts):
    tp = len(parts)
    fs, height, cols = parts[0].shape
    matrix = (fs * height, tp * cols)
    out = (tp * rows[0].shape[0], tp * cols)
    return pl.pallas_call(
        functools.partial(gate_kernel, fs, tp),
        grid_spec=pltpu.PrefetchScalarGridSpec(
            num_scalar_prefetch=1,
            grid=(1,),
            in_specs=[whole(rows[0].shape)] * tp + [whole(parts[0].shape)] * tp,
            out_specs=[whole(matrix), whole(out)],
            scratch_shapes=[pltpu.VMEM((out[0], matrix[0]), bf16)],
        ),
        out_shape=[jax.ShapeDtypeStruct(matrix, bf16), jax.ShapeDtypeStruct(out, f32)],
        compiler_params=params(),
        cost_estimate=cost(2 * out[0] * matrix[0] * matrix[1], 4 * matrix[0] * matrix[1]),
    )(me, *rows, *parts)


def up_kernel(tp, *refs):
    x_refs, (matrix_ref, gate_ref, out_ref, rows_ref) = refs[:tp], refs[tp:]
    up = product_of(x_refs, matrix_ref, rows_ref)
    gate = gate_ref[...]
    out_ref[...] = (gate / (1.0 + jnp.exp(-gate)) * up).astype(bf16)


def up_rows(rows, matrix, gate):
    tp = len(rows)
    return pl.pallas_call(
        functools.partial(up_kernel, tp),
        grid=(1,),
        in_specs=[whole(rows[0].shape)] * tp + [whole(matrix.shape), whole(gate.shape)],
        out_specs=whole(gate.shape),
        scratch_shapes=[pltpu.VMEM((gate.shape[0], matrix.shape[0]), bf16)],
        out_shape=jax.ShapeDtypeStruct(gate.shape, bf16),
        compiler_params=params(),
        cost_estimate=cost(2 * gate.size * matrix.shape[0], 2 * matrix.size),
    )(*rows, matrix, gate)


def down_kernel(fs, tp, parts_count, aliased, me_ref, hidden_ref, *refs):
    w_refs, refs = refs[:tp], refs[tp:]
    parts, refs = refs[:parts_count], refs[parts_count:]
    if aliased:
        refs = refs[1:]
    matrix_ref, outs = refs[0], refs[1:]
    if parts_count == 1:
        matrix_ref[...] = parts[0][...]
    else:
        rows = parts[0].shape[0]
        for r in range(fs):
            origin = lax.rem(me_ref[0] - r + fs, fs)
            matrix_ref[pl.ds(pl.multiple_of(origin * rows, rows), rows), :] = parts[r][...]
    product = jnp.dot(hidden_ref[...], matrix_ref[...], preferred_element_type=f32)
    product = product.astype(bf16).astype(f32)
    count = w_refs[0].shape[0]
    lane = lax.broadcasted_iota(jnp.int32, (count, lanes), 1)
    mine = me_ref[1]
    chosen = (lane == mine) | (lane == mine + tp) | (lane == mine + 2 * tp)
    for q in range(tp):
        weight = jnp.sum(
            jnp.where(chosen, w_refs[q][...].astype(f32), 0.0), axis=1, keepdims=True
        )
        outs[q][...] = (product[q * count : (q + 1) * count] * weight).astype(bf16)


def down_rows(me, fs, hidden, rows, parts, low, width, prior):
    tp = len(rows)
    count = rows[0].shape[0]
    depth = hidden.shape[1]
    size = parts[0].shape[1]
    col_block = low // size
    weight_block = width // lanes
    in_specs = [whole(hidden.shape)]
    in_specs += [pl.BlockSpec((count, lanes), lambda k, m: (0, weight_block))] * tp
    in_specs += [whole(part.shape) for part in parts]
    args = [hidden, *rows, *parts]
    aliases = {}
    if prior is not None:
        in_specs.append(pl.BlockSpec(memory_space=pl.ANY))
        args.append(prior)
        aliases = {len(args): 0}
    outs = pl.pallas_call(
        functools.partial(down_kernel, fs, tp, len(parts), prior is not None),
        grid_spec=pltpu.PrefetchScalarGridSpec(
            num_scalar_prefetch=1,
            grid=(1,),
            in_specs=in_specs,
            out_specs=[pl.BlockSpec((depth, size), lambda k, m: (0, col_block))]
            + [whole((count, size))] * tp,
        ),
        out_shape=[jax.ShapeDtypeStruct((depth, width), bf16)]
        + [jax.ShapeDtypeStruct((count, size), bf16)] * tp,
        input_output_aliases=aliases,
        compiler_params=params(),
        cost_estimate=cost(2 * tp * count * depth * size, 4 * depth * size),
    )(me, *args)
    return outs[0], outs[1:]


def final_kernel(fs, tp, ids_ref, *refs):
    out_ref = refs[-1]
    onehot = slot_onehot(group_of(ids_ref[0:1, :], fs, tp), ids_ref.shape[1] // fs)
    low = 0
    for ref in refs[:-1]:
        high = low + ref.shape[1]
        out_ref[:, low:high] = jnp.dot(onehot, ref[...], preferred_element_type=f32).astype(bf16)
        low = high


def shards(tokens, norm_gain, gate_proj, up_proj, down_proj, expert_ids, route_weight):
    fs = lax.axis_size("fs")
    tp = lax.axis_size("tp")
    me = jnp.stack([lax.axis_index("fs"), lax.axis_index("tp")]).astype(jnp.int32)
    count, width = tokens.shape
    per_group = count // fs
    first = width // 2

    def shift(n, step):
        return [(k, (k + step) % n) for k in range(n)]

    def rotate(parts, axis, back=False):
        n = len(parts)
        return [parts[0]] + [
            lax.ppermute(parts[r], axis, shift(n, n - r if back else r)) for r in range(1, n)
        ]

    def swap_fs(value):
        return lax.all_to_all(value, "fs", 0, 0, tiled=True)

    def by_expert(matrix):
        return matrix.reshape((fs, tp) + matrix.shape[1:])

    ids, weights = expert_ids.T, route_weight.T
    scale = norm_gain[None, :]

    sorted_rows = pl.pallas_call(
        functools.partial(prep_kernel, fs, tp),
        out_shape=jax.ShapeDtypeStruct((count, width + lanes), bf16),
        compiler_params=params(),
        cost_estimate=cost(2 * count * count * width, 4 * count * width),
    )(tokens, ids, weights)
    landed = swap_fs(sorted_rows.reshape(fs, per_group, width + lanes))
    landed = landed.reshape(count, width + lanes)
    gate_parts = cast_along(me, by_expert(gate_proj), scale, 0)
    gate_parts = rotate(gate_parts, "fs")
    up_parts = cast_along(me, by_expert(up_proj), scale, 1)
    up_parts = rotate(up_parts, "tp")
    rows = rotate([landed] * tp, "tp")
    up_here = merge(me, up_parts)
    new_up = swap_fs(up_here)
    new_up = new_up.reshape(-1, new_up.shape[2])
    down_parts = cast_along(me, by_expert(down_proj), None, 1)
    down_parts = rotate(down_parts, "tp")
    gate_parts = regroup(me, gate_parts)
    gate_parts = rotate(gate_parts, "tp")
    down_first, down_last = merge_down(me, down_parts, first)
    down_first = rotate(down_first, "fs")
    new_gate, gate = gate_rows(me, rows, gate_parts)
    down_last = swap_fs(down_last)
    down_last = down_last.reshape(-1, down_last.shape[2])
    hidden = up_rows(rows, new_up, gate)

    def add(parts):
        return sum(part.astype(f32) for part in parts).astype(bf16)

    def back_fs(value):
        return swap_fs(value.reshape(fs, per_group, -1)).reshape(count, -1)

    new_down, partial = down_rows(me, fs, hidden, rows, down_first, 0, width, None)
    partial = rotate(partial, "tp", back=True)
    back_first = back_fs(add(partial))
    new_down, partial = down_rows(me, fs, hidden, rows, [down_last], first, width, new_down)
    partial = rotate(partial, "tp", back=True)
    back_last = back_fs(add(partial))
    mixed = pl.pallas_call(
        functools.partial(final_kernel, fs, tp),
        out_shape=jax.ShapeDtypeStruct((count, width), bf16),
        compiler_params=params(),
        cost_estimate=cost(2 * count * count * width, 4 * count * width),
    )(ids, back_first, back_last)
    return (mixed, new_gate[None], new_up[None], new_down[None])


def solution(mesh):
    in_specs = (
        P(("fs", "tp"), None),
        P("fs"),
        P(None, "fs", "tp"),
        P(None, "fs", "tp"),
        P(None, "fs", "tp"),
        P(("fs", "tp"), None),
        P(("fs", "tp"), None),
    )
    out_specs = (
        P(("fs", "tp"), None),
        P(("fs", "tp"), None, None),
        P(("fs", "tp"), None, None),
        P(("fs", "tp"), None, None),
    )

    return jax.shard_map(shards, mesh=mesh, in_specs=in_specs, out_specs=out_specs, check_vma=False)
```

time: 291 us -> 271 us (0.931)
  starting transfers between devices: 16.4 us -> 98.5 us
  blocking collectives: 55.9 us -> 0 us
  local copies, waits for them, and re-layouts: 51.3 us -> 20.2 us
  Pallas kernels: 0 us -> 22.5 us
  other arithmetic: 18 us -> 3.88 us
  waiting for transfers between devices: 138 us -> 124 us
  matrix products: 9.6 us -> 0 us
    all_to_all x4 -> x5, waiting for transfers between devices: 138 us -> 17.2 us  [swap_fs(): return lax.all_to_all(value, 'fs', 0, 0, tiled=True)]
    ppermute x0 -> x32, waiting for transfers between devices: none -> 107 us  [rotate(): lax.ppermute(parts[r], axis, shift(n, n - r if back else r))]
    ppermute x0 -> x32, starting transfers between devices: none -> 66.8 us  [rotate(): lax.ppermute(parts[r], axis, shift(n, n - r if back else r))]
    all_to_all x1 -> x0, blocking collectives: 55.9 us -> none  [shards(): lax.all_to_all(expand(gate_low), ('fs', 'tp'), split_axis=0, concat_axis=...]
    reshape x6 -> x0, local copies, waits for them, and re-layouts: 23.3 us -> none  [the longest x3 12.6 us: assemble(): return tiled.reshape(1, width_fs * row_count, width_tp * col_count)]
    pallas_call x0 -> x12, Pallas kernels: none -> 22.5 us  [the longest x3 6.15 us: cast_along(): pl.pallas_call(functools.partial(cast_kernel, steps, scale is not None, a...]
    all_to_all x4 -> x5, starting transfers between devices: 16.4 us -> 31.7 us  [swap_fs(): return lax.all_to_all(value, 'fs', 0, 0, tiled=True)]
    reshape x2 -> x0, other arithmetic: 9.79 us -> none  [expand(): return matrix.reshape((matrix.shape[0], 1) + matrix.shape[1:])]
  transfers between devices with their start and end apart: 4 -> 37, of which waited for: 4 -> 12; matrix products, arithmetic and copies ran while one was open for 19% -> 1% of each run, Pallas kernels for 0% -> 7%
where the time goes in v1:
time: 271 us; the launch traced here: 270 us
  waiting for transfers between devices  124 us (46%)
  starting transfers between devices  98.5 us (36%)
  Pallas kernels  22.5 us (8%)
  local copies, waits for them, and re-layouts  20.2 us (7%)
  other arithmetic  3.88 us (1%)
    ppermute x32, waiting for transfers between devices, rotate(): lax.ppermute(parts[r], axis, shift(n, n - r if back else r))  107 us
    ppermute x32, starting transfers between devices, rotate(): lax.ppermute(parts[r], axis, shift(n, n - r if back else r))  66.8 us
    all_to_all x5, starting transfers between devices, swap_fs(): return lax.all_to_all(value, 'fs', 0, 0, tiled=True)  31.7 us
    unnamed x75, local copies, waits for them, and re-layouts  20.2 us
    all_to_all x5, waiting for transfers between devices, swap_fs(): return lax.all_to_all(value, 'fs', 0, 0, tiled=True)  17.2 us
    pallas_call x3, Pallas kernels, cast_along(): pl.pallas_call(functools.partial(cast_kernel, steps, scale is not None, a...  6.15 us
    pallas_call x2, Pallas kernels, down_rows(): pl.pallas_call(functools.partial(down_kernel, fs, tp, len(parts), prior i...  5.59 us
  transfers between devices with their start and end apart: 37, of which 12 were waited for; matrix products, arithmetic and copies ran while one was open for 1% of the time, Pallas kernels for 7%

profile of v1, /device:TPU:0, one launch (start us, length us, event | category | flops | bytes accessed | tf_op | source)
XLA Modules:
  0.0 270.0 jit_solution(15389015456690965509)
XLA Ops:
  4.4 7.3 %all-to-all-start = ((bf16[8,16,2176]{2,1,0:T(8,128)(2,1)}), bf16[8,16,2176]{2,1,0:T(8,128)(2,1)S(1)}, u32[]{:S(2)}, u32[]{:S(2)}) async-start(bf16[8,16,2176]{2,1,0:T(8,128)(2,1)} %bitcast.4), calls=%async_computation | async-start | bytes 1114112 | tf_op jit(solution)/shard_map/all_to_all | solution.py:361
  11.7 2.2 copy-done.7
  18.7 10.6 %collective-permute-done.3.refs_1_ = bf16[8,256,128]{2,1,0:T(8,128)(2,1)S(1)} collective-permute-done((bf16[8,256,128]{2,1,0:T(8,128)(2,1)S(1)}, bf16[8,256,128]{2,1,0:T(8,128)(2,1)S(1)}, u32[]{:S(2)}, u32[]{:S(2)}) %collective-permute-start.3) | collective-permute-done | bytes 524320 | tf_op jit(solution)/shard_map/ppermute | solution.py:357
  30.6 9.6 %collective-permute-done.5.refs_3_ = bf16[8,256,128]{2,1,0:T(8,128)(2,1)S(1)} collective-permute-done((bf16[8,256,128]{2,1,0:T(8,128)(2,1)S(1)}, bf16[8,256,128]{2,1,0:T(8,128)(2,1)S(1)}, u32[]{:S(2)}, u32[]{:S(2)}) %collective-permute-start.5) | collective-permute-done | bytes 524320 | tf_op jit(solution)/shard_map/ppermute | solution.py:357
  42.6 6.0 %all-to-all-start.1 = ((bf16[8,256,512]{2,1,0:T(8,128)(2,1)}), bf16[8,256,512]{2,1,0:T(8,128)(2,1)S(1)}, u32[]{:S(2)}, u32[]{:S(2)}) async-start(bf16[8,256,512]{2,1,0:T(8,128)(2,1)} %copy-done.4), calls=%async_computation.1 | async-start | bytes 4194304 | tf_op jit(solution)/shard_map/all_to_all | solution.py:361
  48.7 2.2 copy-done.9
  54.4 3.0 %shard_map.105 = (bf16[4,256,128]{2,1,0:T(8,128)(2,1)S(1)}, bf16[4,256,128]{2,1,0:T(8,128)(2,1)S(1)}, bf16[4,256,128]{2,1,0:T(8,128)(2,1)S(1)}, bf16[4,256,128]{...) custom-call(s32[2]{0:T(128)S(1)} %pad_add_fusion.me_ref, ...), custom_call_target="tpu_custom_call" | custom-call | flops 1000000000 | bytes 6291456 | tf_op jit(solution)/shard_map/pallas_call | solution.py:107
  57.4 2.0 collective-permute-start.6
  60.8 33.8 %collective-permute-done.6.refs_1_ = bf16[4,256,128]{2,1,0:T(8,128)(2,1)S(1)} collective-permute-done((bf16[4,256,128]{2,1,0:T(8,128)(2,1)S(1)}, bf16[4,256,128]{2,1,0:T(8,128)(2,1)S(1)}, u32[]{:S(2)}, u32[]{:S(2)}) %collective-permute-start.6) | collective-permute-done | bytes 262176 | tf_op jit(solution)/shard_map/ppermute | solution.py:357
  95.3 8.4 %collective-permute-start.8 = (bf16[4,256,128]{2,1,0:T(8,128)(2,1)}, bf16[4,256,128]{2,1,0:T(8,128)(2,1)}, u32[]{:S(2)}, u32[]{:S(2)}) collective-permute-start(bf16[4,256,128]{2,1,0:T(8,128)(2,1)} %get-tuple-element.52), channel_id=1, source_target_pairs={{0,12},{4,16},{8,20},{12,24},{16,28},{20,0},{24,4},{28,8},{1,13},{... | collective-permute-start | bytes 786440 | tf_op jit(solution)/shard_map/ppermute | solution.py:357
  104.4 1.9 collective-permute-start.9
  106.4 10.5 %collective-permute-start.10 = (bf16[4,256,128]{2,1,0:T(8,128)(2,1)}, bf16[4,256,128]{2,1,0:T(8,128)(2,1)}, u32[]{:S(2)}, u32[]{:S(2)}) collective-permute-start(bf16[4,256,128]{2,1,0:T(8,128)(2,1)} %get-tuple-element.54), channel_id=1, source_target_pairs={{0,20},{4,24},{8,28},{12,0},{16,4},{20,8},{24,12},{28,16},{1,21},{... | collective-permute-start | bytes 786440 | tf_op jit(solution)/shard_map/ppermute | solution.py:357
  125.4 5.7 %all-to-all-start.3 = ((bf16[8,64,1024]{2,1,0:T(8,128)(2,1)}), bf16[8,64,1024]{2,1,0:T(8,128)(2,1)}, u32[]{:S(2)}, u32[]{:S(2)}) async-start(bf16[8,64,1024]{2,1,0:T(8,128)(2,1)} %copy-done.10), calls=%async_computation.3 | async-start | bytes 2097152 | tf_op jit(solution)/shard_map/all_to_all | solution.py:361
  131.3 7.5 %collective-permute-done.11.refs_6_ = bf16[4,256,128]{2,1,0:T(8,128)(2,1)} collective-permute-done((bf16[4,256,128]{2,1,0:T(8,128)(2,1)}, bf16[4,256,128]{2,1,0:T(8,128)(2,1)}, u32[]{:S(2)}, u32[]{:S(2)}) %collective-permute-start.11) | collective-permute-done | bytes 262176 | tf_op jit(solution)/shard_map/ppermute | solution.py:357
  138.8 1.9 shard_map.106
  140.8 11.3 %collective-permute-start.19 = (bf16[64,1024]{1,0:T(8,128)(2,1)S(1)}, bf16[64,1024]{1,0:T(8,128)(2,1)S(1)}, u32[]{:S(2)}, u32[]{:S(2)}) collective-permute-start(bf16[64,1024]{1,0:T(8,128)(2,1)S(1)} %copy-done.36), channel_id=1, source_target_pairs={{0,4},{4,8},{8,12},{12,16},{16,20},{20,24},{24,28},{28,0},{1,5},{5... | collective-permute-start | bytes 393224 | tf_op jit(solution)/shard_map/ppermute | solution.py:357
  152.1 6.7 %collective-permute-start.20 = (bf16[64,1024]{1,0:T(8,128)(2,1)S(1)}, bf16[64,1024]{1,0:T(8,128)(2,1)S(1)}, u32[]{:S(2)}, u32[]{:S(2)}) collective-permute-start(bf16[64,1024]{1,0:T(8,128)(2,1)S(1)} %copy-done.34), channel_id=1, source_target_pairs={{0,8},{4,12},{8,16},{12,20},{16,24},{20,28},{24,0},{28,4},{1,9},{5... | collective-permute-start | bytes 393224 | tf_op jit(solution)/shard_map/ppermute | solution.py:357
  160.4 3.4 %collective-permute-done.19.refs_5_ = bf16[64,1024]{1,0:T(8,128)(2,1)S(1)} collective-permute-done((bf16[64,1024]{1,0:T(8,128)(2,1)S(1)}, bf16[64,1024]{1,0:T(8,128)(2,1)S(1)}, u32[]{:S(2)}, u32[]{:S(2)}) %collective-permute-start.19) | collective-permute-done | bytes 131104 | tf_op jit(solution)/shard_map/ppermute | solution.py:357
  165.9 31.1 %collective-permute-done.14.refs_6_ = bf16[8,256,128]{2,1,0:T(8,128)(2,1)S(1)} collective-permute-done((bf16[8,256,128]{2,1,0:T(8,128)(2,1)S(1)}, bf16[8,256,128]{2,1,0:T(8,128)(2,1)S(1)}, u32[]{:S(2)}, u32[]{:S(2)}) %collective-permute-start.14) | collective-permute-done | bytes 524320 | tf_op jit(solution)/shard_map/ppermute | solution.py:357
  197.4 4.1 %collective-permute-done.15.refs_7_ = bf16[8,256,128]{2,1,0:T(8,128)(2,1)S(1)} collective-permute-done((bf16[8,256,128]{2,1,0:T(8,128)(2,1)S(1)}, bf16[8,256,128]{2,1,0:T(8,128)(2,1)S(1)}, u32[]{:S(2)}, u32[]{:S(2)}) %collective-permute-start.15) | collective-permute-done | bytes 524320 | tf_op jit(solution)/shard_map/ppermute | solution.py:357
  201.5 1.9 collective-permute-start.22
  204.1 6.1 %collective-permute-start.24 = (bf16[64,1024]{1,0:T(8,128)(2,1)S(1)}, bf16[64,1024]{1,0:T(8,128)(2,1)S(1)}, u32[]{:S(2)}, u32[]{:S(2)}) collective-permute-start(bf16[64,1024]{1,0:T(8,128)(2,1)S(1)} %copy-done.26), channel_id=1, source_target_pairs={{0,24},{4,28},{8,0},{12,4},{16,8},{20,12},{24,16},{28,20},{1,25},{... | collective-permute-start | bytes 393224 | tf_op jit(solution)/shard_map/ppermute | solution.py:357
  210.3 3.0 %shard_map.107 = (bf16[2048,512]{1,0:T(8,128)(2,1)}, f32[512,512]{1,0:T(8,128)S(1)}) custom-call(s32[2]{0:T(128)S(1)} %pad_add_fusion.me_ref, bf16[128,2176]{1,0:T(8,128)(2,1)S(1)} %bitcast.24, bf16[128,2176]{1,0:T(8,128)(2,1)S(1)} %collective-permute-done.refs_1_, bf16[128,2176]{1,0:T(8,128)(2,1)S(1)} %collective-permute-done.1.refs_2_, ...), custom_call_target="tpu_custom_call" | custom-call | flops 1073741824 | bytes 4194304 | tf_op jit(solution)/shard_map/pallas_call | solution.py:237
  214.7 2.2 collective-permute-done.25.refs_11_
  216.9 2.2 shard_map.111
  224.9 3.4 %shard_map.112 = (bf16[512,2048]{1,0:T(8,128)(2,1)}, bf16[128,1024]{1,0:T(8,128)(2,1)S(1)}, bf16[128,1024]{1,0:T(8,128)(2,1)}, bf16[128,1024]{1,0:T(8,128)(2,1)}, bf16[128,1024]{1,0:T(8,128)(2,1)}) custom-call(s32[2]{0:T(128)S(1)} %pad_add_fusion.me_ref, bf16[512,512]{1,0:T(8,128)(2,1)S(1)} %copy-done.6, ...), custom_call_target="tpu_custom_call", output_to_operand_aliasing={{0}: (7, {})} | custom-call | flops 536870912 | bytes 2097152 | tf_op jit(solution)/shard_map/pallas_call | solution.py:315
  230.6 3.1 %collective-permute-done.26 = bf16[128,1024]{1,0:T(8,128)(2,1)} collective-permute-done((bf16[128,1024]{1,0:T(8,128)(2,1)}, bf16[128,1024]{1,0:T(8,128)(2,1)}, u32[]{:S(2)}, u32[]{:S(2)}) %collective-permute-start.26) | collective-permute-done | bytes 262176 | tf_op jit(solution)/shard_map/ppermute | solution.py:357
  233.7 2.0 add_convert_fusion.1
  235.7 9.1 %all-to-all-start.2 = ((bf16[8,16,1024]{2,1,0:T(8,128)(2,1)}), bf16[8,16,1024]{2,1,0:T(8,128)(2,1)S(1)}, u32[]{:S(2)}, u32[]{:S(2)}) async-start(bf16[8,16,1024]{2,1,0:T(8,128)(2,1)} %bitcast.11), calls=%async_computation.2 | async-start | bytes 524288 | tf_op jit(solution)/shard_map/all_to_all | solution.py:361
  246.6 8.0 %all-to-all-done.2 = bf16[8,16,1024]{2,1,0:T(8,128)(2,1)S(1)} async-done(((bf16[8,16,1024]{2,1,0:T(8,128)(2,1)}), bf16[8,16,1024]{2,1,0:T(8,128)(2,1)S(1)}, u32[]{:S(2)}, u32[]{:S(2)}) %all-to-all-start.2) | async-done | bytes 262176 | tf_op jit(solution)/shard_map/all_to_all | solution.py:361
  254.7 3.6 %all-to-all-start.4 = ((bf16[8,16,1024]{2,1,0:T(8,128)(2,1)}), bf16[8,16,1024]{2,1,0:T(8,128)(2,1)S(1)}, u32[]{:S(2)}, u32[]{:S(2)}) async-start(bf16[8,16,1024]{2,1,0:T(8,128)(2,1)} %bitcast.14), calls=%async_computation.4 | async-start | bytes 524288 | tf_op jit(solution)/shard_map/all_to_all | solution.py:361
  258.3 9.2 %all-to-all-done.4 = bf16[8,16,1024]{2,1,0:T(8,128)(2,1)S(1)} async-done(((bf16[8,16,1024]{2,1,0:T(8,128)(2,1)}), bf16[8,16,1024]{2,1,0:T(8,128)(2,1)S(1)}, u32[]{:S(2)}, u32[]{:S(2)}) %all-to-all-start.4) | async-done | bytes 262176 | tf_op jit(solution)/shard_map/all_to_all | solution.py:361
  (132 shorter events, 45.9 us)
Async XLA Ops:
  4.4 38.3 %all-to-all-start = ((bf16[8,16,2176]{2,1,0:T(8,128)(2,1)}), bf16[8,16,2176]{2,1,0:T(8,128)(2,1)S(1)}, u32[]{:S(2)}, u32[]{:S(2)}) async-start(bf16[8,16,2176]{2,1,0:T(8,128)(2,1)} %bitcast.4), calls=%async_computation | async-start | bytes 1114112 | tf_op jit(solution)/shard_map/all_to_all | solution.py:361
  15.6 13.6 %collective-permute-start.3 = (bf16[8,256,128]{2,1,0:T(8,128)(2,1)S(1)}, bf16[8,256,128]{2,1,0:T(8,128)(2,1)S(1)}, u32[]{:S(2)}, u32[]{:S(2)}) collective-permute-start(bf16[8,256,128]{2,1,0:T(8,128)(2,1)S(1)} %get-tuple-element.46), channel_id=1, source_target_pairs={{0,1},{1,2},{2,3},{3,0},{4,5},{5,6},{6,7},{7,4},{8,9},{9,10},{10,1... | collective-permute-start | bytes 1572872 | tf_op jit(solution)/shard_map/ppermute | solution.py:357
  15.7 14.9 %collective-permute-start.4 = (bf16[8,256,128]{2,1,0:T(8,128)(2,1)S(1)}, bf16[8,256,128]{2,1,0:T(8,128)(2,1)S(1)}, u32[]{:S(2)}, u32[]{:S(2)}) collective-permute-start(bf16[8,256,128]{2,1,0:T(8,128)(2,1)S(1)} %get-tuple-element.47), channel_id=1, source_target_pairs={{0,2},{1,3},{2,0},{3,1},{4,6},{5,7},{6,4},{7,5},{8,10},{9,11},{10,... | collective-permute-start | bytes 1572872 | tf_op jit(solution)/shard_map/ppermute | solution.py:357
  17.3 22.9 %collective-permute-start.5 = (bf16[8,256,128]{2,1,0:T(8,128)(2,1)S(1)}, bf16[8,256,128]{2,1,0:T(8,128)(2,1)S(1)}, u32[]{:S(2)}, u32[]{:S(2)}) collective-permute-start(bf16[8,256,128]{2,1,0:T(8,128)(2,1)S(1)} %get-tuple-element.48), channel_id=1, source_target_pairs={{0,3},{1,0},{2,1},{3,2},{4,7},{5,4},{6,5},{7,6},{8,11},{9,8},{10,9... | collective-permute-start | bytes 1572872 | tf_op jit(solution)/shard_map/ppermute | solution.py:357
  42.6 82.8 %all-to-all-start.1 = ((bf16[8,256,512]{2,1,0:T(8,128)(2,1)}), bf16[8,256,512]{2,1,0:T(8,128)(2,1)S(1)}, u32[]{:S(2)}, u32[]{:S(2)}) async-start(bf16[8,256,512]{2,1,0:T(8,128)(2,1)} %copy-done.4), calls=%async_computation.1 | async-start | bytes 4194304 | tf_op jit(solution)/shard_map/all_to_all | solution.py:361
  52.3 54.1 %collective-permute-start.16 = (bf16[8,64,512]{2,1,0:T(8,128)(2,1)S(1)}, bf16[8,64,512]{2,1,0:T(8,128)(2,1)S(1)}, u32[]{:S(2)}, u32[]{:S(2)}) collective-permute-start(bf16[8,64,512]{2,1,0:T(8,128)(2,1)S(1)} %get-tuple-element.63), channel_id=1, source_target_pairs={{0,1},{1,2},{2,3},{3,0},{4,5},{5,6},{6,7},{7,4},{8,9},{9,10},{10,1... | collective-permute-start | bytes 1572872 | tf_op jit(solution)/shard_map/ppermute | solution.py:357
  52.8 64.1 %collective-permute-start.17 = (bf16[8,64,512]{2,1,0:T(8,128)(2,1)S(1)}, bf16[8,64,512]{2,1,0:T(8,128)(2,1)S(1)}, u32[]{:S(2)}, u32[]{:S(2)}) collective-permute-start(bf16[8,64,512]{2,1,0:T(8,128)(2,1)S(1)} %get-tuple-element.64), channel_id=1, source_target_pairs={{0,2},{1,3},{2,0},{3,1},{4,6},{5,7},{6,4},{7,5},{8,10},{9,11},{10,... | collective-permute-start | bytes 1572872 | tf_op jit(solution)/shard_map/ppermute | solution.py:357
  54.4 62.6 %collective-permute-start.18 = (bf16[8,64,512]{2,1,0:T(8,128)(2,1)S(1)}, bf16[8,64,512]{2,1,0:T(8,128)(2,1)S(1)}, u32[]{:S(2)}, u32[]{:S(2)}) collective-permute-start(bf16[8,64,512]{2,1,0:T(8,128)(2,1)S(1)} %get-tuple-element.65), channel_id=1, source_target_pairs={{0,3},{1,0},{2,1},{3,2},{4,7},{5,4},{6,5},{7,6},{8,11},{9,8},{10,9... | collective-permute-start | bytes 1572872 | tf_op jit(solution)/shard_map/ppermute | solution.py:357
  57.4 37.3 %collective-permute-start.6 = (bf16[4,256,128]{2,1,0:T(8,128)(2,1)S(1)}, bf16[4,256,128]{2,1,0:T(8,128)(2,1)S(1)}, u32[]{:S(2)}, u32[]{:S(2)}) collective-permute-start(bf16[4,256,128]{2,1,0:T(8,128)(2,1)S(1)} %get-tuple-element.50), channel_id=1, source_target_pairs={{0,4},{4,8},{8,12},{12,16},{16,20},{20,24},{24,28},{28,0},{1,5},{5... | collective-permute-start | bytes 786440 | tf_op jit(solution)/shard_map/ppermute | solution.py:357
  59.3 44.4 %collective-permute-start.7 = (bf16[4,256,128]{2,1,0:T(8,128)(2,1)S(1)}, bf16[4,256,128]{2,1,0:T(8,128)(2,1)S(1)}, u32[]{:S(2)}, u32[]{:S(2)}) collective-permute-start(bf16[4,256,128]{2,1,0:T(8,128)(2,1)S(1)} %get-tuple-element.51), channel_id=1, source_target_pairs={{0,8},{4,12},{8,16},{12,20},{16,24},{20,28},{24,0},{28,4},{1,9},{5... | collective-permute-start | bytes 786440 | tf_op jit(solution)/shard_map/ppermute | solution.py:357
  95.3 35.9 %collective-permute-start.8 = (bf16[4,256,128]{2,1,0:T(8,128)(2,1)}, bf16[4,256,128]{2,1,0:T(8,128)(2,1)}, u32[]{:S(2)}, u32[]{:S(2)}) collective-permute-start(bf16[4,256,128]{2,1,0:T(8,128)(2,1)} %get-tuple-element.52), channel_id=1, source_target_pairs={{0,12},{4,16},{8,20},{12,24},{16,28},{20,0},{24,4},{28,8},{1,13},{... | collective-permute-start | bytes 786440 | tf_op jit(solution)/shard_map/ppermute | solution.py:357
  104.4 26.8 %collective-permute-start.9 = (bf16[4,256,128]{2,1,0:T(8,128)(2,1)}, bf16[4,256,128]{2,1,0:T(8,128)(2,1)}, u32[]{:S(2)}, u32[]{:S(2)}) collective-permute-start(bf16[4,256,128]{2,1,0:T(8,128)(2,1)} %get-tuple-element.53), channel_id=1, source_target_pairs={{0,16},{4,20},{8,24},{12,28},{16,0},{20,4},{24,8},{28,12},{1,17},{... | collective-permute-start | bytes 786440 | tf_op jit(solution)/shard_map/ppermute | solution.py:357
  106.4 24.9 %collective-permute-start.10 = (bf16[4,256,128]{2,1,0:T(8,128)(2,1)}, bf16[4,256,128]{2,1,0:T(8,128)(2,1)}, u32[]{:S(2)}, u32[]{:S(2)}) collective-permute-start(bf16[4,256,128]{2,1,0:T(8,128)(2,1)} %get-tuple-element.54), channel_id=1, source_target_pairs={{0,20},{4,24},{8,28},{12,0},{16,4},{20,8},{24,12},{28,16},{1,21},{... | collective-permute-start | bytes 786440 | tf_op jit(solution)/shard_map/ppermute | solution.py:357
  116.9 21.8 %collective-permute-start.11 = (bf16[4,256,128]{2,1,0:T(8,128)(2,1)}, bf16[4,256,128]{2,1,0:T(8,128)(2,1)}, u32[]{:S(2)}, u32[]{:S(2)}) collective-permute-start(bf16[4,256,128]{2,1,0:T(8,128)(2,1)} %get-tuple-element.55), channel_id=1, source_target_pairs={{0,24},{4,28},{8,0},{12,4},{16,8},{20,12},{24,16},{28,20},{1,25},{... | collective-permute-start | bytes 786440 | tf_op jit(solution)/shard_map/ppermute | solution.py:357
  116.9 21.8 %collective-permute-start.12 = (bf16[4,256,128]{2,1,0:T(8,128)(2,1)}, bf16[4,256,128]{2,1,0:T(8,128)(2,1)}, u32[]{:S(2)}, u32[]{:S(2)}) collective-permute-start(bf16[4,256,128]{2,1,0:T(8,128)(2,1)} %get-tuple-element.56), channel_id=1, source_target_pairs={{0,28},{4,0},{8,4},{12,8},{16,12},{20,16},{24,20},{28,24},{1,29},{... | collective-permute-start | bytes 786440 | tf_op jit(solution)/shard_map/ppermute | solution.py:357
  125.4 96.3 %all-to-all-start.3 = ((bf16[8,64,1024]{2,1,0:T(8,128)(2,1)}), bf16[8,64,1024]{2,1,0:T(8,128)(2,1)}, u32[]{:S(2)}, u32[]{:S(2)}) async-start(bf16[8,64,1024]{2,1,0:T(8,128)(2,1)} %copy-done.10), calls=%async_computation.3 | async-start | bytes 2097152 | tf_op jit(solution)/shard_map/all_to_all | solution.py:361
  140.7 25.0 %collective-permute-start.13 = (bf16[8,256,128]{2,1,0:T(8,128)(2,1)S(1)}, bf16[8,256,128]{2,1,0:T(8,128)(2,1)S(1)}, u32[]{:S(2)}, u32[]{:S(2)}) collective-permute-start(bf16[8,256,128]{2,1,0:T(8,128)(2,1)S(1)} %get-tuple-element.58), channel_id=1, source_target_pairs={{0,1},{1,2},{2,3},{3,0},{4,5},{5,6},{6,7},{7,4},{8,9},{9,10},{10,1... | collective-permute-start | bytes 1572872 | tf_op jit(solution)/shard_map/ppermute | solution.py:357
  140.8 23.0 %collective-permute-start.19 = (bf16[64,1024]{1,0:T(8,128)(2,1)S(1)}, bf16[64,1024]{1,0:T(8,128)(2,1)S(1)}, u32[]{:S(2)}, u32[]{:S(2)}) collective-permute-start(bf16[64,1024]{1,0:T(8,128)(2,1)S(1)} %copy-done.36), channel_id=1, source_target_pairs={{0,4},{4,8},{8,12},{12,16},{16,20},{20,24},{24,28},{28,0},{1,5},{5... | collective-permute-start | bytes 393224 | tf_op jit(solution)/shard_map/ppermute | solution.py:357
  152.1 12.7 %collective-permute-start.20 = (bf16[64,1024]{1,0:T(8,128)(2,1)S(1)}, bf16[64,1024]{1,0:T(8,128)(2,1)S(1)}, u32[]{:S(2)}, u32[]{:S(2)}) collective-permute-start(bf16[64,1024]{1,0:T(8,128)(2,1)S(1)} %copy-done.34), channel_id=1, source_target_pairs={{0,8},{4,12},{8,16},{12,20},{16,24},{20,28},{24,0},{28,4},{1,9},{5... | collective-permute-start | bytes 393224 | tf_op jit(solution)/shard_map/ppermute | solution.py:357
  158.9 44.5 %collective-permute-start = (bf16[128,2176]{1,0:T(8,128)(2,1)S(1)}, bf16[128,2176]{1,0:T(8,128)(2,1)S(1)}, u32[]{:S(2)}, u32[]{:S(2)}) collective-permute-start(bf16[128,2176]{1,0:T(8,128)(2,1)S(1)} %bitcast.21), channel_id=1, source_target_pairs={{0,1},{1,2},{2,3},{3,0},{4,5},{5,6},{6,7},{7,4},{8,9},{9,10},{10,1... | collective-permute-start | bytes 1671176 | tf_op jit(solution)/shard_map/ppermute | solution.py:357
  158.9 45.2 %collective-permute-start.1 = (bf16[128,2176]{1,0:T(8,128)(2,1)S(1)}, bf16[128,2176]{1,0:T(8,128)(2,1)S(1)}, u32[]{:S(2)}, u32[]{:S(2)}) collective-permute-start(bf16[128,2176]{1,0:T(8,128)(2,1)S(1)} %bitcast.22), channel_id=1, source_target_pairs={{0,2},{1,3},{2,0},{3,1},{4,6},{5,7},{6,4},{7,5},{8,10},{9,11},{10,... | collective-permute-start | bytes 1671176 | tf_op jit(solution)/shard_map/ppermute | solution.py:357
  163.8 46.4 %collective-permute-start.2 = (bf16[128,2176]{1,0:T(8,128)(2,1)S(1)}, bf16[128,2176]{1,0:T(8,128)(2,1)S(1)}, u32[]{:S(2)}, u32[]{:S(2)}) collective-permute-start(bf16[128,2176]{1,0:T(8,128)(2,1)S(1)} %bitcast.23), channel_id=1, source_target_pairs={{0,3},{1,0},{2,1},{3,2},{4,7},{5,4},{6,5},{7,6},{8,11},{9,8},{10,9... | collective-permute-start | bytes 1671176 | tf_op jit(solution)/shard_map/ppermute | solution.py:357
  164.8 32.2 %collective-permute-start.14 = (bf16[8,256,128]{2,1,0:T(8,128)(2,1)S(1)}, bf16[8,256,128]{2,1,0:T(8,128)(2,1)S(1)}, u32[]{:S(2)}, u32[]{:S(2)}) collective-permute-start(bf16[8,256,128]{2,1,0:T(8,128)(2,1)S(1)} %get-tuple-element.59), channel_id=1, source_target_pairs={{0,2},{1,3},{2,0},{3,1},{4,6},{5,7},{6,4},{7,5},{8,10},{9,11},{10,... | collective-permute-start | bytes 1572872 | tf_op jit(solution)/shard_map/ppermute | solution.py:357
  165.7 35.8 %collective-permute-start.15 = (bf16[8,256,128]{2,1,0:T(8,128)(2,1)S(1)}, bf16[8,256,128]{2,1,0:T(8,128)(2,1)S(1)}, u32[]{:S(2)}, u32[]{:S(2)}) collective-permute-start(bf16[8,256,128]{2,1,0:T(8,128)(2,1)S(1)} %get-tuple-element.60), channel_id=1, source_target_pairs={{0,3},{1,0},{2,1},{3,2},{4,7},{5,4},{6,5},{7,6},{8,11},{9,8},{10,9... | collective-permute-start | bytes 1572872 | tf_op jit(solution)/shard_map/ppermute | solution.py:357
  197.0 17.7 %collective-permute-start.21 = (bf16[64,1024]{1,0:T(8,128)(2,1)S(1)}, bf16[64,1024]{1,0:T(8,128)(2,1)S(1)}, u32[]{:S(2)}, u32[]{:S(2)}) collective-permute-start(bf16[64,1024]{1,0:T(8,128)(2,1)S(1)} %copy-done.32), channel_id=1, source_target_pairs={{0,12},{4,16},{8,20},{12,24},{16,28},{20,0},{24,4},{28,8},{1,13},{... | collective-permute-start | bytes 393224 | tf_op jit(solution)/shard_map/ppermute | solution.py:357
  201.5 13.2 %collective-permute-start.22 = (bf16[64,1024]{1,0:T(8,128)(2,1)S(1)}, bf16[64,1024]{1,0:T(8,128)(2,1)S(1)}, u32[]{:S(2)}, u32[]{:S(2)}) collective-permute-start(bf16[64,1024]{1,0:T(8,128)(2,1)S(1)} %copy-done.30), channel_id=1, source_target_pairs={{0,16},{4,20},{8,24},{12,28},{16,0},{20,4},{24,8},{28,12},{1,17},{... | collective-permute-start | bytes 393224 | tf_op jit(solution)/shard_map/ppermute | solution.py:357
  221.1 12.6 %collective-permute-start.26 = (bf16[128,1024]{1,0:T(8,128)(2,1)}, bf16[128,1024]{1,0:T(8,128)(2,1)}, u32[]{:S(2)}, u32[]{:S(2)}) collective-permute-start(bf16[128,1024]{1,0:T(8,128)(2,1)} %get-tuple-element.75), channel_id=1, source_target_pairs={{0,3},{1,0},{2,1},{3,2},{4,7},{5,4},{6,5},{7,6},{8,11},{9,8},{10,9... | collective-permute-start | bytes 786440 | tf_op jit(solution)/shard_map/ppermute | solution.py:357
  228.3 16.5 %collective-permute-start.31 = (bf16[128,1024]{1,0:T(8,128)(2,1)}, bf16[128,1024]{1,0:T(8,128)(2,1)S(1)}, u32[]{:S(2)}, u32[]{:S(2)}) collective-permute-start(bf16[128,1024]{1,0:T(8,128)(2,1)} %get-tuple-element.83), channel_id=1, source_target_pairs={{0,1},{1,2},{2,3},{3,0},{4,5},{5,6},{6,7},{7,4},{8,9},{9,10},{10,1... | collective-permute-start | bytes 786440 | tf_op jit(solution)/shard_map/ppermute | solution.py:357
  228.3 16.5 %collective-permute-start.30 = (bf16[128,1024]{1,0:T(8,128)(2,1)}, bf16[128,1024]{1,0:T(8,128)(2,1)S(1)}, u32[]{:S(2)}, u32[]{:S(2)}) collective-permute-start(bf16[128,1024]{1,0:T(8,128)(2,1)} %get-tuple-element.82), channel_id=1, source_target_pairs={{0,2},{1,3},{2,0},{3,1},{4,6},{5,7},{6,4},{7,5},{8,10},{9,11},{10,... | collective-permute-start | bytes 786440 | tf_op jit(solution)/shard_map/ppermute | solution.py:357
  229.2 15.6 %collective-permute-start.29 = (bf16[128,1024]{1,0:T(8,128)(2,1)}, bf16[128,1024]{1,0:T(8,128)(2,1)S(1)}, u32[]{:S(2)}, u32[]{:S(2)}) collective-permute-start(bf16[128,1024]{1,0:T(8,128)(2,1)} %get-tuple-element.81), channel_id=1, source_target_pairs={{0,3},{1,0},{2,1},{3,2},{4,7},{5,4},{6,5},{7,6},{8,11},{9,8},{10,9... | collective-permute-start | bytes 786440 | tf_op jit(solution)/shard_map/ppermute | solution.py:357
  235.7 19.0 %all-to-all-start.2 = ((bf16[8,16,1024]{2,1,0:T(8,128)(2,1)}), bf16[8,16,1024]{2,1,0:T(8,128)(2,1)S(1)}, u32[]{:S(2)}, u32[]{:S(2)}) async-start(bf16[8,16,1024]{2,1,0:T(8,128)(2,1)} %bitcast.11), calls=%async_computation.2 | async-start | bytes 524288 | tf_op jit(solution)/shard_map/all_to_all | solution.py:361
  254.7 12.7 %all-to-all-start.4 = ((bf16[8,16,1024]{2,1,0:T(8,128)(2,1)}), bf16[8,16,1024]{2,1,0:T(8,128)(2,1)S(1)}, u32[]{:S(2)}, u32[]{:S(2)}) async-start(bf16[8,16,1024]{2,1,0:T(8,128)(2,1)} %bitcast.14), calls=%async_computation.4 | async-start | bytes 524288 | tf_op jit(solution)/shard_map/all_to_all | solution.py:361
  (42 other events, 574.9 us)

commit v2 on v1

--- a/solution.py
+++ b/solution.py
@@ -12,15 +12,19 @@
 lanes = 128
 bf16 = jnp.bfloat16
 f32 = jnp.float32
-grant = 24 * 1024 * 1024
+small = pltpu.CompilerParams(vmem_limit_bytes=16 * 1024 * 1024)
+
+
+def cuts_of(width):
+    half, rest = width // 2, width // 2 + width // 4
+    return [(0, half), (half, rest), (rest, width)]
+
+
+returns = [(0, 1), (2,)]
 
 
 def cost(flops, nbytes):
     return pl.CostEstimate(flops=int(flops), bytes_accessed=int(nbytes), transcendentals=0)
-
-
-def params():
-    return pltpu.CompilerParams(vmem_limit_bytes=grant)
 
 
 def whole(shape):
@@ -37,12 +41,15 @@
     return jnp.sum(jnp.where(down == across, row, jnp.zeros((), row.dtype)), axis=1, keepdims=True)
 
 
-def slot_onehot(group_row, per_group):
-    down, across = square(group_row.shape[1])
+def slot_onehot(group_row, me, fs):
+    count = group_row.shape[1]
+    down, across = square(count)
     group_col = to_col(group_row)
     earlier = jnp.where((group_col == group_row) & (across < down), 1.0, 0.0)
-    rank = jnp.sum(earlier, axis=1, keepdims=True)
-    slot = (group_col * float(per_group) + rank).astype(jnp.int32)
+    rank = jnp.sum(earlier, axis=1, keepdims=True).astype(jnp.int32)
+    ahead = group_col.astype(jnp.int32) - me
+    ahead = jnp.where(ahead < 0, ahead + fs, ahead)
+    slot = ahead * (count // fs) + rank
     return jnp.where(slot == across, 1.0, 0.0).astype(bf16)
 
 
@@ -53,10 +60,10 @@
     return group
 
 
-def prep_kernel(fs, tp, tok_ref, ids_ref, weight_ref, out_ref):
+def prep_kernel(fs, tp, me_ref, tok_ref, ids_ref, weight_ref, *outs):
     count, width = tok_ref.shape
     group = group_of(ids_ref[0:1, :], fs, tp)
-    onehot = slot_onehot(group, count // fs)
+    onehot = slot_onehot(group, me_ref[0], fs)
     wide = tok_ref[...].astype(f32)
     scale = lax.rsqrt(jnp.mean(wide * wide, axis=-1, keepdims=True) + norm_eps)
     normed = (wide * scale).astype(bf16)
@@ -71,10 +78,52 @@
             extra = extra + jnp.where(lane == local + part * tp, piece, 0.0)
             rest = rest - piece
     dims = (((0,), (0,)), ((), ()))
-    out_ref[:, :width] = lax.dot_general(onehot, normed, dims, preferred_element_type=f32).astype(bf16)
-    out_ref[:, width:] = lax.dot_general(
-        onehot, extra.astype(bf16), dims, preferred_element_type=f32
-    ).astype(bf16)
+    rows = lax.dot_general(onehot, normed, dims, preferred_element_type=f32).astype(bf16)
+    extra = lax.dot_general(onehot, extra.astype(bf16), dims, preferred_element_type=f32).astype(bf16)
+    each = count // fs
+    for r in range(fs):
+        outs[r][:, :width] = rows[r * each : (r + 1) * each]
+        outs[r][:, width:] = extra[r * each : (r + 1) * each]
+
+
+def join_kernel(*refs):
+    each = refs[0].shape[0]
+    for r, ref in enumerate(refs[:-1]):
+        refs[-1][r * each : (r + 1) * each, :] = ref[...]
+
+
+def join(parts):
+    each, width = parts[0].shape
+    return pl.pallas_call(
+        join_kernel,
+        out_shape=jax.ShapeDtypeStruct((each * len(parts), width), bf16),
+        compiler_params=small,
+        cost_estimate=cost(1e9, 4 * len(parts) * parts[0].size),
+    )(*parts)
+
+
+def add_kernel(fs, tp, *refs):
+    ins, outs = refs[:-fs], refs[-fs:]
+    each = outs[0].shape[0]
+    low = 0
+    for k in range(0, len(ins), tp):
+        total = sum(ref[...].astype(f32) for ref in ins[k : k + tp]).astype(bf16)
+        high = low + total.shape[1]
+        for r in range(fs):
+            outs[r][:, low:high] = total[r * each : (r + 1) * each]
+        low = high
+
+
+def add(fs, groups):
+    tp = len(groups[0])
+    count = groups[0][0].shape[0]
+    width = sum(group[0].shape[1] for group in groups)
+    return pl.pallas_call(
+        functools.partial(add_kernel, fs, tp),
+        out_shape=[jax.ShapeDtypeStruct((count // fs, width), bf16)] * fs,
+        compiler_params=small,
+        cost_estimate=cost(1e9, 2 * (tp + 1) * count * width),
+    )(*[part for group in groups for part in group])
 
 
 def cast_kernel(steps, scaled, squeeze, me_ref, in_ref, *refs):
@@ -110,7 +159,6 @@
             num_scalar_prefetch=1, grid=(steps,), in_specs=in_specs, out_specs=[whole(shape)] * steps
         ),
         out_shape=[jax.ShapeDtypeStruct(shape, bf16)] * steps,
-        compiler_params=params(),
         cost_estimate=cost(1e9, 6 * matrix.size),
     )(me, *args)
 
@@ -144,30 +192,29 @@
             out_specs=pl.BlockSpec((1, rows, tp * cols), lambda g, m: (g, 0, 0)),
         ),
         out_shape=jax.ShapeDtypeStruct((fs, rows, tp * cols), bf16),
-        compiler_params=params(),
         cost_estimate=cost(1e9, 4 * tp * parts[0].size),
     )(me, *parts)
 
 
-def merge_down_kernel(fs, tp, first, me_ref, *refs):
+def merge_down_kernel(fs, tp, cuts, me_ref, *refs):
     ins, outs = refs[:tp], refs[tp:]
 
     def store(order):
         for r in range(fs):
             group = lax.rem(me_ref[0] + r, fs)
             full = jnp.concatenate([ins[q][group] for q in order], axis=-1)
-            outs[r][...] = full[:, :first]
-            outs[fs][group] = full[:, first:]
+            for k, (low, high) in enumerate(cuts):
+                outs[k * fs + r][...] = full[:, low:high]
 
     in_order(me_ref, tp, store)
 
 
-def merge_down(me, parts, first):
+def merge_down(me, parts, cuts):
     tp = len(parts)
-    fs, rows, cols = parts[0].shape
-    shapes = [(rows, first)] * fs + [(fs, rows, tp * cols - first)]
+    fs, rows, _ = parts[0].shape
+    shapes = [(rows, high - low) for low, high in cuts for _ in range(fs)]
     outs = pl.pallas_call(
-        functools.partial(merge_down_kernel, fs, tp, first),
+        functools.partial(merge_down_kernel, fs, tp, cuts),
         grid_spec=pltpu.PrefetchScalarGridSpec(
             num_scalar_prefetch=1,
             grid=(1,),
@@ -175,10 +222,9 @@
             out_specs=[whole(shape) for shape in shapes],
         ),
         out_shape=[jax.ShapeDtypeStruct(shape, bf16) for shape in shapes],
-        compiler_params=params(),
         cost_estimate=cost(1e9, 4 * tp * parts[0].size),
     )(me, *parts)
-    return outs[:fs], outs[fs]
+    return [outs[k * fs : (k + 1) * fs] for k in range(len(cuts))]
 
 
 def regroup_kernel(fs, tp, me_ref, *refs):
@@ -201,7 +247,6 @@
             out_specs=[whole(shape)] * tp,
         ),
         out_shape=[jax.ShapeDtypeStruct(shape, bf16)] * tp,
-        compiler_params=params(),
         cost_estimate=cost(1e9, 4 * fs * parts[0].size),
     )(me, *parts)
 
@@ -244,14 +289,14 @@
             scratch_shapes=[pltpu.VMEM((out[0], matrix[0]), bf16)],
         ),
         out_shape=[jax.ShapeDtypeStruct(matrix, bf16), jax.ShapeDtypeStruct(out, f32)],
-        compiler_params=params(),
         cost_estimate=cost(2 * out[0] * matrix[0] * matrix[1], 4 * matrix[0] * matrix[1]),
     )(me, *rows, *parts)
 
 
 def up_kernel(tp, *refs):
-    x_refs, (matrix_ref, gate_ref, out_ref, rows_ref) = refs[:tp], refs[tp:]
-    up = product_of(x_refs, matrix_ref, rows_ref)
+    x_refs, (in_ref, gate_ref, matrix_ref, out_ref, rows_ref) = refs[:tp], refs[tp:]
+    matrix_ref[...] = in_ref[...]
+    up = product_of(x_refs, in_ref, rows_ref)
     gate = gate_ref[...]
     out_ref[...] = (gate / (1.0 + jnp.exp(-gate)) * up).astype(bf16)
 
@@ -262,11 +307,13 @@
         functools.partial(up_kernel, tp),
         grid=(1,),
         in_specs=[whole(rows[0].shape)] * tp + [whole(matrix.shape), whole(gate.shape)],
-        out_specs=whole(gate.shape),
+        out_specs=[whole(matrix.shape), whole(gate.shape)],
         scratch_shapes=[pltpu.VMEM((gate.shape[0], matrix.shape[0]), bf16)],
-        out_shape=jax.ShapeDtypeStruct(gate.shape, bf16),
-        compiler_params=params(),
-        cost_estimate=cost(2 * gate.size * matrix.shape[0], 2 * matrix.size),
+        out_shape=[
+            jax.ShapeDtypeStruct(matrix.shape, bf16),
+            jax.ShapeDtypeStruct(gate.shape, bf16),
+        ],
+        cost_estimate=cost(2 * gate.size * matrix.shape[0], 4 * matrix.size),
     )(*rows, matrix, gate)
 
 
@@ -324,19 +371,20 @@
         out_shape=[jax.ShapeDtypeStruct((depth, width), bf16)]
         + [jax.ShapeDtypeStruct((count, size), bf16)] * tp,
         input_output_aliases=aliases,
-        compiler_params=params(),
+        compiler_params=small,
         cost_estimate=cost(2 * tp * count * depth * size, 4 * depth * size),
     )(me, *args)
     return outs[0], outs[1:]
 
 
-def final_kernel(fs, tp, ids_ref, *refs):
-    out_ref = refs[-1]
-    onehot = slot_onehot(group_of(ids_ref[0:1, :], fs, tp), ids_ref.shape[1] // fs)
+def final_kernel(fs, tp, me_ref, ids_ref, *refs):
+    ins, out_ref = refs[:-1], refs[-1]
+    onehot = slot_onehot(group_of(ids_ref[0:1, :], fs, tp), me_ref[0], fs)
     low = 0
-    for ref in refs[:-1]:
-        high = low + ref.shape[1]
-        out_ref[:, low:high] = jnp.dot(onehot, ref[...], preferred_element_type=f32).astype(bf16)
+    for k in range(0, len(ins), fs):
+        back = jnp.concatenate([ref[...] for ref in ins[k : k + fs]], axis=0)
+        high = low + back.shape[1]
+        out_ref[:, low:high] = jnp.dot(onehot, back, preferred_element_type=f32).astype(bf16)
         low = high
 
 
@@ -345,20 +393,17 @@
     tp = lax.axis_size("tp")
     me = jnp.stack([lax.axis_index("fs"), lax.axis_index("tp")]).astype(jnp.int32)
     count, width = tokens.shape
-    per_group = count // fs
-    first = width // 2
-
-    def shift(n, step):
-        return [(k, (k + step) % n) for k in range(n)]
+    cuts = cuts_of(width)
+    in_smem = pl.BlockSpec(memory_space=pltpu.SMEM)
+    in_vmem = pl.BlockSpec(memory_space=pltpu.VMEM)
 
     def rotate(parts, axis, back=False):
         n = len(parts)
-        return [parts[0]] + [
-            lax.ppermute(parts[r], axis, shift(n, n - r if back else r)) for r in range(1, n)
-        ]
-
-    def swap_fs(value):
-        return lax.all_to_all(value, "fs", 0, 0, tiled=True)
+        out = [parts[0]]
+        for r in range(1, n):
+            step = n - r if back else r
+            out.append(lax.ppermute(parts[r], axis, [(k, (k + step) % n) for k in range(n)]))
+        return out
 
     def by_expert(matrix):
         return matrix.reshape((fs, tp) + matrix.shape[1:])
@@ -366,51 +411,49 @@
     ids, weights = expert_ids.T, route_weight.T
     scale = norm_gain[None, :]
 
-    sorted_rows = pl.pallas_call(
-        functools.partial(prep_kernel, fs, tp),
-        out_shape=jax.ShapeDtypeStruct((count, width + lanes), bf16),
-        compiler_params=params(),
-        cost_estimate=cost(2 * count * count * width, 4 * count * width),
-    )(tokens, ids, weights)
-    landed = swap_fs(sorted_rows.reshape(fs, per_group, width + lanes))
-    landed = landed.reshape(count, width + lanes)
     gate_parts = cast_along(me, by_expert(gate_proj), scale, 0)
     gate_parts = rotate(gate_parts, "fs")
     up_parts = cast_along(me, by_expert(up_proj), scale, 1)
     up_parts = rotate(up_parts, "tp")
-    rows = rotate([landed] * tp, "tp")
-    up_here = merge(me, up_parts)
-    new_up = swap_fs(up_here)
-    new_up = new_up.reshape(-1, new_up.shape[2])
+    sent = pl.pallas_call(
+        functools.partial(prep_kernel, fs, tp),
+        in_specs=[in_smem, in_vmem, in_vmem, in_vmem],
+        out_shape=[jax.ShapeDtypeStruct((count // fs, width + lanes), bf16)] * fs,
+        cost_estimate=cost(2 * count * count * width, 4 * count * width),
+    )(me, tokens, ids, weights)
+    landed = rotate(sent, "fs")
     down_parts = cast_along(me, by_expert(down_proj), None, 1)
     down_parts = rotate(down_parts, "tp")
+    up_here = merge(me, up_parts)
+    up_here = lax.all_to_all(up_here, "fs", 0, 0, tiled=True)
+    up_here = up_here.reshape(-1, up_here.shape[2])
     gate_parts = regroup(me, gate_parts)
     gate_parts = rotate(gate_parts, "tp")
-    down_first, down_last = merge_down(me, down_parts, first)
-    down_first = rotate(down_first, "fs")
+    landed = join(landed)
+    rows = rotate([landed] * tp, "tp")
+    down_parts = merge_down(me, down_parts, cuts)
+    for k in range(len(cuts)):
+        down_parts[k] = rotate(down_parts[k], "fs")
     new_gate, gate = gate_rows(me, rows, gate_parts)
-    down_last = swap_fs(down_last)
-    down_last = down_last.reshape(-1, down_last.shape[2])
-    hidden = up_rows(rows, new_up, gate)
-
-    def add(parts):
-        return sum(part.astype(f32) for part in parts).astype(bf16)
-
-    def back_fs(value):
-        return swap_fs(value.reshape(fs, per_group, -1)).reshape(count, -1)
-
-    new_down, partial = down_rows(me, fs, hidden, rows, down_first, 0, width, None)
-    partial = rotate(partial, "tp", back=True)
-    back_first = back_fs(add(partial))
-    new_down, partial = down_rows(me, fs, hidden, rows, [down_last], first, width, new_down)
-    partial = rotate(partial, "tp", back=True)
-    back_last = back_fs(add(partial))
+    new_up, hidden = up_rows(rows, up_here, gate)
+    new_down = None
+    partials = []
+    for k, (low, _) in enumerate(cuts):
+        new_down, partial = down_rows(
+            me, fs, hidden, rows, down_parts[k], low, width, new_down
+        )
+        partials.append(rotate(partial, "tp", back=True))
+    backs = []
+    for members in returns:
+        summed = add(fs, [partials[m] for m in members])
+        backs += rotate(summed, "fs", back=True)
     mixed = pl.pallas_call(
         functools.partial(final_kernel, fs, tp),
+        in_specs=[in_smem] + [in_vmem] * (1 + len(backs)),
         out_shape=jax.ShapeDtypeStruct((count, width), bf16),
-        compiler_params=params(),
+        compiler_params=small,
         cost_estimate=cost(2 * count * count * width, 4 * count * width),
-    )(ids, back_first, back_last)
+    )(me, ids, *backs)
     return (mixed, new_gate[None], new_up[None], new_down[None])
 
 

time: 271 us -> 306 us (1.13)
  Pallas kernels: 22.5 us -> 52.2 us
  waiting for transfers between devices: 124 us -> 151 us
  local copies, waits for them, and re-layouts: 20.2 us -> 4.96 us
  starting transfers between devices: 98.5 us -> 94.8 us
  other arithmetic: 3.88 us -> 0.58 us
    ppermute x32 -> x70, waiting for transfers between devices: 107 us -> 151 us  [rotate(): lax.ppermute(parts[r], axis, [(k, (k + step) % n) for k in range(n)])]
    all_to_all x5 -> x1, starting transfers between devices: 31.7 us -> 5.81 us  [shards(): up_here = lax.all_to_all(up_here, 'fs', 0, 0, tiled=True)]
    ppermute x32 -> x70, starting transfers between devices: 66.8 us -> 89 us  [rotate(): lax.ppermute(parts[r], axis, [(k, (k + step) % n) for k in range(n)])]
    all_to_all x5 -> x1, waiting for transfers between devices: 17.2 us -> 0.01 us  [shards(): up_here = lax.all_to_all(up_here, 'fs', 0, 0, tiled=True)]
    unnamed x75 -> x86, local copies, waits for them, and re-layouts: 20.2 us -> 4.96 us
    pallas_call x3, Pallas kernels: 6.15 us -> 17.8 us  [cast_along(): pl.pallas_call(functools.partial(cast_kernel, steps, scale is not None, a...]
    pallas_call x1, Pallas kernels: 1.13 us -> 6.43 us  [merge(): pl.pallas_call(functools.partial(merge_kernel, tp), grid_spec=pltpu.Prefe...]
    pallas_call x3 -> x6, Pallas kernels: 3.31 us -> 8.23 us  [the longest x1 3.76 us: merge_down(): pl.pallas_call(functools.partial(merge_down_kernel, fs, tp, cuts), grid_s...]
  transfers between devices with their start and end apart: 37 -> 71, of which waited for: 12 -> 29; matrix products, arithmetic and copies ran while one was open for 1% -> 0% of each run, Pallas kernels for 7% -> 13%
where the time goes in v2:
time: 306 us; the launch traced here: 305 us
  waiting for transfers between devices  151 us (49%)
  starting transfers between devices  94.8 us (31%)
  Pallas kernels  52.2 us (17%)
  local copies, waits for them, and re-layouts  4.96 us (2%)
    ppermute x70, waiting for transfers between devices, rotate(): lax.ppermute(parts[r], axis, [(k, (k + step) % n) for k in range(n)])  151 us
    ppermute x70, starting transfers between devices, rotate(): lax.ppermute(parts[r], axis, [(k, (k + step) % n) for k in range(n)])  89 us
    pallas_call x3, Pallas kernels, cast_along(): pl.pallas_call(functools.partial(cast_kernel, steps, scale is not None, a...  17.8 us
    pallas_call x1, Pallas kernels, merge(): pl.pallas_call(functools.partial(merge_kernel, tp), grid_spec=pltpu.Prefe...  6.43 us
  transfers between devices with their start and end apart: 71, of which 29 were waited for; matrix products, arithmetic and copies ran while one was open for 0% of the time, Pallas kernels for 13%

profile of v2, /device:TPU:0, one launch (start us, length us, event | category | flops | bytes accessed | tf_op | source)
XLA Modules:
  0.0 304.7 jit_solution(16199398512888180988)
XLA Ops:
  1.2 5.3 %shard_map.104 = (bf16[8,256,128]{2,1,0:T(8,128)(2,1)}, bf16[8,256,128]{2,1,0:T(8,128)(2,1)}, bf16[8,256,128]{2,1,0:T(8,128)(2,1)}, bf16[8,256,128]{2,1,0:T(8,128)(2,1)}) custom-call(s32[2]{0:T(128)} %pad_add_fusion.me_ref, f32[8,4,256,128]{3,2,1,0:T(8,128)} %bitcast.15, f32[1,256]{1,0:T(1,128)} %bitcast.18), custom_call_target="tpu_custom_call" | custom-call | flops 1000000000 | bytes 6291456 | tf_op jit(solution)/shard_map/pallas_call | solution.py:156
  11.0 9.8 %collective-permute-done.10.refs_1_ = bf16[8,256,128]{2,1,0:T(8,128)(2,1)S(1)} collective-permute-done((bf16[8,256,128]{2,1,0:T(8,128)(2,1)}, bf16[8,256,128]{2,1,0:T(8,128)(2,1)S(1)}, u32[]{:S(2)}, u32[]{:S(2)}) %collective-permute-start.10) | collective-permute-done | bytes 524320 | tf_op jit(solution)/shard_map/ppermute | solution.py:405
  22.5 10.3 %collective-permute-done.12.refs_3_ = bf16[8,256,128]{2,1,0:T(8,128)(2,1)S(1)} collective-permute-done((bf16[8,256,128]{2,1,0:T(8,128)(2,1)}, bf16[8,256,128]{2,1,0:T(8,128)(2,1)S(1)}, u32[]{:S(2)}, u32[]{:S(2)}) %collective-permute-start.12) | collective-permute-done | bytes 524320 | tf_op jit(solution)/shard_map/ppermute | solution.py:405
  33.6 6.4 %shard_map.105 = bf16[8,256,512]{2,1,0:T(8,128)(2,1)} custom-call(s32[2]{0:T(128)} %pad_add_fusion.me_ref, bf16[8,256,128]{2,1,0:T(8,128)(2,1)} %get-tuple-element.99.refs_0_, bf16[8,256,128]{2,1,0:T(8,128)(2,1)} %copy-done.30, bf16[8,256,128]{2,1,0:T(8,128)(2,1)} %copy-done.31, bf16[8,256,128]{2,1,0:T(8,128)(2,1)} %copy-done.32), custom_call_target="tpu_custom_call" | custom-call | flops 1000000000 | bytes 4194304 | tf_op jit(solution)/shard_map/pallas_call | solution.py:186
  40.0 5.8 %all-to-all-start = ((bf16[8,256,512]{2,1,0:T(8,128)(2,1)}), bf16[8,256,512]{2,1,0:T(8,128)(2,1)}, u32[]{:S(2)}, u32[]{:S(2)}) async-start(bf16[8,256,512]{2,1,0:T(8,128)(2,1)} %shard_map.105), calls=%async_computation | async-start | bytes 4194304 | tf_op jit(solution)/shard_map/all_to_all | solution.py:428
  57.9 7.3 %shard_map.106 = (bf16[4,256,128]{2,1,0:T(8,128)(2,1)}, bf16[4,256,128]{2,1,0:T(8,128)(2,1)}, bf16[4,256,128]{2,1,0:T(8,128)(2,1)}, bf16[4,256,128]{2,1,0:T(8,12...) custom-call(s32[2]{0:T(128)} %pad_add_fusion.me_ref, ...), custom_call_target="tpu_custom_call" | custom-call | flops 1000000000 | bytes 6291456 | tf_op jit(solution)/shard_map/pallas_call | solution.py:156
  65.1 22.5 %collective-permute-done.refs_1_ = bf16[16,2176]{1,0:T(8,128)(2,1)S(1)} collective-permute-done((bf16[16,2176]{1,0:T(8,128)(2,1)}, bf16[16,2176]{1,0:T(8,128)(2,1)S(1)}, u32[]{:S(2)}, u32[]{:S(2)}) %collective-permute-start) | collective-permute-done | bytes 69664 | tf_op jit(solution)/shard_map/ppermute | solution.py:405
  87.7 5.2 %shard_map.110 = (bf16[8,64,512]{2,1,0:T(8,128)(2,1)}, bf16[8,64,512]{2,1,0:T(8,128)(2,1)}, bf16[8,64,512]{2,1,0:T(8,128)(2,1)}, bf16[8,64,512]{2,1,0:T(8,128)(2,1)}) custom-call(s32[2]{0:T(128)} %pad_add_fusion.me_ref, f32[8,4,64,512]{3,2,1,0:T(8,128)} %bitcast.17), custom_call_target="tpu_custom_call" | custom-call | flops 1000000000 | bytes 6291456 | tf_op jit(solution)/shard_map/pallas_call | solution.py:156
  92.9 16.5 %collective-permute-done.2.refs_3_ = bf16[16,2176]{1,0:T(8,128)(2,1)S(1)} collective-permute-done((bf16[16,2176]{1,0:T(8,128)(2,1)}, bf16[16,2176]{1,0:T(8,128)(2,1)S(1)}, u32[]{:S(2)}, u32[]{:S(2)}) %collective-permute-start.2) | collective-permute-done | bytes 69664 | tf_op jit(solution)/shard_map/ppermute | solution.py:405
  109.8 4.9 %collective-permute-done.5.refs_6_ = bf16[16,2176]{1,0:T(8,128)(2,1)S(1)} collective-permute-done((bf16[16,2176]{1,0:T(8,128)(2,1)S(1)}, bf16[16,2176]{1,0:T(8,128)(2,1)S(1)}, u32[]{:S(2)}, u32[]{:S(2)}) %collective-permute-start.5) | collective-permute-done | bytes 69664 | tf_op jit(solution)/shard_map/ppermute | solution.py:405
  114.7 2.9 collective-permute-start.6
  121.6 9.3 %collective-permute-done.14.refs_2_ = bf16[4,256,128]{2,1,0:T(8,128)(2,1)S(1)} collective-permute-done((bf16[4,256,128]{2,1,0:T(8,128)(2,1)}, bf16[4,256,128]{2,1,0:T(8,128)(2,1)S(1)}, u32[]{:S(2)}, u32[]{:S(2)}) %collective-permute-start.14) | collective-permute-done | bytes 262176 | tf_op jit(solution)/shard_map/ppermute | solution.py:405
  130.9 15.7 %collective-permute-done.15.refs_3_ = bf16[4,256,128]{2,1,0:T(8,128)(2,1)S(1)} collective-permute-done((bf16[4,256,128]{2,1,0:T(8,128)(2,1)}, bf16[4,256,128]{2,1,0:T(8,128)(2,1)S(1)}, u32[]{:S(2)}, u32[]{:S(2)}) %collective-permute-start.15) | collective-permute-done | bytes 262176 | tf_op jit(solution)/shard_map/ppermute | solution.py:405
  147.4 4.7 %collective-permute-start.19 = (bf16[4,256,128]{2,1,0:T(8,128)(2,1)}, bf16[4,256,128]{2,1,0:T(8,128)(2,1)}, u32[]{:S(2)}, u32[]{:S(2)}) collective-permute-start(bf16[4,256,128]{2,1,0:T(8,128)(2,1)} %get-tuple-element.110), channel_id=1, source_target_pairs={{0,28},{4,0},{8,4},{12,8},{16,12},{20,16},{24,20},{28,24},{1,29},{... | collective-permute-start | bytes 786440 | tf_op jit(solution)/shard_map/ppermute | solution.py:405
  152.1 3.8 %shard_map.111 = (bf16[64,1024]{1,0:T(8,128)(2,1)}, bf16[64,1024]{1,0:T(8,128)(2,1)}, bf16[64,1024]{1,0:T(8,128)(2,1)}, bf16[64,1024]{1,0:T(8,128)(2,1)}, bf16[6...) custom-call(s32[2]{0:T(128)} %pad_add_fusion.me_ref, ...), custom_call_target="tpu_custom_call" | custom-call | flops 1000000000 | bytes 4194304 | tf_op jit(solution)/shard_map/pallas_call | solution.py:216
  157.1 4.3 %collective-permute-done.17.refs_5_ = bf16[4,256,128]{2,1,0:T(8,128)(2,1)} collective-permute-done((bf16[4,256,128]{2,1,0:T(8,128)(2,1)}, bf16[4,256,128]{2,1,0:T(8,128)(2,1)}, u32[]{:S(2)}, u32[]{:S(2)}) %collective-permute-start.17) | collective-permute-done | bytes 262176 | tf_op jit(solution)/shard_map/ppermute | solution.py:405
  161.5 7.1 %collective-permute-done.18.refs_6_ = bf16[4,256,128]{2,1,0:T(8,128)(2,1)} collective-permute-done((bf16[4,256,128]{2,1,0:T(8,128)(2,1)}, bf16[4,256,128]{2,1,0:T(8,128)(2,1)}, u32[]{:S(2)}, u32[]{:S(2)}) %collective-permute-start.18) | collective-permute-done | bytes 262176 | tf_op jit(solution)/shard_map/ppermute | solution.py:405
  168.6 4.1 %collective-permute-done.19.refs_7_ = bf16[4,256,128]{2,1,0:T(8,128)(2,1)} collective-permute-done((bf16[4,256,128]{2,1,0:T(8,128)(2,1)}, bf16[4,256,128]{2,1,0:T(8,128)(2,1)}, u32[]{:S(2)}, u32[]{:S(2)}) %collective-permute-start.19) | collective-permute-done | bytes 262176 | tf_op jit(solution)/shard_map/ppermute | solution.py:405
  175.5 3.4 %collective-permute-start.40 = (bf16[64,512]{1,0:T(8,128)(2,1)}, bf16[64,512]{1,0:T(8,128)(2,1)S(1)}, u32[]{:S(2)}, u32[]{:S(2)}) collective-permute-start(bf16[64,512]{1,0:T(8,128)(2,1)} %get-tuple-element.138), channel_id=1, source_target_pairs={{0,20},{4,24},{8,28},{12,0},{16,4},{20,8},{24,12},{28,16},{1,21},{... | collective-permute-start | bytes 196616 | tf_op jit(solution)/shard_map/ppermute | solution.py:405
  183.7 3.1 %collective-permute-start.42 = (bf16[64,512]{1,0:T(8,128)(2,1)}, bf16[64,512]{1,0:T(8,128)(2,1)S(1)}, u32[]{:S(2)}, u32[]{:S(2)}) collective-permute-start(bf16[64,512]{1,0:T(8,128)(2,1)} %get-tuple-element.140), channel_id=1, source_target_pairs={{0,28},{4,0},{8,4},{12,8},{16,12},{20,16},{24,20},{28,24},{1,29},{... | collective-permute-start | bytes 196616 | tf_op jit(solution)/shard_map/ppermute | solution.py:405
  190.8 3.6 %shard_map.107 = (bf16[8,256,128]{2,1,0:T(8,128)(2,1)}, bf16[8,256,128]{2,1,0:T(8,128)(2,1)}, bf16[8,256,128]{2,1,0:T(8,128)(2,1)}, bf16[8,256,128]{2,1,0:T(8,128)(2,1)}) custom-call(s32[2]{0:T(128)} %pad_add_fusion.me_ref, bf16[4,256,128]{2,1,0:T(8,128)(2,1)} %get-tuple-element.103.refs_0_, bf16[4,256,128]{2,1,0:T(8,128)(2,1)} %copy-done.36, ...), custom_call_target="tpu_custom_call" | custom-call | flops 1000000000 | bytes 4194304 | tf_op jit(solution)/shard_map/pallas_call | solution.py:241
  204.6 5.7 %collective-permute-done.26.refs_5_ = bf16[64,1024]{1,0:T(8,128)(2,1)S(1)} collective-permute-done((bf16[64,1024]{1,0:T(8,128)(2,1)}, bf16[64,1024]{1,0:T(8,128)(2,1)S(1)}, u32[]{:S(2)}, u32[]{:S(2)}) %collective-permute-start.26) | collective-permute-done | bytes 131104 | tf_op jit(solution)/shard_map/ppermute | solution.py:405
  210.8 3.9 %collective-permute-start.30 = (bf16[64,1024]{1,0:T(8,128)(2,1)}, bf16[64,1024]{1,0:T(8,128)(2,1)S(1)}, u32[]{:S(2)}, u32[]{:S(2)}) collective-permute-start(bf16[64,1024]{1,0:T(8,128)(2,1)} %get-tuple-element.126), channel_id=1, source_target_pairs={{0,20},{4,24},{8,28},{12,0},{16,4},{20,8},{24,12},{28,16},{1,21},{... | collective-permute-start | bytes 393224 | tf_op jit(solution)/shard_map/ppermute | solution.py:405
  214.8 7.5 %collective-permute-done.22.refs_7_ = bf16[8,256,128]{2,1,0:T(8,128)(2,1)S(1)} collective-permute-done((bf16[8,256,128]{2,1,0:T(8,128)(2,1)}, bf16[8,256,128]{2,1,0:T(8,128)(2,1)S(1)}, u32[]{:S(2)}, u32[]{:S(2)}) %collective-permute-start.22) | collective-permute-done | bytes 524320 | tf_op jit(solution)/shard_map/ppermute | solution.py:405
  222.4 3.8 %collective-permute-start.32 = (bf16[64,1024]{1,0:T(8,128)(2,1)}, bf16[64,1024]{1,0:T(8,128)(2,1)S(1)}, u32[]{:S(2)}, u32[]{:S(2)}) collective-permute-start(bf16[64,1024]{1,0:T(8,128)(2,1)} %get-tuple-element.128), channel_id=1, source_target_pairs={{0,28},{4,0},{8,4},{12,8},{16,12},{20,16},{24,20},{28,24},{1,29},{... | collective-permute-start | bytes 393224 | tf_op jit(solution)/shard_map/ppermute | solution.py:405
  226.2 5.3 %shard_map.108 = (bf16[2048,512]{1,0:T(8,128)(2,1)}, f32[512,512]{1,0:T(8,128)}) custom-call(s32[2]{0:T(128)} %pad_add_fusion.me_ref, bf16[128,2176]{1,0:T(8,128)(2,1)} %copy-done, bf16[128,2176]{1,0:T(8,128)(2,1)} %copy-done.6, bf16[128,2176]{1,0:T(8,128)(2,1)} %copy-done.4, bf16[128,2176]{1,0:T(8,128)(2,1)} %copy-done.2, ...), custom_call_target="tpu_custom_call" | custom-call | flops 1073741824 | bytes 4194304 | tf_op jit(solution)/shard_map/pallas_call | solution.py:282
  231.7 5.5 %shard_map.109 = (bf16[2048,512]{1,0:T(8,128)(2,1)}, bf16[512,512]{1,0:T(8,128)(2,1)}) custom-call(bf16[128,2176]{1,0:T(8,128)(2,1)} %copy-done, bf16[128,2176]{1,0:T(8,128)(2,1)} %copy-done.6, bf16[128,2176]{1,0:T(8,128)(2,1)} %copy-done.4, bf16[128,2176]{1,0:T(8,128)(2,1)} %copy-done.2, bf16[2048,512]{1,0:T(8,128)(2,1)} %bitcast.6.refs_4_, ...), custom_call_target="tpu_custom_call" | custom-call | flops 1073741824 | bytes 4194304 | tf_op jit(solution)/shard_map/pallas_call | solution.py:306
  255.6 8.3 %collective-permute-done.61.refs_2_ = bf16[128,512]{1,0:T(8,128)(2,1)S(1)} collective-permute-done((bf16[128,512]{1,0:T(8,128)(2,1)S(1)}, bf16[128,512]{1,0:T(8,128)(2,1)S(1)}, u32[]{:S(2)}, u32[]{:S(2)}) %collective-permute-start.61) | collective-permute-done | bytes 131104 | tf_op jit(solution)/shard_map/ppermute | solution.py:405
  266.5 5.9 %collective-permute-done.44.refs_6_ = bf16[128,512]{1,0:T(8,128)(2,1)S(1)} collective-permute-done((bf16[128,512]{1,0:T(8,128)(2,1)S(1)}, bf16[128,512]{1,0:T(8,128)(2,1)S(1)}, u32[]{:S(2)}, u32[]{:S(2)}) %collective-permute-start.44) | collective-permute-done | bytes 131104 | tf_op jit(solution)/shard_map/ppermute | solution.py:405
  272.4 4.0 %collective-permute-start.63 = (bf16[16,512]{1,0:T(8,128)(2,1)S(1)}, bf16[16,512]{1,0:T(8,128)(2,1)S(1)}, u32[]{:S(2)}, u32[]{:S(2)}) collective-permute-start(bf16[16,512]{1,0:T(8,128)(2,1)S(1)} %get-tuple-element.168), channel_id=1, source_target_pairs={{0,28},{4,0},{8,4},{12,8},{16,12},{20,16},{24,20},{28,24},{1,29},{... | collective-permute-start | bytes 49160 | tf_op jit(solution)/shard_map/ppermute | solution.py:405
  293.0 3.1 %collective-permute-start.51 = (bf16[16,1536]{1,0:T(8,128)(2,1)S(1)}, bf16[16,1536]{1,0:T(8,128)(2,1)S(1)}, u32[]{:S(2)}, u32[]{:S(2)}) collective-permute-start(bf16[16,1536]{1,0:T(8,128)(2,1)S(1)} %get-tuple-element.152), channel_id=1, source_target_pairs={{0,8},{4,12},{8,16},{12,20},{16,24},{20,28},{24,0},{28,4},{1,9},{5... | collective-permute-start | bytes 147464 | tf_op jit(solution)/shard_map/ppermute | solution.py:405
  299.1 3.8 %collective-permute-done.52.refs_7_ = bf16[16,1536]{1,0:T(8,128)(2,1)S(1)} collective-permute-done((bf16[16,1536]{1,0:T(8,128)(2,1)S(1)}, bf16[16,1536]{1,0:T(8,128)(2,1)S(1)}, u32[]{:S(2)}, u32[]{:S(2)}) %collective-permute-start.52) | collective-permute-done | bytes 49184 | tf_op jit(solution)/shard_map/ppermute | solution.py:405
  (213 shorter events, 90.5 us)
Async XLA Ops:
  7.0 15.5 %collective-permute-start.11 = (bf16[8,256,128]{2,1,0:T(8,128)(2,1)}, bf16[8,256,128]{2,1,0:T(8,128)(2,1)S(1)}, u32[]{:S(2)}, u32[]{:S(2)}) collective-permute-start(bf16[8,256,128]{2,1,0:T(8,128)(2,1)} %get-tuple-element.101), channel_id=1, source_target_pairs={{0,2},{1,3},{2,0},{3,1},{4,6},{5,7},{6,4},{7,5},{8,10},{9,11},{10,... | collective-permute-start | bytes 1572872 | tf_op jit(solution)/shard_map/ppermute | solution.py:405
  9.5 23.3 %collective-permute-start.12 = (bf16[8,256,128]{2,1,0:T(8,128)(2,1)}, bf16[8,256,128]{2,1,0:T(8,128)(2,1)S(1)}, u32[]{:S(2)}, u32[]{:S(2)}) collective-permute-start(bf16[8,256,128]{2,1,0:T(8,128)(2,1)} %get-tuple-element.102), channel_id=1, source_target_pairs={{0,3},{1,0},{2,1},{3,2},{4,7},{5,4},{6,5},{7,6},{8,11},{9,8},{10,9... | collective-permute-start | bytes 1572872 | tf_op jit(solution)/shard_map/ppermute | solution.py:405
  40.0 191.6 %all-to-all-start = ((bf16[8,256,512]{2,1,0:T(8,128)(2,1)}), bf16[8,256,512]{2,1,0:T(8,128)(2,1)}, u32[]{:S(2)}, u32[]{:S(2)}) async-start(bf16[8,256,512]{2,1,0:T(8,128)(2,1)} %shard_map.105), calls=%async_computation | async-start | bytes 4194304 | tf_op jit(solution)/shard_map/all_to_all | solution.py:428
  48.2 39.5 %collective-permute-start = (bf16[16,2176]{1,0:T(8,128)(2,1)}, bf16[16,2176]{1,0:T(8,128)(2,1)S(1)}, u32[]{:S(2)}, u32[]{:S(2)}) collective-permute-start(bf16[16,2176]{1,0:T(8,128)(2,1)} %get-tuple-element.92), channel_id=1, source_target_pairs={{0,4},{4,8},{8,12},{12,16},{16,20},{20,24},{24,28},{28,0},{1,5},{5... | collective-permute-start | bytes 208904 | tf_op jit(solution)/shard_map/ppermute | solution.py:405
  50.2 42.7 %collective-permute-start.1 = (bf16[16,2176]{1,0:T(8,128)(2,1)}, bf16[16,2176]{1,0:T(8,128)(2,1)S(1)}, u32[]{:S(2)}, u32[]{:S(2)}) collective-permute-start(bf16[16,2176]{1,0:T(8,128)(2,1)} %get-tuple-element.93), channel_id=1, source_target_pairs={{0,8},{4,12},{8,16},{12,20},{16,24},{20,28},{24,0},{28,4},{1,9},{5... | collective-permute-start | bytes 208904 | tf_op jit(solution)/shard_map/ppermute | solution.py:405
  51.7 57.8 %collective-permute-start.2 = (bf16[16,2176]{1,0:T(8,128)(2,1)}, bf16[16,2176]{1,0:T(8,128)(2,1)S(1)}, u32[]{:S(2)}, u32[]{:S(2)}) collective-permute-start(bf16[16,2176]{1,0:T(8,128)(2,1)} %get-tuple-element.94), channel_id=1, source_target_pairs={{0,12},{4,16},{8,20},{12,24},{16,28},{20,0},{24,4},{28,8},{1,13},{... | collective-permute-start | bytes 208904 | tf_op jit(solution)/shard_map/ppermute | solution.py:405
  54.0 55.4 %collective-permute-start.3 = (bf16[16,2176]{1,0:T(8,128)(2,1)}, bf16[16,2176]{1,0:T(8,128)(2,1)S(1)}, u32[]{:S(2)}, u32[]{:S(2)}) collective-permute-start(bf16[16,2176]{1,0:T(8,128)(2,1)} %get-tuple-element.95), channel_id=1, source_target_pairs={{0,16},{4,20},{8,24},{12,28},{16,0},{20,4},{24,8},{28,12},{1,17},{... | collective-permute-start | bytes 208904 | tf_op jit(solution)/shard_map/ppermute | solution.py:405
  55.5 54.2 %collective-permute-start.4 = (bf16[16,2176]{1,0:T(8,128)(2,1)}, bf16[16,2176]{1,0:T(8,128)(2,1)S(1)}, u32[]{:S(2)}, u32[]{:S(2)}) collective-permute-start(bf16[16,2176]{1,0:T(8,128)(2,1)} %get-tuple-element.96), channel_id=1, source_target_pairs={{0,20},{4,24},{8,28},{12,0},{16,4},{20,8},{24,12},{28,16},{1,21},{... | collective-permute-start | bytes 208904 | tf_op jit(solution)/shard_map/ppermute | solution.py:405
  87.7 33.4 %collective-permute-start.13 = (bf16[4,256,128]{2,1,0:T(8,128)(2,1)}, bf16[4,256,128]{2,1,0:T(8,128)(2,1)S(1)}, u32[]{:S(2)}, u32[]{:S(2)}) collective-permute-start(bf16[4,256,128]{2,1,0:T(8,128)(2,1)} %get-tuple-element.104), channel_id=1, source_target_pairs={{0,4},{4,8},{8,12},{12,16},{16,20},{20,24},{24,28},{28,0},{1,5},{5... | collective-permute-start | bytes 786440 | tf_op jit(solution)/shard_map/ppermute | solution.py:405
  92.9 53.7 %collective-permute-start.23 = (bf16[8,64,512]{2,1,0:T(8,128)(2,1)}, bf16[8,64,512]{2,1,0:T(8,128)(2,1)S(1)}, u32[]{:S(2)}, u32[]{:S(2)}) collective-permute-start(bf16[8,64,512]{2,1,0:T(8,128)(2,1)} %get-tuple-element.118), channel_id=1, source_target_pairs={{0,1},{1,2},{2,3},{3,0},{4,5},{5,6},{6,7},{7,4},{8,9},{9,10},{10,1... | collective-permute-start | bytes 1572872 | tf_op jit(solution)/shard_map/ppermute | solution.py:405
  109.4 37.3 %collective-permute-start.24 = (bf16[8,64,512]{2,1,0:T(8,128)(2,1)}, bf16[8,64,512]{2,1,0:T(8,128)(2,1)S(1)}, u32[]{:S(2)}, u32[]{:S(2)}) collective-permute-start(bf16[8,64,512]{2,1,0:T(8,128)(2,1)} %get-tuple-element.119), channel_id=1, source_target_pairs={{0,2},{1,3},{2,0},{3,1},{4,6},{5,7},{6,4},{7,5},{8,10},{9,11},{10,... | collective-permute-start | bytes 1572872 | tf_op jit(solution)/shard_map/ppermute | solution.py:405
  109.5 37.4 %collective-permute-start.25 = (bf16[8,64,512]{2,1,0:T(8,128)(2,1)}, bf16[8,64,512]{2,1,0:T(8,128)(2,1)S(1)}, u32[]{:S(2)}, u32[]{:S(2)}) collective-permute-start(bf16[8,64,512]{2,1,0:T(8,128)(2,1)} %get-tuple-element.120), channel_id=1, source_target_pairs={{0,3},{1,0},{2,1},{3,2},{4,7},{5,4},{6,5},{7,6},{8,11},{9,8},{10,9... | collective-permute-start | bytes 1572872 | tf_op jit(solution)/shard_map/ppermute | solution.py:405
  121.0 25.6 %collective-permute-start.15 = (bf16[4,256,128]{2,1,0:T(8,128)(2,1)}, bf16[4,256,128]{2,1,0:T(8,128)(2,1)S(1)}, u32[]{:S(2)}, u32[]{:S(2)}) collective-permute-start(bf16[4,256,128]{2,1,0:T(8,128)(2,1)} %get-tuple-element.106), channel_id=1, source_target_pairs={{0,12},{4,16},{8,20},{12,24},{16,28},{20,0},{24,4},{28,8},{1,13},{... | collective-permute-start | bytes 786440 | tf_op jit(solution)/shard_map/ppermute | solution.py:405
  130.9 69.1 %collective-permute-start.9 = (bf16[128,2176]{1,0:T(8,128)(2,1)S(1)}, bf16[128,2176]{1,0:T(8,128)(2,1)S(1)}, u32[]{:S(2)}, u32[]{:S(2)}) collective-permute-start(bf16[128,2176]{1,0:T(8,128)(2,1)S(1)} %shard_map.103.refs_0_), channel_id=1, source_target_pairs={{0,3},{1,0},{2,1},{3,2},{4,7},{5,4},{6,5},{7,6},{8,11},{9,8},{10,9... | collective-permute-start | bytes 1671176 | tf_op jit(solution)/shard_map/ppermute | solution.py:405
  146.8 21.9 %collective-permute-start.18 = (bf16[4,256,128]{2,1,0:T(8,128)(2,1)}, bf16[4,256,128]{2,1,0:T(8,128)(2,1)}, u32[]{:S(2)}, u32[]{:S(2)}) collective-permute-start(bf16[4,256,128]{2,1,0:T(8,128)(2,1)} %get-tuple-element.109), channel_id=1, source_target_pairs={{0,24},{4,28},{8,0},{12,4},{16,8},{20,12},{24,16},{28,20},{1,25},{... | collective-permute-start | bytes 786440 | tf_op jit(solution)/shard_map/ppermute | solution.py:405
  147.4 25.4 %collective-permute-start.19 = (bf16[4,256,128]{2,1,0:T(8,128)(2,1)}, bf16[4,256,128]{2,1,0:T(8,128)(2,1)}, u32[]{:S(2)}, u32[]{:S(2)}) collective-permute-start(bf16[4,256,128]{2,1,0:T(8,128)(2,1)} %get-tuple-element.110), channel_id=1, source_target_pairs={{0,28},{4,0},{8,4},{12,8},{16,12},{20,16},{24,20},{28,24},{1,29},{... | collective-permute-start | bytes 786440 | tf_op jit(solution)/shard_map/ppermute | solution.py:405
  156.9 18.5 %collective-permute-start.36 = (bf16[64,512]{1,0:T(8,128)(2,1)}, bf16[64,512]{1,0:T(8,128)(2,1)S(1)}, u32[]{:S(2)}, u32[]{:S(2)}) collective-permute-start(bf16[64,512]{1,0:T(8,128)(2,1)} %get-tuple-element.134), channel_id=1, source_target_pairs={{0,4},{4,8},{8,12},{12,16},{16,20},{20,24},{24,28},{28,0},{1,5},{5... | collective-permute-start | bytes 196616 | tf_op jit(solution)/shard_map/ppermute | solution.py:405
  161.5 17.4 %collective-permute-start.37 = (bf16[64,512]{1,0:T(8,128)(2,1)}, bf16[64,512]{1,0:T(8,128)(2,1)S(1)}, u32[]{:S(2)}, u32[]{:S(2)}) collective-permute-start(bf16[64,512]{1,0:T(8,128)(2,1)} %get-tuple-element.135), channel_id=1, source_target_pairs={{0,8},{4,12},{8,16},{12,20},{16,24},{20,28},{24,0},{28,4},{1,9},{5... | collective-permute-start | bytes 196616 | tf_op jit(solution)/shard_map/ppermute | solution.py:405
  178.9 22.3 %collective-permute-start.8 = (bf16[128,2176]{1,0:T(8,128)(2,1)S(1)}, bf16[128,2176]{1,0:T(8,128)(2,1)S(1)}, u32[]{:S(2)}, u32[]{:S(2)}) collective-permute-start(bf16[128,2176]{1,0:T(8,128)(2,1)S(1)} %shard_map.103.refs_0_), channel_id=1, source_target_pairs={{0,2},{1,3},{2,0},{3,1},{4,6},{5,7},{6,4},{7,5},{8,10},{9,11},{10,... | collective-permute-start | bytes 1671176 | tf_op jit(solution)/shard_map/ppermute | solution.py:405
  180.7 21.6 %collective-permute-start.7 = (bf16[128,2176]{1,0:T(8,128)(2,1)S(1)}, bf16[128,2176]{1,0:T(8,128)(2,1)S(1)}, u32[]{:S(2)}, u32[]{:S(2)}) collective-permute-start(bf16[128,2176]{1,0:T(8,128)(2,1)S(1)} %shard_map.103.refs_0_), channel_id=1, source_target_pairs={{0,1},{1,2},{2,3},{3,0},{4,5},{5,6},{6,7},{7,4},{8,9},{9,10},{10,1... | collective-permute-start | bytes 1671176 | tf_op jit(solution)/shard_map/ppermute | solution.py:405
  197.7 17.0 %collective-permute-start.21 = (bf16[8,256,128]{2,1,0:T(8,128)(2,1)}, bf16[8,256,128]{2,1,0:T(8,128)(2,1)S(1)}, u32[]{:S(2)}, u32[]{:S(2)}) collective-permute-start(bf16[8,256,128]{2,1,0:T(8,128)(2,1)} %get-tuple-element.113), channel_id=1, source_target_pairs={{0,2},{1,3},{2,0},{3,1},{4,6},{5,7},{6,4},{7,5},{8,10},{9,11},{10,... | collective-permute-start | bytes 1572872 | tf_op jit(solution)/shard_map/ppermute | solution.py:405
  200.1 22.3 %collective-permute-start.22 = (bf16[8,256,128]{2,1,0:T(8,128)(2,1)}, bf16[8,256,128]{2,1,0:T(8,128)(2,1)S(1)}, u32[]{:S(2)}, u32[]{:S(2)}) collective-permute-start(bf16[8,256,128]{2,1,0:T(8,128)(2,1)} %get-tuple-element.114), channel_id=1, source_target_pairs={{0,3},{1,0},{2,1},{3,2},{4,7},{5,4},{6,5},{7,6},{8,11},{9,8},{10,9... | collective-permute-start | bytes 1572872 | tf_op jit(solution)/shard_map/ppermute | solution.py:405
  210.3 26.9 %collective-permute-start.28 = (bf16[64,1024]{1,0:T(8,128)(2,1)}, bf16[64,1024]{1,0:T(8,128)(2,1)S(1)}, u32[]{:S(2)}, u32[]{:S(2)}) collective-permute-start(bf16[64,1024]{1,0:T(8,128)(2,1)} %get-tuple-element.124), channel_id=1, source_target_pairs={{0,12},{4,16},{8,20},{12,24},{16,28},{20,0},{24,4},{28,8},{1,13},{... | collective-permute-start | bytes 393224 | tf_op jit(solution)/shard_map/ppermute | solution.py:405
  210.3 26.9 %collective-permute-start.29 = (bf16[64,1024]{1,0:T(8,128)(2,1)}, bf16[64,1024]{1,0:T(8,128)(2,1)S(1)}, u32[]{:S(2)}, u32[]{:S(2)}) collective-permute-start(bf16[64,1024]{1,0:T(8,128)(2,1)} %get-tuple-element.125), channel_id=1, source_target_pairs={{0,16},{4,20},{8,24},{12,28},{16,0},{20,4},{24,8},{28,12},{1,17},{... | collective-permute-start | bytes 393224 | tf_op jit(solution)/shard_map/ppermute | solution.py:405
  210.8 27.8 %collective-permute-start.30 = (bf16[64,1024]{1,0:T(8,128)(2,1)}, bf16[64,1024]{1,0:T(8,128)(2,1)S(1)}, u32[]{:S(2)}, u32[]{:S(2)}) collective-permute-start(bf16[64,1024]{1,0:T(8,128)(2,1)} %get-tuple-element.126), channel_id=1, source_target_pairs={{0,20},{4,24},{8,28},{12,0},{16,4},{20,8},{24,12},{28,16},{1,21},{... | collective-permute-start | bytes 393224 | tf_op jit(solution)/shard_map/ppermute | solution.py:405
  214.6 26.8 %collective-permute-start.31 = (bf16[64,1024]{1,0:T(8,128)(2,1)}, bf16[64,1024]{1,0:T(8,128)(2,1)S(1)}, u32[]{:S(2)}, u32[]{:S(2)}) collective-permute-start(bf16[64,1024]{1,0:T(8,128)(2,1)} %get-tuple-element.127), channel_id=1, source_target_pairs={{0,24},{4,28},{8,0},{12,4},{16,8},{20,12},{24,16},{28,20},{1,25},{... | collective-permute-start | bytes 393224 | tf_op jit(solution)/shard_map/ppermute | solution.py:405
  222.4 19.6 %collective-permute-start.32 = (bf16[64,1024]{1,0:T(8,128)(2,1)}, bf16[64,1024]{1,0:T(8,128)(2,1)S(1)}, u32[]{:S(2)}, u32[]{:S(2)}) collective-permute-start(bf16[64,1024]{1,0:T(8,128)(2,1)} %get-tuple-element.128), channel_id=1, source_target_pairs={{0,28},{4,0},{8,4},{12,8},{16,12},{20,16},{24,20},{28,24},{1,29},{... | collective-permute-start | bytes 393224 | tf_op jit(solution)/shard_map/ppermute | solution.py:405
  251.6 24.7 %collective-permute-start.33 = (bf16[128,1024]{1,0:T(8,128)(2,1)S(1)}, bf16[128,1024]{1,0:T(8,128)(2,1)S(1)}, u32[]{:S(2)}, u32[]{:S(2)}) collective-permute-start(bf16[128,1024]{1,0:T(8,128)(2,1)S(1)} %get-tuple-element.130), channel_id=1, source_target_pairs={{0,3},{1,0},{2,1},{3,2},{4,7},{5,4},{6,5},{7,6},{8,11},{9,8},{10,9... | collective-permute-start | bytes 786440 | tf_op jit(solution)/shard_map/ppermute | solution.py:405
  253.8 22.6 %collective-permute-start.34 = (bf16[128,1024]{1,0:T(8,128)(2,1)S(1)}, bf16[128,1024]{1,0:T(8,128)(2,1)S(1)}, u32[]{:S(2)}, u32[]{:S(2)}) collective-permute-start(bf16[128,1024]{1,0:T(8,128)(2,1)S(1)} %get-tuple-element.131), channel_id=1, source_target_pairs={{0,2},{1,3},{2,0},{3,1},{4,6},{5,7},{6,4},{7,5},{8,10},{9,11},{10,... | collective-permute-start | bytes 786440 | tf_op jit(solution)/shard_map/ppermute | solution.py:405
  255.5 20.8 %collective-permute-start.35 = (bf16[128,1024]{1,0:T(8,128)(2,1)S(1)}, bf16[128,1024]{1,0:T(8,128)(2,1)S(1)}, u32[]{:S(2)}, u32[]{:S(2)}) collective-permute-start(bf16[128,1024]{1,0:T(8,128)(2,1)S(1)} %get-tuple-element.132), channel_id=1, source_target_pairs={{0,1},{1,2},{2,3},{3,0},{4,5},{5,6},{6,7},{7,4},{8,9},{9,10},{10,1... | collective-permute-start | bytes 786440 | tf_op jit(solution)/shard_map/ppermute | solution.py:405
  276.6 16.4 %collective-permute-start.46 = (bf16[16,1536]{1,0:T(8,128)(2,1)S(1)}, bf16[16,1536]{1,0:T(8,128)(2,1)S(1)}, u32[]{:S(2)}, u32[]{:S(2)}) collective-permute-start(bf16[16,1536]{1,0:T(8,128)(2,1)S(1)} %get-tuple-element.147), channel_id=1, source_target_pairs={{0,28},{4,0},{8,4},{12,8},{16,12},{20,16},{24,20},{28,24},{1,29},{... | collective-permute-start | bytes 147464 | tf_op jit(solution)/shard_map/ppermute | solution.py:405
  278.4 17.7 %collective-permute-start.47 = (bf16[16,1536]{1,0:T(8,128)(2,1)S(1)}, bf16[16,1536]{1,0:T(8,128)(2,1)S(1)}, u32[]{:S(2)}, u32[]{:S(2)}) collective-permute-start(bf16[16,1536]{1,0:T(8,128)(2,1)S(1)} %get-tuple-element.148), channel_id=1, source_target_pairs={{0,24},{4,28},{8,0},{12,4},{16,8},{20,12},{24,16},{28,20},{1,25},{... | collective-permute-start | bytes 147464 | tf_op jit(solution)/shard_map/ppermute | solution.py:405
  (82 other events, 1054.7 us)

commit v3 on v2

--- a/solution.py
+++ b/solution.py
@@ -12,15 +12,22 @@
 lanes = 128
 bf16 = jnp.bfloat16
 f32 = jnp.float32
-small = pltpu.CompilerParams(vmem_limit_bytes=16 * 1024 * 1024)
 
 
 def cuts_of(width):
-    half, rest = width // 2, width // 2 + width // 4
+    half, rest = width // 2, width - width // 8
     return [(0, half), (half, rest), (rest, width)]
 
 
-returns = [(0, 1), (2,)]
+returns = [(0,), (1, 2)]
+
+
+def grant(mib):
+    return pltpu.CompilerParams(vmem_limit_bytes=mib * 1024 * 1024)
+
+
+def far_first(n):
+    return sorted(range(1, n), key=lambda r: (abs(2 * r - n), r))
 
 
 def cost(flops, nbytes):
@@ -97,33 +104,36 @@
     return pl.pallas_call(
         join_kernel,
         out_shape=jax.ShapeDtypeStruct((each * len(parts), width), bf16),
-        compiler_params=small,
+        compiler_params=grant(16),
         cost_estimate=cost(1e9, 4 * len(parts) * parts[0].size),
     )(*parts)
 
 
-def add_kernel(fs, tp, *refs):
-    ins, outs = refs[:-fs], refs[-fs:]
-    each = outs[0].shape[0]
+def add_kernel(tp, me_ref, *refs):
+    ins, out_ref = refs[:-1], refs[-1]
+    fs, each, _ = out_ref.shape
     low = 0
     for k in range(0, len(ins), tp):
         total = sum(ref[...].astype(f32) for ref in ins[k : k + tp]).astype(bf16)
         high = low + total.shape[1]
         for r in range(fs):
-            outs[r][:, low:high] = total[r * each : (r + 1) * each]
+            out_ref[lax.rem(me_ref[0] - r + fs, fs), :, low:high] = total[r * each : (r + 1) * each]
         low = high
 
 
-def add(fs, groups):
+def add(me, fs, groups):
     tp = len(groups[0])
     count = groups[0][0].shape[0]
     width = sum(group[0].shape[1] for group in groups)
-    return pl.pallas_call(
-        functools.partial(add_kernel, fs, tp),
-        out_shape=[jax.ShapeDtypeStruct((count // fs, width), bf16)] * fs,
-        compiler_params=small,
+    terms = [part for group in groups for part in group]
+    return pl.pallas_call(
+        functools.partial(add_kernel, tp),
+        in_specs=[pl.BlockSpec(memory_space=pltpu.SMEM)]
+        + [pl.BlockSpec(memory_space=pltpu.VMEM)] * len(terms),
+        out_shape=jax.ShapeDtypeStruct((fs, count // fs, width), bf16),
+        compiler_params=grant(8),
         cost_estimate=cost(1e9, 2 * (tp + 1) * count * width),
-    )(*[part for group in groups for part in group])
+    )(me, *terms)
 
 
 def cast_kernel(steps, scaled, squeeze, me_ref, in_ref, *refs):
@@ -133,21 +143,28 @@
         value = value * to_col(refs[0][...])[None]
         refs = refs[1:]
     value = value.astype(bf16)
-    for r in range(steps):
-
-        @pl.when(step == r)
-        def _(r=r):
-            refs[r][...] = value
-
-
-def cast_along(me, matrix, scale, axis):
+    for k in range(steps):
+
+        @pl.when(step == k)
+        def _(k=k):
+            refs[k][...] = value
+
+
+def cast_along(me, matrix, scale, axis, distances, params):
     fs, tp, rows, cols = matrix.shape
-    steps = (fs, tp)[axis]
+    steps = len(distances)
+
+    def target(k, m):
+        ahead = jnp.int32(distances[0])
+        for j in range(1, steps):
+            ahead = jnp.where(k == j, jnp.int32(distances[j]), ahead)
+        return lax.rem(m[axis] + ahead, (fs, tp)[axis])
+
     if axis == 0:
-        in_spec = pl.BlockSpec((1, tp, rows, cols), lambda r, m: (lax.rem(m[0] + r, fs), 0, 0, 0))
+        in_spec = pl.BlockSpec((1, tp, rows, cols), lambda k, m: (target(k, m), 0, 0, 0))
         shape = (tp, rows, cols)
     else:
-        in_spec = pl.BlockSpec((fs, 1, rows, cols), lambda r, m: (0, lax.rem(m[1] + r, tp), 0, 0))
+        in_spec = pl.BlockSpec((fs, 1, rows, cols), lambda k, m: (0, target(k, m), 0, 0))
         shape = (fs, rows, cols)
     in_specs, args = [in_spec], [matrix]
     if scale is not None:
@@ -159,7 +176,8 @@
             num_scalar_prefetch=1, grid=(steps,), in_specs=in_specs, out_specs=[whole(shape)] * steps
         ),
         out_shape=[jax.ShapeDtypeStruct(shape, bf16)] * steps,
-        cost_estimate=cost(1e9, 6 * matrix.size),
+        compiler_params=params,
+        cost_estimate=cost(1e9, 6 * matrix.size * steps // (fs, tp)[axis]),
     )(me, *args)
 
 
@@ -171,32 +189,7 @@
             action([(value - j) % tp for j in range(tp)])
 
 
-def merge_kernel(tp, me_ref, *refs):
-    out_ref = refs[tp]
-
-    def store(order):
-        out_ref[0] = jnp.concatenate([refs[q][0] for q in order], axis=-1)
-
-    in_order(me_ref, tp, store)
-
-
-def merge(me, parts):
-    tp = len(parts)
-    fs, rows, cols = parts[0].shape
-    return pl.pallas_call(
-        functools.partial(merge_kernel, tp),
-        grid_spec=pltpu.PrefetchScalarGridSpec(
-            num_scalar_prefetch=1,
-            grid=(fs,),
-            in_specs=[pl.BlockSpec((1, rows, cols), lambda g, m: (g, 0, 0))] * tp,
-            out_specs=pl.BlockSpec((1, rows, tp * cols), lambda g, m: (g, 0, 0)),
-        ),
-        out_shape=jax.ShapeDtypeStruct((fs, rows, tp * cols), bf16),
-        cost_estimate=cost(1e9, 4 * tp * parts[0].size),
-    )(me, *parts)
-
-
-def merge_down_kernel(fs, tp, cuts, me_ref, *refs):
+def merge_kernel(fs, tp, cuts, me_ref, *refs):
     ins, outs = refs[:tp], refs[tp:]
 
     def store(order):
@@ -209,12 +202,12 @@
     in_order(me_ref, tp, store)
 
 
-def merge_down(me, parts, cuts):
+def merge(me, parts, cuts):
     tp = len(parts)
     fs, rows, _ = parts[0].shape
     shapes = [(rows, high - low) for low, high in cuts for _ in range(fs)]
     outs = pl.pallas_call(
-        functools.partial(merge_down_kernel, fs, tp, cuts),
+        functools.partial(merge_kernel, fs, tp, cuts),
         grid_spec=pltpu.PrefetchScalarGridSpec(
             num_scalar_prefetch=1,
             grid=(1,),
@@ -222,6 +215,7 @@
             out_specs=[whole(shape) for shape in shapes],
         ),
         out_shape=[jax.ShapeDtypeStruct(shape, bf16) for shape in shapes],
+        compiler_params=grant(16),
         cost_estimate=cost(1e9, 4 * tp * parts[0].size),
     )(me, *parts)
     return [outs[k * fs : (k + 1) * fs] for k in range(len(cuts))]
@@ -247,6 +241,7 @@
             out_specs=[whole(shape)] * tp,
         ),
         out_shape=[jax.ShapeDtypeStruct(shape, bf16)] * tp,
+        compiler_params=grant(16),
         cost_estimate=cost(1e9, 4 * fs * parts[0].size),
     )(me, *parts)
 
@@ -289,48 +284,57 @@
             scratch_shapes=[pltpu.VMEM((out[0], matrix[0]), bf16)],
         ),
         out_shape=[jax.ShapeDtypeStruct(matrix, bf16), jax.ShapeDtypeStruct(out, f32)],
+        compiler_params=grant(24),
         cost_estimate=cost(2 * out[0] * matrix[0] * matrix[1], 4 * matrix[0] * matrix[1]),
     )(me, *rows, *parts)
 
 
-def up_kernel(tp, *refs):
-    x_refs, (in_ref, gate_ref, matrix_ref, out_ref, rows_ref) = refs[:tp], refs[tp:]
-    matrix_ref[...] = in_ref[...]
-    up = product_of(x_refs, in_ref, rows_ref)
+def assemble(me_ref, parts, matrix_ref):
+    fs, rows = len(parts), parts[0].shape[0]
+    for r in range(fs):
+        origin = lax.rem(me_ref[0] - r + fs, fs)
+        matrix_ref[pl.ds(pl.multiple_of(origin * rows, rows), rows), :] = parts[r][...]
+
+
+def up_kernel(fs, tp, me_ref, *refs):
+    x_refs, parts, refs = refs[:tp], refs[tp : tp + fs], refs[tp + fs :]
+    gate_ref, matrix_ref, out_ref, rows_ref = refs
+    assemble(me_ref, parts, matrix_ref)
+    up = product_of(x_refs, matrix_ref, rows_ref)
     gate = gate_ref[...]
     out_ref[...] = (gate / (1.0 + jnp.exp(-gate)) * up).astype(bf16)
 
 
-def up_rows(rows, matrix, gate):
-    tp = len(rows)
-    return pl.pallas_call(
-        functools.partial(up_kernel, tp),
-        grid=(1,),
-        in_specs=[whole(rows[0].shape)] * tp + [whole(matrix.shape), whole(gate.shape)],
-        out_specs=[whole(matrix.shape), whole(gate.shape)],
-        scratch_shapes=[pltpu.VMEM((gate.shape[0], matrix.shape[0]), bf16)],
-        out_shape=[
-            jax.ShapeDtypeStruct(matrix.shape, bf16),
-            jax.ShapeDtypeStruct(gate.shape, bf16),
-        ],
-        cost_estimate=cost(2 * gate.size * matrix.shape[0], 4 * matrix.size),
-    )(*rows, matrix, gate)
-
-
-def down_kernel(fs, tp, parts_count, aliased, me_ref, hidden_ref, *refs):
+def up_rows(me, rows, parts, gate):
+    tp, fs = len(rows), len(parts)
+    matrix = (fs * parts[0].shape[0], parts[0].shape[1])
+    return pl.pallas_call(
+        functools.partial(up_kernel, fs, tp),
+        grid_spec=pltpu.PrefetchScalarGridSpec(
+            num_scalar_prefetch=1,
+            grid=(1,),
+            in_specs=[whole(rows[0].shape)] * tp
+            + [whole(parts[0].shape)] * fs
+            + [whole(gate.shape)],
+            out_specs=[whole(matrix), whole(gate.shape)],
+            scratch_shapes=[pltpu.VMEM((gate.shape[0], matrix[0]), bf16)],
+        ),
+        out_shape=[jax.ShapeDtypeStruct(matrix, bf16), jax.ShapeDtypeStruct(gate.shape, bf16)],
+        compiler_params=grant(24),
+        cost_estimate=cost(2 * gate.size * matrix[0], 4 * matrix[0] * matrix[1]),
+    )(me, *rows, *parts, gate)
+
+
+def down_kernel(fs, tp, low, aliased, me_ref, hidden_ref, *refs):
     w_refs, refs = refs[:tp], refs[tp:]
-    parts, refs = refs[:parts_count], refs[parts_count:]
+    parts, refs = refs[:fs], refs[fs:]
     if aliased:
         refs = refs[1:]
-    matrix_ref, outs = refs[0], refs[1:]
-    if parts_count == 1:
-        matrix_ref[...] = parts[0][...]
-    else:
-        rows = parts[0].shape[0]
-        for r in range(fs):
-            origin = lax.rem(me_ref[0] - r + fs, fs)
-            matrix_ref[pl.ds(pl.multiple_of(origin * rows, rows), rows), :] = parts[r][...]
-    product = jnp.dot(hidden_ref[...], matrix_ref[...], preferred_element_type=f32)
+    matrix_ref, outs, block, done = refs[0], refs[1 : 1 + tp], refs[1 + tp], refs[2 + tp]
+    assemble(me_ref, parts, block)
+    copy = pltpu.make_async_copy(block, matrix_ref.at[:, pl.ds(low, block.shape[1])], done)
+    copy.start()
+    product = jnp.dot(hidden_ref[...], block[...], preferred_element_type=f32)
     product = product.astype(bf16).astype(f32)
     count = w_refs[0].shape[0]
     lane = lax.broadcasted_iota(jnp.int32, (count, lanes), 1)
@@ -341,14 +345,14 @@
             jnp.where(chosen, w_refs[q][...].astype(f32), 0.0), axis=1, keepdims=True
         )
         outs[q][...] = (product[q * count : (q + 1) * count] * weight).astype(bf16)
-
-
-def down_rows(me, fs, hidden, rows, parts, low, width, prior):
-    tp = len(rows)
+    copy.wait()
+
+
+def down_rows(me, hidden, rows, parts, low, width, prior):
+    tp, fs = len(rows), len(parts)
     count = rows[0].shape[0]
     depth = hidden.shape[1]
     size = parts[0].shape[1]
-    col_block = low // size
     weight_block = width // lanes
     in_specs = [whole(hidden.shape)]
     in_specs += [pl.BlockSpec((count, lanes), lambda k, m: (0, weight_block))] * tp
@@ -360,18 +364,18 @@
         args.append(prior)
         aliases = {len(args): 0}
     outs = pl.pallas_call(
-        functools.partial(down_kernel, fs, tp, len(parts), prior is not None),
+        functools.partial(down_kernel, fs, tp, low, prior is not None),
         grid_spec=pltpu.PrefetchScalarGridSpec(
             num_scalar_prefetch=1,
             grid=(1,),
             in_specs=in_specs,
-            out_specs=[pl.BlockSpec((depth, size), lambda k, m: (0, col_block))]
-            + [whole((count, size))] * tp,
+            out_specs=[pl.BlockSpec(memory_space=pl.ANY)] + [whole((count, size))] * tp,
+            scratch_shapes=[pltpu.VMEM((depth, size), bf16), pltpu.SemaphoreType.DMA],
         ),
         out_shape=[jax.ShapeDtypeStruct((depth, width), bf16)]
         + [jax.ShapeDtypeStruct((count, size), bf16)] * tp,
         input_output_aliases=aliases,
-        compiler_params=small,
+        compiler_params=grant(16),
         cost_estimate=cost(2 * tp * count * depth * size, 4 * depth * size),
     )(me, *args)
     return outs[0], outs[1:]
@@ -381,8 +385,8 @@
     ins, out_ref = refs[:-1], refs[-1]
     onehot = slot_onehot(group_of(ids_ref[0:1, :], fs, tp), me_ref[0], fs)
     low = 0
-    for k in range(0, len(ins), fs):
-        back = jnp.concatenate([ref[...] for ref in ins[k : k + fs]], axis=0)
+    for ref in ins:
+        back = jnp.concatenate([ref[lax.rem(me_ref[0] + r, fs)] for r in range(fs)], axis=0)
         high = low + back.shape[1]
         out_ref[:, low:high] = jnp.dot(onehot, back, preferred_element_type=f32).astype(bf16)
         low = high
@@ -397,12 +401,12 @@
     in_smem = pl.BlockSpec(memory_space=pltpu.SMEM)
     in_vmem = pl.BlockSpec(memory_space=pltpu.VMEM)
 
-    def rotate(parts, axis, back=False):
+    def rotate(parts, axis, back=False, distances=None):
         n = len(parts)
-        out = [parts[0]]
-        for r in range(1, n):
+        out = list(parts)
+        for r in distances or far_first(n):
             step = n - r if back else r
-            out.append(lax.ppermute(parts[r], axis, [(k, (k + step) % n) for k in range(n)]))
+            out[r] = lax.ppermute(parts[r], axis, [(k, (k + step) % n) for k in range(n)])
         return out
 
     def by_expert(matrix):
@@ -411,47 +415,50 @@
     ids, weights = expert_ids.T, route_weight.T
     scale = norm_gain[None, :]
 
-    gate_parts = cast_along(me, by_expert(gate_proj), scale, 0)
-    gate_parts = rotate(gate_parts, "fs")
-    up_parts = cast_along(me, by_expert(up_proj), scale, 1)
+    gate_parts = [None] * fs
+    early, late = far_first(fs)[:3], far_first(fs)[3:]
+    for k, distances in enumerate((early, late + [0])):
+        cut = cast_along(me, by_expert(gate_proj), scale, 0, distances, None if k == 0 else grant(16))
+        for r, part in zip(distances, cut):
+            gate_parts[r] = part
+        gate_parts = rotate(gate_parts, "fs", distances=[r for r in distances if r > 0])
+    up_parts = cast_along(me, by_expert(up_proj), scale, 1, range(tp), grant(16))
     up_parts = rotate(up_parts, "tp")
     sent = pl.pallas_call(
         functools.partial(prep_kernel, fs, tp),
         in_specs=[in_smem, in_vmem, in_vmem, in_vmem],
         out_shape=[jax.ShapeDtypeStruct((count // fs, width + lanes), bf16)] * fs,
+        compiler_params=grant(16),
         cost_estimate=cost(2 * count * count * width, 4 * count * width),
     )(me, tokens, ids, weights)
     landed = rotate(sent, "fs")
-    down_parts = cast_along(me, by_expert(down_proj), None, 1)
+    down_parts = cast_along(me, by_expert(down_proj), None, 1, range(tp), grant(16))
     down_parts = rotate(down_parts, "tp")
-    up_here = merge(me, up_parts)
-    up_here = lax.all_to_all(up_here, "fs", 0, 0, tiled=True)
-    up_here = up_here.reshape(-1, up_here.shape[2])
+    (up_parts,) = merge(me, up_parts, [(0, tp * up_parts[0].shape[2])])
+    up_parts = rotate(up_parts, "fs")
     gate_parts = regroup(me, gate_parts)
     gate_parts = rotate(gate_parts, "tp")
     landed = join(landed)
     rows = rotate([landed] * tp, "tp")
-    down_parts = merge_down(me, down_parts, cuts)
+    down_parts = merge(me, down_parts, cuts)
     for k in range(len(cuts)):
         down_parts[k] = rotate(down_parts[k], "fs")
     new_gate, gate = gate_rows(me, rows, gate_parts)
-    new_up, hidden = up_rows(rows, up_here, gate)
+    new_up, hidden = up_rows(me, rows, up_parts, gate)
     new_down = None
     partials = []
     for k, (low, _) in enumerate(cuts):
-        new_down, partial = down_rows(
-            me, fs, hidden, rows, down_parts[k], low, width, new_down
-        )
+        new_down, partial = down_rows(me, hidden, rows, down_parts[k], low, width, new_down)
         partials.append(rotate(partial, "tp", back=True))
     backs = []
     for members in returns:
-        summed = add(fs, [partials[m] for m in members])
-        backs += rotate(summed, "fs", back=True)
+        summed = add(me, fs, [partials[m] for m in members])
+        backs.append(lax.all_to_all(summed, "fs", 0, 0, tiled=True))
     mixed = pl.pallas_call(
         functools.partial(final_kernel, fs, tp),
         in_specs=[in_smem] + [in_vmem] * (1 + len(backs)),
         out_shape=jax.ShapeDtypeStruct((count, width), bf16),
-        compiler_params=small,
+        compiler_params=grant(16),
         cost_estimate=cost(2 * count * count * width, 4 * count * width),
     )(me, ids, *backs)
     return (mixed, new_gate[None], new_up[None], new_down[None])

time: 306 us -> 284 us (0.928)
  waiting for transfers between devices: 151 us -> 112 us
  starting transfers between devices: 94.8 us -> 128 us
  Pallas kernels: 52.2 us -> 26.2 us
  blocking collectives: 0 us -> 14.3 us
    ppermute x70 -> x63, waiting for transfers between devices: 151 us -> 112 us  [rotate(): lax.ppermute(parts[r], axis, [(k, (k + step) % n) for k in range(n)])]
    ppermute x70 -> x63, starting transfers between devices: 89 us -> 121 us  [rotate(): lax.ppermute(parts[r], axis, [(k, (k + step) % n) for k in range(n)])]
    all_to_all x0 -> x1, blocking collectives: none -> 14.3 us  [shards(): backs.append(lax.all_to_all(summed, 'fs', 0, 0, tiled=True))]
    pallas_call x8, Pallas kernels: 21.2 us -> 11.1 us  [the longest x3 5.2 us: down_rows(): pl.pallas_call(functools.partial(down_kernel, fs, tp, low, prior is not N...]
    pallas_call x3 -> x4, Pallas kernels: 17.8 us -> 8.58 us  [cast_along(): pl.pallas_call(functools.partial(cast_kernel, steps, scale is not None, a...]
  transfers between devices with their start and end apart: 71 -> 64, of which waited for: 29 -> 24; matrix products, arithmetic and copies ran while one was open for 0% -> 0% of each run, Pallas kernels for 13% -> 7%
where the time goes in v3:
time: 284 us
  starting transfers between devices  128 us (45%)
  waiting for transfers between devices  112 us (39%)
  Pallas kernels  26.2 us (9%)
  blocking collectives  14.3 us (5%)
    ppermute x63, starting transfers between devices, rotate(): lax.ppermute(parts[r], axis, [(k, (k + step) % n) for k in range(n)])  121 us
    ppermute x63, waiting for transfers between devices, rotate(): lax.ppermute(parts[r], axis, [(k, (k + step) % n) for k in range(n)])  112 us
    all_to_all x1, blocking collectives, shards(): backs.append(lax.all_to_all(summed, 'fs', 0, 0, tiled=True))  14.3 us
    pallas_call x4, Pallas kernels, cast_along(): pl.pallas_call(functools.partial(cast_kernel, steps, scale is not None, a...  8.58 us
    all_to_all x1, starting transfers between devices, shards(): backs.append(lax.all_to_all(summed, 'fs', 0, 0, tiled=True))  6.27 us
  transfers between devices with their start and end apart: 64, of which 24 were waited for; matrix products, arithmetic and copies ran while one was open for 0% of the time, Pallas kernels for 7%

profile of v3, /device:TPU:0, one launch (start us, length us, event | category | flops | bytes accessed | tf_op | source)
XLA Modules:
  0.0 283.9 jit_solution(6682773206802146449)
XLA Ops:
  1.2 4.1 %shard_map.107 = (bf16[4,256,128]{2,1,0:T(8,128)(2,1)}, bf16[4,256,128]{2,1,0:T(8,128)(2,1)}, bf16[4,256,128]{2,1,0:T(8,128)(2,1)}) custom-call(s32[2]{0:T(128)} %pad_add_fusion.me_ref, f32[8,4,256,128]{3,2,1,0:T(8,128)} %bitcast.11, f32[1,256]{1,0:T(1,128)} %bitcast.15), custom_call_target="tpu_custom_call" | custom-call | flops 1000000000 | bytes 2359296 | tf_op jit(solution)/shard_map/pallas_call | solution.py:173
  5.3 4.0 %collective-permute-start.22 = (bf16[4,256,128]{2,1,0:T(8,128)(2,1)}, bf16[4,256,128]{2,1,0:T(8,128)(2,1)S(1)}, u32[]{:S(2)}, u32[]{:S(2)}) collective-permute-start(bf16[4,256,128]{2,1,0:T(8,128)(2,1)} %get-tuple-element.106), channel_id=1, source_target_pairs={{0,12},{4,16},{8,20},{12,24},{16,28},{20,0},{24,4},{28,8},{1,13},{... | collective-permute-start | bytes 786440 | tf_op jit(solution)/shard_map/ppermute | solution.py:409
  13.9 3.4 %collective-permute-start.2 = (bf16[16,2176]{1,0:T(8,128)(2,1)S(1)}, bf16[16,2176]{1,0:T(8,128)(2,1)S(1)}, u32[]{:S(2)}, u32[]{:S(2)}) collective-permute-start(bf16[16,2176]{1,0:T(8,128)(2,1)S(1)} %get-tuple-element.86), channel_id=1, source_target_pairs={{0,12},{4,16},{8,20},{12,24},{16,28},{20,0},{24,4},{28,8},{1,13},{... | collective-permute-start | bytes 208904 | tf_op jit(solution)/shard_map/ppermute | solution.py:409
  17.3 3.2 %collective-permute-done.refs_1_ = bf16[16,2176]{1,0:T(8,128)(2,1)S(1)} collective-permute-done((bf16[16,2176]{1,0:T(8,128)(2,1)S(1)}, bf16[16,2176]{1,0:T(8,128)(2,1)S(1)}, u32[]{:S(2)}, u32[]{:S(2)}) %collective-permute-start) | collective-permute-done | bytes 69664 | tf_op jit(solution)/shard_map/ppermute | solution.py:409
  20.5 16.2 %collective-permute-start.3 = (bf16[16,2176]{1,0:T(8,128)(2,1)S(1)}, bf16[16,2176]{1,0:T(8,128)(2,1)S(1)}, u32[]{:S(2)}, u32[]{:S(2)}) collective-permute-start(bf16[16,2176]{1,0:T(8,128)(2,1)S(1)} %get-tuple-element.87), channel_id=1, source_target_pairs={{0,16},{4,20},{8,24},{12,28},{16,0},{20,4},{24,8},{28,12},{1,17},{... | collective-permute-start | bytes 208904 | tf_op jit(solution)/shard_map/ppermute | solution.py:409
  38.2 3.8 %collective-permute-done.2.refs_3_ = bf16[16,2176]{1,0:T(8,128)(2,1)S(1)} collective-permute-done((bf16[16,2176]{1,0:T(8,128)(2,1)S(1)}, bf16[16,2176]{1,0:T(8,128)(2,1)S(1)}, u32[]{:S(2)}, u32[]{:S(2)}) %collective-permute-start.2) | collective-permute-done | bytes 69664 | tf_op jit(solution)/shard_map/ppermute | solution.py:409
  42.0 5.7 %collective-permute-start.5 = (bf16[16,2176]{1,0:T(8,128)(2,1)S(1)}, bf16[16,2176]{1,0:T(8,128)(2,1)S(1)}, u32[]{:S(2)}, u32[]{:S(2)}) collective-permute-start(bf16[16,2176]{1,0:T(8,128)(2,1)S(1)} %get-tuple-element.89), channel_id=1, source_target_pairs={{0,24},{4,28},{8,0},{12,4},{16,8},{20,12},{24,16},{28,20},{1,25},{... | collective-permute-start | bytes 208904 | tf_op jit(solution)/shard_map/ppermute | solution.py:409
  53.4 2.9 %collective-permute-start.21 = (bf16[4,256,128]{2,1,0:T(8,128)(2,1)S(1)}, bf16[4,256,128]{2,1,0:T(8,128)(2,1)S(1)}, u32[]{:S(2)}, u32[]{:S(2)}) collective-permute-start(bf16[4,256,128]{2,1,0:T(8,128)(2,1)S(1)} %get-tuple-element.105), channel_id=1, source_target_pairs={{0,8},{4,12},{8,16},{12,20},{16,24},{20,28},{24,0},{28,4},{1,9},{5... | collective-permute-start | bytes 786440 | tf_op jit(solution)/shard_map/ppermute | solution.py:409
  60.8 8.4 %collective-permute-done.24.refs_5_ = bf16[4,256,128]{2,1,0:T(8,128)(2,1)S(1)} collective-permute-done((bf16[4,256,128]{2,1,0:T(8,128)(2,1)}, bf16[4,256,128]{2,1,0:T(8,128)(2,1)S(1)}, u32[]{:S(2)}, u32[]{:S(2)}) %collective-permute-start.24) | collective-permute-done | bytes 262176 | tf_op jit(solution)/shard_map/ppermute | solution.py:409
  76.0 6.2 %collective-permute-done.26.refs_7_ = bf16[4,256,128]{2,1,0:T(8,128)(2,1)S(1)} collective-permute-done((bf16[4,256,128]{2,1,0:T(8,128)(2,1)S(1)}, bf16[4,256,128]{2,1,0:T(8,128)(2,1)S(1)}, u32[]{:S(2)}, u32[]{:S(2)}) %collective-permute-start.26) | collective-permute-done | bytes 262176 | tf_op jit(solution)/shard_map/ppermute | solution.py:409
  86.0 8.4 %collective-permute-done.32.refs_3_ = bf16[8,64,512]{2,1,0:T(8,128)(2,1)S(1)} collective-permute-done((bf16[8,64,512]{2,1,0:T(8,128)(2,1)S(1)}, bf16[8,64,512]{2,1,0:T(8,128)(2,1)S(1)}, u32[]{:S(2)}, u32[]{:S(2)}) %collective-permute-start.32) | collective-permute-done | bytes 524320 | tf_op jit(solution)/shard_map/ppermute | solution.py:409
  95.9 10.6 %collective-permute-done.11.refs_2_ = bf16[8,256,128]{2,1,0:T(8,128)(2,1)S(1)} collective-permute-done((bf16[8,256,128]{2,1,0:T(8,128)(2,1)S(1)}, bf16[8,256,128]{2,1,0:T(8,128)(2,1)S(1)}, u32[]{:S(2)}, u32[]{:S(2)}) %collective-permute-start.11) | collective-permute-done | bytes 524320 | tf_op jit(solution)/shard_map/ppermute | solution.py:409
  107.2 9.6 %collective-permute-done.12.refs_3_ = bf16[8,256,128]{2,1,0:T(8,128)(2,1)S(1)} collective-permute-done((bf16[8,256,128]{2,1,0:T(8,128)(2,1)S(1)}, bf16[8,256,128]{2,1,0:T(8,128)(2,1)S(1)}, u32[]{:S(2)}, u32[]{:S(2)}) %collective-permute-start.12) | collective-permute-done | bytes 524320 | tf_op jit(solution)/shard_map/ppermute | solution.py:409
  117.5 6.7 %collective-permute-done.44.refs_6_ = bf16[64,768]{1,0:T(8,128)(2,1)S(1)} collective-permute-done((bf16[64,768]{1,0:T(8,128)(2,1)S(1)}, bf16[64,768]{1,0:T(8,128)(2,1)S(1)}, u32[]{:S(2)}, u32[]{:S(2)}) %collective-permute-start.44) | collective-permute-done | bytes 98336 | tf_op jit(solution)/shard_map/ppermute | solution.py:409
  124.2 4.3 %collective-permute-done.9.refs_3_ = bf16[128,2176]{1,0:T(8,128)(2,1)S(1)} collective-permute-done((bf16[128,2176]{1,0:T(8,128)(2,1)S(1)}, bf16[128,2176]{1,0:T(8,128)(2,1)S(1)}, u32[]{:S(2)}, u32[]{:S(2)}) %collective-permute-start.9) | collective-permute-done | bytes 557088 | tf_op jit(solution)/shard_map/ppermute | solution.py:409
  129.2 6.2 %collective-permute-done.8.refs_2_ = bf16[128,2176]{1,0:T(8,128)(2,1)S(1)} collective-permute-done((bf16[128,2176]{1,0:T(8,128)(2,1)S(1)}, bf16[128,2176]{1,0:T(8,128)(2,1)S(1)}, u32[]{:S(2)}, u32[]{:S(2)}) %collective-permute-start.8) | collective-permute-done | bytes 557088 | tf_op jit(solution)/shard_map/ppermute | solution.py:409
  138.4 3.0 %collective-permute-start.37 = (bf16[64,1024]{1,0:T(8,128)(2,1)S(1)}, bf16[64,1024]{1,0:T(8,128)(2,1)S(1)}, u32[]{:S(2)}, u32[]{:S(2)}) collective-permute-start(bf16[64,1024]{1,0:T(8,128)(2,1)S(1)} %get-tuple-element.126), channel_id=1, source_target_pairs={{0,20},{4,24},{8,28},{12,0},{16,4},{20,8},{24,12},{28,16},{1,21},{... | collective-permute-start | bytes 393224 | tf_op jit(solution)/shard_map/ppermute | solution.py:409
  141.5 4.6 %collective-permute-done.36.refs_8_ = bf16[64,1024]{1,0:T(8,128)(2,1)S(1)} collective-permute-done((bf16[64,1024]{1,0:T(8,128)(2,1)S(1)}, bf16[64,1024]{1,0:T(8,128)(2,1)S(1)}, u32[]{:S(2)}, u32[]{:S(2)}) %collective-permute-start.36) | collective-permute-done | bytes 131104 | tf_op jit(solution)/shard_map/ppermute | solution.py:409
  146.7 7.7 %collective-permute-start.39 = (bf16[64,1024]{1,0:T(8,128)(2,1)S(1)}, bf16[64,1024]{1,0:T(8,128)(2,1)S(1)}, u32[]{:S(2)}, u32[]{:S(2)}) collective-permute-start(bf16[64,1024]{1,0:T(8,128)(2,1)S(1)} %get-tuple-element.128), channel_id=1, source_target_pairs={{0,28},{4,0},{8,4},{12,8},{16,12},{20,16},{24,20},{28,24},{1,29},{... | collective-permute-start | bytes 393224 | tf_op jit(solution)/shard_map/ppermute | solution.py:409
  159.7 5.0 %collective-permute-start.16 = (bf16[256,512]{1,0:T(8,128)(2,1)S(1)}, bf16[256,512]{1,0:T(8,128)(2,1)S(1)}, u32[]{:S(2)}, u32[]{:S(2)}) collective-permute-start(bf16[256,512]{1,0:T(8,128)(2,1)S(1)} %get-tuple-element.99), channel_id=1, source_target_pairs={{0,16},{4,20},{8,24},{12,28},{16,0},{20,4},{24,8},{28,12},{1,17},{... | collective-permute-start | bytes 786440 | tf_op jit(solution)/shard_map/ppermute | solution.py:409
  164.8 3.8 %collective-permute-start.17 = (bf16[256,512]{1,0:T(8,128)(2,1)S(1)}, bf16[256,512]{1,0:T(8,128)(2,1)S(1)}, u32[]{:S(2)}, u32[]{:S(2)}) collective-permute-start(bf16[256,512]{1,0:T(8,128)(2,1)S(1)} %get-tuple-element.100), channel_id=1, source_target_pairs={{0,20},{4,24},{8,28},{12,0},{16,4},{20,8},{24,12},{28,16},{1,21},{... | collective-permute-start | bytes 786440 | tf_op jit(solution)/shard_map/ppermute | solution.py:409
  168.5 2.9 %collective-permute-done.14.refs_6_ = bf16[256,512]{1,0:T(8,128)(2,1)S(1)} collective-permute-done((bf16[256,512]{1,0:T(8,128)(2,1)S(1)}, bf16[256,512]{1,0:T(8,128)(2,1)S(1)}, u32[]{:S(2)}, u32[]{:S(2)}) %collective-permute-start.14) | collective-permute-done | bytes 262176 | tf_op jit(solution)/shard_map/ppermute | solution.py:409
  172.6 3.0 %shard_map.109 = (bf16[2048,512]{1,0:T(8,128)(2,1)}, f32[512,512]{1,0:T(8,128)S(1)}) custom-call(s32[2]{0:T(128)S(1)} %copy-done.4, bf16[128,2176]{1,0:T(8,128)(2,1)S(1)} %shard_map.103.refs_0_, bf16[128,2176]{1,0:T(8,128)(2,1)S(1)} %collective-permute-done.7.refs_1_, bf16[128,2176]{1,0:T(8,128)(2,1)S(1)} %collective-permute-done.8.refs_2_, ...), custom_call_target="tpu_custom_call" | custom-call | flops 1073741824 | bytes 4194304 | tf_op jit(solution)/shard_map/pallas_call | solution.py:277
  175.6 12.8 %collective-permute-done.15.refs_7_ = bf16[256,512]{1,0:T(8,128)(2,1)S(1)} collective-permute-done((bf16[256,512]{1,0:T(8,128)(2,1)S(1)}, bf16[256,512]{1,0:T(8,128)(2,1)S(1)}, u32[]{:S(2)}, u32[]{:S(2)}) %collective-permute-start.15) | collective-permute-done | bytes 262176 | tf_op jit(solution)/shard_map/ppermute | solution.py:409
  188.4 8.5 %collective-permute-start.45 = (bf16[64,768]{1,0:T(8,128)(2,1)S(1)}, bf16[64,768]{1,0:T(8,128)(2,1)S(1)}, u32[]{:S(2)}, u32[]{:S(2)}) collective-permute-start(bf16[64,768]{1,0:T(8,128)(2,1)S(1)} %get-tuple-element.136), channel_id=1, source_target_pairs={{0,12},{4,16},{8,20},{12,24},{16,28},{20,0},{24,4},{28,8},{1,13},{... | collective-permute-start | bytes 294920 | tf_op jit(solution)/shard_map/ppermute | solution.py:409
  196.9 4.4 %collective-permute-start.47 = (bf16[64,768]{1,0:T(8,128)(2,1)S(1)}, bf16[64,768]{1,0:T(8,128)(2,1)S(1)}, u32[]{:S(2)}, u32[]{:S(2)}) collective-permute-start(bf16[64,768]{1,0:T(8,128)(2,1)S(1)} %get-tuple-element.138), channel_id=1, source_target_pairs={{0,20},{4,24},{8,28},{12,0},{16,4},{20,8},{24,12},{28,16},{1,21},{... | collective-permute-start | bytes 294920 | tf_op jit(solution)/shard_map/ppermute | solution.py:409
  201.3 10.1 %collective-permute-start.48 = (bf16[64,768]{1,0:T(8,128)(2,1)S(1)}, bf16[64,768]{1,0:T(8,128)(2,1)S(1)}, u32[]{:S(2)}, u32[]{:S(2)}) collective-permute-start(bf16[64,768]{1,0:T(8,128)(2,1)S(1)} %get-tuple-element.139), channel_id=1, source_target_pairs={{0,24},{4,28},{8,0},{12,4},{16,8},{20,12},{24,16},{28,20},{1,25},{... | collective-permute-start | bytes 294920 | tf_op jit(solution)/shard_map/ppermute | solution.py:409
  218.6 4.4 %collective-permute-start.54 = (bf16[64,256]{1,0:T(8,128)(2,1)S(1)}, bf16[64,256]{1,0:T(8,128)(2,1)S(1)}, u32[]{:S(2)}, u32[]{:S(2)}) collective-permute-start(bf16[64,256]{1,0:T(8,128)(2,1)S(1)} %get-tuple-element.148), channel_id=1, source_target_pairs={{0,8},{4,12},{8,16},{12,20},{16,24},{20,28},{24,0},{28,4},{1,9},{5... | collective-permute-start | bytes 98312 | tf_op jit(solution)/shard_map/ppermute | solution.py:409
  248.1 6.3 %all-to-all-start.1 = ((bf16[8,16,1024]{2,1,0:T(8,128)(2,1)}), bf16[8,16,1024]{2,1,0:T(8,128)(2,1)S(1)}, u32[]{:S(2)}, u32[]{:S(2)}) async-start(bf16[8,16,1024]{2,1,0:T(8,128)(2,1)} %shard_map.117), calls=%async_computation.1 | async-start | bytes 524288 | tf_op jit(solution)/shard_map/all_to_all | solution.py:456
  254.9 6.2 %collective-permute-done.40.refs_1_ = bf16[128,1024]{1,0:T(8,128)(2,1)S(1)} collective-permute-done((bf16[128,1024]{1,0:T(8,128)(2,1)S(1)}, bf16[128,1024]{1,0:T(8,128)(2,1)S(1)}, u32[]{:S(2)}, u32[]{:S(2)}) %collective-permute-start.40) | collective-permute-done | bytes 262176 | tf_op jit(solution)/shard_map/ppermute | solution.py:409
  261.0 5.4 %collective-permute-done.41.refs_2_ = bf16[128,1024]{1,0:T(8,128)(2,1)S(1)} collective-permute-done((bf16[128,1024]{1,0:T(8,128)(2,1)S(1)}, bf16[128,1024]{1,0:T(8,128)(2,1)S(1)}, u32[]{:S(2)}, u32[]{:S(2)}) %collective-permute-start.41) | collective-permute-done | bytes 262176 | tf_op jit(solution)/shard_map/ppermute | solution.py:409
  267.8 14.3 %all_to_all.10.refs_0_ = bf16[8,16,1024]{2,1,0:T(8,128)(2,1)S(1)} all-to-all(bf16[8,16,1024]{2,1,0:T(8,128)(2,1)S(1)} %shard_map.114), channel_id=1, replica_groups=mesh['fs'=8,'tp'=4] {'fs'}, dimensions={0} | all-to-all | bytes 524288 | tf_op jit(solution)/shard_map/all_to_all | solution.py:456
  (131 shorter events, 76.9 us)
Async XLA Ops:
  5.3 50.9 %collective-permute-start.22 = (bf16[4,256,128]{2,1,0:T(8,128)(2,1)}, bf16[4,256,128]{2,1,0:T(8,128)(2,1)S(1)}, u32[]{:S(2)}, u32[]{:S(2)}) collective-permute-start(bf16[4,256,128]{2,1,0:T(8,128)(2,1)} %get-tuple-element.106), channel_id=1, source_target_pairs={{0,12},{4,16},{8,20},{12,24},{16,28},{20,0},{24,4},{28,8},{1,13},{... | collective-permute-start | bytes 786440 | tf_op jit(solution)/shard_map/ppermute | solution.py:409
  12.0 24.8 %collective-permute-start.1 = (bf16[16,2176]{1,0:T(8,128)(2,1)S(1)}, bf16[16,2176]{1,0:T(8,128)(2,1)S(1)}, u32[]{:S(2)}, u32[]{:S(2)}) collective-permute-start(bf16[16,2176]{1,0:T(8,128)(2,1)S(1)} %get-tuple-element.85), channel_id=1, source_target_pairs={{0,8},{4,12},{8,16},{12,20},{16,24},{20,28},{24,0},{28,4},{1,9},{5... | collective-permute-start | bytes 208904 | tf_op jit(solution)/shard_map/ppermute | solution.py:409
  13.6 45.4 %collective-permute-start.23 = (bf16[4,256,128]{2,1,0:T(8,128)(2,1)}, bf16[4,256,128]{2,1,0:T(8,128)(2,1)S(1)}, u32[]{:S(2)}, u32[]{:S(2)}) collective-permute-start(bf16[4,256,128]{2,1,0:T(8,128)(2,1)} %get-tuple-element.107), channel_id=1, source_target_pairs={{0,16},{4,20},{8,24},{12,28},{16,0},{20,4},{24,8},{28,12},{1,17},{... | collective-permute-start | bytes 786440 | tf_op jit(solution)/shard_map/ppermute | solution.py:409
  13.9 28.1 %collective-permute-start.2 = (bf16[16,2176]{1,0:T(8,128)(2,1)S(1)}, bf16[16,2176]{1,0:T(8,128)(2,1)S(1)}, u32[]{:S(2)}, u32[]{:S(2)}) collective-permute-start(bf16[16,2176]{1,0:T(8,128)(2,1)S(1)} %get-tuple-element.86), channel_id=1, source_target_pairs={{0,12},{4,16},{8,20},{12,24},{16,28},{20,0},{24,4},{28,8},{1,13},{... | collective-permute-start | bytes 208904 | tf_op jit(solution)/shard_map/ppermute | solution.py:409
  20.5 27.2 %collective-permute-start.3 = (bf16[16,2176]{1,0:T(8,128)(2,1)S(1)}, bf16[16,2176]{1,0:T(8,128)(2,1)S(1)}, u32[]{:S(2)}, u32[]{:S(2)}) collective-permute-start(bf16[16,2176]{1,0:T(8,128)(2,1)S(1)} %get-tuple-element.87), channel_id=1, source_target_pairs={{0,16},{4,20},{8,24},{12,28},{16,0},{20,4},{24,8},{28,12},{1,17},{... | collective-permute-start | bytes 208904 | tf_op jit(solution)/shard_map/ppermute | solution.py:409
  49.1 20.1 %collective-permute-start.24 = (bf16[4,256,128]{2,1,0:T(8,128)(2,1)}, bf16[4,256,128]{2,1,0:T(8,128)(2,1)S(1)}, u32[]{:S(2)}, u32[]{:S(2)}) collective-permute-start(bf16[4,256,128]{2,1,0:T(8,128)(2,1)} %get-tuple-element.108), channel_id=1, source_target_pairs={{0,20},{4,24},{8,28},{12,0},{16,4},{20,8},{24,12},{28,16},{1,21},{... | collective-permute-start | bytes 786440 | tf_op jit(solution)/shard_map/ppermute | solution.py:409
  52.7 16.6 %collective-permute-start.20 = (bf16[4,256,128]{2,1,0:T(8,128)(2,1)S(1)}, bf16[4,256,128]{2,1,0:T(8,128)(2,1)S(1)}, u32[]{:S(2)}, u32[]{:S(2)}) collective-permute-start(bf16[4,256,128]{2,1,0:T(8,128)(2,1)S(1)} %get-tuple-element.104), channel_id=1, source_target_pairs={{0,4},{4,8},{8,12},{12,16},{16,20},{20,24},{24,28},{28,0},{1,5},{5... | collective-permute-start | bytes 786440 | tf_op jit(solution)/shard_map/ppermute | solution.py:409
  53.4 17.4 %collective-permute-start.21 = (bf16[4,256,128]{2,1,0:T(8,128)(2,1)S(1)}, bf16[4,256,128]{2,1,0:T(8,128)(2,1)S(1)}, u32[]{:S(2)}, u32[]{:S(2)}) collective-permute-start(bf16[4,256,128]{2,1,0:T(8,128)(2,1)S(1)} %get-tuple-element.105), channel_id=1, source_target_pairs={{0,8},{4,12},{8,16},{12,20},{16,24},{20,28},{24,0},{28,4},{1,9},{5... | collective-permute-start | bytes 786440 | tf_op jit(solution)/shard_map/ppermute | solution.py:409
  56.2 17.7 %collective-permute-start.25 = (bf16[4,256,128]{2,1,0:T(8,128)(2,1)S(1)}, bf16[4,256,128]{2,1,0:T(8,128)(2,1)S(1)}, u32[]{:S(2)}, u32[]{:S(2)}) collective-permute-start(bf16[4,256,128]{2,1,0:T(8,128)(2,1)S(1)} %get-tuple-element.109), channel_id=1, source_target_pairs={{0,24},{4,28},{8,0},{12,4},{16,8},{20,12},{24,16},{28,20},{1,25},{... | collective-permute-start | bytes 786440 | tf_op jit(solution)/shard_map/ppermute | solution.py:409
  58.9 24.8 %collective-permute-start.10 = (bf16[8,256,128]{2,1,0:T(8,128)(2,1)S(1)}, bf16[8,256,128]{2,1,0:T(8,128)(2,1)S(1)}, u32[]{:S(2)}, u32[]{:S(2)}) collective-permute-start(bf16[8,256,128]{2,1,0:T(8,128)(2,1)S(1)} %get-tuple-element.92), channel_id=1, source_target_pairs={{0,1},{1,2},{2,3},{3,0},{4,5},{5,6},{6,7},{7,4},{8,9},{9,10},{10,1... | collective-permute-start | bytes 1572872 | tf_op jit(solution)/shard_map/ppermute | solution.py:409
  70.8 23.5 %collective-permute-start.32 = (bf16[8,64,512]{2,1,0:T(8,128)(2,1)S(1)}, bf16[8,64,512]{2,1,0:T(8,128)(2,1)S(1)}, u32[]{:S(2)}, u32[]{:S(2)}) collective-permute-start(bf16[8,64,512]{2,1,0:T(8,128)(2,1)S(1)} %get-tuple-element.120), channel_id=1, source_target_pairs={{0,3},{1,0},{2,1},{3,2},{4,7},{5,4},{6,5},{7,6},{8,11},{9,8},{10,9... | collective-permute-start | bytes 1572872 | tf_op jit(solution)/shard_map/ppermute | solution.py:409
  82.2 24.3 %collective-permute-start.11 = (bf16[8,256,128]{2,1,0:T(8,128)(2,1)S(1)}, bf16[8,256,128]{2,1,0:T(8,128)(2,1)S(1)}, u32[]{:S(2)}, u32[]{:S(2)}) collective-permute-start(bf16[8,256,128]{2,1,0:T(8,128)(2,1)S(1)} %get-tuple-element.93), channel_id=1, source_target_pairs={{0,2},{1,3},{2,0},{3,1},{4,6},{5,7},{6,4},{7,5},{8,10},{9,11},{10,... | collective-permute-start | bytes 1572872 | tf_op jit(solution)/shard_map/ppermute | solution.py:409
  83.7 33.1 %collective-permute-start.12 = (bf16[8,256,128]{2,1,0:T(8,128)(2,1)S(1)}, bf16[8,256,128]{2,1,0:T(8,128)(2,1)S(1)}, u32[]{:S(2)}, u32[]{:S(2)}) collective-permute-start(bf16[8,256,128]{2,1,0:T(8,128)(2,1)S(1)} %get-tuple-element.94), channel_id=1, source_target_pairs={{0,3},{1,0},{2,1},{3,2},{4,7},{5,4},{6,5},{7,6},{8,11},{9,8},{10,9... | collective-permute-start | bytes 1572872 | tf_op jit(solution)/shard_map/ppermute | solution.py:409
  83.8 44.7 %collective-permute-start.9 = (bf16[128,2176]{1,0:T(8,128)(2,1)S(1)}, bf16[128,2176]{1,0:T(8,128)(2,1)S(1)}, u32[]{:S(2)}, u32[]{:S(2)}) collective-permute-start(bf16[128,2176]{1,0:T(8,128)(2,1)S(1)} %shard_map.103.refs_0_), channel_id=1, source_target_pairs={{0,3},{1,0},{2,1},{3,2},{4,7},{5,4},{6,5},{7,6},{8,11},{9,8},{10,9... | collective-permute-start | bytes 1671176 | tf_op jit(solution)/shard_map/ppermute | solution.py:409
  84.4 51.0 %collective-permute-start.8 = (bf16[128,2176]{1,0:T(8,128)(2,1)S(1)}, bf16[128,2176]{1,0:T(8,128)(2,1)S(1)}, u32[]{:S(2)}, u32[]{:S(2)}) collective-permute-start(bf16[128,2176]{1,0:T(8,128)(2,1)S(1)} %shard_map.103.refs_0_), channel_id=1, source_target_pairs={{0,2},{1,3},{2,0},{3,1},{4,6},{5,7},{6,4},{7,5},{8,10},{9,11},{10,... | collective-permute-start | bytes 1671176 | tf_op jit(solution)/shard_map/ppermute | solution.py:409
  94.3 41.1 %collective-permute-start.7 = (bf16[128,2176]{1,0:T(8,128)(2,1)S(1)}, bf16[128,2176]{1,0:T(8,128)(2,1)S(1)}, u32[]{:S(2)}, u32[]{:S(2)}) collective-permute-start(bf16[128,2176]{1,0:T(8,128)(2,1)S(1)} %shard_map.103.refs_0_), channel_id=1, source_target_pairs={{0,1},{1,2},{2,3},{3,0},{4,5},{5,6},{6,7},{7,4},{8,9},{9,10},{10,1... | collective-permute-start | bytes 1671176 | tf_op jit(solution)/shard_map/ppermute | solution.py:409
  116.8 20.2 %collective-permute-start.33 = (bf16[64,1024]{1,0:T(8,128)(2,1)S(1)}, bf16[64,1024]{1,0:T(8,128)(2,1)S(1)}, u32[]{:S(2)}, u32[]{:S(2)}) collective-permute-start(bf16[64,1024]{1,0:T(8,128)(2,1)S(1)} %get-tuple-element.122), channel_id=1, source_target_pairs={{0,4},{4,8},{8,12},{12,16},{16,20},{20,24},{24,28},{28,0},{1,5},{5... | collective-permute-start | bytes 393224 | tf_op jit(solution)/shard_map/ppermute | solution.py:409
  135.4 24.3 %collective-permute-start.27 = (bf16[8,256,128]{2,1,0:T(8,128)(2,1)S(1)}, bf16[8,256,128]{2,1,0:T(8,128)(2,1)S(1)}, u32[]{:S(2)}, u32[]{:S(2)}) collective-permute-start(bf16[8,256,128]{2,1,0:T(8,128)(2,1)S(1)} %get-tuple-element.112), channel_id=1, source_target_pairs={{0,1},{1,2},{2,3},{3,0},{4,5},{5,6},{6,7},{7,4},{8,9},{9,10},{10,1... | collective-permute-start | bytes 1572872 | tf_op jit(solution)/shard_map/ppermute | solution.py:409
  135.4 24.3 %collective-permute-start.28 = (bf16[8,256,128]{2,1,0:T(8,128)(2,1)S(1)}, bf16[8,256,128]{2,1,0:T(8,128)(2,1)S(1)}, u32[]{:S(2)}, u32[]{:S(2)}) collective-permute-start(bf16[8,256,128]{2,1,0:T(8,128)(2,1)S(1)} %get-tuple-element.113), channel_id=1, source_target_pairs={{0,2},{1,3},{2,0},{3,1},{4,6},{5,7},{6,4},{7,5},{8,10},{9,11},{10,... | collective-permute-start | bytes 1572872 | tf_op jit(solution)/shard_map/ppermute | solution.py:409
  137.0 27.8 %collective-permute-start.29 = (bf16[8,256,128]{2,1,0:T(8,128)(2,1)S(1)}, bf16[8,256,128]{2,1,0:T(8,128)(2,1)S(1)}, u32[]{:S(2)}, u32[]{:S(2)}) collective-permute-start(bf16[8,256,128]{2,1,0:T(8,128)(2,1)S(1)} %get-tuple-element.114), channel_id=1, source_target_pairs={{0,3},{1,0},{2,1},{3,2},{4,7},{5,4},{6,5},{7,6},{8,11},{9,8},{10,9... | collective-permute-start | bytes 1572872 | tf_op jit(solution)/shard_map/ppermute | solution.py:409
  159.7 28.7 %collective-permute-start.15 = (bf16[256,512]{1,0:T(8,128)(2,1)S(1)}, bf16[256,512]{1,0:T(8,128)(2,1)S(1)}, u32[]{:S(2)}, u32[]{:S(2)}) collective-permute-start(bf16[256,512]{1,0:T(8,128)(2,1)S(1)} %get-tuple-element.98), channel_id=1, source_target_pairs={{0,12},{4,16},{8,20},{12,24},{16,28},{20,0},{24,4},{28,8},{1,13},{... | collective-permute-start | bytes 786440 | tf_op jit(solution)/shard_map/ppermute | solution.py:409
  159.7 37.2 %collective-permute-start.16 = (bf16[256,512]{1,0:T(8,128)(2,1)S(1)}, bf16[256,512]{1,0:T(8,128)(2,1)S(1)}, u32[]{:S(2)}, u32[]{:S(2)}) collective-permute-start(bf16[256,512]{1,0:T(8,128)(2,1)S(1)} %get-tuple-element.99), channel_id=1, source_target_pairs={{0,16},{4,20},{8,24},{12,28},{16,0},{20,4},{24,8},{28,12},{1,17},{... | collective-permute-start | bytes 786440 | tf_op jit(solution)/shard_map/ppermute | solution.py:409
  164.8 32.2 %collective-permute-start.17 = (bf16[256,512]{1,0:T(8,128)(2,1)S(1)}, bf16[256,512]{1,0:T(8,128)(2,1)S(1)}, u32[]{:S(2)}, u32[]{:S(2)}) collective-permute-start(bf16[256,512]{1,0:T(8,128)(2,1)S(1)} %get-tuple-element.100), channel_id=1, source_target_pairs={{0,20},{4,24},{8,28},{12,0},{16,4},{20,8},{24,12},{28,16},{1,21},{... | collective-permute-start | bytes 786440 | tf_op jit(solution)/shard_map/ppermute | solution.py:409
  168.5 32.8 %collective-permute-start.18 = (bf16[256,512]{1,0:T(8,128)(2,1)S(1)}, bf16[256,512]{1,0:T(8,128)(2,1)S(1)}, u32[]{:S(2)}, u32[]{:S(2)}) collective-permute-start(bf16[256,512]{1,0:T(8,128)(2,1)S(1)} %get-tuple-element.101), channel_id=1, source_target_pairs={{0,24},{4,28},{8,0},{12,4},{16,8},{20,12},{24,16},{28,20},{1,25},{... | collective-permute-start | bytes 786440 | tf_op jit(solution)/shard_map/ppermute | solution.py:409
  171.5 40.0 %collective-permute-start.19 = (bf16[256,512]{1,0:T(8,128)(2,1)S(1)}, bf16[256,512]{1,0:T(8,128)(2,1)S(1)}, u32[]{:S(2)}, u32[]{:S(2)}) collective-permute-start(bf16[256,512]{1,0:T(8,128)(2,1)S(1)} %get-tuple-element.102), channel_id=1, source_target_pairs={{0,28},{4,0},{8,4},{12,8},{16,12},{20,16},{24,20},{28,24},{1,29},{... | collective-permute-start | bytes 786440 | tf_op jit(solution)/shard_map/ppermute | solution.py:409
  188.4 28.8 %collective-permute-start.45 = (bf16[64,768]{1,0:T(8,128)(2,1)S(1)}, bf16[64,768]{1,0:T(8,128)(2,1)S(1)}, u32[]{:S(2)}, u32[]{:S(2)}) collective-permute-start(bf16[64,768]{1,0:T(8,128)(2,1)S(1)} %get-tuple-element.136), channel_id=1, source_target_pairs={{0,12},{4,16},{8,20},{12,24},{16,28},{20,0},{24,4},{28,8},{1,13},{... | collective-permute-start | bytes 294920 | tf_op jit(solution)/shard_map/ppermute | solution.py:409
  196.9 21.7 %collective-permute-start.46 = (bf16[64,768]{1,0:T(8,128)(2,1)S(1)}, bf16[64,768]{1,0:T(8,128)(2,1)S(1)}, u32[]{:S(2)}, u32[]{:S(2)}) collective-permute-start(bf16[64,768]{1,0:T(8,128)(2,1)S(1)} %get-tuple-element.137), channel_id=1, source_target_pairs={{0,16},{4,20},{8,24},{12,28},{16,0},{20,4},{24,8},{28,12},{1,17},{... | collective-permute-start | bytes 294920 | tf_op jit(solution)/shard_map/ppermute | solution.py:409
  196.9 26.1 %collective-permute-start.47 = (bf16[64,768]{1,0:T(8,128)(2,1)S(1)}, bf16[64,768]{1,0:T(8,128)(2,1)S(1)}, u32[]{:S(2)}, u32[]{:S(2)}) collective-permute-start(bf16[64,768]{1,0:T(8,128)(2,1)S(1)} %get-tuple-element.138), channel_id=1, source_target_pairs={{0,20},{4,24},{8,28},{12,0},{16,4},{20,8},{24,12},{28,16},{1,21},{... | collective-permute-start | bytes 294920 | tf_op jit(solution)/shard_map/ppermute | solution.py:409
  201.3 24.3 %collective-permute-start.48 = (bf16[64,768]{1,0:T(8,128)(2,1)S(1)}, bf16[64,768]{1,0:T(8,128)(2,1)S(1)}, u32[]{:S(2)}, u32[]{:S(2)}) collective-permute-start(bf16[64,768]{1,0:T(8,128)(2,1)S(1)} %get-tuple-element.139), channel_id=1, source_target_pairs={{0,24},{4,28},{8,0},{12,4},{16,8},{20,12},{24,16},{28,20},{1,25},{... | collective-permute-start | bytes 294920 | tf_op jit(solution)/shard_map/ppermute | solution.py:409
  229.9 16.8 %collective-permute-start.50 = (bf16[128,768]{1,0:T(8,128)(2,1)S(1)}, bf16[128,768]{1,0:T(8,128)(2,1)S(1)}, u32[]{:S(2)}, u32[]{:S(2)}) collective-permute-start(bf16[128,768]{1,0:T(8,128)(2,1)S(1)} %get-tuple-element.143), channel_id=1, source_target_pairs={{0,3},{1,0},{2,1},{3,2},{4,7},{5,4},{6,5},{7,6},{8,11},{9,8},{10,9... | collective-permute-start | bytes 589832 | tf_op jit(solution)/shard_map/ppermute | solution.py:409
  230.0 16.7 %collective-permute-start.51 = (bf16[128,768]{1,0:T(8,128)(2,1)S(1)}, bf16[128,768]{1,0:T(8,128)(2,1)S(1)}, u32[]{:S(2)}, u32[]{:S(2)}) collective-permute-start(bf16[128,768]{1,0:T(8,128)(2,1)S(1)} %get-tuple-element.144), channel_id=1, source_target_pairs={{0,2},{1,3},{2,0},{3,1},{4,6},{5,7},{6,4},{7,5},{8,10},{9,11},{10,... | collective-permute-start | bytes 589832 | tf_op jit(solution)/shard_map/ppermute | solution.py:409
  248.1 19.8 %all-to-all-start.1 = ((bf16[8,16,1024]{2,1,0:T(8,128)(2,1)}), bf16[8,16,1024]{2,1,0:T(8,128)(2,1)S(1)}, u32[]{:S(2)}, u32[]{:S(2)}) async-start(bf16[8,16,1024]{2,1,0:T(8,128)(2,1)} %shard_map.117), calls=%async_computation.1 | async-start | bytes 524288 | tf_op jit(solution)/shard_map/all_to_all | solution.py:456
  (40 other events, 400.6 us)

commit v4 on v3

--- a/solution.py
+++ b/solution.py
@@ -48,15 +48,13 @@
     return jnp.sum(jnp.where(down == across, row, jnp.zeros((), row.dtype)), axis=1, keepdims=True)
 
 
-def slot_onehot(group_row, me, fs):
+def slot_onehot(group_row, fs):
     count = group_row.shape[1]
     down, across = square(count)
     group_col = to_col(group_row)
     earlier = jnp.where((group_col == group_row) & (across < down), 1.0, 0.0)
-    rank = jnp.sum(earlier, axis=1, keepdims=True).astype(jnp.int32)
-    ahead = group_col.astype(jnp.int32) - me
-    ahead = jnp.where(ahead < 0, ahead + fs, ahead)
-    slot = ahead * (count // fs) + rank
+    rank = jnp.sum(earlier, axis=1, keepdims=True)
+    slot = (group_col * float(count // fs) + rank).astype(jnp.int32)
     return jnp.where(slot == across, 1.0, 0.0).astype(bf16)
 
 
@@ -67,10 +65,10 @@
     return group
 
 
-def prep_kernel(fs, tp, me_ref, tok_ref, ids_ref, weight_ref, *outs):
+def prep_kernel(fs, tp, tok_ref, ids_ref, weight_ref, out_ref):
     count, width = tok_ref.shape
     group = group_of(ids_ref[0:1, :], fs, tp)
-    onehot = slot_onehot(group, me_ref[0], fs)
+    onehot = slot_onehot(group, fs)
     wide = tok_ref[...].astype(f32)
     scale = lax.rsqrt(jnp.mean(wide * wide, axis=-1, keepdims=True) + norm_eps)
     normed = (wide * scale).astype(bf16)
@@ -87,29 +85,11 @@
     dims = (((0,), (0,)), ((), ()))
     rows = lax.dot_general(onehot, normed, dims, preferred_element_type=f32).astype(bf16)
     extra = lax.dot_general(onehot, extra.astype(bf16), dims, preferred_element_type=f32).astype(bf16)
-    each = count // fs
-    for r in range(fs):
-        outs[r][:, :width] = rows[r * each : (r + 1) * each]
-        outs[r][:, width:] = extra[r * each : (r + 1) * each]
-
-
-def join_kernel(*refs):
-    each = refs[0].shape[0]
-    for r, ref in enumerate(refs[:-1]):
-        refs[-1][r * each : (r + 1) * each, :] = ref[...]
-
-
-def join(parts):
-    each, width = parts[0].shape
-    return pl.pallas_call(
-        join_kernel,
-        out_shape=jax.ShapeDtypeStruct((each * len(parts), width), bf16),
-        compiler_params=grant(16),
-        cost_estimate=cost(1e9, 4 * len(parts) * parts[0].size),
-    )(*parts)
-
-
-def add_kernel(tp, me_ref, *refs):
+    out_ref[:, :width] = rows
+    out_ref[:, width:] = extra
+
+
+def add_kernel(tp, *refs):
     ins, out_ref = refs[:-1], refs[-1]
     fs, each, _ = out_ref.shape
     low = 0
@@ -117,23 +97,21 @@
         total = sum(ref[...].astype(f32) for ref in ins[k : k + tp]).astype(bf16)
         high = low + total.shape[1]
         for r in range(fs):
-            out_ref[lax.rem(me_ref[0] - r + fs, fs), :, low:high] = total[r * each : (r + 1) * each]
+            out_ref[r, :, low:high] = total[r * each : (r + 1) * each]
         low = high
 
 
-def add(me, fs, groups):
+def add(fs, groups):
     tp = len(groups[0])
     count = groups[0][0].shape[0]
     width = sum(group[0].shape[1] for group in groups)
     terms = [part for group in groups for part in group]
     return pl.pallas_call(
         functools.partial(add_kernel, tp),
-        in_specs=[pl.BlockSpec(memory_space=pltpu.SMEM)]
-        + [pl.BlockSpec(memory_space=pltpu.VMEM)] * len(terms),
         out_shape=jax.ShapeDtypeStruct((fs, count // fs, width), bf16),
         compiler_params=grant(8),
         cost_estimate=cost(1e9, 2 * (tp + 1) * count * width),
-    )(me, *terms)
+    )(*terms)
 
 
 def cast_kernel(steps, scaled, squeeze, me_ref, in_ref, *refs):
@@ -381,12 +359,12 @@
     return outs[0], outs[1:]
 
 
-def final_kernel(fs, tp, me_ref, ids_ref, *refs):
+def final_kernel(fs, tp, ids_ref, *refs):
     ins, out_ref = refs[:-1], refs[-1]
-    onehot = slot_onehot(group_of(ids_ref[0:1, :], fs, tp), me_ref[0], fs)
+    onehot = slot_onehot(group_of(ids_ref[0:1, :], fs, tp), fs)
     low = 0
     for ref in ins:
-        back = jnp.concatenate([ref[lax.rem(me_ref[0] + r, fs)] for r in range(fs)], axis=0)
+        back = jnp.concatenate([ref[g] for g in range(fs)], axis=0)
         high = low + back.shape[1]
         out_ref[:, low:high] = jnp.dot(onehot, back, preferred_element_type=f32).astype(bf16)
         low = high
@@ -398,15 +376,12 @@
     me = jnp.stack([lax.axis_index("fs"), lax.axis_index("tp")]).astype(jnp.int32)
     count, width = tokens.shape
     cuts = cuts_of(width)
-    in_smem = pl.BlockSpec(memory_space=pltpu.SMEM)
-    in_vmem = pl.BlockSpec(memory_space=pltpu.VMEM)
-
-    def rotate(parts, axis, back=False, distances=None):
+
+    def rotate(parts, axis, distances=None):
         n = len(parts)
         out = list(parts)
         for r in distances or far_first(n):
-            step = n - r if back else r
-            out[r] = lax.ppermute(parts[r], axis, [(k, (k + step) % n) for k in range(n)])
+            out[r] = lax.ppermute(parts[r], axis, [(k, (k + r) % n) for k in range(n)])
         return out
 
     def by_expert(matrix):
@@ -415,31 +390,41 @@
     ids, weights = expert_ids.T, route_weight.T
     scale = norm_gain[None, :]
 
+    sent = pl.pallas_call(
+        functools.partial(prep_kernel, fs, tp),
+        out_shape=jax.ShapeDtypeStruct((count, width + lanes), bf16),
+        cost_estimate=cost(2 * count * count * width, 4 * count * width),
+    )(tokens, ids, weights)
+    landed = lax.all_to_all(sent.reshape(fs, count // fs, -1), "fs", 0, 0, tiled=True)
+    landed = landed.reshape(count, -1)
     gate_parts = [None] * fs
     early, late = far_first(fs)[:3], far_first(fs)[3:]
-    for k, distances in enumerate((early, late + [0])):
-        cut = cast_along(me, by_expert(gate_proj), scale, 0, distances, None if k == 0 else grant(16))
+
+    def cut_gate(distances, params):
+        cut = cast_along(me, by_expert(gate_proj), scale, 0, distances, params)
         for r, part in zip(distances, cut):
             gate_parts[r] = part
-        gate_parts = rotate(gate_parts, "fs", distances=[r for r in distances if r > 0])
+        gate_parts[:] = rotate(gate_parts, "fs", distances=[r for r in distances if r > 0])
+
+    cut_gate(early, None)
     up_parts = cast_along(me, by_expert(up_proj), scale, 1, range(tp), grant(16))
     up_parts = rotate(up_parts, "tp")
-    sent = pl.pallas_call(
-        functools.partial(prep_kernel, fs, tp),
-        in_specs=[in_smem, in_vmem, in_vmem, in_vmem],
-        out_shape=[jax.ShapeDtypeStruct((count // fs, width + lanes), bf16)] * fs,
-        compiler_params=grant(16),
-        cost_estimate=cost(2 * count * count * width, 4 * count * width),
-    )(me, tokens, ids, weights)
-    landed = rotate(sent, "fs")
+    cut_gate(late + [0], grant(16))
     down_parts = cast_along(me, by_expert(down_proj), None, 1, range(tp), grant(16))
     down_parts = rotate(down_parts, "tp")
+    source = [
+        [((j ^ core) - step) % tp for j in range(tp)] for core in (0, 1) for step in range(0, tp, 2)
+    ]
+    rows = [landed] + [
+        lax.ppermute(landed, "tp", [(k, (k + step) % tp) for k in range(tp)])
+        for step in range(2, tp, 2)
+    ]
+    rows += [lax.ppermute(part, "tp", [(k, k ^ 1) for k in range(tp)]) for part in rows]
     (up_parts,) = merge(me, up_parts, [(0, tp * up_parts[0].shape[2])])
-    up_parts = rotate(up_parts, "fs")
+    for distances in (early, late):
+        up_parts = rotate(up_parts, "fs", distances)
     gate_parts = regroup(me, gate_parts)
     gate_parts = rotate(gate_parts, "tp")
-    landed = join(landed)
-    rows = rotate([landed] * tp, "tp")
     down_parts = merge(me, down_parts, cuts)
     for k in range(len(cuts)):
         down_parts[k] = rotate(down_parts[k], "fs")
@@ -449,18 +434,23 @@
     partials = []
     for k, (low, _) in enumerate(cuts):
         new_down, partial = down_rows(me, hidden, rows, down_parts[k], low, width, new_down)
-        partials.append(rotate(partial, "tp", back=True))
+        partials.append(
+            [partial[0]]
+            + [
+                lax.ppermute(term, "tp", list(enumerate(places)))
+                for term, places in zip(partial[1:], source[1:])
+            ]
+        )
     backs = []
     for members in returns:
-        summed = add(me, fs, [partials[m] for m in members])
+        summed = add(fs, [partials[m] for m in members])
         backs.append(lax.all_to_all(summed, "fs", 0, 0, tiled=True))
     mixed = pl.pallas_call(
         functools.partial(final_kernel, fs, tp),
-        in_specs=[in_smem] + [in_vmem] * (1 + len(backs)),
         out_shape=jax.ShapeDtypeStruct((count, width), bf16),
         compiler_params=grant(16),
         cost_estimate=cost(2 * count * count * width, 4 * count * width),
-    )(me, ids, *backs)
+    )(ids, *backs)
     return (mixed, new_gate[None], new_up[None], new_down[None])
 
 

time: 284 us -> 253 us (0.89)
  waiting for transfers between devices: 112 us -> 88.7 us
  starting transfers between devices: 128 us -> 105 us
  local copies, waits for them, and re-layouts: 2.58 us -> 12.6 us
    ppermute x63 -> x56, starting transfers between devices: 121 us -> 92.3 us  [the longest x44 83.8 us: rotate(): out[r] = lax.ppermute(parts[r], axis, [(k, (k + r) % n) for k in range(n)])]
    ppermute x63 -> x56, waiting for transfers between devices: 112 us -> 88.7 us  [the longest x44 71.9 us: rotate(): out[r] = lax.ppermute(parts[r], axis, [(k, (k + r) % n) for k in range(n)])]
    unnamed x16 -> x48, local copies, waits for them, and re-layouts: 2.58 us -> 12.6 us
    all_to_all x0 -> x1, starting transfers between devices: none -> 7.28 us  [shards(): lax.all_to_all(sent.reshape(fs, count // fs, -1), 'fs', 0, 0, tiled=True)]
  transfers between devices with their start and end apart: 64 -> 58, of which waited for: 24 -> 18; matrix products, arithmetic and copies ran while one was open for 0% -> 0% of each run, Pallas kernels for 7% -> 10%
where the time goes in v4:
time: 253 us; the launch traced here: 252 us
  starting transfers between devices  105 us (42%)
  waiting for transfers between devices  88.7 us (35%)
  Pallas kernels  28.7 us (11%)
  blocking collectives  15.4 us (6%)
  local copies, waits for them, and re-layouts  12.6 us (5%)
    ppermute x44, starting transfers between devices, rotate(): out[r] = lax.ppermute(parts[r], axis, [(k, (k + r) % n) for k in range(n)])  83.8 us
    ppermute x44, waiting for transfers between devices, rotate(): out[r] = lax.ppermute(parts[r], axis, [(k, (k + r) % n) for k in range(n)])  71.9 us
    ppermute x9, waiting for transfers between devices, shards(): lax.ppermute(term, 'tp', list(enumerate(places)))  16.8 us
    all_to_all x1, blocking collectives, shards(): backs.append(lax.all_to_all(summed, 'fs', 0, 0, tiled=True))  15.4 us
    unnamed x48, local copies, waits for them, and re-layouts  12.6 us
    pallas_call x4, Pallas kernels, cast_along(): pl.pallas_call(functools.partial(cast_kernel, steps, scale is not None, a...  10.4 us
    all_to_all x1, starting transfers between devices, shards(): lax.all_to_all(sent.reshape(fs, count // fs, -1), 'fs', 0, 0, tiled=True)  7.28 us
    ppermute x9, starting transfers between devices, shards(): lax.ppermute(term, 'tp', list(enumerate(places)))  7.05 us
  transfers between devices with their start and end apart: 58, of which 18 were waited for; matrix products, arithmetic and copies ran while one was open for 0% of the time, Pallas kernels for 10%

profile of v4, /device:TPU:0, one launch (start us, length us, event | category | flops | bytes accessed | tf_op | source)
XLA Modules:
  0.0 252.2 jit_solution(6644574418683369636)
XLA Ops:
  0.6 2.4 shard_map.102
  3.0 7.3 %all-to-all-start = ((bf16[8,16,2176]{2,1,0:T(8,128)(2,1)}), bf16[8,16,2176]{2,1,0:T(8,128)(2,1)S(1)}, u32[]{:S(2)}, u32[]{:S(2)}) async-start(bf16[8,16,2176]{2,1,0:T(8,128)(2,1)} %bitcast.30), calls=%async_computation | async-start | bytes 1114112 | tf_op jit(solution)/shard_map/all_to_all | solution.py:398
  10.9 4.1 %shard_map.106 = (bf16[4,256,128]{2,1,0:T(8,128)(2,1)}, bf16[4,256,128]{2,1,0:T(8,128)(2,1)}, bf16[4,256,128]{2,1,0:T(8,128)(2,1)}) custom-call(s32[2]{0:T(128)} %pad_add_fusion.me_ref, f32[8,4,256,128]{3,2,1,0:T(8,128)} %bitcast.20, f32[1,256]{1,0:T(1,128)} %bitcast.24), custom_call_target="tpu_custom_call" | custom-call | flops 1000000000 | bytes 2359296 | tf_op jit(solution)/shard_map/pallas_call | solution.py:151
  15.0 2.9 %collective-permute-start.15 = (bf16[4,256,128]{2,1,0:T(8,128)(2,1)}, bf16[4,256,128]{2,1,0:T(8,128)(2,1)S(1)}, u32[]{:S(2)}, u32[]{:S(2)}) collective-permute-start(bf16[4,256,128]{2,1,0:T(8,128)(2,1)} %get-tuple-element.90), channel_id=1, source_target_pairs={{0,12},{4,16},{8,20},{12,24},{16,28},{20,0},{24,4},{28,8},{1,13},{... | collective-permute-start | bytes 786440 | tf_op jit(solution)/shard_map/ppermute | solution.py:384
  30.3 19.5 %collective-permute-done.15.refs_3_ = bf16[4,256,128]{2,1,0:T(8,128)(2,1)S(1)} collective-permute-done((bf16[4,256,128]{2,1,0:T(8,128)(2,1)}, bf16[4,256,128]{2,1,0:T(8,128)(2,1)S(1)}, u32[]{:S(2)}, u32[]{:S(2)}) %collective-permute-start.15) | collective-permute-done | bytes 262176 | tf_op jit(solution)/shard_map/ppermute | solution.py:384
  52.8 3.8 %collective-permute-start.18 = (bf16[4,256,128]{2,1,0:T(8,128)(2,1)S(1)}, bf16[4,256,128]{2,1,0:T(8,128)(2,1)S(1)}, u32[]{:S(2)}, u32[]{:S(2)}) collective-permute-start(bf16[4,256,128]{2,1,0:T(8,128)(2,1)S(1)} %get-tuple-element.93), channel_id=1, source_target_pairs={{0,24},{4,28},{8,0},{12,4},{16,8},{20,12},{24,16},{28,20},{1,25},{... | collective-permute-start | bytes 786440 | tf_op jit(solution)/shard_map/ppermute | solution.py:384
  57.3 2.9 %shard_map.103 = (bf16[8,256,128]{2,1,0:T(8,128)(2,1)S(1)}, bf16[8,256,128]{2,1,0:T(8,128)(2,1)}, bf16[8,256,128]{2,1,0:T(8,128)(2,1)}, bf16[8,256,128]{2,1,0:T(8,128)(2,1)}) custom-call(s32[2]{0:T(128)S(1)} %copy-done.3, f32[8,4,256,128]{3,2,1,0:T(8,128)S(1)} %bitcast.22, f32[1,256]{1,0:T(1,128)S(1)} %bitcast.26), custom_call_target="tpu_custom_call" | custom-call | flops 1000000000 | bytes 6291456 | tf_op jit(solution)/shard_map/pallas_call | solution.py:151
  60.2 2.5 %collective-permute-done.14.refs_2_ = bf16[4,256,128]{2,1,0:T(8,128)(2,1)S(1)} collective-permute-done((bf16[4,256,128]{2,1,0:T(8,128)(2,1)S(1)}, bf16[4,256,128]{2,1,0:T(8,128)(2,1)S(1)}, u32[]{:S(2)}, u32[]{:S(2)}) %collective-permute-start.14) | collective-permute-done | bytes 262176 | tf_op jit(solution)/shard_map/ppermute | solution.py:384
  63.4 8.4 %collective-permute-done.18.refs_6_ = bf16[4,256,128]{2,1,0:T(8,128)(2,1)S(1)} collective-permute-done((bf16[4,256,128]{2,1,0:T(8,128)(2,1)S(1)}, bf16[4,256,128]{2,1,0:T(8,128)(2,1)S(1)}, u32[]{:S(2)}, u32[]{:S(2)}) %collective-permute-start.18) | collective-permute-done | bytes 262176 | tf_op jit(solution)/shard_map/ppermute | solution.py:384
  90.0 5.0 %collective-permute-done.5.refs_3_ = bf16[8,256,128]{2,1,0:T(8,128)(2,1)S(1)} collective-permute-done((bf16[8,256,128]{2,1,0:T(8,128)(2,1)}, bf16[8,256,128]{2,1,0:T(8,128)(2,1)S(1)}, u32[]{:S(2)}, u32[]{:S(2)}) %collective-permute-start.5) | collective-permute-done | bytes 524320 | tf_op jit(solution)/shard_map/ppermute | solution.py:384
  95.0 5.0 %collective-permute-start.27 = (bf16[64,1024]{1,0:T(8,128)(2,1)S(1)}, bf16[64,1024]{1,0:T(8,128)(2,1)S(1)}, u32[]{:S(2)}, u32[]{:S(2)}) collective-permute-start(bf16[64,1024]{1,0:T(8,128)(2,1)S(1)} %get-tuple-element.107), channel_id=1, source_target_pairs={{0,8},{4,12},{8,16},{12,20},{16,24},{20,28},{24,0},{28,4},{1,9},{5... | collective-permute-start | bytes 393224 | tf_op jit(solution)/shard_map/ppermute | solution.py:384
  100.1 3.8 %collective-permute-start.30 = (bf16[64,1024]{1,0:T(8,128)(2,1)S(1)}, bf16[64,1024]{1,0:T(8,128)(2,1)S(1)}, u32[]{:S(2)}, u32[]{:S(2)}) collective-permute-start(bf16[64,1024]{1,0:T(8,128)(2,1)S(1)} %get-tuple-element.110), channel_id=1, source_target_pairs={{0,20},{4,24},{8,28},{12,0},{16,4},{20,8},{24,12},{28,16},{1,21},{... | collective-permute-start | bytes 393224 | tf_op jit(solution)/shard_map/ppermute | solution.py:384
  107.3 6.5 %collective-permute-done.28.refs_7_ = bf16[64,1024]{1,0:T(8,128)(2,1)S(1)} collective-permute-done((bf16[64,1024]{1,0:T(8,128)(2,1)S(1)}, bf16[64,1024]{1,0:T(8,128)(2,1)S(1)}, u32[]{:S(2)}, u32[]{:S(2)}) %collective-permute-start.28) | collective-permute-done | bytes 131104 | tf_op jit(solution)/shard_map/ppermute | solution.py:384
  114.6 2.6 %collective-permute-start.31 = (bf16[64,1024]{1,0:T(8,128)(2,1)S(1)}, bf16[64,1024]{1,0:T(8,128)(2,1)S(1)}, u32[]{:S(2)}, u32[]{:S(2)}) collective-permute-start(bf16[64,1024]{1,0:T(8,128)(2,1)S(1)} %get-tuple-element.111), channel_id=1, source_target_pairs={{0,24},{4,28},{8,0},{12,4},{16,8},{20,12},{24,16},{28,20},{1,25},{... | collective-permute-start | bytes 393224 | tf_op jit(solution)/shard_map/ppermute | solution.py:384
  117.2 3.2 %collective-permute-start.32 = (bf16[64,1024]{1,0:T(8,128)(2,1)S(1)}, bf16[64,1024]{1,0:T(8,128)(2,1)S(1)}, u32[]{:S(2)}, u32[]{:S(2)}) collective-permute-start(bf16[64,1024]{1,0:T(8,128)(2,1)S(1)} %get-tuple-element.112), channel_id=1, source_target_pairs={{0,28},{4,0},{8,4},{12,8},{16,12},{20,16},{24,20},{28,24},{1,29},{... | collective-permute-start | bytes 393224 | tf_op jit(solution)/shard_map/ppermute | solution.py:384
  121.7 2.8 %collective-permute-done.32.refs_11_ = bf16[64,1024]{1,0:T(8,128)(2,1)S(1)} collective-permute-done((bf16[64,1024]{1,0:T(8,128)(2,1)S(1)}, bf16[64,1024]{1,0:T(8,128)(2,1)S(1)}, u32[]{:S(2)}, u32[]{:S(2)}) %collective-permute-start.32) | collective-permute-done | bytes 131104 | tf_op jit(solution)/shard_map/ppermute | solution.py:384
  127.9 3.8 %collective-permute-done.22.refs_7_ = bf16[8,256,128]{2,1,0:T(8,128)(2,1)S(1)} collective-permute-done((bf16[8,256,128]{2,1,0:T(8,128)(2,1)S(1)}, bf16[8,256,128]{2,1,0:T(8,128)(2,1)S(1)}, u32[]{:S(2)}, u32[]{:S(2)}) %collective-permute-start.22) | collective-permute-done | bytes 524320 | tf_op jit(solution)/shard_map/ppermute | solution.py:384
  132.3 5.8 %collective-permute-done.6.refs_5_ = bf16[256,512]{1,0:T(8,128)(2,1)S(1)} collective-permute-done((bf16[256,512]{1,0:T(8,128)(2,1)S(1)}, bf16[256,512]{1,0:T(8,128)(2,1)S(1)}, u32[]{:S(2)}, u32[]{:S(2)}) %collective-permute-start.6) | collective-permute-done | bytes 262176 | tf_op jit(solution)/shard_map/ppermute | solution.py:384
  138.1 3.9 %collective-permute-start.10 = (bf16[256,512]{1,0:T(8,128)(2,1)S(1)}, bf16[256,512]{1,0:T(8,128)(2,1)S(1)}, u32[]{:S(2)}, u32[]{:S(2)}) collective-permute-start(bf16[256,512]{1,0:T(8,128)(2,1)S(1)} %get-tuple-element.84), channel_id=1, source_target_pairs={{0,20},{4,24},{8,28},{12,0},{16,4},{20,8},{24,12},{28,16},{1,21},{... | collective-permute-start | bytes 786440 | tf_op jit(solution)/shard_map/ppermute | solution.py:384
  144.2 3.0 %shard_map.108 = (bf16[2048,512]{1,0:T(8,128)(2,1)}, f32[512,512]{1,0:T(8,128)S(1)}) custom-call(s32[2]{0:T(128)S(1)} %copy-done.3, bf16[128,2176]{1,0:T(8,128)(2,1)S(1)} %bitcast.15, bf16[128,2176]{1,0:T(8,128)(2,1)S(1)} %collective-permute-done.refs_1_, bf16[128,2176]{1,0:T(8,128)(2,1)S(1)} %collective-permute-done.1.refs_2_, ...), custom_call_target="tpu_custom_call" | custom-call | flops 1073741824 | bytes 4194304 | tf_op jit(solution)/shard_map/pallas_call | solution.py:255
  147.2 12.1 %collective-permute-done.8.refs_7_ = bf16[256,512]{1,0:T(8,128)(2,1)S(1)} collective-permute-done((bf16[256,512]{1,0:T(8,128)(2,1)S(1)}, bf16[256,512]{1,0:T(8,128)(2,1)S(1)}, u32[]{:S(2)}, u32[]{:S(2)}) %collective-permute-start.8) | collective-permute-done | bytes 262176 | tf_op jit(solution)/shard_map/ppermute | solution.py:384
  159.3 10.3 %collective-permute-start.38 = (bf16[64,768]{1,0:T(8,128)(2,1)S(1)}, bf16[64,768]{1,0:T(8,128)(2,1)S(1)}, u32[]{:S(2)}, u32[]{:S(2)}) collective-permute-start(bf16[64,768]{1,0:T(8,128)(2,1)S(1)} %get-tuple-element.120), channel_id=1, source_target_pairs={{0,12},{4,16},{8,20},{12,24},{16,28},{20,0},{24,4},{28,8},{1,13},{... | collective-permute-start | bytes 294920 | tf_op jit(solution)/shard_map/ppermute | solution.py:384
  169.6 2.5 %collective-permute-start.40 = (bf16[64,768]{1,0:T(8,128)(2,1)S(1)}, bf16[64,768]{1,0:T(8,128)(2,1)S(1)}, u32[]{:S(2)}, u32[]{:S(2)}) collective-permute-start(bf16[64,768]{1,0:T(8,128)(2,1)S(1)} %get-tuple-element.122), channel_id=1, source_target_pairs={{0,20},{4,24},{8,28},{12,0},{16,4},{20,8},{24,12},{28,16},{1,21},{... | collective-permute-start | bytes 294920 | tf_op jit(solution)/shard_map/ppermute | solution.py:384
  172.2 12.0 %collective-permute-start.41 = (bf16[64,768]{1,0:T(8,128)(2,1)S(1)}, bf16[64,768]{1,0:T(8,128)(2,1)S(1)}, u32[]{:S(2)}, u32[]{:S(2)}) collective-permute-start(bf16[64,768]{1,0:T(8,128)(2,1)S(1)} %get-tuple-element.123), channel_id=1, source_target_pairs={{0,24},{4,28},{8,0},{12,4},{16,8},{20,12},{24,16},{28,20},{1,25},{... | collective-permute-start | bytes 294920 | tf_op jit(solution)/shard_map/ppermute | solution.py:384
  191.4 3.3 %collective-permute-start.49 = (bf16[64,256]{1,0:T(8,128)(2,1)S(1)}, bf16[64,256]{1,0:T(8,128)(2,1)S(1)}, u32[]{:S(2)}, u32[]{:S(2)}) collective-permute-start(bf16[64,256]{1,0:T(8,128)(2,1)S(1)} %get-tuple-element.134), channel_id=1, source_target_pairs={{0,16},{4,20},{8,24},{12,28},{16,0},{20,4},{24,8},{28,12},{1,17},{... | collective-permute-start | bytes 98312 | tf_op jit(solution)/shard_map/ppermute | solution.py:384
  196.7 2.7 %collective-permute-start.43 = (bf16[128,768]{1,0:T(8,128)(2,1)S(1)}, bf16[128,768]{1,0:T(8,128)(2,1)S(1)}, u32[]{:S(2)}, u32[]{:S(2)}) collective-permute-start(bf16[128,768]{1,0:T(8,128)(2,1)S(1)} %get-tuple-element.127), channel_id=1, source_target_pairs={{0,2},{1,3},{2,0},{3,1},{4,6},{5,7},{6,4},{7,5},{8,10},{9,11},{10,... | collective-permute-start | bytes 589832 | tf_op jit(solution)/shard_map/ppermute | solution.py:440
  199.7 2.9 %collective-permute-start.51 = (bf16[64,256]{1,0:T(8,128)(2,1)S(1)}, bf16[64,256]{1,0:T(8,128)(2,1)S(1)}, u32[]{:S(2)}, u32[]{:S(2)}) collective-permute-start(bf16[64,256]{1,0:T(8,128)(2,1)S(1)} %get-tuple-element.136), channel_id=1, source_target_pairs={{0,24},{4,28},{8,0},{12,4},{16,8},{20,12},{24,16},{28,20},{1,25},{... | collective-permute-start | bytes 98312 | tf_op jit(solution)/shard_map/ppermute | solution.py:384
  212.3 3.9 %collective-permute-done.55.refs_7_ = bf16[128,256]{1,0:T(8,128)(2,1)S(1)} collective-permute-done((bf16[128,256]{1,0:T(8,128)(2,1)S(1)}, bf16[128,256]{1,0:T(8,128)(2,1)S(1)}, u32[]{:S(2)}, u32[]{:S(2)}) %collective-permute-start.55) | collective-permute-done | bytes 65568 | tf_op jit(solution)/shard_map/ppermute | solution.py:440
  217.0 5.7 %all-to-all-start.2 = ((bf16[8,16,1024]{2,1,0:T(8,128)(2,1)}), bf16[8,16,1024]{2,1,0:T(8,128)(2,1)S(1)}, u32[]{:S(2)}, u32[]{:S(2)}) async-start(bf16[8,16,1024]{2,1,0:T(8,128)(2,1)} %shard_map.116), calls=%async_computation.2 | async-start | bytes 524288 | tf_op jit(solution)/shard_map/all_to_all | solution.py:447
  224.9 7.0 %collective-permute-done.33.refs_1_ = bf16[128,1024]{1,0:T(8,128)(2,1)S(1)} collective-permute-done((bf16[128,1024]{1,0:T(8,128)(2,1)S(1)}, bf16[128,1024]{1,0:T(8,128)(2,1)S(1)}, u32[]{:S(2)}, u32[]{:S(2)}) %collective-permute-start.33) | collective-permute-done | bytes 262176 | tf_op jit(solution)/shard_map/ppermute | solution.py:440
  231.9 3.5 %collective-permute-done.35.refs_3_ = bf16[128,1024]{1,0:T(8,128)(2,1)S(1)} collective-permute-done((bf16[128,1024]{1,0:T(8,128)(2,1)S(1)}, bf16[128,1024]{1,0:T(8,128)(2,1)S(1)}, u32[]{:S(2)}, u32[]{:S(2)}) %collective-permute-start.35) | collective-permute-done | bytes 262176 | tf_op jit(solution)/shard_map/ppermute | solution.py:440
  235.6 15.4 %all_to_all.15.refs_0_ = bf16[8,16,1024]{2,1,0:T(8,128)(2,1)S(1)} all-to-all(bf16[8,16,1024]{2,1,0:T(8,128)(2,1)S(1)} %shard_map.113), channel_id=1, replica_groups=mesh['fs'=8,'tp'=4] {'fs'}, dimensions={0} | all-to-all | bytes 524288 | tf_op jit(solution)/shard_map/all_to_all | solution.py:447
  (150 shorter events, 70.8 us)
Async XLA Ops:
  3.0 75.0 %all-to-all-start = ((bf16[8,16,2176]{2,1,0:T(8,128)(2,1)}), bf16[8,16,2176]{2,1,0:T(8,128)(2,1)S(1)}, u32[]{:S(2)}, u32[]{:S(2)}) async-start(bf16[8,16,2176]{2,1,0:T(8,128)(2,1)} %bitcast.30), calls=%async_computation | async-start | bytes 1114112 | tf_op jit(solution)/shard_map/all_to_all | solution.py:398
  15.0 34.9 %collective-permute-start.15 = (bf16[4,256,128]{2,1,0:T(8,128)(2,1)}, bf16[4,256,128]{2,1,0:T(8,128)(2,1)S(1)}, u32[]{:S(2)}, u32[]{:S(2)}) collective-permute-start(bf16[4,256,128]{2,1,0:T(8,128)(2,1)} %get-tuple-element.90), channel_id=1, source_target_pairs={{0,12},{4,16},{8,20},{12,24},{16,28},{20,0},{24,4},{28,8},{1,13},{... | collective-permute-start | bytes 786440 | tf_op jit(solution)/shard_map/ppermute | solution.py:384
  17.9 33.5 %collective-permute-start.16 = (bf16[4,256,128]{2,1,0:T(8,128)(2,1)}, bf16[4,256,128]{2,1,0:T(8,128)(2,1)S(1)}, u32[]{:S(2)}, u32[]{:S(2)}) collective-permute-start(bf16[4,256,128]{2,1,0:T(8,128)(2,1)} %get-tuple-element.91), channel_id=1, source_target_pairs={{0,16},{4,20},{8,24},{12,28},{16,0},{20,4},{24,8},{28,12},{1,17},{... | collective-permute-start | bytes 786440 | tf_op jit(solution)/shard_map/ppermute | solution.py:384
  20.3 31.8 %collective-permute-start.17 = (bf16[4,256,128]{2,1,0:T(8,128)(2,1)}, bf16[4,256,128]{2,1,0:T(8,128)(2,1)S(1)}, u32[]{:S(2)}, u32[]{:S(2)}) collective-permute-start(bf16[4,256,128]{2,1,0:T(8,128)(2,1)} %get-tuple-element.92), channel_id=1, source_target_pairs={{0,20},{4,24},{8,28},{12,0},{16,4},{20,8},{24,12},{28,16},{1,21},{... | collective-permute-start | bytes 786440 | tf_op jit(solution)/shard_map/ppermute | solution.py:384
  25.4 48.7 %collective-permute-start.23 = (bf16[8,64,512]{2,1,0:T(8,128)(2,1)S(1)}, bf16[8,64,512]{2,1,0:T(8,128)(2,1)S(1)}, u32[]{:S(2)}, u32[]{:S(2)}) collective-permute-start(bf16[8,64,512]{2,1,0:T(8,128)(2,1)S(1)} %get-tuple-element.102), channel_id=1, source_target_pairs={{0,1},{1,2},{2,3},{3,0},{4,5},{5,6},{6,7},{7,4},{8,9},{9,10},{10,1... | collective-permute-start | bytes 1572872 | tf_op jit(solution)/shard_map/ppermute | solution.py:384
  28.9 27.8 %collective-permute-start.13 = (bf16[4,256,128]{2,1,0:T(8,128)(2,1)S(1)}, bf16[4,256,128]{2,1,0:T(8,128)(2,1)S(1)}, u32[]{:S(2)}, u32[]{:S(2)}) collective-permute-start(bf16[4,256,128]{2,1,0:T(8,128)(2,1)S(1)} %get-tuple-element.88), channel_id=1, source_target_pairs={{0,4},{4,8},{8,12},{12,16},{16,20},{20,24},{24,28},{28,0},{1,5},{5... | collective-permute-start | bytes 786440 | tf_op jit(solution)/shard_map/ppermute | solution.py:384
  49.8 25.1 %collective-permute-start.24 = (bf16[8,64,512]{2,1,0:T(8,128)(2,1)S(1)}, bf16[8,64,512]{2,1,0:T(8,128)(2,1)S(1)}, u32[]{:S(2)}, u32[]{:S(2)}) collective-permute-start(bf16[8,64,512]{2,1,0:T(8,128)(2,1)S(1)} %get-tuple-element.103), channel_id=1, source_target_pairs={{0,2},{1,3},{2,0},{3,1},{4,6},{5,7},{6,4},{7,5},{8,10},{9,11},{10,... | collective-permute-start | bytes 1572872 | tf_op jit(solution)/shard_map/ppermute | solution.py:384
  52.8 19.1 %collective-permute-start.18 = (bf16[4,256,128]{2,1,0:T(8,128)(2,1)S(1)}, bf16[4,256,128]{2,1,0:T(8,128)(2,1)S(1)}, u32[]{:S(2)}, u32[]{:S(2)}) collective-permute-start(bf16[4,256,128]{2,1,0:T(8,128)(2,1)S(1)} %get-tuple-element.93), channel_id=1, source_target_pairs={{0,24},{4,28},{8,0},{12,4},{16,8},{20,12},{24,16},{28,20},{1,25},{... | collective-permute-start | bytes 786440 | tf_op jit(solution)/shard_map/ppermute | solution.py:384
  57.3 19.9 %collective-permute-start.25 = (bf16[8,64,512]{2,1,0:T(8,128)(2,1)S(1)}, bf16[8,64,512]{2,1,0:T(8,128)(2,1)S(1)}, u32[]{:S(2)}, u32[]{:S(2)}) collective-permute-start(bf16[8,64,512]{2,1,0:T(8,128)(2,1)S(1)} %get-tuple-element.104), channel_id=1, source_target_pairs={{0,3},{1,0},{2,1},{3,2},{4,7},{5,4},{6,5},{7,6},{8,11},{9,8},{10,9... | collective-permute-start | bytes 1572872 | tf_op jit(solution)/shard_map/ppermute | solution.py:384
  63.4 23.0 %collective-permute-start.3 = (bf16[8,256,128]{2,1,0:T(8,128)(2,1)}, bf16[8,256,128]{2,1,0:T(8,128)(2,1)S(1)}, u32[]{:S(2)}, u32[]{:S(2)}) collective-permute-start(bf16[8,256,128]{2,1,0:T(8,128)(2,1)} %get-tuple-element.76), channel_id=1, source_target_pairs={{0,1},{1,2},{2,3},{3,0},{4,5},{5,6},{6,7},{7,4},{8,9},{9,10},{10,1... | collective-permute-start | bytes 1572872 | tf_op jit(solution)/shard_map/ppermute | solution.py:384
  72.6 15.7 %collective-permute-start.4 = (bf16[8,256,128]{2,1,0:T(8,128)(2,1)}, bf16[8,256,128]{2,1,0:T(8,128)(2,1)S(1)}, u32[]{:S(2)}, u32[]{:S(2)}) collective-permute-start(bf16[8,256,128]{2,1,0:T(8,128)(2,1)} %get-tuple-element.77), channel_id=1, source_target_pairs={{0,2},{1,3},{2,0},{3,1},{4,6},{5,7},{6,4},{7,5},{8,10},{9,11},{10,... | collective-permute-start | bytes 1572872 | tf_op jit(solution)/shard_map/ppermute | solution.py:384
  74.9 20.1 %collective-permute-start.5 = (bf16[8,256,128]{2,1,0:T(8,128)(2,1)}, bf16[8,256,128]{2,1,0:T(8,128)(2,1)S(1)}, u32[]{:S(2)}, u32[]{:S(2)}) collective-permute-start(bf16[8,256,128]{2,1,0:T(8,128)(2,1)} %get-tuple-element.78), channel_id=1, source_target_pairs={{0,3},{1,0},{2,1},{3,2},{4,7},{5,4},{6,5},{7,6},{8,11},{9,8},{10,9... | collective-permute-start | bytes 1572872 | tf_op jit(solution)/shard_map/ppermute | solution.py:384
  78.0 43.6 %collective-permute-start = (bf16[128,2176]{1,0:T(8,128)(2,1)S(1)}, bf16[128,2176]{1,0:T(8,128)(2,1)S(1)}, u32[]{:S(2)}, u32[]{:S(2)}) collective-permute-start(bf16[128,2176]{1,0:T(8,128)(2,1)S(1)} %bitcast.13), channel_id=1, source_target_pairs={{0,2},{1,3},{2,0},{3,1},{4,6},{5,7},{6,4},{7,5},{8,10},{9,11},{10,... | collective-permute-start | bytes 1671176 | tf_op jit(solution)/shard_map/ppermute | solution.py:419
  84.7 15.2 %collective-permute-start.36 = (bf16[64,768]{1,0:T(8,128)(2,1)S(1)}, bf16[64,768]{1,0:T(8,128)(2,1)S(1)}, u32[]{:S(2)}, u32[]{:S(2)}) collective-permute-start(bf16[64,768]{1,0:T(8,128)(2,1)S(1)} %get-tuple-element.118), channel_id=1, source_target_pairs={{0,4},{4,8},{8,12},{12,16},{16,20},{20,24},{24,28},{28,0},{1,5},{5... | collective-permute-start | bytes 294920 | tf_op jit(solution)/shard_map/ppermute | solution.py:384
  100.0 14.6 %collective-permute-start.29 = (bf16[64,1024]{1,0:T(8,128)(2,1)S(1)}, bf16[64,1024]{1,0:T(8,128)(2,1)S(1)}, u32[]{:S(2)}, u32[]{:S(2)}) collective-permute-start(bf16[64,1024]{1,0:T(8,128)(2,1)S(1)} %get-tuple-element.109), channel_id=1, source_target_pairs={{0,16},{4,20},{8,24},{12,28},{16,0},{20,4},{24,8},{28,12},{1,17},{... | collective-permute-start | bytes 393224 | tf_op jit(solution)/shard_map/ppermute | solution.py:384
  100.1 17.1 %collective-permute-start.30 = (bf16[64,1024]{1,0:T(8,128)(2,1)S(1)}, bf16[64,1024]{1,0:T(8,128)(2,1)S(1)}, u32[]{:S(2)}, u32[]{:S(2)}) collective-permute-start(bf16[64,1024]{1,0:T(8,128)(2,1)S(1)} %get-tuple-element.110), channel_id=1, source_target_pairs={{0,20},{4,24},{8,28},{12,0},{16,4},{20,8},{24,12},{28,16},{1,21},{... | collective-permute-start | bytes 393224 | tf_op jit(solution)/shard_map/ppermute | solution.py:384
  105.5 20.1 %collective-permute-start.20 = (bf16[8,256,128]{2,1,0:T(8,128)(2,1)S(1)}, bf16[8,256,128]{2,1,0:T(8,128)(2,1)S(1)}, u32[]{:S(2)}, u32[]{:S(2)}) collective-permute-start(bf16[8,256,128]{2,1,0:T(8,128)(2,1)S(1)} %get-tuple-element.96), channel_id=1, source_target_pairs={{0,1},{1,2},{2,3},{3,0},{4,5},{5,6},{6,7},{7,4},{8,9},{9,10},{10,1... | collective-permute-start | bytes 1572872 | tf_op jit(solution)/shard_map/ppermute | solution.py:384
  120.7 21.3 %collective-permute-start.1 = (bf16[128,2176]{1,0:T(8,128)(2,1)S(1)}, bf16[128,2176]{1,0:T(8,128)(2,1)S(1)}, u32[]{:S(2)}, u32[]{:S(2)}) collective-permute-start(bf16[128,2176]{1,0:T(8,128)(2,1)S(1)} %bitcast.14), channel_id=1, source_target_pairs={{0,1},{1,0},{2,3},{3,2},{4,5},{5,4},{6,7},{7,6},{8,9},{9,8},{10,11... | collective-permute-start | bytes 1671176 | tf_op jit(solution)/shard_map/ppermute | solution.py:422
  121.6 22.6 %collective-permute-start.2 = (bf16[128,2176]{1,0:T(8,128)(2,1)S(1)}, bf16[128,2176]{1,0:T(8,128)(2,1)S(1)}, u32[]{:S(2)}, u32[]{:S(2)}) collective-permute-start(bf16[128,2176]{1,0:T(8,128)(2,1)S(1)} %collective-permute-done.refs_1_), channel_id=1, source_target_pairs={{0,1},{1,0},{2,3},{3,2},{4,5},{5,4},{6,7},{7,6},{8,9},{9,8},{10,11... | collective-permute-start | bytes 1671176 | tf_op jit(solution)/shard_map/ppermute | solution.py:422
  131.7 27.6 %collective-permute-start.8 = (bf16[256,512]{1,0:T(8,128)(2,1)S(1)}, bf16[256,512]{1,0:T(8,128)(2,1)S(1)}, u32[]{:S(2)}, u32[]{:S(2)}) collective-permute-start(bf16[256,512]{1,0:T(8,128)(2,1)S(1)} %get-tuple-element.82), channel_id=1, source_target_pairs={{0,12},{4,16},{8,20},{12,24},{16,28},{20,0},{24,4},{28,8},{1,13},{... | collective-permute-start | bytes 786440 | tf_op jit(solution)/shard_map/ppermute | solution.py:384
  138.1 31.5 %collective-permute-start.9 = (bf16[256,512]{1,0:T(8,128)(2,1)S(1)}, bf16[256,512]{1,0:T(8,128)(2,1)S(1)}, u32[]{:S(2)}, u32[]{:S(2)}) collective-permute-start(bf16[256,512]{1,0:T(8,128)(2,1)S(1)} %get-tuple-element.83), channel_id=1, source_target_pairs={{0,16},{4,20},{8,24},{12,28},{16,0},{20,4},{24,8},{28,12},{1,17},{... | collective-permute-start | bytes 786440 | tf_op jit(solution)/shard_map/ppermute | solution.py:384
  138.1 31.5 %collective-permute-start.10 = (bf16[256,512]{1,0:T(8,128)(2,1)S(1)}, bf16[256,512]{1,0:T(8,128)(2,1)S(1)}, u32[]{:S(2)}, u32[]{:S(2)}) collective-permute-start(bf16[256,512]{1,0:T(8,128)(2,1)S(1)} %get-tuple-element.84), channel_id=1, source_target_pairs={{0,20},{4,24},{8,28},{12,0},{16,4},{20,8},{24,12},{28,16},{1,21},{... | collective-permute-start | bytes 786440 | tf_op jit(solution)/shard_map/ppermute | solution.py:384
  142.0 30.1 %collective-permute-start.11 = (bf16[256,512]{1,0:T(8,128)(2,1)S(1)}, bf16[256,512]{1,0:T(8,128)(2,1)S(1)}, u32[]{:S(2)}, u32[]{:S(2)}) collective-permute-start(bf16[256,512]{1,0:T(8,128)(2,1)S(1)} %get-tuple-element.85), channel_id=1, source_target_pairs={{0,24},{4,28},{8,0},{12,4},{16,8},{20,12},{24,16},{28,20},{1,25},{... | collective-permute-start | bytes 786440 | tf_op jit(solution)/shard_map/ppermute | solution.py:384
  144.2 40.0 %collective-permute-start.12 = (bf16[256,512]{1,0:T(8,128)(2,1)S(1)}, bf16[256,512]{1,0:T(8,128)(2,1)S(1)}, u32[]{:S(2)}, u32[]{:S(2)}) collective-permute-start(bf16[256,512]{1,0:T(8,128)(2,1)S(1)} %get-tuple-element.86), channel_id=1, source_target_pairs={{0,28},{4,0},{8,4},{12,8},{16,12},{20,16},{24,20},{28,24},{1,29},{... | collective-permute-start | bytes 786440 | tf_op jit(solution)/shard_map/ppermute | solution.py:384
  159.3 29.4 %collective-permute-start.38 = (bf16[64,768]{1,0:T(8,128)(2,1)S(1)}, bf16[64,768]{1,0:T(8,128)(2,1)S(1)}, u32[]{:S(2)}, u32[]{:S(2)}) collective-permute-start(bf16[64,768]{1,0:T(8,128)(2,1)S(1)} %get-tuple-element.120), channel_id=1, source_target_pairs={{0,12},{4,16},{8,20},{12,24},{16,28},{20,0},{24,4},{28,8},{1,13},{... | collective-permute-start | bytes 294920 | tf_op jit(solution)/shard_map/ppermute | solution.py:384
  169.6 21.2 %collective-permute-start.39 = (bf16[64,768]{1,0:T(8,128)(2,1)S(1)}, bf16[64,768]{1,0:T(8,128)(2,1)S(1)}, u32[]{:S(2)}, u32[]{:S(2)}) collective-permute-start(bf16[64,768]{1,0:T(8,128)(2,1)S(1)} %get-tuple-element.121), channel_id=1, source_target_pairs={{0,16},{4,20},{8,24},{12,28},{16,0},{20,4},{24,8},{28,12},{1,17},{... | collective-permute-start | bytes 294920 | tf_op jit(solution)/shard_map/ppermute | solution.py:384
  169.6 21.2 %collective-permute-start.40 = (bf16[64,768]{1,0:T(8,128)(2,1)S(1)}, bf16[64,768]{1,0:T(8,128)(2,1)S(1)}, u32[]{:S(2)}, u32[]{:S(2)}) collective-permute-start(bf16[64,768]{1,0:T(8,128)(2,1)S(1)} %get-tuple-element.122), channel_id=1, source_target_pairs={{0,20},{4,24},{8,28},{12,0},{16,4},{20,8},{24,12},{28,16},{1,21},{... | collective-permute-start | bytes 294920 | tf_op jit(solution)/shard_map/ppermute | solution.py:384
  172.2 19.3 %collective-permute-start.41 = (bf16[64,768]{1,0:T(8,128)(2,1)S(1)}, bf16[64,768]{1,0:T(8,128)(2,1)S(1)}, u32[]{:S(2)}, u32[]{:S(2)}) collective-permute-start(bf16[64,768]{1,0:T(8,128)(2,1)S(1)} %get-tuple-element.123), channel_id=1, source_target_pairs={{0,24},{4,28},{8,0},{12,4},{16,8},{20,12},{24,16},{28,20},{1,25},{... | collective-permute-start | bytes 294920 | tf_op jit(solution)/shard_map/ppermute | solution.py:384
  196.7 19.4 %collective-permute-start.43 = (bf16[128,768]{1,0:T(8,128)(2,1)S(1)}, bf16[128,768]{1,0:T(8,128)(2,1)S(1)}, u32[]{:S(2)}, u32[]{:S(2)}) collective-permute-start(bf16[128,768]{1,0:T(8,128)(2,1)S(1)} %get-tuple-element.127), channel_id=1, source_target_pairs={{0,2},{1,3},{2,0},{3,1},{4,6},{5,7},{6,4},{7,5},{8,10},{9,11},{10,... | collective-permute-start | bytes 589832 | tf_op jit(solution)/shard_map/ppermute | solution.py:440
  199.4 16.7 %collective-permute-start.44 = (bf16[128,768]{1,0:T(8,128)(2,1)S(1)}, bf16[128,768]{1,0:T(8,128)(2,1)S(1)}, u32[]{:S(2)}, u32[]{:S(2)}) collective-permute-start(bf16[128,768]{1,0:T(8,128)(2,1)S(1)} %get-tuple-element.128), channel_id=1, source_target_pairs={{0,1},{1,0},{2,3},{3,2},{4,5},{5,4},{6,7},{7,6},{8,9},{9,8},{10,11... | collective-permute-start | bytes 589832 | tf_op jit(solution)/shard_map/ppermute | solution.py:440
  199.5 16.7 %collective-permute-start.45 = (bf16[128,768]{1,0:T(8,128)(2,1)S(1)}, bf16[128,768]{1,0:T(8,128)(2,1)S(1)}, u32[]{:S(2)}, u32[]{:S(2)}) collective-permute-start(bf16[128,768]{1,0:T(8,128)(2,1)S(1)} %get-tuple-element.129), channel_id=1, source_target_pairs={{0,3},{1,2},{2,1},{3,0},{4,7},{5,6},{6,5},{7,4},{8,11},{9,10},{10,... | collective-permute-start | bytes 589832 | tf_op jit(solution)/shard_map/ppermute | solution.py:440
  217.0 18.5 %all-to-all-start.2 = ((bf16[8,16,1024]{2,1,0:T(8,128)(2,1)}), bf16[8,16,1024]{2,1,0:T(8,128)(2,1)S(1)}, u32[]{:S(2)}, u32[]{:S(2)}) async-start(bf16[8,16,1024]{2,1,0:T(8,128)(2,1)} %shard_map.116), calls=%async_computation.2 | async-start | bytes 524288 | tf_op jit(solution)/shard_map/all_to_all | solution.py:447
  (50 other events, 434.4 us)

commit v5 on v4

--- a/solution.py
+++ b/solution.py
@@ -15,11 +15,8 @@
 
 
 def cuts_of(width):
-    half, rest = width // 2, width - width // 8
-    return [(0, half), (half, rest), (rest, width)]
-
-
-returns = [(0,), (1, 2)]
+    first = width // 8 * 5
+    return [(0, first), (first, width)]
 
 
 def grant(mib):
@@ -89,28 +86,21 @@
     out_ref[:, width:] = extra
 
 
-def add_kernel(tp, *refs):
-    ins, out_ref = refs[:-1], refs[-1]
+def add_kernel(*refs):
+    out_ref = refs[-1]
     fs, each, _ = out_ref.shape
-    low = 0
-    for k in range(0, len(ins), tp):
-        total = sum(ref[...].astype(f32) for ref in ins[k : k + tp]).astype(bf16)
-        high = low + total.shape[1]
-        for r in range(fs):
-            out_ref[r, :, low:high] = total[r * each : (r + 1) * each]
-        low = high
-
-
-def add(fs, groups):
-    tp = len(groups[0])
-    count = groups[0][0].shape[0]
-    width = sum(group[0].shape[1] for group in groups)
-    terms = [part for group in groups for part in group]
+    total = sum(ref[...].astype(f32) for ref in refs[:-1]).astype(bf16)
+    for i in range(fs):
+        out_ref[i] = total[i * each : (i + 1) * each]
+
+
+def add(fs, terms):
+    count, width = terms[0].shape
     return pl.pallas_call(
-        functools.partial(add_kernel, tp),
+        add_kernel,
         out_shape=jax.ShapeDtypeStruct((fs, count // fs, width), bf16),
         compiler_params=grant(8),
-        cost_estimate=cost(1e9, 2 * (tp + 1) * count * width),
+        cost_estimate=cost(1e9, 2 * (len(terms) + 1) * count * width),
     )(*terms)
 
 
@@ -174,8 +164,9 @@
         for r in range(fs):
             group = lax.rem(me_ref[0] + r, fs)
             full = jnp.concatenate([ins[q][group] for q in order], axis=-1)
-            for k, (low, high) in enumerate(cuts):
+            for k, (low, high) in enumerate(cuts[:-1]):
                 outs[k * fs + r][...] = full[:, low:high]
+            outs[-1][group] = full[:, cuts[-1][0] :]
 
     in_order(me_ref, tp, store)
 
@@ -183,7 +174,8 @@
 def merge(me, parts, cuts):
     tp = len(parts)
     fs, rows, _ = parts[0].shape
-    shapes = [(rows, high - low) for low, high in cuts for _ in range(fs)]
+    shapes = [(rows, high - low) for low, high in cuts[:-1] for _ in range(fs)]
+    shapes.append((fs, rows, cuts[-1][1] - cuts[-1][0]))
     outs = pl.pallas_call(
         functools.partial(merge_kernel, fs, tp, cuts),
         grid_spec=pltpu.PrefetchScalarGridSpec(
@@ -196,7 +188,7 @@
         compiler_params=grant(16),
         cost_estimate=cost(1e9, 4 * tp * parts[0].size),
     )(me, *parts)
-    return [outs[k * fs : (k + 1) * fs] for k in range(len(cuts))]
+    return [outs[k * fs : (k + 1) * fs] for k in range(len(cuts) - 1)] + [outs[-1]]
 
 
 def regroup_kernel(fs, tp, me_ref, *refs):
@@ -269,13 +261,16 @@
 
 def assemble(me_ref, parts, matrix_ref):
     fs, rows = len(parts), parts[0].shape[0]
+    if fs == 1:
+        matrix_ref[...] = parts[0][...]
+        return
     for r in range(fs):
         origin = lax.rem(me_ref[0] - r + fs, fs)
         matrix_ref[pl.ds(pl.multiple_of(origin * rows, rows), rows), :] = parts[r][...]
 
 
-def up_kernel(fs, tp, me_ref, *refs):
-    x_refs, parts, refs = refs[:tp], refs[tp : tp + fs], refs[tp + fs :]
+def up_kernel(tp, me_ref, *refs):
+    x_refs, parts, refs = refs[:tp], refs[tp:-4], refs[-4:]
     gate_ref, matrix_ref, out_ref, rows_ref = refs
     assemble(me_ref, parts, matrix_ref)
     up = product_of(x_refs, matrix_ref, rows_ref)
@@ -284,15 +279,15 @@
 
 
 def up_rows(me, rows, parts, gate):
-    tp, fs = len(rows), len(parts)
-    matrix = (fs * parts[0].shape[0], parts[0].shape[1])
+    tp = len(rows)
+    matrix = (len(parts) * parts[0].shape[0], parts[0].shape[1])
     return pl.pallas_call(
-        functools.partial(up_kernel, fs, tp),
+        functools.partial(up_kernel, tp),
         grid_spec=pltpu.PrefetchScalarGridSpec(
             num_scalar_prefetch=1,
             grid=(1,),
             in_specs=[whole(rows[0].shape)] * tp
-            + [whole(parts[0].shape)] * fs
+            + [whole(part.shape) for part in parts]
             + [whole(gate.shape)],
             out_specs=[whole(matrix), whole(gate.shape)],
             scratch_shapes=[pltpu.VMEM((gate.shape[0], matrix[0]), bf16)],
@@ -303,9 +298,9 @@
     )(me, *rows, *parts, gate)
 
 
-def down_kernel(fs, tp, low, aliased, me_ref, hidden_ref, *refs):
+def down_kernel(count_parts, tp, low, aliased, me_ref, hidden_ref, *refs):
     w_refs, refs = refs[:tp], refs[tp:]
-    parts, refs = refs[:fs], refs[fs:]
+    parts, refs = refs[:count_parts], refs[count_parts:]
     if aliased:
         refs = refs[1:]
     matrix_ref, outs, block, done = refs[0], refs[1 : 1 + tp], refs[1 + tp], refs[2 + tp]
@@ -327,7 +322,7 @@
 
 
 def down_rows(me, hidden, rows, parts, low, width, prior):
-    tp, fs = len(rows), len(parts)
+    tp = len(rows)
     count = rows[0].shape[0]
     depth = hidden.shape[1]
     size = parts[0].shape[1]
@@ -342,7 +337,7 @@
         args.append(prior)
         aliases = {len(args): 0}
     outs = pl.pallas_call(
-        functools.partial(down_kernel, fs, tp, low, prior is not None),
+        functools.partial(down_kernel, len(parts), tp, low, prior is not None),
         grid_spec=pltpu.PrefetchScalarGridSpec(
             num_scalar_prefetch=1,
             grid=(1,),
@@ -364,9 +359,8 @@
     onehot = slot_onehot(group_of(ids_ref[0:1, :], fs, tp), fs)
     low = 0
     for ref in ins:
-        back = jnp.concatenate([ref[g] for g in range(fs)], axis=0)
-        high = low + back.shape[1]
-        out_ref[:, low:high] = jnp.dot(onehot, back, preferred_element_type=f32).astype(bf16)
+        high = low + ref.shape[1]
+        out_ref[:, low:high] = jnp.dot(onehot, ref[...], preferred_element_type=f32).astype(bf16)
         low = high
 
 
@@ -384,6 +378,10 @@
             out[r] = lax.ppermute(parts[r], axis, [(k, (k + r) % n) for k in range(n)])
         return out
 
+    def swap_fs(value):
+        out = lax.all_to_all(value, "fs", 0, 0, tiled=True)
+        return out.reshape(-1, out.shape[2])
+
     def by_expert(matrix):
         return matrix.reshape((fs, tp) + matrix.shape[1:])
 
@@ -395,8 +393,7 @@
         out_shape=jax.ShapeDtypeStruct((count, width + lanes), bf16),
         cost_estimate=cost(2 * count * count * width, 4 * count * width),
     )(tokens, ids, weights)
-    landed = lax.all_to_all(sent.reshape(fs, count // fs, -1), "fs", 0, 0, tiled=True)
-    landed = landed.reshape(count, -1)
+    landed = swap_fs(sent.reshape(fs, count // fs, -1))
     gate_parts = [None] * fs
     early, late = far_first(fs)[:3], far_first(fs)[3:]
 
@@ -420,15 +417,14 @@
         for step in range(2, tp, 2)
     ]
     rows += [lax.ppermute(part, "tp", [(k, k ^ 1) for k in range(tp)]) for part in rows]
-    (up_parts,) = merge(me, up_parts, [(0, tp * up_parts[0].shape[2])])
-    for distances in (early, late):
-        up_parts = rotate(up_parts, "fs", distances)
+    (up_here,) = merge(me, up_parts, [(0, tp * up_parts[0].shape[2])])
+    up_parts = [swap_fs(up_here)]
     gate_parts = regroup(me, gate_parts)
     gate_parts = rotate(gate_parts, "tp")
     down_parts = merge(me, down_parts, cuts)
-    for k in range(len(cuts)):
-        down_parts[k] = rotate(down_parts[k], "fs")
     new_gate, gate = gate_rows(me, rows, gate_parts)
+    down_parts[0] = rotate(down_parts[0], "fs")
+    down_parts[1] = [swap_fs(down_parts[1])]
     new_up, hidden = up_rows(me, rows, up_parts, gate)
     new_down = None
     partials = []
@@ -442,9 +438,9 @@
             ]
         )
     backs = []
-    for members in returns:
-        summed = add(fs, [partials[m] for m in members])
-        backs.append(lax.all_to_all(summed, "fs", 0, 0, tiled=True))
+    for partial in partials:
+        summed = add(fs, partial)
+        backs.append(swap_fs(summed))
     mixed = pl.pallas_call(
         functools.partial(final_kernel, fs, tp),
         out_shape=jax.ShapeDtypeStruct((count, width), bf16),

time: 253 us -> 268 us (1.059)
  waiting for transfers between devices: 88.7 us -> 114 us
  starting transfers between devices: 105 us -> 86.5 us
  local copies, waits for them, and re-layouts: 12.6 us -> 18.6 us
    ppermute x44 -> x23, starting transfers between devices: 83.8 us -> 50.4 us  [rotate(): out[r] = lax.ppermute(parts[r], axis, [(k, (k + r) % n) for k in range(n)])]
    all_to_all x2 -> x4, waiting for transfers between devices: 0.01 us -> 26.8 us  [swap_fs(): out = lax.all_to_all(value, 'fs', 0, 0, tiled=True)]
    all_to_all x2 -> x4, starting transfers between devices: 13 us -> 31.9 us  [swap_fs(): out = lax.all_to_all(value, 'fs', 0, 0, tiled=True)]
    ppermute x9 -> x6, waiting for transfers between devices: 16.8 us -> 9.94 us  [shards(): lax.ppermute(term, 'tp', list(enumerate(places)))]
    unnamed x48 -> x62, local copies, waits for them, and re-layouts: 12.6 us -> 18.6 us
    ppermute x44 -> x23, waiting for transfers between devices: 71.9 us -> 77.7 us  [rotate(): out[r] = lax.ppermute(parts[r], axis, [(k, (k + r) % n) for k in range(n)])]
    ppermute x9 -> x6, starting transfers between devices: 7.05 us -> 3.72 us  [shards(): lax.ppermute(term, 'tp', list(enumerate(places)))]
    pallas_call x6 -> x5, Pallas kernels: 8.43 us -> 8.78 us  [the longest x2 5.09 us: down_rows(): pl.pallas_call(functools.partial(down_kernel, len(parts), tp, low, prior...]
  transfers between devices with their start and end apart: 58 -> 36, of which waited for: 18 -> 14; matrix products, arithmetic and copies ran while one was open for 0% -> 0% of each run, Pallas kernels for 10% -> 9%
where the time goes in v5:
time: 268 us; the launch traced here: 267 us
  waiting for transfers between devices  114 us (43%)
  starting transfers between devices  86.5 us (32%)
  Pallas kernels  30.4 us (11%)
  local copies, waits for them, and re-layouts  18.6 us (7%)
  blocking collectives  16.2 us (6%)
    ppermute x23, waiting for transfers between devices, rotate(): out[r] = lax.ppermute(parts[r], axis, [(k, (k + r) % n) for k in range(n)])  77.7 us
    ppermute x23, starting transfers between devices, rotate(): out[r] = lax.ppermute(parts[r], axis, [(k, (k + r) % n) for k in range(n)])  50.4 us
    all_to_all x4, starting transfers between devices, swap_fs(): out = lax.all_to_all(value, 'fs', 0, 0, tiled=True)  31.9 us
    all_to_all x4, waiting for transfers between devices, swap_fs(): out = lax.all_to_all(value, 'fs', 0, 0, tiled=True)  26.8 us
    unnamed x62, local copies, waits for them, and re-layouts  18.6 us
    all_to_all x1, blocking collectives, swap_fs(): out = lax.all_to_all(value, 'fs', 0, 0, tiled=True)  16.2 us
    pallas_call x4, Pallas kernels, cast_along(): pl.pallas_call(functools.partial(cast_kernel, steps, scale is not None, a...  10.4 us
    ppermute x6, waiting for transfers between devices, shards(): lax.ppermute(term, 'tp', list(enumerate(places)))  9.94 us
  transfers between devices with their start and end apart: 36, of which 14 were waited for; matrix products, arithmetic and copies ran while one was open for 0% of the time, Pallas kernels for 9%

profile of v5, /device:TPU:0, one launch (start us, length us, event | category | flops | bytes accessed | tf_op | source)
XLA Modules:
  0.0 267.0 jit_solution(758892564467997076)
XLA Ops:
  0.6 2.4 shard_map.102
  3.0 7.3 %all-to-all-start = ((bf16[8,16,2176]{2,1,0:T(8,128)(2,1)}), bf16[8,16,2176]{2,1,0:T(8,128)(2,1)S(1)}, u32[]{:S(2)}, u32[]{:S(2)}) async-start(bf16[8,16,2176]{2,1,0:T(8,128)(2,1)} %bitcast.36), calls=%async_computation | async-start | bytes 1114112 | tf_op jit(solution)/shard_map/all_to_all | solution.py:382
  10.4 2.2 copy-done.4
  17.3 10.6 %collective-permute-done.3.refs_1_ = bf16[8,256,128]{2,1,0:T(8,128)(2,1)S(1)} collective-permute-done((bf16[8,256,128]{2,1,0:T(8,128)(2,1)S(1)}, bf16[8,256,128]{2,1,0:T(8,128)(2,1)S(1)}, u32[]{:S(2)}, u32[]{:S(2)}) %collective-permute-start.3) | collective-permute-done | bytes 524320 | tf_op jit(solution)/shard_map/ppermute | solution.py:378
  29.2 9.6 %collective-permute-done.5.refs_3_ = bf16[8,256,128]{2,1,0:T(8,128)(2,1)S(1)} collective-permute-done((bf16[8,256,128]{2,1,0:T(8,128)(2,1)S(1)}, bf16[8,256,128]{2,1,0:T(8,128)(2,1)S(1)}, u32[]{:S(2)}, u32[]{:S(2)}) %collective-permute-start.5) | collective-permute-done | bytes 524320 | tf_op jit(solution)/shard_map/ppermute | solution.py:378
  41.0 6.0 %all-to-all-start.1 = ((bf16[8,256,512]{2,1,0:T(8,128)(2,1)}), bf16[8,256,512]{2,1,0:T(8,128)(2,1)S(1)}, u32[]{:S(2)}, u32[]{:S(2)}) async-start(bf16[8,256,512]{2,1,0:T(8,128)(2,1)} %copy-done.3), calls=%async_computation.1 | async-start | bytes 4194304 | tf_op jit(solution)/shard_map/all_to_all | solution.py:382
  47.0 2.2 copy-done.5
  49.2 2.6 shard_map.110
  60.1 4.0 %shard_map.106 = (bf16[4,256,128]{2,1,0:T(8,128)(2,1)}, bf16[4,256,128]{2,1,0:T(8,128)(2,1)}, bf16[4,256,128]{2,1,0:T(8,128)(2,1)}) custom-call(s32[2]{0:T(128)} %copy-done.9, f32[8,4,256,128]{3,2,1,0:T(8,128)} %bitcast.17, f32[1,256]{1,0:T(1,128)} %bitcast.31), custom_call_target="tpu_custom_call" | custom-call | flops 1000000000 | bytes 2359296 | tf_op jit(solution)/shard_map/pallas_call | solution.py:141
  65.9 3.2 %collective-permute-start.8 = (bf16[4,256,128]{2,1,0:T(8,128)(2,1)}, bf16[4,256,128]{2,1,0:T(8,128)(2,1)}, u32[]{:S(2)}, u32[]{:S(2)}) collective-permute-start(bf16[4,256,128]{2,1,0:T(8,128)(2,1)} %get-tuple-element.54), channel_id=1, source_target_pairs={{0,12},{4,16},{8,20},{12,24},{16,28},{20,0},{24,4},{28,8},{1,13},{... | collective-permute-start | bytes 786440 | tf_op jit(solution)/shard_map/ppermute | solution.py:378
  69.2 6.4 %collective-permute-done.18.refs_3_ = bf16[8,64,512]{2,1,0:T(8,128)(2,1)} collective-permute-done((bf16[8,64,512]{2,1,0:T(8,128)(2,1)}, bf16[8,64,512]{2,1,0:T(8,128)(2,1)}, u32[]{:S(2)}, u32[]{:S(2)}) %collective-permute-start.18) | collective-permute-done | bytes 524320 | tf_op jit(solution)/shard_map/ppermute | solution.py:378
  85.9 21.6 %all-to-all-done.1 = bf16[8,256,512]{2,1,0:T(8,128)(2,1)S(1)} async-done(((bf16[8,256,512]{2,1,0:T(8,128)(2,1)}), bf16[8,256,512]{2,1,0:T(8,128)(2,1)S(1)}, u32[]{:S(2)}, u32[]{:S(2)}) %all-to-all-start.1) | async-done | bytes 2097184 | tf_op jit(solution)/shard_map/all_to_all | solution.py:382
  108.8 8.8 %all-to-all-start.3 = ((bf16[8,64,768]{2,1,0:T(8,128)(2,1)}), bf16[8,64,768]{2,1,0:T(8,128)(2,1)S(1)}, u32[]{:S(2)}, u32[]{:S(2)}) async-start(bf16[8,64,768]{2,1,0:T(8,128)(2,1)} %copy-done.6), calls=%async_computation.3 | async-start | bytes 1572864 | tf_op jit(solution)/shard_map/all_to_all | solution.py:382
  117.6 2.9 %collective-permute-start.9 = (bf16[4,256,128]{2,1,0:T(8,128)(2,1)}, bf16[4,256,128]{2,1,0:T(8,128)(2,1)S(1)}, u32[]{:S(2)}, u32[]{:S(2)}) collective-permute-start(bf16[4,256,128]{2,1,0:T(8,128)(2,1)} %get-tuple-element.55), channel_id=1, source_target_pairs={{0,16},{4,20},{8,24},{12,28},{16,0},{20,4},{24,8},{28,12},{1,17},{... | collective-permute-start | bytes 786440 | tf_op jit(solution)/shard_map/ppermute | solution.py:378
  122.2 3.0 %collective-permute-start.11 = (bf16[4,256,128]{2,1,0:T(8,128)(2,1)}, bf16[4,256,128]{2,1,0:T(8,128)(2,1)S(1)}, u32[]{:S(2)}, u32[]{:S(2)}) collective-permute-start(bf16[4,256,128]{2,1,0:T(8,128)(2,1)} %copy-done.23), channel_id=1, source_target_pairs={{0,24},{4,28},{8,0},{12,4},{16,8},{20,12},{24,16},{28,20},{1,25},{... | collective-permute-start | bytes 786440 | tf_op jit(solution)/shard_map/ppermute | solution.py:378
  125.8 30.1 %collective-permute-done.9.refs_4_ = bf16[4,256,128]{2,1,0:T(8,128)(2,1)S(1)} collective-permute-done((bf16[4,256,128]{2,1,0:T(8,128)(2,1)}, bf16[4,256,128]{2,1,0:T(8,128)(2,1)S(1)}, u32[]{:S(2)}, u32[]{:S(2)}) %collective-permute-start.9) | collective-permute-done | bytes 262176 | tf_op jit(solution)/shard_map/ppermute | solution.py:378
  156.0 13.5 %collective-permute-start.20 = (bf16[64,1280]{1,0:T(8,128)(2,1)}, bf16[64,1280]{1,0:T(8,128)(2,1)S(1)}, u32[]{:S(2)}, u32[]{:S(2)}) collective-permute-start(bf16[64,1280]{1,0:T(8,128)(2,1)} %copy-done.29), channel_id=1, source_target_pairs={{0,8},{4,12},{8,16},{12,20},{16,24},{20,28},{24,0},{28,4},{1,9},{5... | collective-permute-start | bytes 491528 | tf_op jit(solution)/shard_map/ppermute | solution.py:378
  172.8 2.5 collective-permute-start.14
  176.7 10.0 %collective-permute-done.13.refs_5_ = bf16[8,256,128]{2,1,0:T(8,128)(2,1)S(1)} collective-permute-done((bf16[8,256,128]{2,1,0:T(8,128)(2,1)S(1)}, bf16[8,256,128]{2,1,0:T(8,128)(2,1)S(1)}, u32[]{:S(2)}, u32[]{:S(2)}) %collective-permute-start.13) | collective-permute-done | bytes 524320 | tf_op jit(solution)/shard_map/ppermute | solution.py:378
  186.6 5.5 %collective-permute-start.21 = (bf16[64,1280]{1,0:T(8,128)(2,1)}, bf16[64,1280]{1,0:T(8,128)(2,1)S(1)}, u32[]{:S(2)}, u32[]{:S(2)}) collective-permute-start(bf16[64,1280]{1,0:T(8,128)(2,1)} %copy-done.28), channel_id=1, source_target_pairs={{0,12},{4,16},{8,20},{12,24},{16,28},{20,0},{24,4},{28,8},{1,13},{... | collective-permute-start | bytes 491528 | tf_op jit(solution)/shard_map/ppermute | solution.py:378
  192.2 6.0 %collective-permute-done.15.refs_7_ = bf16[8,256,128]{2,1,0:T(8,128)(2,1)S(1)} collective-permute-done((bf16[8,256,128]{2,1,0:T(8,128)(2,1)S(1)}, bf16[8,256,128]{2,1,0:T(8,128)(2,1)S(1)}, u32[]{:S(2)}, u32[]{:S(2)}) %collective-permute-start.15) | collective-permute-done | bytes 524320 | tf_op jit(solution)/shard_map/ppermute | solution.py:378
  198.2 4.2 %collective-permute-start.23 = (bf16[64,1280]{1,0:T(8,128)(2,1)}, bf16[64,1280]{1,0:T(8,128)(2,1)S(1)}, u32[]{:S(2)}, u32[]{:S(2)}) collective-permute-start(bf16[64,1280]{1,0:T(8,128)(2,1)} %copy-done.26), channel_id=1, source_target_pairs={{0,20},{4,24},{8,28},{12,0},{16,4},{20,8},{24,12},{28,16},{1,21},{... | collective-permute-start | bytes 491528 | tf_op jit(solution)/shard_map/ppermute | solution.py:378
  202.4 3.3 %collective-permute-start.24 = (bf16[64,1280]{1,0:T(8,128)(2,1)}, bf16[64,1280]{1,0:T(8,128)(2,1)S(1)}, u32[]{:S(2)}, u32[]{:S(2)}) collective-permute-start(bf16[64,1280]{1,0:T(8,128)(2,1)} %copy-done.25), channel_id=1, source_target_pairs={{0,24},{4,28},{8,0},{12,4},{16,8},{20,12},{24,16},{28,20},{1,25},{... | collective-permute-start | bytes 491528 | tf_op jit(solution)/shard_map/ppermute | solution.py:378
  205.7 3.1 %shard_map.108 = (bf16[2048,512]{1,0:T(8,128)(2,1)}, f32[512,512]{1,0:T(8,128)S(1)}) custom-call(s32[2]{0:T(128)S(1)} %copy-done.10, bf16[128,2176]{1,0:T(8,128)(2,1)S(1)} %bitcast.21, bf16[128,2176]{1,0:T(8,128)(2,1)S(1)} %collective-permute-done.refs_1_, bf16[128,2176]{1,0:T(8,128)(2,1)S(1)} %collective-permute-done.1.refs_2_, ...), custom_call_target="tpu_custom_call" | custom-call | flops 1073741824 | bytes 4194304 | tf_op jit(solution)/shard_map/pallas_call | solution.py:247
  208.8 2.7 %shard_map.109 = (bf16[2048,512]{1,0:T(8,128)(2,1)}, bf16[512,512]{1,0:T(8,128)(2,1)S(1)}) custom-call(s32[2]{0:T(128)S(1)} %copy-done.10, bf16[128,2176]{1,0:T(8,128)(2,1)S(1)} %bitcast.22, bf16[128,2176]{1,0:T(8,128)(2,1)S(1)} %collective-permute-done.refs_1_, bf16[128,2176]{1,0:T(8,128)(2,1)S(1)} %collective-permute-done.1.refs_2_, ...), custom_call_target="tpu_custom_call" | custom-call | flops 1073741824 | bytes 4194304 | tf_op jit(solution)/shard_map/pallas_call | solution.py:284
  211.5 2.5 collective-permute-done.25.refs_11_
  214.1 3.4 %shard_map.112 = (bf16[512,2048]{1,0:T(8,128)(2,1)}, bf16[128,1280]{1,0:T(8,128)(2,1)S(1)}, bf16[128,1280]{1,0:T(8,128)(2,1)}, bf16[128,1280]{1,0:T(8,128)(2,1)}, bf16[128,1280]{1,0:T(8,128)(2,1)}) custom-call(s32[2]{0:T(128)S(1)} %copy-done.10, bf16[512,512]{1,0:T(8,128)(2,1)S(1)} %get-tuple-element.64.hidden_ref, bf16[128,2176]{1,0:T(8,128)(2,1)S(1)} %bitcast.23, ...), custom_call_target="tpu_custom_call" | custom-call | flops 671088640 | bytes 2621440 | tf_op jit(solution)/shard_map/pallas_call | solution.py:339
  223.4 4.4 %collective-permute-done.29.refs_1_ = bf16[128,768]{1,0:T(8,128)(2,1)S(1)} collective-permute-done((bf16[128,768]{1,0:T(8,128)(2,1)S(1)}, bf16[128,768]{1,0:T(8,128)(2,1)S(1)}, u32[]{:S(2)}, u32[]{:S(2)}) %collective-permute-start.29) | collective-permute-done | bytes 196640 | tf_op jit(solution)/shard_map/ppermute | solution.py:436
  231.0 9.8 %all-to-all-start.4 = ((bf16[8,16,768]{2,1,0:T(8,128)(2,1)}), bf16[8,16,768]{2,1,0:T(8,128)(2,1)S(1)}, u32[]{:S(2)}, u32[]{:S(2)}) async-start(bf16[8,16,768]{2,1,0:T(8,128)(2,1)} %shard_map.115), calls=%async_computation.4 | async-start | bytes 393216 | tf_op jit(solution)/shard_map/all_to_all | solution.py:382
  240.8 3.4 %collective-permute-done.28.refs_3_ = bf16[128,1280]{1,0:T(8,128)(2,1)S(1)} collective-permute-done((bf16[128,1280]{1,0:T(8,128)(2,1)}, bf16[128,1280]{1,0:T(8,128)(2,1)S(1)}, u32[]{:S(2)}, u32[]{:S(2)}) %collective-permute-start.28) | collective-permute-done | bytes 327712 | tf_op jit(solution)/shard_map/ppermute | solution.py:436
  244.4 5.2 %all-to-all-done.4 = bf16[8,16,768]{2,1,0:T(8,128)(2,1)S(1)} async-done(((bf16[8,16,768]{2,1,0:T(8,128)(2,1)}), bf16[8,16,768]{2,1,0:T(8,128)(2,1)S(1)}, u32[]{:S(2)}, u32[]{:S(2)}) %all-to-all-start.4) | async-done | bytes 196640 | tf_op jit(solution)/shard_map/all_to_all | solution.py:382
  249.6 16.2 %all_to_all.25 = bf16[8,16,1280]{2,1,0:T(8,128)(2,1)S(1)} all-to-all(bf16[8,16,1280]{2,1,0:T(8,128)(2,1)S(1)} %shard_map.113), channel_id=1, replica_groups=mesh['fs'=8,'tp'=4] {'fs'}, dimensions={0} | all-to-all | bytes 655360 | tf_op jit(solution)/shard_map/all_to_all | solution.py:382
  (119 shorter events, 47.6 us)
Async XLA Ops:
  3.0 38.0 %all-to-all-start = ((bf16[8,16,2176]{2,1,0:T(8,128)(2,1)}), bf16[8,16,2176]{2,1,0:T(8,128)(2,1)S(1)}, u32[]{:S(2)}, u32[]{:S(2)}) async-start(bf16[8,16,2176]{2,1,0:T(8,128)(2,1)} %bitcast.36), calls=%async_computation | async-start | bytes 1114112 | tf_op jit(solution)/shard_map/all_to_all | solution.py:382
  14.3 13.6 %collective-permute-start.3 = (bf16[8,256,128]{2,1,0:T(8,128)(2,1)S(1)}, bf16[8,256,128]{2,1,0:T(8,128)(2,1)S(1)}, u32[]{:S(2)}, u32[]{:S(2)}) collective-permute-start(bf16[8,256,128]{2,1,0:T(8,128)(2,1)S(1)} %get-tuple-element.48), channel_id=1, source_target_pairs={{0,1},{1,2},{2,3},{3,0},{4,5},{5,6},{6,7},{7,4},{8,9},{9,10},{10,1... | collective-permute-start | bytes 1572872 | tf_op jit(solution)/shard_map/ppermute | solution.py:378
  14.4 14.9 %collective-permute-start.4 = (bf16[8,256,128]{2,1,0:T(8,128)(2,1)S(1)}, bf16[8,256,128]{2,1,0:T(8,128)(2,1)S(1)}, u32[]{:S(2)}, u32[]{:S(2)}) collective-permute-start(bf16[8,256,128]{2,1,0:T(8,128)(2,1)S(1)} %get-tuple-element.49), channel_id=1, source_target_pairs={{0,2},{1,3},{2,0},{3,1},{4,6},{5,7},{6,4},{7,5},{8,10},{9,11},{10,... | collective-permute-start | bytes 1572872 | tf_op jit(solution)/shard_map/ppermute | solution.py:378
  16.0 22.9 %collective-permute-start.5 = (bf16[8,256,128]{2,1,0:T(8,128)(2,1)S(1)}, bf16[8,256,128]{2,1,0:T(8,128)(2,1)S(1)}, u32[]{:S(2)}, u32[]{:S(2)}) collective-permute-start(bf16[8,256,128]{2,1,0:T(8,128)(2,1)S(1)} %get-tuple-element.50), channel_id=1, source_target_pairs={{0,3},{1,0},{2,1},{3,2},{4,7},{5,4},{6,5},{7,6},{8,11},{9,8},{10,9... | collective-permute-start | bytes 1572872 | tf_op jit(solution)/shard_map/ppermute | solution.py:378
  41.0 66.4 %all-to-all-start.1 = ((bf16[8,256,512]{2,1,0:T(8,128)(2,1)}), bf16[8,256,512]{2,1,0:T(8,128)(2,1)S(1)}, u32[]{:S(2)}, u32[]{:S(2)}) async-start(bf16[8,256,512]{2,1,0:T(8,128)(2,1)} %copy-done.3), calls=%async_computation.1 | async-start | bytes 4194304 | tf_op jit(solution)/shard_map/all_to_all | solution.py:382
  51.8 13.4 %collective-permute-start.16 = (bf16[8,64,512]{2,1,0:T(8,128)(2,1)}, bf16[8,64,512]{2,1,0:T(8,128)(2,1)S(1)}, u32[]{:S(2)}, u32[]{:S(2)}) collective-permute-start(bf16[8,64,512]{2,1,0:T(8,128)(2,1)} %get-tuple-element.66), channel_id=1, source_target_pairs={{0,1},{1,2},{2,3},{3,0},{4,5},{5,6},{6,7},{7,4},{8,9},{9,10},{10,1... | collective-permute-start | bytes 1572872 | tf_op jit(solution)/shard_map/ppermute | solution.py:378
  52.3 16.8 %collective-permute-start.17 = (bf16[8,64,512]{2,1,0:T(8,128)(2,1)}, bf16[8,64,512]{2,1,0:T(8,128)(2,1)}, u32[]{:S(2)}, u32[]{:S(2)}) collective-permute-start(bf16[8,64,512]{2,1,0:T(8,128)(2,1)} %get-tuple-element.67), channel_id=1, source_target_pairs={{0,2},{1,3},{2,0},{3,1},{4,6},{5,7},{6,4},{7,5},{8,10},{9,11},{10,... | collective-permute-start | bytes 1572872 | tf_op jit(solution)/shard_map/ppermute | solution.py:378
  53.8 21.8 %collective-permute-start.18 = (bf16[8,64,512]{2,1,0:T(8,128)(2,1)}, bf16[8,64,512]{2,1,0:T(8,128)(2,1)}, u32[]{:S(2)}, u32[]{:S(2)}) collective-permute-start(bf16[8,64,512]{2,1,0:T(8,128)(2,1)} %get-tuple-element.68), channel_id=1, source_target_pairs={{0,3},{1,0},{2,1},{3,2},{4,7},{5,4},{6,5},{7,6},{8,11},{9,8},{10,9... | collective-permute-start | bytes 1572872 | tf_op jit(solution)/shard_map/ppermute | solution.py:378
  56.7 63.8 %collective-permute-start.6 = (bf16[4,256,128]{2,1,0:T(8,128)(2,1)}, bf16[4,256,128]{2,1,0:T(8,128)(2,1)}, u32[]{:S(2)}, u32[]{:S(2)}) collective-permute-start(bf16[4,256,128]{2,1,0:T(8,128)(2,1)} %get-tuple-element.52), channel_id=1, source_target_pairs={{0,4},{4,8},{8,12},{12,16},{16,20},{20,24},{24,28},{28,0},{1,5},{5... | collective-permute-start | bytes 786440 | tf_op jit(solution)/shard_map/ppermute | solution.py:378
  58.6 63.6 %collective-permute-start.7 = (bf16[4,256,128]{2,1,0:T(8,128)(2,1)}, bf16[4,256,128]{2,1,0:T(8,128)(2,1)}, u32[]{:S(2)}, u32[]{:S(2)}) collective-permute-start(bf16[4,256,128]{2,1,0:T(8,128)(2,1)} %get-tuple-element.53), channel_id=1, source_target_pairs={{0,8},{4,12},{8,16},{12,20},{16,24},{20,28},{24,0},{28,4},{1,9},{5... | collective-permute-start | bytes 786440 | tf_op jit(solution)/shard_map/ppermute | solution.py:378
  65.9 59.3 %collective-permute-start.8 = (bf16[4,256,128]{2,1,0:T(8,128)(2,1)}, bf16[4,256,128]{2,1,0:T(8,128)(2,1)}, u32[]{:S(2)}, u32[]{:S(2)}) collective-permute-start(bf16[4,256,128]{2,1,0:T(8,128)(2,1)} %get-tuple-element.54), channel_id=1, source_target_pairs={{0,12},{4,16},{8,20},{12,24},{16,28},{20,0},{24,4},{28,8},{1,13},{... | collective-permute-start | bytes 786440 | tf_op jit(solution)/shard_map/ppermute | solution.py:378
  69.2 100.3 %collective-permute-start = (bf16[128,2176]{1,0:T(8,128)(2,1)S(1)}, bf16[128,2176]{1,0:T(8,128)(2,1)S(1)}, u32[]{:S(2)}, u32[]{:S(2)}) collective-permute-start(bf16[128,2176]{1,0:T(8,128)(2,1)S(1)} %bitcast.19), channel_id=1, source_target_pairs={{0,2},{1,3},{2,0},{3,1},{4,6},{5,7},{6,4},{7,5},{8,10},{9,11},{10,... | collective-permute-start | bytes 1671176 | tf_op jit(solution)/shard_map/ppermute | solution.py:416
  108.8 109.5 %all-to-all-start.3 = ((bf16[8,64,768]{2,1,0:T(8,128)(2,1)}), bf16[8,64,768]{2,1,0:T(8,128)(2,1)S(1)}, u32[]{:S(2)}, u32[]{:S(2)}) async-start(bf16[8,64,768]{2,1,0:T(8,128)(2,1)} %copy-done.6), calls=%async_computation.3 | async-start | bytes 1572864 | tf_op jit(solution)/shard_map/all_to_all | solution.py:382
  117.6 38.4 %collective-permute-start.9 = (bf16[4,256,128]{2,1,0:T(8,128)(2,1)}, bf16[4,256,128]{2,1,0:T(8,128)(2,1)S(1)}, u32[]{:S(2)}, u32[]{:S(2)}) collective-permute-start(bf16[4,256,128]{2,1,0:T(8,128)(2,1)} %get-tuple-element.55), channel_id=1, source_target_pairs={{0,16},{4,20},{8,24},{12,28},{16,0},{20,4},{24,8},{28,12},{1,17},{... | collective-permute-start | bytes 786440 | tf_op jit(solution)/shard_map/ppermute | solution.py:378
  120.5 35.5 %collective-permute-start.10 = (bf16[4,256,128]{2,1,0:T(8,128)(2,1)}, bf16[4,256,128]{2,1,0:T(8,128)(2,1)S(1)}, u32[]{:S(2)}, u32[]{:S(2)}) collective-permute-start(bf16[4,256,128]{2,1,0:T(8,128)(2,1)} %get-tuple-element.56), channel_id=1, source_target_pairs={{0,20},{4,24},{8,28},{12,0},{16,4},{20,8},{24,12},{28,16},{1,21},{... | collective-permute-start | bytes 786440 | tf_op jit(solution)/shard_map/ppermute | solution.py:378
  122.2 47.2 %collective-permute-start.11 = (bf16[4,256,128]{2,1,0:T(8,128)(2,1)}, bf16[4,256,128]{2,1,0:T(8,128)(2,1)S(1)}, u32[]{:S(2)}, u32[]{:S(2)}) collective-permute-start(bf16[4,256,128]{2,1,0:T(8,128)(2,1)} %copy-done.23), channel_id=1, source_target_pairs={{0,24},{4,28},{8,0},{12,4},{16,8},{20,12},{24,16},{28,20},{1,25},{... | collective-permute-start | bytes 786440 | tf_op jit(solution)/shard_map/ppermute | solution.py:378
  125.2 44.7 %collective-permute-start.12 = (bf16[4,256,128]{2,1,0:T(8,128)(2,1)S(1)}, bf16[4,256,128]{2,1,0:T(8,128)(2,1)S(1)}, u32[]{:S(2)}, u32[]{:S(2)}) collective-permute-start(bf16[4,256,128]{2,1,0:T(8,128)(2,1)S(1)} %copy-done.22), channel_id=1, source_target_pairs={{0,28},{4,0},{8,4},{12,8},{16,12},{20,16},{24,20},{28,24},{1,29},{... | collective-permute-start | bytes 786440 | tf_op jit(solution)/shard_map/ppermute | solution.py:378
  155.9 16.9 %collective-permute-start.19 = (bf16[64,1280]{1,0:T(8,128)(2,1)}, bf16[64,1280]{1,0:T(8,128)(2,1)S(1)}, u32[]{:S(2)}, u32[]{:S(2)}) collective-permute-start(bf16[64,1280]{1,0:T(8,128)(2,1)} %copy-done.30), channel_id=1, source_target_pairs={{0,4},{4,8},{8,12},{12,16},{16,20},{20,24},{24,28},{28,0},{1,5},{5... | collective-permute-start | bytes 491528 | tf_op jit(solution)/shard_map/ppermute | solution.py:378
  156.0 19.3 %collective-permute-start.20 = (bf16[64,1280]{1,0:T(8,128)(2,1)}, bf16[64,1280]{1,0:T(8,128)(2,1)S(1)}, u32[]{:S(2)}, u32[]{:S(2)}) collective-permute-start(bf16[64,1280]{1,0:T(8,128)(2,1)} %copy-done.29), channel_id=1, source_target_pairs={{0,8},{4,12},{8,16},{12,20},{16,24},{20,28},{24,0},{28,4},{1,9},{5... | collective-permute-start | bytes 491528 | tf_op jit(solution)/shard_map/ppermute | solution.py:378
  169.4 33.0 %collective-permute-start.1 = (bf16[128,2176]{1,0:T(8,128)(2,1)S(1)}, bf16[128,2176]{1,0:T(8,128)(2,1)S(1)}, u32[]{:S(2)}, u32[]{:S(2)}) collective-permute-start(bf16[128,2176]{1,0:T(8,128)(2,1)S(1)} %bitcast.20), channel_id=1, source_target_pairs={{0,1},{1,0},{2,3},{3,2},{4,5},{5,4},{6,7},{7,6},{8,9},{9,8},{10,11... | collective-permute-start | bytes 1671176 | tf_op jit(solution)/shard_map/ppermute | solution.py:419
  169.4 36.2 %collective-permute-start.2 = (bf16[128,2176]{1,0:T(8,128)(2,1)S(1)}, bf16[128,2176]{1,0:T(8,128)(2,1)S(1)}, u32[]{:S(2)}, u32[]{:S(2)}) collective-permute-start(bf16[128,2176]{1,0:T(8,128)(2,1)S(1)} %collective-permute-done.refs_1_), channel_id=1, source_target_pairs={{0,1},{1,0},{2,3},{3,2},{4,5},{5,4},{6,7},{7,6},{8,9},{9,8},{10,11... | collective-permute-start | bytes 1671176 | tf_op jit(solution)/shard_map/ppermute | solution.py:419
  172.7 14.0 %collective-permute-start.13 = (bf16[8,256,128]{2,1,0:T(8,128)(2,1)S(1)}, bf16[8,256,128]{2,1,0:T(8,128)(2,1)S(1)}, u32[]{:S(2)}, u32[]{:S(2)}) collective-permute-start(bf16[8,256,128]{2,1,0:T(8,128)(2,1)S(1)} %get-tuple-element.60), channel_id=1, source_target_pairs={{0,1},{1,2},{2,3},{3,0},{4,5},{5,6},{6,7},{7,4},{8,9},{9,10},{10,1... | collective-permute-start | bytes 1572872 | tf_op jit(solution)/shard_map/ppermute | solution.py:378
  172.8 19.4 %collective-permute-start.14 = (bf16[8,256,128]{2,1,0:T(8,128)(2,1)S(1)}, bf16[8,256,128]{2,1,0:T(8,128)(2,1)S(1)}, u32[]{:S(2)}, u32[]{:S(2)}) collective-permute-start(bf16[8,256,128]{2,1,0:T(8,128)(2,1)S(1)} %get-tuple-element.61), channel_id=1, source_target_pairs={{0,2},{1,3},{2,0},{3,1},{4,6},{5,7},{6,4},{7,5},{8,10},{9,11},{10,... | collective-permute-start | bytes 1572872 | tf_op jit(solution)/shard_map/ppermute | solution.py:378
  175.3 22.9 %collective-permute-start.15 = (bf16[8,256,128]{2,1,0:T(8,128)(2,1)S(1)}, bf16[8,256,128]{2,1,0:T(8,128)(2,1)S(1)}, u32[]{:S(2)}, u32[]{:S(2)}) collective-permute-start(bf16[8,256,128]{2,1,0:T(8,128)(2,1)S(1)} %get-tuple-element.62), channel_id=1, source_target_pairs={{0,3},{1,0},{2,1},{3,2},{4,7},{5,4},{6,5},{7,6},{8,11},{9,8},{10,9... | collective-permute-start | bytes 1572872 | tf_op jit(solution)/shard_map/ppermute | solution.py:378
  186.6 24.9 %collective-permute-start.21 = (bf16[64,1280]{1,0:T(8,128)(2,1)}, bf16[64,1280]{1,0:T(8,128)(2,1)S(1)}, u32[]{:S(2)}, u32[]{:S(2)}) collective-permute-start(bf16[64,1280]{1,0:T(8,128)(2,1)} %copy-done.28), channel_id=1, source_target_pairs={{0,12},{4,16},{8,20},{12,24},{16,28},{20,0},{24,4},{28,8},{1,13},{... | collective-permute-start | bytes 491528 | tf_op jit(solution)/shard_map/ppermute | solution.py:378
  192.2 19.3 %collective-permute-start.22 = (bf16[64,1280]{1,0:T(8,128)(2,1)}, bf16[64,1280]{1,0:T(8,128)(2,1)S(1)}, u32[]{:S(2)}, u32[]{:S(2)}) collective-permute-start(bf16[64,1280]{1,0:T(8,128)(2,1)} %copy-done.27), channel_id=1, source_target_pairs={{0,16},{4,20},{8,24},{12,28},{16,0},{20,4},{24,8},{28,12},{1,17},{... | collective-permute-start | bytes 491528 | tf_op jit(solution)/shard_map/ppermute | solution.py:378
  198.2 13.3 %collective-permute-start.23 = (bf16[64,1280]{1,0:T(8,128)(2,1)}, bf16[64,1280]{1,0:T(8,128)(2,1)S(1)}, u32[]{:S(2)}, u32[]{:S(2)}) collective-permute-start(bf16[64,1280]{1,0:T(8,128)(2,1)} %copy-done.26), channel_id=1, source_target_pairs={{0,20},{4,24},{8,28},{12,0},{16,4},{20,8},{24,12},{28,16},{1,21},{... | collective-permute-start | bytes 491528 | tf_op jit(solution)/shard_map/ppermute | solution.py:378
  202.4 9.1 %collective-permute-start.24 = (bf16[64,1280]{1,0:T(8,128)(2,1)}, bf16[64,1280]{1,0:T(8,128)(2,1)S(1)}, u32[]{:S(2)}, u32[]{:S(2)}) collective-permute-start(bf16[64,1280]{1,0:T(8,128)(2,1)} %copy-done.25), channel_id=1, source_target_pairs={{0,24},{4,28},{8,0},{12,4},{16,8},{20,12},{24,16},{28,20},{1,25},{... | collective-permute-start | bytes 491528 | tf_op jit(solution)/shard_map/ppermute | solution.py:378
  222.2 18.7 %collective-permute-start.26 = (bf16[128,1280]{1,0:T(8,128)(2,1)}, bf16[128,1280]{1,0:T(8,128)(2,1)S(1)}, u32[]{:S(2)}, u32[]{:S(2)}) collective-permute-start(bf16[128,1280]{1,0:T(8,128)(2,1)} %get-tuple-element.78), channel_id=1, source_target_pairs={{0,2},{1,3},{2,0},{3,1},{4,6},{5,7},{6,4},{7,5},{8,10},{9,11},{10,... | collective-permute-start | bytes 983048 | tf_op jit(solution)/shard_map/ppermute | solution.py:436
  223.2 17.6 %collective-permute-start.27 = (bf16[128,1280]{1,0:T(8,128)(2,1)}, bf16[128,1280]{1,0:T(8,128)(2,1)S(1)}, u32[]{:S(2)}, u32[]{:S(2)}) collective-permute-start(bf16[128,1280]{1,0:T(8,128)(2,1)} %get-tuple-element.79), channel_id=1, source_target_pairs={{0,1},{1,0},{2,3},{3,2},{4,5},{5,4},{6,7},{7,6},{8,9},{9,8},{10,11... | collective-permute-start | bytes 983048 | tf_op jit(solution)/shard_map/ppermute | solution.py:436
  227.8 16.5 %collective-permute-start.28 = (bf16[128,1280]{1,0:T(8,128)(2,1)}, bf16[128,1280]{1,0:T(8,128)(2,1)S(1)}, u32[]{:S(2)}, u32[]{:S(2)}) collective-permute-start(bf16[128,1280]{1,0:T(8,128)(2,1)} %get-tuple-element.80), channel_id=1, source_target_pairs={{0,3},{1,2},{2,1},{3,0},{4,7},{5,6},{6,5},{7,4},{8,11},{9,10},{10,... | collective-permute-start | bytes 983048 | tf_op jit(solution)/shard_map/ppermute | solution.py:436
  231.0 18.6 %all-to-all-start.4 = ((bf16[8,16,768]{2,1,0:T(8,128)(2,1)}), bf16[8,16,768]{2,1,0:T(8,128)(2,1)S(1)}, u32[]{:S(2)}, u32[]{:S(2)}) async-start(bf16[8,16,768]{2,1,0:T(8,128)(2,1)} %shard_map.115), calls=%async_computation.4 | async-start | bytes 393216 | tf_op jit(solution)/shard_map/all_to_all | solution.py:382
  (35 other events, 241.4 us)

commit v6 on v5

--- a/solution.py
+++ b/solution.py
@@ -164,9 +164,10 @@
         for r in range(fs):
             group = lax.rem(me_ref[0] + r, fs)
             full = jnp.concatenate([ins[q][group] for q in order], axis=-1)
-            for k, (low, high) in enumerate(cuts[:-1]):
-                outs[k * fs + r][...] = full[:, low:high]
-            outs[-1][group] = full[:, cuts[-1][0] :]
+            low, high = cuts[0]
+            outs[r][...] = full[:, low:high]
+            for out, (low, high) in zip(outs[fs:], cuts[1:]):
+                out[group] = full[:, low:high]
 
     in_order(me_ref, tp, store)
 
@@ -174,8 +175,8 @@
 def merge(me, parts, cuts):
     tp = len(parts)
     fs, rows, _ = parts[0].shape
-    shapes = [(rows, high - low) for low, high in cuts[:-1] for _ in range(fs)]
-    shapes.append((fs, rows, cuts[-1][1] - cuts[-1][0]))
+    sizes = [high - low for low, high in cuts]
+    shapes = [(rows, sizes[0])] * fs + [(fs, rows, size) for size in sizes[1:]]
     outs = pl.pallas_call(
         functools.partial(merge_kernel, fs, tp, cuts),
         grid_spec=pltpu.PrefetchScalarGridSpec(
@@ -188,7 +189,7 @@
         compiler_params=grant(16),
         cost_estimate=cost(1e9, 4 * tp * parts[0].size),
     )(me, *parts)
-    return [outs[k * fs : (k + 1) * fs] for k in range(len(cuts) - 1)] + [outs[-1]]
+    return [outs[:fs], *outs[fs:]]
 
 
 def regroup_kernel(fs, tp, me_ref, *refs):
@@ -417,8 +418,8 @@
         for step in range(2, tp, 2)
     ]
     rows += [lax.ppermute(part, "tp", [(k, k ^ 1) for k in range(tp)]) for part in rows]
-    (up_here,) = merge(me, up_parts, [(0, tp * up_parts[0].shape[2])])
-    up_parts = [swap_fs(up_here)]
+    (up_parts,) = merge(me, up_parts, [(0, tp * up_parts[0].shape[2])])
+    up_parts = rotate(up_parts, "fs")
     gate_parts = regroup(me, gate_parts)
     gate_parts = rotate(gate_parts, "tp")
     down_parts = merge(me, down_parts, cuts)

time: 268 us -> 248 us (0.925)
  waiting for transfers between devices: 114 us -> 78.8 us
  starting transfers between devices: 86.5 us -> 106 us
    ppermute x23 -> x30, starting transfers between devices: 50.4 us -> 74.4 us  [rotate(): out[r] = lax.ppermute(parts[r], axis, [(k, (k + r) % n) for k in range(n)])]
    all_to_all x4 -> x3, waiting for transfers between devices: 26.8 us -> 5.43 us  [swap_fs(): out = lax.all_to_all(value, 'fs', 0, 0, tiled=True)]
    ppermute x23 -> x30, waiting for transfers between devices: 77.7 us -> 65.3 us  [rotate(): out[r] = lax.ppermute(parts[r], axis, [(k, (k + r) % n) for k in range(n)])]
    all_to_all x4 -> x3, starting transfers between devices: 31.9 us -> 21.2 us  [swap_fs(): out = lax.all_to_all(value, 'fs', 0, 0, tiled=True)]
    ppermute x6, starting transfers between devices: 3.72 us -> 8.74 us  [shards(): lax.ppermute(term, 'tp', list(enumerate(places)))]
    unnamed x62 -> x76, local copies, waits for them, and re-layouts: 18.6 us -> 16.3 us
  transfers between devices with their start and end apart: 36 -> 42, of which waited for: 14 -> 12; matrix products, arithmetic and copies ran while one was open for 0% -> 0% of each run, Pallas kernels for 9% -> 10%
where the time goes in v6:
time: 248 us
  starting transfers between devices  106 us (43%)
  waiting for transfers between devices  78.8 us (32%)
  Pallas kernels  29.7 us (12%)
  local copies, waits for them, and re-layouts  16.3 us (7%)
  blocking collectives  15.5 us (6%)
    ppermute x30, starting transfers between devices, rotate(): out[r] = lax.ppermute(parts[r], axis, [(k, (k + r) % n) for k in range(n)])  74.4 us
    ppermute x30, waiting for transfers between devices, rotate(): out[r] = lax.ppermute(parts[r], axis, [(k, (k + r) % n) for k in range(n)])  65.3 us
    all_to_all x3, starting transfers between devices, swap_fs(): out = lax.all_to_all(value, 'fs', 0, 0, tiled=True)  21.2 us
    unnamed x76, local copies, waits for them, and re-layouts  16.3 us
    all_to_all x1, blocking collectives, swap_fs(): out = lax.all_to_all(value, 'fs', 0, 0, tiled=True)  15.5 us
    pallas_call x4, Pallas kernels, cast_along(): pl.pallas_call(functools.partial(cast_kernel, steps, scale is not None, a...  10.2 us
    ppermute x6, starting transfers between devices, shards(): lax.ppermute(term, 'tp', list(enumerate(places)))  8.74 us
    ppermute x6, waiting for transfers between devices, shards(): lax.ppermute(term, 'tp', list(enumerate(places)))  8.1 us
  transfers between devices with their start and end apart: 42, of which 12 were waited for; matrix products, arithmetic and copies ran while one was open for 0% of the time, Pallas kernels for 10%

profile of v6, /device:TPU:0, one launch (start us, length us, event | category | flops | bytes accessed | tf_op | source)
XLA Modules:
  0.0 247.8 jit_solution(6389944843013778508)
XLA Ops:
  0.6 2.4 shard_map.102
  3.0 7.3 %all-to-all-start = ((bf16[8,16,2176]{2,1,0:T(8,128)(2,1)}), bf16[8,16,2176]{2,1,0:T(8,128)(2,1)S(1)}, u32[]{:S(2)}, u32[]{:S(2)}) async-start(bf16[8,16,2176]{2,1,0:T(8,128)(2,1)} %bitcast.34), calls=%async_computation | async-start | bytes 1114112 | tf_op jit(solution)/shard_map/all_to_all | solution.py:383
  12.6 2.5 %shard_map.103 = (bf16[8,256,128]{2,1,0:T(8,128)(2,1)S(1)}, bf16[8,256,128]{2,1,0:T(8,128)(2,1)}, bf16[8,256,128]{2,1,0:T(8,128)(2,1)S(1)}, bf16[8,256,128]{2,1,0:T(8,128)(2,1)S(1)}) custom-call(s32[2]{0:T(128)S(1)} %pad_add_fusion.me_ref, f32[8,4,256,128]{3,2,1,0:T(8,128)S(1)} %bitcast.24, f32[1,256]{1,0:T(1,128)S(1)} %bitcast.30), custom_call_target="tpu_custom_call" | custom-call | flops 1000000000 | bytes 6291456 | tf_op jit(solution)/shard_map/pallas_call | solution.py:141
  15.1 2.3 shard_map.105
  20.9 3.9 %shard_map.106 = (bf16[4,256,128]{2,1,0:T(8,128)(2,1)}, bf16[4,256,128]{2,1,0:T(8,128)(2,1)}, bf16[4,256,128]{2,1,0:T(8,128)(2,1)}) custom-call(s32[2]{0:T(128)} %copy-done.7, f32[8,4,256,128]{3,2,1,0:T(8,128)} %bitcast.16, f32[1,256]{1,0:T(1,128)} %bitcast.29), custom_call_target="tpu_custom_call" | custom-call | flops 1000000000 | bytes 2359296 | tf_op jit(solution)/shard_map/pallas_call | solution.py:141
  24.9 2.4 collective-permute-start.15
  28.7 2.2 copy-done.2
  34.6 20.9 %collective-permute-done.15.refs_3_ = bf16[4,256,128]{2,1,0:T(8,128)(2,1)S(1)} collective-permute-done((bf16[4,256,128]{2,1,0:T(8,128)(2,1)}, bf16[4,256,128]{2,1,0:T(8,128)(2,1)S(1)}, u32[]{:S(2)}, u32[]{:S(2)}) %collective-permute-start.15) | collective-permute-done | bytes 262176 | tf_op jit(solution)/shard_map/ppermute | solution.py:379
  58.8 3.3 %collective-permute-start.17 = (bf16[4,256,128]{2,1,0:T(8,128)(2,1)S(1)}, bf16[4,256,128]{2,1,0:T(8,128)(2,1)}, u32[]{:S(2)}, u32[]{:S(2)}) collective-permute-start(bf16[4,256,128]{2,1,0:T(8,128)(2,1)S(1)} %copy-done.37), channel_id=1, source_target_pairs={{0,20},{4,24},{8,28},{12,0},{16,4},{20,8},{24,12},{28,16},{1,21},{... | collective-permute-start | bytes 786440 | tf_op jit(solution)/shard_map/ppermute | solution.py:379
  63.6 3.2 %collective-permute-done.25.refs_3_ = bf16[8,64,512]{2,1,0:T(8,128)(2,1)S(1)} collective-permute-done((bf16[8,64,512]{2,1,0:T(8,128)(2,1)S(1)}, bf16[8,64,512]{2,1,0:T(8,128)(2,1)S(1)}, u32[]{:S(2)}, u32[]{:S(2)}) %collective-permute-start.25) | collective-permute-done | bytes 524320 | tf_op jit(solution)/shard_map/ppermute | solution.py:379
  73.1 3.0 %collective-permute-done.4.refs_2_ = bf16[8,256,128]{2,1,0:T(8,128)(2,1)S(1)} collective-permute-done((bf16[8,256,128]{2,1,0:T(8,128)(2,1)S(1)}, bf16[8,256,128]{2,1,0:T(8,128)(2,1)S(1)}, u32[]{:S(2)}, u32[]{:S(2)}) %collective-permute-start.4) | collective-permute-done | bytes 524320 | tf_op jit(solution)/shard_map/ppermute | solution.py:379
  76.9 2.8 %collective-permute-done.5.refs_3_ = bf16[8,256,128]{2,1,0:T(8,128)(2,1)S(1)} collective-permute-done((bf16[8,256,128]{2,1,0:T(8,128)(2,1)S(1)}, bf16[8,256,128]{2,1,0:T(8,128)(2,1)S(1)}, u32[]{:S(2)}, u32[]{:S(2)}) %collective-permute-start.5) | collective-permute-done | bytes 524320 | tf_op jit(solution)/shard_map/ppermute | solution.py:379
  82.1 5.5 %all-to-all-start.2 = ((bf16[8,64,768]{2,1,0:T(8,128)(2,1)}), bf16[8,64,768]{2,1,0:T(8,128)(2,1)S(1)}, u32[]{:S(2)}, u32[]{:S(2)}) async-start(bf16[8,64,768]{2,1,0:T(8,128)(2,1)} %get-tuple-element.97), calls=%async_computation.2 | async-start | bytes 1572864 | tf_op jit(solution)/shard_map/all_to_all | solution.py:383
  94.1 2.4 collective-permute-start.8
  97.2 23.3 %collective-permute-done.27.refs_6_ = bf16[64,1280]{1,0:T(8,128)(2,1)S(1)} collective-permute-done((bf16[64,1280]{1,0:T(8,128)(2,1)S(1)}, bf16[64,1280]{1,0:T(8,128)(2,1)S(1)}, u32[]{:S(2)}, u32[]{:S(2)}) %collective-permute-start.27) | collective-permute-done | bytes 163872 | tf_op jit(solution)/shard_map/ppermute | solution.py:379
  120.4 3.4 %collective-permute-start.9 = (bf16[256,512]{1,0:T(8,128)(2,1)S(1)}, bf16[256,512]{1,0:T(8,128)(2,1)S(1)}, u32[]{:S(2)}, u32[]{:S(2)}) collective-permute-start(bf16[256,512]{1,0:T(8,128)(2,1)S(1)} %get-tuple-element.63), channel_id=1, source_target_pairs={{0,16},{4,20},{8,24},{12,28},{16,0},{20,4},{24,8},{28,12},{1,17},{... | collective-permute-start | bytes 786440 | tf_op jit(solution)/shard_map/ppermute | solution.py:379
  123.8 12.7 %collective-permute-start.10 = (bf16[256,512]{1,0:T(8,128)(2,1)S(1)}, bf16[256,512]{1,0:T(8,128)(2,1)S(1)}, u32[]{:S(2)}, u32[]{:S(2)}) collective-permute-start(bf16[256,512]{1,0:T(8,128)(2,1)S(1)} %get-tuple-element.64), channel_id=1, source_target_pairs={{0,20},{4,24},{8,28},{12,0},{16,4},{20,8},{24,12},{28,16},{1,21},{... | collective-permute-start | bytes 786440 | tf_op jit(solution)/shard_map/ppermute | solution.py:379
  140.5 2.8 %collective-permute-done.10.refs_9_ = bf16[256,512]{1,0:T(8,128)(2,1)S(1)} collective-permute-done((bf16[256,512]{1,0:T(8,128)(2,1)S(1)}, bf16[256,512]{1,0:T(8,128)(2,1)S(1)}, u32[]{:S(2)}, u32[]{:S(2)}) %collective-permute-start.10) | collective-permute-done | bytes 262176 | tf_op jit(solution)/shard_map/ppermute | solution.py:379
  143.3 8.0 %collective-permute-done.11.refs_10_ = bf16[256,512]{1,0:T(8,128)(2,1)S(1)} collective-permute-done((bf16[256,512]{1,0:T(8,128)(2,1)S(1)}, bf16[256,512]{1,0:T(8,128)(2,1)S(1)}, u32[]{:S(2)}, u32[]{:S(2)}) %collective-permute-start.11) | collective-permute-done | bytes 262176 | tf_op jit(solution)/shard_map/ppermute | solution.py:379
  153.7 19.7 %collective-permute-start.28 = (bf16[64,1280]{1,0:T(8,128)(2,1)S(1)}, bf16[64,1280]{1,0:T(8,128)(2,1)S(1)}, u32[]{:S(2)}, u32[]{:S(2)}) collective-permute-start(bf16[64,1280]{1,0:T(8,128)(2,1)S(1)} %copy-done.34), channel_id=1, source_target_pairs={{0,12},{4,16},{8,20},{12,24},{16,28},{20,0},{24,4},{28,8},{1,13},{... | collective-permute-start | bytes 491528 | tf_op jit(solution)/shard_map/ppermute | solution.py:379
  173.4 4.6 %collective-permute-start.29 = (bf16[64,1280]{1,0:T(8,128)(2,1)S(1)}, bf16[64,1280]{1,0:T(8,128)(2,1)S(1)}, u32[]{:S(2)}, u32[]{:S(2)}) collective-permute-start(bf16[64,1280]{1,0:T(8,128)(2,1)S(1)} %copy-done.32), channel_id=1, source_target_pairs={{0,16},{4,20},{8,24},{12,28},{16,0},{20,4},{24,8},{28,12},{1,17},{... | collective-permute-start | bytes 491528 | tf_op jit(solution)/shard_map/ppermute | solution.py:379
  178.2 8.2 %collective-permute-start.31 = (bf16[64,1280]{1,0:T(8,128)(2,1)S(1)}, bf16[64,1280]{1,0:T(8,128)(2,1)S(1)}, u32[]{:S(2)}, u32[]{:S(2)}) collective-permute-start(bf16[64,1280]{1,0:T(8,128)(2,1)S(1)} %copy-done.28), channel_id=1, source_target_pairs={{0,24},{4,28},{8,0},{12,4},{16,8},{20,12},{24,16},{28,20},{1,25},{... | collective-permute-start | bytes 491528 | tf_op jit(solution)/shard_map/ppermute | solution.py:379
  187.9 3.2 %shard_map.108 = (bf16[2048,512]{1,0:T(8,128)(2,1)}, f32[512,512]{1,0:T(8,128)S(1)}) custom-call(s32[2]{0:T(128)S(1)} %copy-done.8, bf16[128,2176]{1,0:T(8,128)(2,1)S(1)} %bitcast.20, bf16[128,2176]{1,0:T(8,128)(2,1)S(1)} %collective-permute-done.refs_1_, bf16[128,2176]{1,0:T(8,128)(2,1)S(1)} %collective-permute-done.1.refs_2_, ...), custom_call_target="tpu_custom_call" | custom-call | flops 1073741824 | bytes 4194304 | tf_op jit(solution)/shard_map/pallas_call | solution.py:248
  191.1 2.3 shard_map.109
  193.4 3.4 %shard_map.112 = (bf16[512,2048]{1,0:T(8,128)(2,1)}, bf16[128,1280]{1,0:T(8,128)(2,1)S(1)}, bf16[128,1280]{1,0:T(8,128)(2,1)}, bf16[128,1280]{1,0:T(8,128)(2,1)}, bf16[128,1280]{1,0:T(8,128)(2,1)}) custom-call(s32[2]{0:T(128)S(1)} %copy-done.8, bf16[512,512]{1,0:T(8,128)(2,1)S(1)} %get-tuple-element.80.hidden_ref, bf16[128,2176]{1,0:T(8,128)(2,1)S(1)} %bitcast.22, ...), custom_call_target="tpu_custom_call" | custom-call | flops 671088640 | bytes 2621440 | tf_op jit(solution)/shard_map/pallas_call | solution.py:340
  200.4 2.3 collective-permute-start.37
  205.4 3.4 %collective-permute-start.35 = (bf16[128,1280]{1,0:T(8,128)(2,1)}, bf16[128,1280]{1,0:T(8,128)(2,1)S(1)}, u32[]{:S(2)}, u32[]{:S(2)}) collective-permute-start(bf16[128,1280]{1,0:T(8,128)(2,1)} %get-tuple-element.96), channel_id=1, source_target_pairs={{0,3},{1,2},{2,1},{3,0},{4,7},{5,6},{6,5},{7,4},{8,11},{9,10},{10,... | collective-permute-start | bytes 983048 | tf_op jit(solution)/shard_map/ppermute | solution.py:437
  208.8 3.7 %collective-permute-done.38.refs_3_ = bf16[128,768]{1,0:T(8,128)(2,1)S(1)} collective-permute-done((bf16[128,768]{1,0:T(8,128)(2,1)S(1)}, bf16[128,768]{1,0:T(8,128)(2,1)S(1)}, u32[]{:S(2)}, u32[]{:S(2)}) %collective-permute-start.38) | collective-permute-done | bytes 196640 | tf_op jit(solution)/shard_map/ppermute | solution.py:437
  213.3 8.5 %all-to-all-start.3 = ((bf16[8,16,768]{2,1,0:T(8,128)(2,1)}), bf16[8,16,768]{2,1,0:T(8,128)(2,1)S(1)}, u32[]{:S(2)}, u32[]{:S(2)}) async-start(bf16[8,16,768]{2,1,0:T(8,128)(2,1)} %shard_map.115), calls=%async_computation.3 | async-start | bytes 393216 | tf_op jit(solution)/shard_map/all_to_all | solution.py:383
  221.8 3.6 %collective-permute-done.35.refs_3_ = bf16[128,1280]{1,0:T(8,128)(2,1)S(1)} collective-permute-done((bf16[128,1280]{1,0:T(8,128)(2,1)}, bf16[128,1280]{1,0:T(8,128)(2,1)S(1)}, u32[]{:S(2)}, u32[]{:S(2)}) %collective-permute-start.35) | collective-permute-done | bytes 327712 | tf_op jit(solution)/shard_map/ppermute | solution.py:437
  225.6 5.4 %all-to-all-done.3 = bf16[8,16,768]{2,1,0:T(8,128)(2,1)S(1)} async-done(((bf16[8,16,768]{2,1,0:T(8,128)(2,1)}), bf16[8,16,768]{2,1,0:T(8,128)(2,1)S(1)}, u32[]{:S(2)}, u32[]{:S(2)}) %all-to-all-start.3) | async-done | bytes 196640 | tf_op jit(solution)/shard_map/all_to_all | solution.py:383
  231.0 15.5 %all_to_all.20 = bf16[8,16,1280]{2,1,0:T(8,128)(2,1)S(1)} all-to-all(bf16[8,16,1280]{2,1,0:T(8,128)(2,1)S(1)} %shard_map.113), channel_id=1, replica_groups=mesh['fs'=8,'tp'=4] {'fs'}, dimensions={0} | all-to-all | bytes 655360 | tf_op jit(solution)/shard_map/all_to_all | solution.py:383
  (145 shorter events, 48.8 us)
Async XLA Ops:
  3.0 77.5 %all-to-all-start = ((bf16[8,16,2176]{2,1,0:T(8,128)(2,1)}), bf16[8,16,2176]{2,1,0:T(8,128)(2,1)S(1)}, u32[]{:S(2)}, u32[]{:S(2)}) async-start(bf16[8,16,2176]{2,1,0:T(8,128)(2,1)} %bitcast.34), calls=%async_computation | async-start | bytes 1114112 | tf_op jit(solution)/shard_map/all_to_all | solution.py:383
  15.1 43.3 %collective-permute-start.3 = (bf16[8,256,128]{2,1,0:T(8,128)(2,1)}, bf16[8,256,128]{2,1,0:T(8,128)(2,1)S(1)}, u32[]{:S(2)}, u32[]{:S(2)}) collective-permute-start(bf16[8,256,128]{2,1,0:T(8,128)(2,1)} %get-tuple-element.56), channel_id=1, source_target_pairs={{0,1},{1,2},{2,3},{3,0},{4,5},{5,6},{6,7},{7,4},{8,9},{9,10},{10,1... | collective-permute-start | bytes 1572872 | tf_op jit(solution)/shard_map/ppermute | solution.py:379
  24.9 30.6 %collective-permute-start.15 = (bf16[4,256,128]{2,1,0:T(8,128)(2,1)}, bf16[4,256,128]{2,1,0:T(8,128)(2,1)S(1)}, u32[]{:S(2)}, u32[]{:S(2)}) collective-permute-start(bf16[4,256,128]{2,1,0:T(8,128)(2,1)} %get-tuple-element.70), channel_id=1, source_target_pairs={{0,12},{4,16},{8,20},{12,24},{16,28},{20,0},{24,4},{28,8},{1,13},{... | collective-permute-start | bytes 786440 | tf_op jit(solution)/shard_map/ppermute | solution.py:379
  27.2 29.0 %collective-permute-start.16 = (bf16[4,256,128]{2,1,0:T(8,128)(2,1)}, bf16[4,256,128]{2,1,0:T(8,128)(2,1)S(1)}, u32[]{:S(2)}, u32[]{:S(2)}) collective-permute-start(bf16[4,256,128]{2,1,0:T(8,128)(2,1)} %get-tuple-element.71), channel_id=1, source_target_pairs={{0,16},{4,20},{8,24},{12,28},{16,0},{20,4},{24,8},{28,12},{1,17},{... | collective-permute-start | bytes 786440 | tf_op jit(solution)/shard_map/ppermute | solution.py:379
  33.1 25.7 %collective-permute-start.23 = (bf16[8,64,512]{2,1,0:T(8,128)(2,1)S(1)}, bf16[8,64,512]{2,1,0:T(8,128)(2,1)S(1)}, u32[]{:S(2)}, u32[]{:S(2)}) collective-permute-start(bf16[8,64,512]{2,1,0:T(8,128)(2,1)S(1)} %get-tuple-element.82), channel_id=1, source_target_pairs={{0,1},{1,2},{2,3},{3,0},{4,5},{5,6},{6,7},{7,4},{8,9},{9,10},{10,1... | collective-permute-start | bytes 1572872 | tf_op jit(solution)/shard_map/ppermute | solution.py:379
  33.6 28.5 %collective-permute-start.24 = (bf16[8,64,512]{2,1,0:T(8,128)(2,1)S(1)}, bf16[8,64,512]{2,1,0:T(8,128)(2,1)S(1)}, u32[]{:S(2)}, u32[]{:S(2)}) collective-permute-start(bf16[8,64,512]{2,1,0:T(8,128)(2,1)S(1)} %get-tuple-element.83), channel_id=1, source_target_pairs={{0,2},{1,3},{2,0},{3,1},{4,6},{5,7},{6,4},{7,5},{8,10},{9,11},{10,... | collective-permute-start | bytes 1572872 | tf_op jit(solution)/shard_map/ppermute | solution.py:379
  56.9 19.2 %collective-permute-start.4 = (bf16[8,256,128]{2,1,0:T(8,128)(2,1)S(1)}, bf16[8,256,128]{2,1,0:T(8,128)(2,1)S(1)}, u32[]{:S(2)}, u32[]{:S(2)}) collective-permute-start(bf16[8,256,128]{2,1,0:T(8,128)(2,1)S(1)} %get-tuple-element.57), channel_id=1, source_target_pairs={{0,2},{1,3},{2,0},{3,1},{4,6},{5,7},{6,4},{7,5},{8,10},{9,11},{10,... | collective-permute-start | bytes 1572872 | tf_op jit(solution)/shard_map/ppermute | solution.py:379
  58.4 21.3 %collective-permute-start.5 = (bf16[8,256,128]{2,1,0:T(8,128)(2,1)S(1)}, bf16[8,256,128]{2,1,0:T(8,128)(2,1)S(1)}, u32[]{:S(2)}, u32[]{:S(2)}) collective-permute-start(bf16[8,256,128]{2,1,0:T(8,128)(2,1)S(1)} %get-tuple-element.58), channel_id=1, source_target_pairs={{0,3},{1,0},{2,1},{3,2},{4,7},{5,4},{6,5},{7,6},{8,11},{9,8},{10,9... | collective-permute-start | bytes 1572872 | tf_op jit(solution)/shard_map/ppermute | solution.py:379
  58.8 31.8 %collective-permute-start.17 = (bf16[4,256,128]{2,1,0:T(8,128)(2,1)S(1)}, bf16[4,256,128]{2,1,0:T(8,128)(2,1)}, u32[]{:S(2)}, u32[]{:S(2)}) collective-permute-start(bf16[4,256,128]{2,1,0:T(8,128)(2,1)S(1)} %copy-done.37), channel_id=1, source_target_pairs={{0,20},{4,24},{8,28},{12,0},{16,4},{20,8},{24,12},{28,16},{1,21},{... | collective-permute-start | bytes 786440 | tf_op jit(solution)/shard_map/ppermute | solution.py:379
  62.1 30.6 %collective-permute-start.18 = (bf16[4,256,128]{2,1,0:T(8,128)(2,1)}, bf16[4,256,128]{2,1,0:T(8,128)(2,1)}, u32[]{:S(2)}, u32[]{:S(2)}) collective-permute-start(bf16[4,256,128]{2,1,0:T(8,128)(2,1)} %get-tuple-element.73), channel_id=1, source_target_pairs={{0,24},{4,28},{8,0},{12,4},{16,8},{20,12},{24,16},{28,20},{1,25},{... | collective-permute-start | bytes 786440 | tf_op jit(solution)/shard_map/ppermute | solution.py:379
  66.7 27.3 %collective-permute-start.19 = (bf16[4,256,128]{2,1,0:T(8,128)(2,1)}, bf16[4,256,128]{2,1,0:T(8,128)(2,1)}, u32[]{:S(2)}, u32[]{:S(2)}) collective-permute-start(bf16[4,256,128]{2,1,0:T(8,128)(2,1)} %get-tuple-element.74), channel_id=1, source_target_pairs={{0,28},{4,0},{8,4},{12,8},{16,12},{20,16},{24,20},{28,24},{1,29},{... | collective-permute-start | bytes 786440 | tf_op jit(solution)/shard_map/ppermute | solution.py:379
  76.9 19.6 %collective-permute-start.26 = (bf16[64,1280]{1,0:T(8,128)(2,1)}, bf16[64,1280]{1,0:T(8,128)(2,1)S(1)}, u32[]{:S(2)}, u32[]{:S(2)}) collective-permute-start(bf16[64,1280]{1,0:T(8,128)(2,1)} %get-tuple-element.86), channel_id=1, source_target_pairs={{0,4},{4,8},{8,12},{12,16},{16,20},{20,24},{24,28},{28,0},{1,5},{5... | collective-permute-start | bytes 491528 | tf_op jit(solution)/shard_map/ppermute | solution.py:379
  80.5 57.5 %collective-permute-start = (bf16[128,2176]{1,0:T(8,128)(2,1)S(1)}, bf16[128,2176]{1,0:T(8,128)(2,1)S(1)}, u32[]{:S(2)}, u32[]{:S(2)}) collective-permute-start(bf16[128,2176]{1,0:T(8,128)(2,1)S(1)} %bitcast.18), channel_id=1, source_target_pairs={{0,2},{1,3},{2,0},{3,1},{4,6},{5,7},{6,4},{7,5},{8,10},{9,11},{10,... | collective-permute-start | bytes 1671176 | tf_op jit(solution)/shard_map/ppermute | solution.py:417
  82.1 115.5 %all-to-all-start.2 = ((bf16[8,64,768]{2,1,0:T(8,128)(2,1)}), bf16[8,64,768]{2,1,0:T(8,128)(2,1)S(1)}, u32[]{:S(2)}, u32[]{:S(2)}) async-start(bf16[8,64,768]{2,1,0:T(8,128)(2,1)} %get-tuple-element.97), calls=%async_computation.2 | async-start | bytes 1572864 | tf_op jit(solution)/shard_map/all_to_all | solution.py:383
  90.5 33.3 %collective-permute-start.6 = (bf16[256,512]{1,0:T(8,128)(2,1)S(1)}, bf16[256,512]{1,0:T(8,128)(2,1)S(1)}, u32[]{:S(2)}, u32[]{:S(2)}) collective-permute-start(bf16[256,512]{1,0:T(8,128)(2,1)S(1)} %get-tuple-element.60), channel_id=1, source_target_pairs={{0,4},{4,8},{8,12},{12,16},{16,20},{20,24},{24,28},{28,0},{1,5},{5... | collective-permute-start | bytes 786440 | tf_op jit(solution)/shard_map/ppermute | solution.py:379
  92.6 43.9 %collective-permute-start.7 = (bf16[256,512]{1,0:T(8,128)(2,1)S(1)}, bf16[256,512]{1,0:T(8,128)(2,1)S(1)}, u32[]{:S(2)}, u32[]{:S(2)}) collective-permute-start(bf16[256,512]{1,0:T(8,128)(2,1)S(1)} %get-tuple-element.61), channel_id=1, source_target_pairs={{0,8},{4,12},{8,16},{12,20},{16,24},{20,28},{24,0},{28,4},{1,9},{5... | collective-permute-start | bytes 786440 | tf_op jit(solution)/shard_map/ppermute | solution.py:379
  94.1 42.9 %collective-permute-start.8 = (bf16[256,512]{1,0:T(8,128)(2,1)S(1)}, bf16[256,512]{1,0:T(8,128)(2,1)S(1)}, u32[]{:S(2)}, u32[]{:S(2)}) collective-permute-start(bf16[256,512]{1,0:T(8,128)(2,1)S(1)} %get-tuple-element.62), channel_id=1, source_target_pairs={{0,12},{4,16},{8,20},{12,24},{16,28},{20,0},{24,4},{28,8},{1,13},{... | collective-permute-start | bytes 786440 | tf_op jit(solution)/shard_map/ppermute | solution.py:379
  97.1 23.3 %collective-permute-start.27 = (bf16[64,1280]{1,0:T(8,128)(2,1)S(1)}, bf16[64,1280]{1,0:T(8,128)(2,1)S(1)}, u32[]{:S(2)}, u32[]{:S(2)}) collective-permute-start(bf16[64,1280]{1,0:T(8,128)(2,1)S(1)} %copy-done.36), channel_id=1, source_target_pairs={{0,8},{4,12},{8,16},{12,20},{16,24},{20,28},{24,0},{28,4},{1,9},{5... | collective-permute-start | bytes 491528 | tf_op jit(solution)/shard_map/ppermute | solution.py:379
  120.4 17.6 %collective-permute-start.9 = (bf16[256,512]{1,0:T(8,128)(2,1)S(1)}, bf16[256,512]{1,0:T(8,128)(2,1)S(1)}, u32[]{:S(2)}, u32[]{:S(2)}) collective-permute-start(bf16[256,512]{1,0:T(8,128)(2,1)S(1)} %get-tuple-element.63), channel_id=1, source_target_pairs={{0,16},{4,20},{8,24},{12,28},{16,0},{20,4},{24,8},{28,12},{1,17},{... | collective-permute-start | bytes 786440 | tf_op jit(solution)/shard_map/ppermute | solution.py:379
  123.8 19.4 %collective-permute-start.10 = (bf16[256,512]{1,0:T(8,128)(2,1)S(1)}, bf16[256,512]{1,0:T(8,128)(2,1)S(1)}, u32[]{:S(2)}, u32[]{:S(2)}) collective-permute-start(bf16[256,512]{1,0:T(8,128)(2,1)S(1)} %get-tuple-element.64), channel_id=1, source_target_pairs={{0,20},{4,24},{8,28},{12,0},{16,4},{20,8},{24,12},{28,16},{1,21},{... | collective-permute-start | bytes 786440 | tf_op jit(solution)/shard_map/ppermute | solution.py:379
  137.0 16.7 %collective-permute-start.12 = (bf16[256,512]{1,0:T(8,128)(2,1)S(1)}, bf16[256,512]{1,0:T(8,128)(2,1)S(1)}, u32[]{:S(2)}, u32[]{:S(2)}) collective-permute-start(bf16[256,512]{1,0:T(8,128)(2,1)S(1)} %get-tuple-element.66), channel_id=1, source_target_pairs={{0,28},{4,0},{8,4},{12,8},{16,12},{20,16},{24,20},{28,24},{1,29},{... | collective-permute-start | bytes 786440 | tf_op jit(solution)/shard_map/ppermute | solution.py:379
  138.1 40.2 %collective-permute-start.1 = (bf16[128,2176]{1,0:T(8,128)(2,1)S(1)}, bf16[128,2176]{1,0:T(8,128)(2,1)S(1)}, u32[]{:S(2)}, u32[]{:S(2)}) collective-permute-start(bf16[128,2176]{1,0:T(8,128)(2,1)S(1)} %bitcast.19), channel_id=1, source_target_pairs={{0,1},{1,0},{2,3},{3,2},{4,5},{5,4},{6,7},{7,6},{8,9},{9,8},{10,11... | collective-permute-start | bytes 1671176 | tf_op jit(solution)/shard_map/ppermute | solution.py:420
  138.1 48.4 %collective-permute-start.2 = (bf16[128,2176]{1,0:T(8,128)(2,1)S(1)}, bf16[128,2176]{1,0:T(8,128)(2,1)S(1)}, u32[]{:S(2)}, u32[]{:S(2)}) collective-permute-start(bf16[128,2176]{1,0:T(8,128)(2,1)S(1)} %collective-permute-done.refs_1_), channel_id=1, source_target_pairs={{0,1},{1,0},{2,3},{3,2},{4,5},{5,4},{6,7},{7,6},{8,9},{9,8},{10,11... | collective-permute-start | bytes 1671176 | tf_op jit(solution)/shard_map/ppermute | solution.py:420
  151.3 22.1 %collective-permute-start.21 = (bf16[8,256,128]{2,1,0:T(8,128)(2,1)S(1)}, bf16[8,256,128]{2,1,0:T(8,128)(2,1)S(1)}, u32[]{:S(2)}, u32[]{:S(2)}) collective-permute-start(bf16[8,256,128]{2,1,0:T(8,128)(2,1)S(1)} %get-tuple-element.77), channel_id=1, source_target_pairs={{0,2},{1,3},{2,0},{3,1},{4,6},{5,7},{6,4},{7,5},{8,10},{9,11},{10,... | collective-permute-start | bytes 1572872 | tf_op jit(solution)/shard_map/ppermute | solution.py:379
  153.6 24.3 %collective-permute-start.22 = (bf16[8,256,128]{2,1,0:T(8,128)(2,1)S(1)}, bf16[8,256,128]{2,1,0:T(8,128)(2,1)S(1)}, u32[]{:S(2)}, u32[]{:S(2)}) collective-permute-start(bf16[8,256,128]{2,1,0:T(8,128)(2,1)S(1)} %get-tuple-element.78), channel_id=1, source_target_pairs={{0,3},{1,0},{2,1},{3,2},{4,7},{5,4},{6,5},{7,6},{8,11},{9,8},{10,9... | collective-permute-start | bytes 1572872 | tf_op jit(solution)/shard_map/ppermute | solution.py:379
  153.7 39.7 %collective-permute-start.28 = (bf16[64,1280]{1,0:T(8,128)(2,1)S(1)}, bf16[64,1280]{1,0:T(8,128)(2,1)S(1)}, u32[]{:S(2)}, u32[]{:S(2)}) collective-permute-start(bf16[64,1280]{1,0:T(8,128)(2,1)S(1)} %copy-done.34), channel_id=1, source_target_pairs={{0,12},{4,16},{8,20},{12,24},{16,28},{20,0},{24,4},{28,8},{1,13},{... | collective-permute-start | bytes 491528 | tf_op jit(solution)/shard_map/ppermute | solution.py:379
  173.4 20.0 %collective-permute-start.29 = (bf16[64,1280]{1,0:T(8,128)(2,1)S(1)}, bf16[64,1280]{1,0:T(8,128)(2,1)S(1)}, u32[]{:S(2)}, u32[]{:S(2)}) collective-permute-start(bf16[64,1280]{1,0:T(8,128)(2,1)S(1)} %copy-done.32), channel_id=1, source_target_pairs={{0,16},{4,20},{8,24},{12,28},{16,0},{20,4},{24,8},{28,12},{1,17},{... | collective-permute-start | bytes 491528 | tf_op jit(solution)/shard_map/ppermute | solution.py:379
  178.0 15.4 %collective-permute-start.30 = (bf16[64,1280]{1,0:T(8,128)(2,1)S(1)}, bf16[64,1280]{1,0:T(8,128)(2,1)S(1)}, u32[]{:S(2)}, u32[]{:S(2)}) collective-permute-start(bf16[64,1280]{1,0:T(8,128)(2,1)S(1)} %copy-done.30), channel_id=1, source_target_pairs={{0,20},{4,24},{8,28},{12,0},{16,4},{20,8},{24,12},{28,16},{1,21},{... | collective-permute-start | bytes 491528 | tf_op jit(solution)/shard_map/ppermute | solution.py:379
  203.4 18.4 %collective-permute-start.33 = (bf16[128,1280]{1,0:T(8,128)(2,1)}, bf16[128,1280]{1,0:T(8,128)(2,1)S(1)}, u32[]{:S(2)}, u32[]{:S(2)}) collective-permute-start(bf16[128,1280]{1,0:T(8,128)(2,1)} %get-tuple-element.94), channel_id=1, source_target_pairs={{0,2},{1,3},{2,0},{3,1},{4,6},{5,7},{6,4},{7,5},{8,10},{9,11},{10,... | collective-permute-start | bytes 983048 | tf_op jit(solution)/shard_map/ppermute | solution.py:437
  204.4 17.4 %collective-permute-start.34 = (bf16[128,1280]{1,0:T(8,128)(2,1)}, bf16[128,1280]{1,0:T(8,128)(2,1)S(1)}, u32[]{:S(2)}, u32[]{:S(2)}) collective-permute-start(bf16[128,1280]{1,0:T(8,128)(2,1)} %get-tuple-element.95), channel_id=1, source_target_pairs={{0,1},{1,0},{2,3},{3,2},{4,5},{5,4},{6,7},{7,6},{8,9},{9,8},{10,11... | collective-permute-start | bytes 983048 | tf_op jit(solution)/shard_map/ppermute | solution.py:437
  205.4 20.0 %collective-permute-start.35 = (bf16[128,1280]{1,0:T(8,128)(2,1)}, bf16[128,1280]{1,0:T(8,128)(2,1)S(1)}, u32[]{:S(2)}, u32[]{:S(2)}) collective-permute-start(bf16[128,1280]{1,0:T(8,128)(2,1)} %get-tuple-element.96), channel_id=1, source_target_pairs={{0,3},{1,2},{2,1},{3,0},{4,7},{5,6},{6,5},{7,4},{8,11},{9,10},{10,... | collective-permute-start | bytes 983048 | tf_op jit(solution)/shard_map/ppermute | solution.py:437
  213.3 17.7 %all-to-all-start.3 = ((bf16[8,16,768]{2,1,0:T(8,128)(2,1)}), bf16[8,16,768]{2,1,0:T(8,128)(2,1)S(1)}, u32[]{:S(2)}, u32[]{:S(2)}) async-start(bf16[8,16,768]{2,1,0:T(8,128)(2,1)} %shard_map.115), calls=%async_computation.3 | async-start | bytes 393216 | tf_op jit(solution)/shard_map/all_to_all | solution.py:383
  (48 other events, 861.6 us)

commit v7 on v6

--- a/solution.py
+++ b/solution.py
@@ -15,7 +15,7 @@
 
 
 def cuts_of(width):
-    first = width // 8 * 5
+    first = width // 2
     return [(0, first), (first, width)]
 
 
@@ -86,6 +86,23 @@
     out_ref[:, width:] = extra
 
 
+def fold_kernel(mine_ref, other_ref, *outs):
+    count = outs[0].shape[0]
+    for k, out in enumerate(outs):
+        block = slice(k * count, (k + 1) * count)
+        out[...] = (mine_ref[block].astype(f32) + other_ref[block].astype(f32)).astype(bf16)
+
+
+def fold(count, mine, other):
+    rows, width = mine.shape
+    return pl.pallas_call(
+        fold_kernel,
+        out_shape=[jax.ShapeDtypeStruct((count, width), bf16)] * (rows // count),
+        compiler_params=grant(8),
+        cost_estimate=cost(1e9, 6 * rows * width),
+    )(mine, other)
+
+
 def add_kernel(*refs):
     out_ref = refs[-1]
     fs, each, _ = out_ref.shape
@@ -164,10 +181,8 @@
         for r in range(fs):
             group = lax.rem(me_ref[0] + r, fs)
             full = jnp.concatenate([ins[q][group] for q in order], axis=-1)
-            low, high = cuts[0]
-            outs[r][...] = full[:, low:high]
-            for out, (low, high) in zip(outs[fs:], cuts[1:]):
-                out[group] = full[:, low:high]
+            for k, (low, high) in enumerate(cuts):
+                outs[k * fs + r][...] = full[:, low:high]
 
     in_order(me_ref, tp, store)
 
@@ -175,8 +190,7 @@
 def merge(me, parts, cuts):
     tp = len(parts)
     fs, rows, _ = parts[0].shape
-    sizes = [high - low for low, high in cuts]
-    shapes = [(rows, sizes[0])] * fs + [(fs, rows, size) for size in sizes[1:]]
+    shapes = [(rows, high - low) for low, high in cuts for _ in range(fs)]
     outs = pl.pallas_call(
         functools.partial(merge_kernel, fs, tp, cuts),
         grid_spec=pltpu.PrefetchScalarGridSpec(
@@ -189,7 +203,7 @@
         compiler_params=grant(16),
         cost_estimate=cost(1e9, 4 * tp * parts[0].size),
     )(me, *parts)
-    return [outs[:fs], *outs[fs:]]
+    return [outs[k * fs : (k + 1) * fs] for k in range(len(cuts))]
 
 
 def regroup_kernel(fs, tp, me_ref, *refs):
@@ -304,7 +318,7 @@
     parts, refs = refs[:count_parts], refs[count_parts:]
     if aliased:
         refs = refs[1:]
-    matrix_ref, outs, block, done = refs[0], refs[1 : 1 + tp], refs[1 + tp], refs[2 + tp]
+    matrix_ref, same_ref, other_ref, block, done = refs
     assemble(me_ref, parts, block)
     copy = pltpu.make_async_copy(block, matrix_ref.at[:, pl.ds(low, block.shape[1])], done)
     copy.start()
@@ -318,7 +332,10 @@
         weight = jnp.sum(
             jnp.where(chosen, w_refs[q][...].astype(f32), 0.0), axis=1, keepdims=True
         )
-        outs[q][...] = (product[q * count : (q + 1) * count] * weight).astype(bf16)
+        out_ref, at = (same_ref, q) if q < tp // 2 else (other_ref, q - tp // 2)
+        out_ref[at * count : (at + 1) * count] = (
+            product[q * count : (q + 1) * count] * weight
+        ).astype(bf16)
     copy.wait()
 
 
@@ -343,16 +360,16 @@
             num_scalar_prefetch=1,
             grid=(1,),
             in_specs=in_specs,
-            out_specs=[pl.BlockSpec(memory_space=pl.ANY)] + [whole((count, size))] * tp,
+            out_specs=[pl.BlockSpec(memory_space=pl.ANY)] + [whole((tp // 2 * count, size))] * 2,
             scratch_shapes=[pltpu.VMEM((depth, size), bf16), pltpu.SemaphoreType.DMA],
         ),
         out_shape=[jax.ShapeDtypeStruct((depth, width), bf16)]
-        + [jax.ShapeDtypeStruct((count, size), bf16)] * tp,
+        + [jax.ShapeDtypeStruct((tp // 2 * count, size), bf16)] * 2,
         input_output_aliases=aliases,
         compiler_params=grant(16),
         cost_estimate=cost(2 * tp * count * depth * size, 4 * depth * size),
     )(me, *args)
-    return outs[0], outs[1:]
+    return outs
 
 
 def final_kernel(fs, tp, ids_ref, *refs):
@@ -383,6 +400,9 @@
         out = lax.all_to_all(value, "fs", 0, 0, tiled=True)
         return out.reshape(-1, out.shape[2])
 
+    def swap_core(value):
+        return lax.ppermute(value, "tp", [(j, j ^ 1) for j in range(tp)])
+
     def by_expert(matrix):
         return matrix.reshape((fs, tp) + matrix.shape[1:])
 
@@ -410,14 +430,11 @@
     cut_gate(late + [0], grant(16))
     down_parts = cast_along(me, by_expert(down_proj), None, 1, range(tp), grant(16))
     down_parts = rotate(down_parts, "tp")
-    source = [
-        [((j ^ core) - step) % tp for j in range(tp)] for core in (0, 1) for step in range(0, tp, 2)
-    ]
     rows = [landed] + [
         lax.ppermute(landed, "tp", [(k, (k + step) % tp) for k in range(tp)])
         for step in range(2, tp, 2)
     ]
-    rows += [lax.ppermute(part, "tp", [(k, k ^ 1) for k in range(tp)]) for part in rows]
+    rows += [swap_core(part) for part in rows]
     (up_parts,) = merge(me, up_parts, [(0, tp * up_parts[0].shape[2])])
     up_parts = rotate(up_parts, "fs")
     gate_parts = regroup(me, gate_parts)
@@ -425,22 +442,21 @@
     down_parts = merge(me, down_parts, cuts)
     new_gate, gate = gate_rows(me, rows, gate_parts)
     down_parts[0] = rotate(down_parts[0], "fs")
-    down_parts[1] = [swap_fs(down_parts[1])]
+    down_parts[1] = rotate(down_parts[1], "fs")
     new_up, hidden = up_rows(me, rows, up_parts, gate)
     new_down = None
-    partials = []
+    backs = []
     for k, (low, _) in enumerate(cuts):
-        new_down, partial = down_rows(me, hidden, rows, down_parts[k], low, width, new_down)
-        partials.append(
-            [partial[0]]
-            + [
-                lax.ppermute(term, "tp", list(enumerate(places)))
-                for term, places in zip(partial[1:], source[1:])
-            ]
+        new_down, mine, other = down_rows(
+            me, hidden, rows, down_parts[k], low, width, new_down
         )
-    backs = []
-    for partial in partials:
-        summed = add(fs, partial)
+        other = swap_core(other)
+        terms = fold(count, mine, other)
+        terms = [terms[0]] + [
+            lax.ppermute(term, "tp", [(j, (j - step) % tp) for j in range(tp)])
+            for term, step in zip(terms[1:], range(2, tp, 2))
+        ]
+        summed = add(fs, terms)
         backs.append(swap_fs(summed))
     mixed = pl.pallas_call(
         functools.partial(final_kernel, fs, tp),

time: 248 us -> 246 us (level)
  waiting for transfers between devices: 78.8 us -> 90 us
  starting transfers between devices: 106 us -> 101 us
  local copies, waits for them, and re-layouts: 16.3 us -> 12.8 us
  blocking collectives: 15.5 us -> 12.9 us
    ppermute x30 -> x37, waiting for transfers between devices: 65.3 us -> 74.3 us  [rotate(): out[r] = lax.ppermute(parts[r], axis, [(k, (k + r) % n) for k in range(n)])]
    all_to_all x3 -> x2, starting transfers between devices: 21.2 us -> 13.7 us  [swap_fs(): out = lax.all_to_all(value, 'fs', 0, 0, tiled=True)]
    ppermute x30 -> x37, starting transfers between devices: 74.4 us -> 81.8 us  [rotate(): out[r] = lax.ppermute(parts[r], axis, [(k, (k + r) % n) for k in range(n)])]
    ppermute x8 -> x6, waiting for transfers between devices: 8.11 us -> 14.8 us  [the longest x2 14.8 us: shards(): lax.ppermute(term, 'tp', [(j, (j - step) % tp) for j in range(tp)])]
    ppermute x8 -> x6, starting transfers between devices: 9.25 us -> 4.58 us  [the longest x4 3 us: swap_core(): return lax.ppermute(value, 'tp', [(j, j ^ 1) for j in range(tp)])]
    all_to_all x3 -> x2, waiting for transfers between devices: 5.43 us -> 0.89 us  [swap_fs(): out = lax.all_to_all(value, 'fs', 0, 0, tiled=True)]
    unnamed x76 -> x42, local copies, waits for them, and re-layouts: 16.3 us -> 12.8 us
    all_to_all x1, blocking collectives: 15.5 us -> 12.9 us  [swap_fs(): out = lax.all_to_all(value, 'fs', 0, 0, tiled=True)]
  transfers between devices with their start and end apart: 42 -> 46, of which waited for: 12 -> 16; matrix products, arithmetic and copies ran while one was open for 0% -> 0% of each run, Pallas kernels for 10% -> 9%
where the time goes in v7:
time: 246 us; the launch traced here: 245 us
  starting transfers between devices  101 us (41%)
  waiting for transfers between devices  90 us (37%)
  Pallas kernels  28 us (11%)
  blocking collectives  12.9 us (5%)
  local copies, waits for them, and re-layouts  12.8 us (5%)
    ppermute x37, starting transfers between devices, rotate(): out[r] = lax.ppermute(parts[r], axis, [(k, (k + r) % n) for k in range(n)])  81.8 us
    ppermute x37, waiting for transfers between devices, rotate(): out[r] = lax.ppermute(parts[r], axis, [(k, (k + r) % n) for k in range(n)])  74.3 us
    ppermute x2, waiting for transfers between devices, shards(): lax.ppermute(term, 'tp', [(j, (j - step) % tp) for j in range(tp)])  14.8 us
    all_to_all x2, starting transfers between devices, swap_fs(): out = lax.all_to_all(value, 'fs', 0, 0, tiled=True)  13.7 us
    all_to_all x1, blocking collectives, swap_fs(): out = lax.all_to_all(value, 'fs', 0, 0, tiled=True)  12.9 us
    unnamed x42, local copies, waits for them, and re-layouts  12.8 us
    pallas_call x4, Pallas kernels, cast_along(): pl.pallas_call(functools.partial(cast_kernel, steps, scale is not None, a...  10.2 us
  transfers between devices with their start and end apart: 46, of which 16 were waited for; matrix products, arithmetic and copies ran while one was open for 0% of the time, Pallas kernels for 9%

profile of v7, /device:TPU:0, one launch (start us, length us, event | category | flops | bytes accessed | tf_op | source)
XLA Modules:
  0.0 245.2 jit_solution(12522449572153083311)
XLA Ops:
  0.6 2.4 shard_map.102
  3.0 7.3 %all-to-all-start = ((bf16[8,16,2176]{2,1,0:T(8,128)(2,1)}), bf16[8,16,2176]{2,1,0:T(8,128)(2,1)S(1)}, u32[]{:S(2)}, u32[]{:S(2)}) async-start(bf16[8,16,2176]{2,1,0:T(8,128)(2,1)} %bitcast.32), calls=%async_computation | async-start | bytes 1114112 | tf_op jit(solution)/shard_map/all_to_all | solution.py:400
  12.6 2.5 %shard_map.103 = (bf16[8,256,128]{2,1,0:T(8,128)(2,1)S(1)}, bf16[8,256,128]{2,1,0:T(8,128)(2,1)}, bf16[8,256,128]{2,1,0:T(8,128)(2,1)S(1)}, bf16[8,256,128]{2,1,0:T(8,128)(2,1)S(1)}) custom-call(s32[2]{0:T(128)S(1)} %pad_add_fusion.me_ref, f32[8,4,256,128]{3,2,1,0:T(8,128)S(1)} %bitcast.23, f32[1,256]{1,0:T(1,128)S(1)} %bitcast.28), custom_call_target="tpu_custom_call" | custom-call | flops 1000000000 | bytes 6291456 | tf_op jit(solution)/shard_map/pallas_call | solution.py:158
  21.6 4.0 %shard_map.106 = (bf16[4,256,128]{2,1,0:T(8,128)(2,1)}, bf16[4,256,128]{2,1,0:T(8,128)(2,1)}, bf16[4,256,128]{2,1,0:T(8,128)(2,1)}) custom-call(s32[2]{0:T(128)} %copy-done.3, f32[8,4,256,128]{3,2,1,0:T(8,128)} %bitcast.15, f32[1,256]{1,0:T(1,128)} %bitcast.27), custom_call_target="tpu_custom_call" | custom-call | flops 1000000000 | bytes 2359296 | tf_op jit(solution)/shard_map/pallas_call | solution.py:158
  25.6 2.4 collective-permute-start.15
  35.3 20.1 %collective-permute-done.15.refs_3_ = bf16[4,256,128]{2,1,0:T(8,128)(2,1)S(1)} collective-permute-done((bf16[4,256,128]{2,1,0:T(8,128)(2,1)}, bf16[4,256,128]{2,1,0:T(8,128)(2,1)S(1)}, u32[]{:S(2)}, u32[]{:S(2)}) %collective-permute-start.15) | collective-permute-done | bytes 262176 | tf_op jit(solution)/shard_map/ppermute | solution.py:396
  59.0 3.1 %collective-permute-start.17 = (bf16[4,256,128]{2,1,0:T(8,128)(2,1)}, bf16[4,256,128]{2,1,0:T(8,128)(2,1)}, u32[]{:S(2)}, u32[]{:S(2)}) collective-permute-start(bf16[4,256,128]{2,1,0:T(8,128)(2,1)} %get-tuple-element.79), channel_id=1, source_target_pairs={{0,20},{4,24},{8,28},{12,0},{16,4},{20,8},{24,12},{28,16},{1,21},{... | collective-permute-start | bytes 786440 | tf_op jit(solution)/shard_map/ppermute | solution.py:396
  64.4 3.7 %collective-permute-done.24.refs_2_ = bf16[8,64,512]{2,1,0:T(8,128)(2,1)S(1)} collective-permute-done((bf16[8,64,512]{2,1,0:T(8,128)(2,1)S(1)}, bf16[8,64,512]{2,1,0:T(8,128)(2,1)S(1)}, u32[]{:S(2)}, u32[]{:S(2)}) %collective-permute-start.24) | collective-permute-done | bytes 524320 | tf_op jit(solution)/shard_map/ppermute | solution.py:396
  68.9 3.9 %collective-permute-done.25.refs_3_ = bf16[8,64,512]{2,1,0:T(8,128)(2,1)S(1)} collective-permute-done((bf16[8,64,512]{2,1,0:T(8,128)(2,1)S(1)}, bf16[8,64,512]{2,1,0:T(8,128)(2,1)S(1)}, u32[]{:S(2)}, u32[]{:S(2)}) %collective-permute-start.25) | collective-permute-done | bytes 524320 | tf_op jit(solution)/shard_map/ppermute | solution.py:396
  78.0 2.4 collective-permute-done.5.refs_3_
  82.4 3.2 %collective-permute-start.7 = (bf16[256,512]{1,0:T(8,128)(2,1)S(1)}, bf16[256,512]{1,0:T(8,128)(2,1)S(1)}, u32[]{:S(2)}, u32[]{:S(2)}) collective-permute-start(bf16[256,512]{1,0:T(8,128)(2,1)S(1)} %get-tuple-element.68), channel_id=1, source_target_pairs={{0,8},{4,12},{8,16},{12,20},{16,24},{20,28},{24,0},{28,4},{1,9},{5... | collective-permute-start | bytes 786440 | tf_op jit(solution)/shard_map/ppermute | solution.py:396
  85.6 3.0 %collective-permute-start.8 = (bf16[256,512]{1,0:T(8,128)(2,1)S(1)}, bf16[256,512]{1,0:T(8,128)(2,1)S(1)}, u32[]{:S(2)}, u32[]{:S(2)}) collective-permute-start(bf16[256,512]{1,0:T(8,128)(2,1)S(1)} %get-tuple-element.69), channel_id=1, source_target_pairs={{0,12},{4,16},{8,20},{12,24},{16,28},{20,0},{24,4},{28,8},{1,13},{... | collective-permute-start | bytes 786440 | tf_op jit(solution)/shard_map/ppermute | solution.py:396
  90.5 14.0 %collective-permute-done.27.refs_6_ = bf16[64,1024]{1,0:T(8,128)(2,1)S(1)} collective-permute-done((bf16[64,1024]{1,0:T(8,128)(2,1)S(1)}, bf16[64,1024]{1,0:T(8,128)(2,1)S(1)}, u32[]{:S(2)}, u32[]{:S(2)}) %collective-permute-start.27) | collective-permute-done | bytes 131104 | tf_op jit(solution)/shard_map/ppermute | solution.py:396
  104.5 9.5 %collective-permute-start.10 = (bf16[256,512]{1,0:T(8,128)(2,1)S(1)}, bf16[256,512]{1,0:T(8,128)(2,1)S(1)}, u32[]{:S(2)}, u32[]{:S(2)}) collective-permute-start(bf16[256,512]{1,0:T(8,128)(2,1)S(1)} %get-tuple-element.71), channel_id=1, source_target_pairs={{0,20},{4,24},{8,28},{12,0},{16,4},{20,8},{24,12},{28,16},{1,21},{... | collective-permute-start | bytes 786440 | tf_op jit(solution)/shard_map/ppermute | solution.py:396
  114.4 6.3 %collective-permute-done.8.refs_7_ = bf16[256,512]{1,0:T(8,128)(2,1)S(1)} collective-permute-done((bf16[256,512]{1,0:T(8,128)(2,1)S(1)}, bf16[256,512]{1,0:T(8,128)(2,1)S(1)}, u32[]{:S(2)}, u32[]{:S(2)}) %collective-permute-start.8) | collective-permute-done | bytes 262176 | tf_op jit(solution)/shard_map/ppermute | solution.py:396
  125.4 5.3 %collective-permute-done.11.refs_10_ = bf16[256,512]{1,0:T(8,128)(2,1)S(1)} collective-permute-done((bf16[256,512]{1,0:T(8,128)(2,1)S(1)}, bf16[256,512]{1,0:T(8,128)(2,1)S(1)}, u32[]{:S(2)}, u32[]{:S(2)}) %collective-permute-start.11) | collective-permute-done | bytes 262176 | tf_op jit(solution)/shard_map/ppermute | solution.py:396
  134.0 16.0 %collective-permute-start.28 = (bf16[64,1024]{1,0:T(8,128)(2,1)S(1)}, bf16[64,1024]{1,0:T(8,128)(2,1)S(1)}, u32[]{:S(2)}, u32[]{:S(2)}) collective-permute-start(bf16[64,1024]{1,0:T(8,128)(2,1)S(1)} %get-tuple-element.95), channel_id=1, source_target_pairs={{0,12},{4,16},{8,20},{12,24},{16,28},{20,0},{24,4},{28,8},{1,13},{... | collective-permute-start | bytes 393224 | tf_op jit(solution)/shard_map/ppermute | solution.py:396
  149.9 7.1 %collective-permute-start.29 = (bf16[64,1024]{1,0:T(8,128)(2,1)S(1)}, bf16[64,1024]{1,0:T(8,128)(2,1)S(1)}, u32[]{:S(2)}, u32[]{:S(2)}) collective-permute-start(bf16[64,1024]{1,0:T(8,128)(2,1)S(1)} %get-tuple-element.96), channel_id=1, source_target_pairs={{0,16},{4,20},{8,24},{12,28},{16,0},{20,4},{24,8},{28,12},{1,17},{... | collective-permute-start | bytes 393224 | tf_op jit(solution)/shard_map/ppermute | solution.py:396
  157.0 6.2 %collective-permute-start.31 = (bf16[64,1024]{1,0:T(8,128)(2,1)S(1)}, bf16[64,1024]{1,0:T(8,128)(2,1)S(1)}, u32[]{:S(2)}, u32[]{:S(2)}) collective-permute-start(bf16[64,1024]{1,0:T(8,128)(2,1)S(1)} %get-tuple-element.98), channel_id=1, source_target_pairs={{0,24},{4,28},{8,0},{12,4},{16,8},{20,12},{24,16},{28,20},{1,25},{... | collective-permute-start | bytes 393224 | tf_op jit(solution)/shard_map/ppermute | solution.py:396
  163.3 4.0 %collective-permute-start.32 = (bf16[64,1024]{1,0:T(8,128)(2,1)S(1)}, bf16[64,1024]{1,0:T(8,128)(2,1)S(1)}, u32[]{:S(2)}, u32[]{:S(2)}) collective-permute-start(bf16[64,1024]{1,0:T(8,128)(2,1)S(1)} %get-tuple-element.99), channel_id=1, source_target_pairs={{0,28},{4,0},{8,4},{12,8},{16,12},{20,16},{24,20},{28,24},{1,29},{... | collective-permute-start | bytes 393224 | tf_op jit(solution)/shard_map/ppermute | solution.py:396
  167.3 3.0 %shard_map.108 = (bf16[2048,512]{1,0:T(8,128)(2,1)}, f32[512,512]{1,0:T(8,128)S(1)}) custom-call(s32[2]{0:T(128)S(1)} %copy-done.4, bf16[128,2176]{1,0:T(8,128)(2,1)S(1)} %bitcast.19, bf16[128,2176]{1,0:T(8,128)(2,1)S(1)} %collective-permute-done.refs_1_, bf16[128,2176]{1,0:T(8,128)(2,1)S(1)} %collective-permute-done.1.refs_2_, ...), custom_call_target="tpu_custom_call" | custom-call | flops 1073741824 | bytes 4194304 | tf_op jit(solution)/shard_map/pallas_call | solution.py:262
  174.4 2.4 collective-permute-start.33
  178.6 2.8 %collective-permute-start.36 = (bf16[64,1024]{1,0:T(8,128)(2,1)S(1)}, bf16[64,1024]{1,0:T(8,128)(2,1)S(1)}, u32[]{:S(2)}, u32[]{:S(2)}) collective-permute-start(bf16[64,1024]{1,0:T(8,128)(2,1)S(1)} %get-tuple-element.106), channel_id=1, source_target_pairs={{0,8},{4,12},{8,16},{12,20},{16,24},{20,28},{24,0},{28,4},{1,9},{5... | collective-permute-start | bytes 393224 | tf_op jit(solution)/shard_map/ppermute | solution.py:396
  183.1 2.8 %collective-permute-done.35.refs_5_ = bf16[64,1024]{1,0:T(8,128)(2,1)S(1)} collective-permute-done((bf16[64,1024]{1,0:T(8,128)(2,1)S(1)}, bf16[64,1024]{1,0:T(8,128)(2,1)S(1)}, u32[]{:S(2)}, u32[]{:S(2)}) %collective-permute-start.35) | collective-permute-done | bytes 131104 | tf_op jit(solution)/shard_map/ppermute | solution.py:396
  186.4 2.6 %collective-permute-start.40 = (bf16[64,1024]{1,0:T(8,128)(2,1)S(1)}, bf16[64,1024]{1,0:T(8,128)(2,1)S(1)}, u32[]{:S(2)}, u32[]{:S(2)}) collective-permute-start(bf16[64,1024]{1,0:T(8,128)(2,1)S(1)} %get-tuple-element.110), channel_id=1, source_target_pairs={{0,24},{4,28},{8,0},{12,4},{16,8},{20,12},{24,16},{28,20},{1,25},{... | collective-permute-start | bytes 393224 | tf_op jit(solution)/shard_map/ppermute | solution.py:396
  189.0 7.8 %collective-permute-done.37.refs_7_ = bf16[64,1024]{1,0:T(8,128)(2,1)S(1)} collective-permute-done((bf16[64,1024]{1,0:T(8,128)(2,1)S(1)}, bf16[64,1024]{1,0:T(8,128)(2,1)S(1)}, u32[]{:S(2)}, u32[]{:S(2)}) %collective-permute-start.37) | collective-permute-done | bytes 131104 | tf_op jit(solution)/shard_map/ppermute | solution.py:396
  196.9 5.3 %collective-permute-start.41 = (bf16[64,1024]{1,0:T(8,128)(2,1)S(1)}, bf16[64,1024]{1,0:T(8,128)(2,1)S(1)}, u32[]{:S(2)}, u32[]{:S(2)}) collective-permute-start(bf16[64,1024]{1,0:T(8,128)(2,1)S(1)} %get-tuple-element.111), channel_id=1, source_target_pairs={{0,28},{4,0},{8,4},{12,8},{16,12},{20,16},{24,20},{28,24},{1,29},{... | collective-permute-start | bytes 393224 | tf_op jit(solution)/shard_map/ppermute | solution.py:396
  202.2 2.5 %collective-permute-done.41.refs_11_ = bf16[64,1024]{1,0:T(8,128)(2,1)S(1)} collective-permute-done((bf16[64,1024]{1,0:T(8,128)(2,1)S(1)}, bf16[64,1024]{1,0:T(8,128)(2,1)S(1)}, u32[]{:S(2)}, u32[]{:S(2)}) %collective-permute-start.41) | collective-permute-done | bytes 131104 | tf_op jit(solution)/shard_map/ppermute | solution.py:396
  207.3 8.0 %collective-permute-done.34.refs_1_ = bf16[128,1024]{1,0:T(8,128)(2,1)S(1)} collective-permute-done((bf16[128,1024]{1,0:T(8,128)(2,1)S(1)}, bf16[128,1024]{1,0:T(8,128)(2,1)S(1)}, u32[]{:S(2)}, u32[]{:S(2)}) %collective-permute-start.34) | collective-permute-done | bytes 262176 | tf_op jit(solution)/shard_map/ppermute | solution.py:456
  216.0 6.4 %all-to-all-start.1 = ((bf16[8,16,1024]{2,1,0:T(8,128)(2,1)}), bf16[8,16,1024]{2,1,0:T(8,128)(2,1)S(1)}, u32[]{:S(2)}, u32[]{:S(2)}) async-start(bf16[8,16,1024]{2,1,0:T(8,128)(2,1)} %shard_map.114), calls=%async_computation.1 | async-start | bytes 524288 | tf_op jit(solution)/shard_map/all_to_all | solution.py:400
  223.4 6.8 %collective-permute-done.43.refs_1_ = bf16[128,1024]{1,0:T(8,128)(2,1)S(1)} collective-permute-done((bf16[128,1024]{1,0:T(8,128)(2,1)S(1)}, bf16[128,1024]{1,0:T(8,128)(2,1)S(1)}, u32[]{:S(2)}, u32[]{:S(2)}) %collective-permute-start.43) | collective-permute-done | bytes 262176 | tf_op jit(solution)/shard_map/ppermute | solution.py:456
  231.1 12.9 %all_to_all.15 = bf16[8,16,1024]{2,1,0:T(8,128)(2,1)S(1)} all-to-all(bf16[8,16,1024]{2,1,0:T(8,128)(2,1)S(1)} %shard_map.117), channel_id=1, replica_groups=mesh['fs'=8,'tp'=4] {'fs'}, dimensions={0} | all-to-all | bytes 524288 | tf_op jit(solution)/shard_map/all_to_all | solution.py:400
  (121 shorter events, 54.6 us)
Async XLA Ops:
  3.0 70.6 %all-to-all-start = ((bf16[8,16,2176]{2,1,0:T(8,128)(2,1)}), bf16[8,16,2176]{2,1,0:T(8,128)(2,1)S(1)}, u32[]{:S(2)}, u32[]{:S(2)}) async-start(bf16[8,16,2176]{2,1,0:T(8,128)(2,1)} %bitcast.32), calls=%async_computation | async-start | bytes 1114112 | tf_op jit(solution)/shard_map/all_to_all | solution.py:400
  15.9 42.5 %collective-permute-start.3 = (bf16[8,256,128]{2,1,0:T(8,128)(2,1)}, bf16[8,256,128]{2,1,0:T(8,128)(2,1)S(1)}, u32[]{:S(2)}, u32[]{:S(2)}) collective-permute-start(bf16[8,256,128]{2,1,0:T(8,128)(2,1)} %get-tuple-element.63), channel_id=1, source_target_pairs={{0,1},{1,2},{2,3},{3,0},{4,5},{5,6},{6,7},{7,4},{8,9},{9,10},{10,1... | collective-permute-start | bytes 1572872 | tf_op jit(solution)/shard_map/ppermute | solution.py:396
  20.1 15.2 %collective-permute-start.14 = (bf16[4,256,128]{2,1,0:T(8,128)(2,1)}, bf16[4,256,128]{2,1,0:T(8,128)(2,1)}, u32[]{:S(2)}, u32[]{:S(2)}) collective-permute-start(bf16[4,256,128]{2,1,0:T(8,128)(2,1)} %get-tuple-element.76), channel_id=1, source_target_pairs={{0,8},{4,12},{8,16},{12,20},{16,24},{20,28},{24,0},{28,4},{1,9},{5... | collective-permute-start | bytes 786440 | tf_op jit(solution)/shard_map/ppermute | solution.py:396
  25.6 29.9 %collective-permute-start.15 = (bf16[4,256,128]{2,1,0:T(8,128)(2,1)}, bf16[4,256,128]{2,1,0:T(8,128)(2,1)S(1)}, u32[]{:S(2)}, u32[]{:S(2)}) collective-permute-start(bf16[4,256,128]{2,1,0:T(8,128)(2,1)} %get-tuple-element.77), channel_id=1, source_target_pairs={{0,12},{4,16},{8,20},{12,24},{16,28},{20,0},{24,4},{28,8},{1,13},{... | collective-permute-start | bytes 786440 | tf_op jit(solution)/shard_map/ppermute | solution.py:396
  28.0 29.7 %collective-permute-start.16 = (bf16[4,256,128]{2,1,0:T(8,128)(2,1)}, bf16[4,256,128]{2,1,0:T(8,128)(2,1)S(1)}, u32[]{:S(2)}, u32[]{:S(2)}) collective-permute-start(bf16[4,256,128]{2,1,0:T(8,128)(2,1)} %get-tuple-element.78), channel_id=1, source_target_pairs={{0,16},{4,20},{8,24},{12,28},{16,0},{20,4},{24,8},{28,12},{1,17},{... | collective-permute-start | bytes 786440 | tf_op jit(solution)/shard_map/ppermute | solution.py:396
  33.8 25.2 %collective-permute-start.4 = (bf16[8,256,128]{2,1,0:T(8,128)(2,1)S(1)}, bf16[8,256,128]{2,1,0:T(8,128)(2,1)S(1)}, u32[]{:S(2)}, u32[]{:S(2)}) collective-permute-start(bf16[8,256,128]{2,1,0:T(8,128)(2,1)S(1)} %copy-done.10), channel_id=1, source_target_pairs={{0,2},{1,3},{2,0},{3,1},{4,6},{5,7},{6,4},{7,5},{8,10},{9,11},{10,... | collective-permute-start | bytes 1572872 | tf_op jit(solution)/shard_map/ppermute | solution.py:396
  35.3 26.8 %collective-permute-start.23 = (bf16[8,64,512]{2,1,0:T(8,128)(2,1)S(1)}, bf16[8,64,512]{2,1,0:T(8,128)(2,1)S(1)}, u32[]{:S(2)}, u32[]{:S(2)}) collective-permute-start(bf16[8,64,512]{2,1,0:T(8,128)(2,1)S(1)} %get-tuple-element.89), channel_id=1, source_target_pairs={{0,1},{1,2},{2,3},{3,0},{4,5},{5,6},{6,7},{7,4},{8,9},{9,10},{10,1... | collective-permute-start | bytes 1572872 | tf_op jit(solution)/shard_map/ppermute | solution.py:396
  58.4 22.0 %collective-permute-start.5 = (bf16[8,256,128]{2,1,0:T(8,128)(2,1)S(1)}, bf16[8,256,128]{2,1,0:T(8,128)(2,1)}, u32[]{:S(2)}, u32[]{:S(2)}) collective-permute-start(bf16[8,256,128]{2,1,0:T(8,128)(2,1)S(1)} %get-tuple-element.65), channel_id=1, source_target_pairs={{0,3},{1,0},{2,1},{3,2},{4,7},{5,4},{6,5},{7,6},{8,11},{9,8},{10,9... | collective-permute-start | bytes 1572872 | tf_op jit(solution)/shard_map/ppermute | solution.py:396
  59.0 23.2 %collective-permute-start.17 = (bf16[4,256,128]{2,1,0:T(8,128)(2,1)}, bf16[4,256,128]{2,1,0:T(8,128)(2,1)}, u32[]{:S(2)}, u32[]{:S(2)}) collective-permute-start(bf16[4,256,128]{2,1,0:T(8,128)(2,1)} %get-tuple-element.79), channel_id=1, source_target_pairs={{0,20},{4,24},{8,28},{12,0},{16,4},{20,8},{24,12},{28,16},{1,21},{... | collective-permute-start | bytes 786440 | tf_op jit(solution)/shard_map/ppermute | solution.py:396
  62.9 19.5 %collective-permute-start.18 = (bf16[4,256,128]{2,1,0:T(8,128)(2,1)}, bf16[4,256,128]{2,1,0:T(8,128)(2,1)}, u32[]{:S(2)}, u32[]{:S(2)}) collective-permute-start(bf16[4,256,128]{2,1,0:T(8,128)(2,1)} %get-tuple-element.80), channel_id=1, source_target_pairs={{0,24},{4,28},{8,0},{12,4},{16,8},{20,12},{24,16},{28,20},{1,25},{... | collective-permute-start | bytes 786440 | tf_op jit(solution)/shard_map/ppermute | solution.py:396
  68.9 16.7 %collective-permute-start.19 = (bf16[4,256,128]{2,1,0:T(8,128)(2,1)}, bf16[4,256,128]{2,1,0:T(8,128)(2,1)}, u32[]{:S(2)}, u32[]{:S(2)}) collective-permute-start(bf16[4,256,128]{2,1,0:T(8,128)(2,1)} %get-tuple-element.81), channel_id=1, source_target_pairs={{0,28},{4,0},{8,4},{12,8},{16,12},{20,16},{24,20},{28,24},{1,29},{... | collective-permute-start | bytes 786440 | tf_op jit(solution)/shard_map/ppermute | solution.py:396
  73.6 49.3 %collective-permute-start = (bf16[128,2176]{1,0:T(8,128)(2,1)S(1)}, bf16[128,2176]{1,0:T(8,128)(2,1)S(1)}, u32[]{:S(2)}, u32[]{:S(2)}) collective-permute-start(bf16[128,2176]{1,0:T(8,128)(2,1)S(1)} %bitcast.17), channel_id=1, source_target_pairs={{0,2},{1,3},{2,0},{3,1},{4,6},{5,7},{6,4},{7,5},{8,10},{9,11},{10,... | collective-permute-start | bytes 1671176 | tf_op jit(solution)/shard_map/ppermute | solution.py:434
  82.3 22.2 %collective-permute-start.6 = (bf16[256,512]{1,0:T(8,128)(2,1)S(1)}, bf16[256,512]{1,0:T(8,128)(2,1)S(1)}, u32[]{:S(2)}, u32[]{:S(2)}) collective-permute-start(bf16[256,512]{1,0:T(8,128)(2,1)S(1)} %get-tuple-element.67), channel_id=1, source_target_pairs={{0,4},{4,8},{8,12},{12,16},{16,20},{20,24},{24,28},{28,0},{1,5},{5... | collective-permute-start | bytes 786440 | tf_op jit(solution)/shard_map/ppermute | solution.py:396
  82.4 31.6 %collective-permute-start.7 = (bf16[256,512]{1,0:T(8,128)(2,1)S(1)}, bf16[256,512]{1,0:T(8,128)(2,1)S(1)}, u32[]{:S(2)}, u32[]{:S(2)}) collective-permute-start(bf16[256,512]{1,0:T(8,128)(2,1)S(1)} %get-tuple-element.68), channel_id=1, source_target_pairs={{0,8},{4,12},{8,16},{12,20},{16,24},{20,28},{24,0},{28,4},{1,9},{5... | collective-permute-start | bytes 786440 | tf_op jit(solution)/shard_map/ppermute | solution.py:396
  85.6 35.2 %collective-permute-start.8 = (bf16[256,512]{1,0:T(8,128)(2,1)S(1)}, bf16[256,512]{1,0:T(8,128)(2,1)S(1)}, u32[]{:S(2)}, u32[]{:S(2)}) collective-permute-start(bf16[256,512]{1,0:T(8,128)(2,1)S(1)} %get-tuple-element.69), channel_id=1, source_target_pairs={{0,12},{4,16},{8,20},{12,24},{16,28},{20,0},{24,4},{28,8},{1,13},{... | collective-permute-start | bytes 786440 | tf_op jit(solution)/shard_map/ppermute | solution.py:396
  104.5 18.4 %collective-permute-start.9 = (bf16[256,512]{1,0:T(8,128)(2,1)S(1)}, bf16[256,512]{1,0:T(8,128)(2,1)S(1)}, u32[]{:S(2)}, u32[]{:S(2)}) collective-permute-start(bf16[256,512]{1,0:T(8,128)(2,1)S(1)} %get-tuple-element.70), channel_id=1, source_target_pairs={{0,16},{4,20},{8,24},{12,28},{16,0},{20,4},{24,8},{28,12},{1,17},{... | collective-permute-start | bytes 786440 | tf_op jit(solution)/shard_map/ppermute | solution.py:396
  104.5 20.8 %collective-permute-start.10 = (bf16[256,512]{1,0:T(8,128)(2,1)S(1)}, bf16[256,512]{1,0:T(8,128)(2,1)S(1)}, u32[]{:S(2)}, u32[]{:S(2)}) collective-permute-start(bf16[256,512]{1,0:T(8,128)(2,1)S(1)} %get-tuple-element.71), channel_id=1, source_target_pairs={{0,20},{4,24},{8,28},{12,0},{16,4},{20,8},{24,12},{28,16},{1,21},{... | collective-permute-start | bytes 786440 | tf_op jit(solution)/shard_map/ppermute | solution.py:396
  114.0 16.8 %collective-permute-start.11 = (bf16[256,512]{1,0:T(8,128)(2,1)S(1)}, bf16[256,512]{1,0:T(8,128)(2,1)S(1)}, u32[]{:S(2)}, u32[]{:S(2)}) collective-permute-start(bf16[256,512]{1,0:T(8,128)(2,1)S(1)} %get-tuple-element.72), channel_id=1, source_target_pairs={{0,24},{4,28},{8,0},{12,4},{16,8},{20,12},{24,16},{28,20},{1,25},{... | collective-permute-start | bytes 786440 | tf_op jit(solution)/shard_map/ppermute | solution.py:396
  122.9 34.1 %collective-permute-start.1 = (bf16[128,2176]{1,0:T(8,128)(2,1)S(1)}, bf16[128,2176]{1,0:T(8,128)(2,1)S(1)}, u32[]{:S(2)}, u32[]{:S(2)}) collective-permute-start(bf16[128,2176]{1,0:T(8,128)(2,1)S(1)} %bitcast.18), channel_id=1, source_target_pairs={{0,1},{1,0},{2,3},{3,2},{4,5},{5,4},{6,7},{7,6},{8,9},{9,8},{10,11... | collective-permute-start | bytes 1671176 | tf_op jit(solution)/shard_map/ppermute | solution.py:404
  122.9 40.3 %collective-permute-start.2 = (bf16[128,2176]{1,0:T(8,128)(2,1)S(1)}, bf16[128,2176]{1,0:T(8,128)(2,1)S(1)}, u32[]{:S(2)}, u32[]{:S(2)}) collective-permute-start(bf16[128,2176]{1,0:T(8,128)(2,1)S(1)} %collective-permute-done.refs_1_), channel_id=1, source_target_pairs={{0,1},{1,0},{2,3},{3,2},{4,5},{5,4},{6,7},{7,6},{8,9},{9,8},{10,11... | collective-permute-start | bytes 1671176 | tf_op jit(solution)/shard_map/ppermute | solution.py:404
  130.7 19.2 %collective-permute-start.21 = (bf16[8,256,128]{2,1,0:T(8,128)(2,1)S(1)}, bf16[8,256,128]{2,1,0:T(8,128)(2,1)S(1)}, u32[]{:S(2)}, u32[]{:S(2)}) collective-permute-start(bf16[8,256,128]{2,1,0:T(8,128)(2,1)S(1)} %get-tuple-element.84), channel_id=1, source_target_pairs={{0,2},{1,3},{2,0},{3,1},{4,6},{5,7},{6,4},{7,5},{8,10},{9,11},{10,... | collective-permute-start | bytes 1572872 | tf_op jit(solution)/shard_map/ppermute | solution.py:396
  131.7 25.4 %collective-permute-start.22 = (bf16[8,256,128]{2,1,0:T(8,128)(2,1)S(1)}, bf16[8,256,128]{2,1,0:T(8,128)(2,1)S(1)}, u32[]{:S(2)}, u32[]{:S(2)}) collective-permute-start(bf16[8,256,128]{2,1,0:T(8,128)(2,1)S(1)} %get-tuple-element.85), channel_id=1, source_target_pairs={{0,3},{1,0},{2,1},{3,2},{4,7},{5,4},{6,5},{7,6},{8,11},{9,8},{10,9... | collective-permute-start | bytes 1572872 | tf_op jit(solution)/shard_map/ppermute | solution.py:396
  134.0 38.6 %collective-permute-start.28 = (bf16[64,1024]{1,0:T(8,128)(2,1)S(1)}, bf16[64,1024]{1,0:T(8,128)(2,1)S(1)}, u32[]{:S(2)}, u32[]{:S(2)}) collective-permute-start(bf16[64,1024]{1,0:T(8,128)(2,1)S(1)} %get-tuple-element.95), channel_id=1, source_target_pairs={{0,12},{4,16},{8,20},{12,24},{16,28},{20,0},{24,4},{28,8},{1,13},{... | collective-permute-start | bytes 393224 | tf_op jit(solution)/shard_map/ppermute | solution.py:396
  149.9 22.6 %collective-permute-start.29 = (bf16[64,1024]{1,0:T(8,128)(2,1)S(1)}, bf16[64,1024]{1,0:T(8,128)(2,1)S(1)}, u32[]{:S(2)}, u32[]{:S(2)}) collective-permute-start(bf16[64,1024]{1,0:T(8,128)(2,1)S(1)} %get-tuple-element.96), channel_id=1, source_target_pairs={{0,16},{4,20},{8,24},{12,28},{16,0},{20,4},{24,8},{28,12},{1,17},{... | collective-permute-start | bytes 393224 | tf_op jit(solution)/shard_map/ppermute | solution.py:396
  157.0 15.6 %collective-permute-start.30 = (bf16[64,1024]{1,0:T(8,128)(2,1)S(1)}, bf16[64,1024]{1,0:T(8,128)(2,1)S(1)}, u32[]{:S(2)}, u32[]{:S(2)}) collective-permute-start(bf16[64,1024]{1,0:T(8,128)(2,1)S(1)} %get-tuple-element.97), channel_id=1, source_target_pairs={{0,20},{4,24},{8,28},{12,0},{16,4},{20,8},{24,12},{28,16},{1,21},{... | collective-permute-start | bytes 393224 | tf_op jit(solution)/shard_map/ppermute | solution.py:396
  157.0 15.6 %collective-permute-start.31 = (bf16[64,1024]{1,0:T(8,128)(2,1)S(1)}, bf16[64,1024]{1,0:T(8,128)(2,1)S(1)}, u32[]{:S(2)}, u32[]{:S(2)}) collective-permute-start(bf16[64,1024]{1,0:T(8,128)(2,1)S(1)} %get-tuple-element.98), channel_id=1, source_target_pairs={{0,24},{4,28},{8,0},{12,4},{16,8},{20,12},{24,16},{28,20},{1,25},{... | collective-permute-start | bytes 393224 | tf_op jit(solution)/shard_map/ppermute | solution.py:396
  174.4 32.0 %collective-permute-start.33 = (bf16[256,1024]{1,0:T(8,128)(2,1)S(1)}, bf16[256,1024]{1,0:T(8,128)(2,1)S(1)}, u32[]{:S(2)}, u32[]{:S(2)}) collective-permute-start(bf16[256,1024]{1,0:T(8,128)(2,1)S(1)} %get-tuple-element.101), channel_id=1, source_target_pairs={{0,1},{1,0},{2,3},{3,2},{4,5},{5,4},{6,7},{7,6},{8,9},{9,8},{10,11... | collective-permute-start | bytes 1572872 | tf_op jit(solution)/shard_map/ppermute | solution.py:404
  181.4 15.5 %collective-permute-start.37 = (bf16[64,1024]{1,0:T(8,128)(2,1)S(1)}, bf16[64,1024]{1,0:T(8,128)(2,1)S(1)}, u32[]{:S(2)}, u32[]{:S(2)}) collective-permute-start(bf16[64,1024]{1,0:T(8,128)(2,1)S(1)} %get-tuple-element.107), channel_id=1, source_target_pairs={{0,12},{4,16},{8,20},{12,24},{16,28},{20,0},{24,4},{28,8},{1,13},{... | collective-permute-start | bytes 393224 | tf_op jit(solution)/shard_map/ppermute | solution.py:396
  181.4 20.8 %collective-permute-start.38 = (bf16[64,1024]{1,0:T(8,128)(2,1)S(1)}, bf16[64,1024]{1,0:T(8,128)(2,1)S(1)}, u32[]{:S(2)}, u32[]{:S(2)}) collective-permute-start(bf16[64,1024]{1,0:T(8,128)(2,1)S(1)} %get-tuple-element.108), channel_id=1, source_target_pairs={{0,16},{4,20},{8,24},{12,28},{16,0},{20,4},{24,8},{28,12},{1,17},{... | collective-permute-start | bytes 393224 | tf_op jit(solution)/shard_map/ppermute | solution.py:396
  185.9 16.3 %collective-permute-start.39 = (bf16[64,1024]{1,0:T(8,128)(2,1)S(1)}, bf16[64,1024]{1,0:T(8,128)(2,1)S(1)}, u32[]{:S(2)}, u32[]{:S(2)}) collective-permute-start(bf16[64,1024]{1,0:T(8,128)(2,1)S(1)} %get-tuple-element.109), channel_id=1, source_target_pairs={{0,20},{4,24},{8,28},{12,0},{16,4},{20,8},{24,12},{28,16},{1,21},{... | collective-permute-start | bytes 393224 | tf_op jit(solution)/shard_map/ppermute | solution.py:396
  186.4 15.7 %collective-permute-start.40 = (bf16[64,1024]{1,0:T(8,128)(2,1)S(1)}, bf16[64,1024]{1,0:T(8,128)(2,1)S(1)}, u32[]{:S(2)}, u32[]{:S(2)}) collective-permute-start(bf16[64,1024]{1,0:T(8,128)(2,1)S(1)} %get-tuple-element.110), channel_id=1, source_target_pairs={{0,24},{4,28},{8,0},{12,4},{16,8},{20,12},{24,16},{28,20},{1,25},{... | collective-permute-start | bytes 393224 | tf_op jit(solution)/shard_map/ppermute | solution.py:396
  206.3 16.2 %collective-permute-start.42 = (bf16[256,1024]{1,0:T(8,128)(2,1)S(1)}, bf16[256,1024]{1,0:T(8,128)(2,1)S(1)}, u32[]{:S(2)}, u32[]{:S(2)}) collective-permute-start(bf16[256,1024]{1,0:T(8,128)(2,1)S(1)} %get-tuple-element.114), channel_id=1, source_target_pairs={{0,1},{1,0},{2,3},{3,2},{4,5},{5,4},{6,7},{7,6},{8,9},{9,8},{10,11... | collective-permute-start | bytes 1572872 | tf_op jit(solution)/shard_map/ppermute | solution.py:404
  (35 other events, 343.6 us)

commit v8 on v7

--- a/solution.py
+++ b/solution.py
@@ -15,7 +15,7 @@
 
 
 def cuts_of(width):
-    first = width // 2
+    first = width // 8 * 5
     return [(0, first), (first, width)]
 
 
@@ -103,22 +103,29 @@
     )(mine, other)
 
 
-def add_kernel(*refs):
-    out_ref = refs[-1]
+def add_kernel(counts, *refs):
+    refs, out_ref = list(refs[:-1]), refs[-1]
     fs, each, _ = out_ref.shape
-    total = sum(ref[...].astype(f32) for ref in refs[:-1]).astype(bf16)
-    for i in range(fs):
-        out_ref[i] = total[i * each : (i + 1) * each]
-
-
-def add(fs, terms):
-    count, width = terms[0].shape
-    return pl.pallas_call(
-        add_kernel,
+    low = 0
+    for count in counts:
+        terms, refs = refs[:count], refs[count:]
+        total = sum(ref[...].astype(f32) for ref in terms).astype(bf16)
+        high = low + total.shape[1]
+        for i in range(fs):
+            out_ref[i, :, low:high] = total[i * each : (i + 1) * each]
+        low = high
+
+
+def add(fs, groups):
+    count = groups[0][0].shape[0]
+    width = sum(terms[0].shape[1] for terms in groups)
+    flat = [term for terms in groups for term in terms]
+    return pl.pallas_call(
+        functools.partial(add_kernel, [len(terms) for terms in groups]),
         out_shape=jax.ShapeDtypeStruct((fs, count // fs, width), bf16),
         compiler_params=grant(8),
-        cost_estimate=cost(1e9, 2 * (len(terms) + 1) * count * width),
-    )(*terms)
+        cost_estimate=cost(1e9, 2 * (len(groups[0]) + 1) * count * width),
+    )(*flat)
 
 
 def cast_kernel(steps, scaled, squeeze, me_ref, in_ref, *refs):
@@ -372,14 +379,9 @@
     return outs
 
 
-def final_kernel(fs, tp, ids_ref, *refs):
-    ins, out_ref = refs[:-1], refs[-1]
+def final_kernel(fs, tp, ids_ref, back_ref, out_ref):
     onehot = slot_onehot(group_of(ids_ref[0:1, :], fs, tp), fs)
-    low = 0
-    for ref in ins:
-        high = low + ref.shape[1]
-        out_ref[:, low:high] = jnp.dot(onehot, ref[...], preferred_element_type=f32).astype(bf16)
-        low = high
+    out_ref[...] = jnp.dot(onehot, back_ref[...], preferred_element_type=f32).astype(bf16)
 
 
 def shards(tokens, norm_gain, gate_proj, up_proj, down_proj, expert_ids, route_weight):
@@ -445,7 +447,7 @@
     down_parts[1] = rotate(down_parts[1], "fs")
     new_up, hidden = up_rows(me, rows, up_parts, gate)
     new_down = None
-    backs = []
+    sums = []
     for k, (low, _) in enumerate(cuts):
         new_down, mine, other = down_rows(
             me, hidden, rows, down_parts[k], low, width, new_down
@@ -456,14 +458,15 @@
             lax.ppermute(term, "tp", [(j, (j - step) % tp) for j in range(tp)])
             for term, step in zip(terms[1:], range(2, tp, 2))
         ]
-        summed = add(fs, terms)
-        backs.append(swap_fs(summed))
+        sums.append(terms)
+    summed = add(fs, sums)
+    back = swap_fs(summed)
     mixed = pl.pallas_call(
         functools.partial(final_kernel, fs, tp),
         out_shape=jax.ShapeDtypeStruct((count, width), bf16),
         compiler_params=grant(16),
         cost_estimate=cost(2 * count * count * width, 4 * count * width),
-    )(ids, *backs)
+    )(ids, back)
     return (mixed, new_gate[None], new_up[None], new_down[None])
 
 

time: 246 us -> 247 us (level)
  waiting for transfers between devices: 90 us -> 81.5 us
  local copies, waits for them, and re-layouts: 12.8 us -> 20.8 us
  blocking collectives: 12.9 us -> 20.5 us
  starting transfers between devices: 101 us -> 95.4 us
    unnamed x42 -> x82, local copies, waits for them, and re-layouts: 12.8 us -> 20.8 us
    all_to_all x1, blocking collectives: 12.9 us -> 20.5 us  [swap_fs(): out = lax.all_to_all(value, 'fs', 0, 0, tiled=True)]
    all_to_all x2 -> x1, starting transfers between devices: 13.7 us -> 7.28 us  [swap_fs(): out = lax.all_to_all(value, 'fs', 0, 0, tiled=True)]
    ppermute x37, waiting for transfers between devices: 74.3 us -> 68.5 us  [rotate(): out[r] = lax.ppermute(parts[r], axis, [(k, (k + r) % n) for k in range(n)])]
    ppermute x2, waiting for transfers between devices: 14.8 us -> 12.1 us  [shards(): lax.ppermute(term, 'tp', [(j, (j - step) % tp) for j in range(tp)])]
  transfers between devices with their start and end apart: 46 -> 45, of which waited for: 16 -> 15; matrix products, arithmetic and copies ran while one was open for 0% -> 0% of each run, Pallas kernels for 9% -> 9%
where the time goes in v8:
time: 247 us; the launch traced here: 246 us
  starting transfers between devices  95.4 us (39%)
  waiting for transfers between devices  81.5 us (33%)
  Pallas kernels  27 us (11%)
  local copies, waits for them, and re-layouts  20.8 us (8%)
  blocking collectives  20.5 us (8%)
    ppermute x37, starting transfers between devices, rotate(): out[r] = lax.ppermute(parts[r], axis, [(k, (k + r) % n) for k in range(n)])  81.3 us
    ppermute x37, waiting for transfers between devices, rotate(): out[r] = lax.ppermute(parts[r], axis, [(k, (k + r) % n) for k in range(n)])  68.5 us
    unnamed x82, local copies, waits for them, and re-layouts  20.8 us
    all_to_all x1, blocking collectives, swap_fs(): out = lax.all_to_all(value, 'fs', 0, 0, tiled=True)  20.5 us
    ppermute x2, waiting for transfers between devices, shards(): lax.ppermute(term, 'tp', [(j, (j - step) % tp) for j in range(tp)])  12.1 us
    pallas_call x4, Pallas kernels, cast_along(): pl.pallas_call(functools.partial(cast_kernel, steps, scale is not None, a...  10.3 us
    all_to_all x1, starting transfers between devices, swap_fs(): out = lax.all_to_all(value, 'fs', 0, 0, tiled=True)  7.28 us
  transfers between devices with their start and end apart: 45, of which 15 were waited for; matrix products, arithmetic and copies ran while one was open for 0% of the time, Pallas kernels for 9%

profile of v8, /device:TPU:0, one launch (start us, length us, event | category | flops | bytes accessed | tf_op | source)
XLA Modules:
  0.0 246.1 jit_solution(898839250468967563)
XLA Ops:
  0.6 2.4 shard_map.102
  3.0 7.3 %all-to-all-start = ((bf16[8,16,2176]{2,1,0:T(8,128)(2,1)}), bf16[8,16,2176]{2,1,0:T(8,128)(2,1)S(1)}, u32[]{:S(2)}, u32[]{:S(2)}) async-start(bf16[8,16,2176]{2,1,0:T(8,128)(2,1)} %bitcast.30), calls=%async_computation | async-start | bytes 1114112 | tf_op jit(solution)/shard_map/all_to_all | solution.py:402
  10.4 2.2 copy-done.1
  12.6 2.5 %shard_map.103 = (bf16[8,256,128]{2,1,0:T(8,128)(2,1)S(1)}, bf16[8,256,128]{2,1,0:T(8,128)(2,1)}, bf16[8,256,128]{2,1,0:T(8,128)(2,1)S(1)}, bf16[8,256,128]{2,1,0:T(8,128)(2,1)S(1)}) custom-call(s32[2]{0:T(128)S(1)} %pad_add_fusion.me_ref, f32[8,4,256,128]{3,2,1,0:T(8,128)S(1)} %bitcast.22, f32[1,256]{1,0:T(1,128)S(1)} %bitcast.26), custom_call_target="tpu_custom_call" | custom-call | flops 1000000000 | bytes 6291456 | tf_op jit(solution)/shard_map/pallas_call | solution.py:165
  15.1 2.3 shard_map.105
  17.4 2.0 collective-permute-start.13
  20.9 4.0 %shard_map.106 = (bf16[4,256,128]{2,1,0:T(8,128)(2,1)}, bf16[4,256,128]{2,1,0:T(8,128)(2,1)}, bf16[4,256,128]{2,1,0:T(8,128)(2,1)}) custom-call(s32[2]{0:T(128)} %copy-done.3, f32[8,4,256,128]{3,2,1,0:T(8,128)} %bitcast.14, f32[1,256]{1,0:T(1,128)} %bitcast.25), custom_call_target="tpu_custom_call" | custom-call | flops 1000000000 | bytes 2359296 | tf_op jit(solution)/shard_map/pallas_call | solution.py:165
  24.9 2.4 collective-permute-start.15
  28.7 2.2 copy-done.2
  34.6 20.9 %collective-permute-done.15.refs_3_ = bf16[4,256,128]{2,1,0:T(8,128)(2,1)S(1)} collective-permute-done((bf16[4,256,128]{2,1,0:T(8,128)(2,1)}, bf16[4,256,128]{2,1,0:T(8,128)(2,1)S(1)}, u32[]{:S(2)}, u32[]{:S(2)}) %collective-permute-start.15) | collective-permute-done | bytes 262176 | tf_op jit(solution)/shard_map/ppermute | solution.py:398
  58.8 3.3 %collective-permute-start.17 = (bf16[4,256,128]{2,1,0:T(8,128)(2,1)}, bf16[4,256,128]{2,1,0:T(8,128)(2,1)}, u32[]{:S(2)}, u32[]{:S(2)}) collective-permute-start(bf16[4,256,128]{2,1,0:T(8,128)(2,1)} %get-tuple-element.79), channel_id=1, source_target_pairs={{0,20},{4,24},{8,28},{12,0},{16,4},{20,8},{24,12},{28,16},{1,21},{... | collective-permute-start | bytes 786440 | tf_op jit(solution)/shard_map/ppermute | solution.py:398
  63.5 3.2 %collective-permute-done.25.refs_3_ = bf16[8,64,512]{2,1,0:T(8,128)(2,1)S(1)} collective-permute-done((bf16[8,64,512]{2,1,0:T(8,128)(2,1)S(1)}, bf16[8,64,512]{2,1,0:T(8,128)(2,1)S(1)}, u32[]{:S(2)}, u32[]{:S(2)}) %collective-permute-start.25) | collective-permute-done | bytes 524320 | tf_op jit(solution)/shard_map/ppermute | solution.py:398
  85.1 3.7 %collective-permute-start.7 = (bf16[256,512]{1,0:T(8,128)(2,1)S(1)}, bf16[256,512]{1,0:T(8,128)(2,1)S(1)}, u32[]{:S(2)}, u32[]{:S(2)}) collective-permute-start(bf16[256,512]{1,0:T(8,128)(2,1)S(1)} %get-tuple-element.68), channel_id=1, source_target_pairs={{0,8},{4,12},{8,16},{12,20},{16,24},{20,28},{24,0},{28,4},{1,9},{5... | collective-permute-start | bytes 786440 | tf_op jit(solution)/shard_map/ppermute | solution.py:398
  88.8 2.7 %collective-permute-start.8 = (bf16[256,512]{1,0:T(8,128)(2,1)S(1)}, bf16[256,512]{1,0:T(8,128)(2,1)S(1)}, u32[]{:S(2)}, u32[]{:S(2)}) collective-permute-start(bf16[256,512]{1,0:T(8,128)(2,1)S(1)} %get-tuple-element.69), channel_id=1, source_target_pairs={{0,12},{4,16},{8,20},{12,24},{16,28},{20,0},{24,4},{28,8},{1,13},{... | collective-permute-start | bytes 786440 | tf_op jit(solution)/shard_map/ppermute | solution.py:398
  92.1 14.6 %collective-permute-done.27.refs_6_ = bf16[64,1280]{1,0:T(8,128)(2,1)S(1)} collective-permute-done((bf16[64,1280]{1,0:T(8,128)(2,1)S(1)}, bf16[64,1280]{1,0:T(8,128)(2,1)S(1)}, u32[]{:S(2)}, u32[]{:S(2)}) %collective-permute-start.27) | collective-permute-done | bytes 163872 | tf_op jit(solution)/shard_map/ppermute | solution.py:398
  106.7 2.9 %collective-permute-start.9 = (bf16[256,512]{1,0:T(8,128)(2,1)S(1)}, bf16[256,512]{1,0:T(8,128)(2,1)S(1)}, u32[]{:S(2)}, u32[]{:S(2)}) collective-permute-start(bf16[256,512]{1,0:T(8,128)(2,1)S(1)} %get-tuple-element.70), channel_id=1, source_target_pairs={{0,16},{4,20},{8,24},{12,28},{16,0},{20,4},{24,8},{28,12},{1,17},{... | collective-permute-start | bytes 786440 | tf_op jit(solution)/shard_map/ppermute | solution.py:398
  109.7 8.7 %collective-permute-start.10 = (bf16[256,512]{1,0:T(8,128)(2,1)S(1)}, bf16[256,512]{1,0:T(8,128)(2,1)S(1)}, u32[]{:S(2)}, u32[]{:S(2)}) collective-permute-start(bf16[256,512]{1,0:T(8,128)(2,1)S(1)} %get-tuple-element.71), channel_id=1, source_target_pairs={{0,20},{4,24},{8,28},{12,0},{16,4},{20,8},{24,12},{28,16},{1,21},{... | collective-permute-start | bytes 786440 | tf_op jit(solution)/shard_map/ppermute | solution.py:398
  119.8 8.2 %collective-permute-done.9.refs_8_ = bf16[256,512]{1,0:T(8,128)(2,1)S(1)} collective-permute-done((bf16[256,512]{1,0:T(8,128)(2,1)S(1)}, bf16[256,512]{1,0:T(8,128)(2,1)S(1)}, u32[]{:S(2)}, u32[]{:S(2)}) %collective-permute-start.9) | collective-permute-done | bytes 262176 | tf_op jit(solution)/shard_map/ppermute | solution.py:398
  135.8 9.7 %collective-permute-done.20.refs_5_ = bf16[8,256,128]{2,1,0:T(8,128)(2,1)S(1)} collective-permute-done((bf16[8,256,128]{2,1,0:T(8,128)(2,1)S(1)}, bf16[8,256,128]{2,1,0:T(8,128)(2,1)S(1)}, u32[]{:S(2)}, u32[]{:S(2)}) %collective-permute-start.20) | collective-permute-done | bytes 524320 | tf_op jit(solution)/shard_map/ppermute | solution.py:398
  145.5 13.0 %collective-permute-start.28 = (bf16[64,1280]{1,0:T(8,128)(2,1)S(1)}, bf16[64,1280]{1,0:T(8,128)(2,1)S(1)}, u32[]{:S(2)}, u32[]{:S(2)}) collective-permute-start(bf16[64,1280]{1,0:T(8,128)(2,1)S(1)} %copy-done.24), channel_id=1, source_target_pairs={{0,12},{4,16},{8,20},{12,24},{16,28},{20,0},{24,4},{28,8},{1,13},{... | collective-permute-start | bytes 491528 | tf_op jit(solution)/shard_map/ppermute | solution.py:398
  158.5 3.6 %collective-permute-start.29 = (bf16[64,1280]{1,0:T(8,128)(2,1)S(1)}, bf16[64,1280]{1,0:T(8,128)(2,1)S(1)}, u32[]{:S(2)}, u32[]{:S(2)}) collective-permute-start(bf16[64,1280]{1,0:T(8,128)(2,1)S(1)} %copy-done.22), channel_id=1, source_target_pairs={{0,16},{4,20},{8,24},{12,28},{16,0},{20,4},{24,8},{28,12},{1,17},{... | collective-permute-start | bytes 491528 | tf_op jit(solution)/shard_map/ppermute | solution.py:398
  162.2 9.4 %collective-permute-start.31 = (bf16[64,1280]{1,0:T(8,128)(2,1)S(1)}, bf16[64,1280]{1,0:T(8,128)(2,1)S(1)}, u32[]{:S(2)}, u32[]{:S(2)}) collective-permute-start(bf16[64,1280]{1,0:T(8,128)(2,1)S(1)} %copy-done.18), channel_id=1, source_target_pairs={{0,24},{4,28},{8,0},{12,4},{16,8},{20,12},{24,16},{28,20},{1,25},{... | collective-permute-start | bytes 491528 | tf_op jit(solution)/shard_map/ppermute | solution.py:398
  172.2 3.0 %shard_map.108 = (bf16[2048,512]{1,0:T(8,128)(2,1)}, f32[512,512]{1,0:T(8,128)S(1)}) custom-call(s32[2]{0:T(128)S(1)} %copy-done.4, bf16[128,2176]{1,0:T(8,128)(2,1)S(1)} %bitcast.18, bf16[128,2176]{1,0:T(8,128)(2,1)S(1)} %collective-permute-done.refs_1_, bf16[128,2176]{1,0:T(8,128)(2,1)S(1)} %collective-permute-done.1.refs_2_, ...), custom_call_target="tpu_custom_call" | custom-call | flops 1073741824 | bytes 4194304 | tf_op jit(solution)/shard_map/pallas_call | solution.py:269
  175.2 2.3 shard_map.109
  179.5 3.4 %collective-permute-start.33 = (bf16[256,1280]{1,0:T(8,128)(2,1)S(1)}, bf16[256,1280]{1,0:T(8,128)(2,1)S(1)}, u32[]{:S(2)}, u32[]{:S(2)}) collective-permute-start(bf16[256,1280]{1,0:T(8,128)(2,1)S(1)} %get-tuple-element.101), channel_id=1, source_target_pairs={{0,1},{1,0},{2,3},{3,2},{4,5},{5,4},{6,7},{7,6},{8,9},{9,8},{10,11... | collective-permute-start | bytes 1966088 | tf_op jit(solution)/shard_map/ppermute | solution.py:406
  184.4 5.0 %collective-permute-start.36 = (bf16[64,768]{1,0:T(8,128)(2,1)S(1)}, bf16[64,768]{1,0:T(8,128)(2,1)S(1)}, u32[]{:S(2)}, u32[]{:S(2)}) collective-permute-start(bf16[64,768]{1,0:T(8,128)(2,1)S(1)} %copy-done.38), channel_id=1, source_target_pairs={{0,8},{4,12},{8,16},{12,20},{16,24},{20,28},{24,0},{28,4},{1,9},{5... | collective-permute-start | bytes 294920 | tf_op jit(solution)/shard_map/ppermute | solution.py:398
  189.4 3.1 %collective-permute-start.38 = (bf16[64,768]{1,0:T(8,128)(2,1)S(1)}, bf16[64,768]{1,0:T(8,128)(2,1)S(1)}, u32[]{:S(2)}, u32[]{:S(2)}) collective-permute-start(bf16[64,768]{1,0:T(8,128)(2,1)S(1)} %copy-done.34), channel_id=1, source_target_pairs={{0,16},{4,20},{8,24},{12,28},{16,0},{20,4},{24,8},{28,12},{1,17},{... | collective-permute-start | bytes 294920 | tf_op jit(solution)/shard_map/ppermute | solution.py:398
  197.4 4.9 %collective-permute-done.37.refs_7_ = bf16[64,768]{1,0:T(8,128)(2,1)S(1)} collective-permute-done((bf16[64,768]{1,0:T(8,128)(2,1)S(1)}, bf16[64,768]{1,0:T(8,128)(2,1)S(1)}, u32[]{:S(2)}, u32[]{:S(2)}) %collective-permute-start.37) | collective-permute-done | bytes 98336 | tf_op jit(solution)/shard_map/ppermute | solution.py:398
  202.3 3.6 %collective-permute-start.41 = (bf16[64,768]{1,0:T(8,128)(2,1)S(1)}, bf16[64,768]{1,0:T(8,128)(2,1)S(1)}, u32[]{:S(2)}, u32[]{:S(2)}) collective-permute-start(bf16[64,768]{1,0:T(8,128)(2,1)S(1)} %copy-done.28), channel_id=1, source_target_pairs={{0,28},{4,0},{8,4},{12,8},{16,12},{20,16},{24,20},{28,24},{1,29},{... | collective-permute-start | bytes 294920 | tf_op jit(solution)/shard_map/ppermute | solution.py:398
  206.0 2.2 collective-permute-done.41.refs_11_
  212.2 12.1 %collective-permute-done.43.refs_3_ = bf16[128,768]{1,0:T(8,128)(2,1)S(1)} collective-permute-done((bf16[128,768]{1,0:T(8,128)(2,1)S(1)}, bf16[128,768]{1,0:T(8,128)(2,1)S(1)}, u32[]{:S(2)}, u32[]{:S(2)}) %collective-permute-start.43) | collective-permute-done | bytes 196640 | tf_op jit(solution)/shard_map/ppermute | solution.py:458
  224.4 20.5 %all_to_all.10 = bf16[8,16,2048]{2,1,0:T(8,128)(2,1)S(1)} all-to-all(bf16[8,16,2048]{2,1,0:T(8,128)(2,1)S(1)} %shard_map.116), channel_id=1, replica_groups=mesh['fs'=8,'tp'=4] {'fs'}, dimensions={0} | all-to-all | bytes 1048576 | tf_op jit(solution)/shard_map/all_to_all | solution.py:402
  (158 shorter events, 54.0 us)
Async XLA Ops:
  3.0 77.5 %all-to-all-start = ((bf16[8,16,2176]{2,1,0:T(8,128)(2,1)}), bf16[8,16,2176]{2,1,0:T(8,128)(2,1)S(1)}, u32[]{:S(2)}, u32[]{:S(2)}) async-start(bf16[8,16,2176]{2,1,0:T(8,128)(2,1)} %bitcast.30), calls=%async_computation | async-start | bytes 1114112 | tf_op jit(solution)/shard_map/all_to_all | solution.py:402
  15.1 43.3 %collective-permute-start.3 = (bf16[8,256,128]{2,1,0:T(8,128)(2,1)}, bf16[8,256,128]{2,1,0:T(8,128)(2,1)S(1)}, u32[]{:S(2)}, u32[]{:S(2)}) collective-permute-start(bf16[8,256,128]{2,1,0:T(8,128)(2,1)} %get-tuple-element.63), channel_id=1, source_target_pairs={{0,1},{1,2},{2,3},{3,0},{4,5},{5,6},{6,7},{7,4},{8,9},{9,10},{10,1... | collective-permute-start | bytes 1572872 | tf_op jit(solution)/shard_map/ppermute | solution.py:398
  17.4 14.9 %collective-permute-start.13 = (bf16[4,256,128]{2,1,0:T(8,128)(2,1)}, bf16[4,256,128]{2,1,0:T(8,128)(2,1)S(1)}, u32[]{:S(2)}, u32[]{:S(2)}) collective-permute-start(bf16[4,256,128]{2,1,0:T(8,128)(2,1)} %get-tuple-element.75), channel_id=1, source_target_pairs={{0,4},{4,8},{8,12},{12,16},{16,20},{20,24},{24,28},{28,0},{1,5},{5... | collective-permute-start | bytes 786440 | tf_op jit(solution)/shard_map/ppermute | solution.py:398
  24.9 30.6 %collective-permute-start.15 = (bf16[4,256,128]{2,1,0:T(8,128)(2,1)}, bf16[4,256,128]{2,1,0:T(8,128)(2,1)S(1)}, u32[]{:S(2)}, u32[]{:S(2)}) collective-permute-start(bf16[4,256,128]{2,1,0:T(8,128)(2,1)} %get-tuple-element.77), channel_id=1, source_target_pairs={{0,12},{4,16},{8,20},{12,24},{16,28},{20,0},{24,4},{28,8},{1,13},{... | collective-permute-start | bytes 786440 | tf_op jit(solution)/shard_map/ppermute | solution.py:398
  27.2 28.9 %collective-permute-start.16 = (bf16[4,256,128]{2,1,0:T(8,128)(2,1)}, bf16[4,256,128]{2,1,0:T(8,128)(2,1)S(1)}, u32[]{:S(2)}, u32[]{:S(2)}) collective-permute-start(bf16[4,256,128]{2,1,0:T(8,128)(2,1)} %get-tuple-element.78), channel_id=1, source_target_pairs={{0,16},{4,20},{8,24},{12,28},{16,0},{20,4},{24,8},{28,12},{1,17},{... | collective-permute-start | bytes 786440 | tf_op jit(solution)/shard_map/ppermute | solution.py:398
  33.1 25.7 %collective-permute-start.23 = (bf16[8,64,512]{2,1,0:T(8,128)(2,1)S(1)}, bf16[8,64,512]{2,1,0:T(8,128)(2,1)S(1)}, u32[]{:S(2)}, u32[]{:S(2)}) collective-permute-start(bf16[8,64,512]{2,1,0:T(8,128)(2,1)S(1)} %get-tuple-element.89), channel_id=1, source_target_pairs={{0,1},{1,2},{2,3},{3,0},{4,5},{5,6},{6,7},{7,4},{8,9},{9,10},{10,1... | collective-permute-start | bytes 1572872 | tf_op jit(solution)/shard_map/ppermute | solution.py:398
  33.6 28.4 %collective-permute-start.24 = (bf16[8,64,512]{2,1,0:T(8,128)(2,1)S(1)}, bf16[8,64,512]{2,1,0:T(8,128)(2,1)S(1)}, u32[]{:S(2)}, u32[]{:S(2)}) collective-permute-start(bf16[8,64,512]{2,1,0:T(8,128)(2,1)S(1)} %get-tuple-element.90), channel_id=1, source_target_pairs={{0,2},{1,3},{2,0},{3,1},{4,6},{5,7},{6,4},{7,5},{8,10},{9,11},{10,... | collective-permute-start | bytes 1572872 | tf_op jit(solution)/shard_map/ppermute | solution.py:398
  56.9 19.2 %collective-permute-start.4 = (bf16[8,256,128]{2,1,0:T(8,128)(2,1)S(1)}, bf16[8,256,128]{2,1,0:T(8,128)(2,1)S(1)}, u32[]{:S(2)}, u32[]{:S(2)}) collective-permute-start(bf16[8,256,128]{2,1,0:T(8,128)(2,1)S(1)} %get-tuple-element.64), channel_id=1, source_target_pairs={{0,2},{1,3},{2,0},{3,1},{4,6},{5,7},{6,4},{7,5},{8,10},{9,11},{10,... | collective-permute-start | bytes 1572872 | tf_op jit(solution)/shard_map/ppermute | solution.py:398
  58.4 21.3 %collective-permute-start.5 = (bf16[8,256,128]{2,1,0:T(8,128)(2,1)S(1)}, bf16[8,256,128]{2,1,0:T(8,128)(2,1)S(1)}, u32[]{:S(2)}, u32[]{:S(2)}) collective-permute-start(bf16[8,256,128]{2,1,0:T(8,128)(2,1)S(1)} %get-tuple-element.65), channel_id=1, source_target_pairs={{0,3},{1,0},{2,1},{3,2},{4,7},{5,4},{6,5},{7,6},{8,11},{9,8},{10,9... | collective-permute-start | bytes 1572872 | tf_op jit(solution)/shard_map/ppermute | solution.py:398
  58.8 26.3 %collective-permute-start.17 = (bf16[4,256,128]{2,1,0:T(8,128)(2,1)}, bf16[4,256,128]{2,1,0:T(8,128)(2,1)}, u32[]{:S(2)}, u32[]{:S(2)}) collective-permute-start(bf16[4,256,128]{2,1,0:T(8,128)(2,1)} %get-tuple-element.79), channel_id=1, source_target_pairs={{0,20},{4,24},{8,28},{12,0},{16,4},{20,8},{24,12},{28,16},{1,21},{... | collective-permute-start | bytes 786440 | tf_op jit(solution)/shard_map/ppermute | solution.py:398
  62.0 23.1 %collective-permute-start.18 = (bf16[4,256,128]{2,1,0:T(8,128)(2,1)}, bf16[4,256,128]{2,1,0:T(8,128)(2,1)}, u32[]{:S(2)}, u32[]{:S(2)}) collective-permute-start(bf16[4,256,128]{2,1,0:T(8,128)(2,1)} %get-tuple-element.80), channel_id=1, source_target_pairs={{0,24},{4,28},{8,0},{12,4},{16,8},{20,12},{24,16},{28,20},{1,25},{... | collective-permute-start | bytes 786440 | tf_op jit(solution)/shard_map/ppermute | solution.py:398
  66.7 22.1 %collective-permute-start.19 = (bf16[4,256,128]{2,1,0:T(8,128)(2,1)}, bf16[4,256,128]{2,1,0:T(8,128)(2,1)}, u32[]{:S(2)}, u32[]{:S(2)}) collective-permute-start(bf16[4,256,128]{2,1,0:T(8,128)(2,1)} %get-tuple-element.81), channel_id=1, source_target_pairs={{0,28},{4,0},{8,4},{12,8},{16,12},{20,16},{24,20},{28,24},{1,29},{... | collective-permute-start | bytes 786440 | tf_op jit(solution)/shard_map/ppermute | solution.py:398
  76.9 14.6 %collective-permute-start.26 = (bf16[64,1280]{1,0:T(8,128)(2,1)}, bf16[64,1280]{1,0:T(8,128)(2,1)S(1)}, u32[]{:S(2)}, u32[]{:S(2)}) collective-permute-start(bf16[64,1280]{1,0:T(8,128)(2,1)} %get-tuple-element.93), channel_id=1, source_target_pairs={{0,4},{4,8},{8,12},{12,16},{16,20},{20,24},{24,28},{28,0},{1,5},{5... | collective-permute-start | bytes 491528 | tf_op jit(solution)/shard_map/ppermute | solution.py:398
  80.5 47.5 %collective-permute-start = (bf16[128,2176]{1,0:T(8,128)(2,1)S(1)}, bf16[128,2176]{1,0:T(8,128)(2,1)S(1)}, u32[]{:S(2)}, u32[]{:S(2)}) collective-permute-start(bf16[128,2176]{1,0:T(8,128)(2,1)S(1)} %bitcast.16), channel_id=1, source_target_pairs={{0,2},{1,3},{2,0},{3,1},{4,6},{5,7},{6,4},{7,5},{8,10},{9,11},{10,... | collective-permute-start | bytes 1671176 | tf_op jit(solution)/shard_map/ppermute | solution.py:436
  85.0 24.6 %collective-permute-start.6 = (bf16[256,512]{1,0:T(8,128)(2,1)S(1)}, bf16[256,512]{1,0:T(8,128)(2,1)S(1)}, u32[]{:S(2)}, u32[]{:S(2)}) collective-permute-start(bf16[256,512]{1,0:T(8,128)(2,1)S(1)} %get-tuple-element.67), channel_id=1, source_target_pairs={{0,4},{4,8},{8,12},{12,16},{16,20},{20,24},{24,28},{28,0},{1,5},{5... | collective-permute-start | bytes 786440 | tf_op jit(solution)/shard_map/ppermute | solution.py:398
  85.1 33.2 %collective-permute-start.7 = (bf16[256,512]{1,0:T(8,128)(2,1)S(1)}, bf16[256,512]{1,0:T(8,128)(2,1)S(1)}, u32[]{:S(2)}, u32[]{:S(2)}) collective-permute-start(bf16[256,512]{1,0:T(8,128)(2,1)S(1)} %get-tuple-element.68), channel_id=1, source_target_pairs={{0,8},{4,12},{8,16},{12,20},{16,24},{20,28},{24,0},{28,4},{1,9},{5... | collective-permute-start | bytes 786440 | tf_op jit(solution)/shard_map/ppermute | solution.py:398
  88.8 29.9 %collective-permute-start.8 = (bf16[256,512]{1,0:T(8,128)(2,1)S(1)}, bf16[256,512]{1,0:T(8,128)(2,1)S(1)}, u32[]{:S(2)}, u32[]{:S(2)}) collective-permute-start(bf16[256,512]{1,0:T(8,128)(2,1)S(1)} %get-tuple-element.69), channel_id=1, source_target_pairs={{0,12},{4,16},{8,20},{12,24},{16,28},{20,0},{24,4},{28,8},{1,13},{... | collective-permute-start | bytes 786440 | tf_op jit(solution)/shard_map/ppermute | solution.py:398
  91.5 15.2 %collective-permute-start.27 = (bf16[64,1280]{1,0:T(8,128)(2,1)S(1)}, bf16[64,1280]{1,0:T(8,128)(2,1)S(1)}, u32[]{:S(2)}, u32[]{:S(2)}) collective-permute-start(bf16[64,1280]{1,0:T(8,128)(2,1)S(1)} %copy-done.26), channel_id=1, source_target_pairs={{0,8},{4,12},{8,16},{12,20},{16,24},{20,28},{24,0},{28,4},{1,9},{5... | collective-permute-start | bytes 491528 | tf_op jit(solution)/shard_map/ppermute | solution.py:398
  106.7 21.3 %collective-permute-start.9 = (bf16[256,512]{1,0:T(8,128)(2,1)S(1)}, bf16[256,512]{1,0:T(8,128)(2,1)S(1)}, u32[]{:S(2)}, u32[]{:S(2)}) collective-permute-start(bf16[256,512]{1,0:T(8,128)(2,1)S(1)} %get-tuple-element.70), channel_id=1, source_target_pairs={{0,16},{4,20},{8,24},{12,28},{16,0},{20,4},{24,8},{28,12},{1,17},{... | collective-permute-start | bytes 786440 | tf_op jit(solution)/shard_map/ppermute | solution.py:398
  109.7 23.6 %collective-permute-start.10 = (bf16[256,512]{1,0:T(8,128)(2,1)S(1)}, bf16[256,512]{1,0:T(8,128)(2,1)S(1)}, u32[]{:S(2)}, u32[]{:S(2)}) collective-permute-start(bf16[256,512]{1,0:T(8,128)(2,1)S(1)} %get-tuple-element.71), channel_id=1, source_target_pairs={{0,20},{4,24},{8,28},{12,0},{16,4},{20,8},{24,12},{28,16},{1,21},{... | collective-permute-start | bytes 786440 | tf_op jit(solution)/shard_map/ppermute | solution.py:398
  118.3 16.4 %collective-permute-start.11 = (bf16[256,512]{1,0:T(8,128)(2,1)S(1)}, bf16[256,512]{1,0:T(8,128)(2,1)S(1)}, u32[]{:S(2)}, u32[]{:S(2)}) collective-permute-start(bf16[256,512]{1,0:T(8,128)(2,1)S(1)} %get-tuple-element.72), channel_id=1, source_target_pairs={{0,24},{4,28},{8,0},{12,4},{16,8},{20,12},{24,16},{28,20},{1,25},{... | collective-permute-start | bytes 786440 | tf_op jit(solution)/shard_map/ppermute | solution.py:398
  118.8 17.0 %collective-permute-start.12 = (bf16[256,512]{1,0:T(8,128)(2,1)S(1)}, bf16[256,512]{1,0:T(8,128)(2,1)S(1)}, u32[]{:S(2)}, u32[]{:S(2)}) collective-permute-start(bf16[256,512]{1,0:T(8,128)(2,1)S(1)} %get-tuple-element.73), channel_id=1, source_target_pairs={{0,28},{4,0},{8,4},{12,8},{16,12},{20,16},{24,20},{28,24},{1,29},{... | collective-permute-start | bytes 786440 | tf_op jit(solution)/shard_map/ppermute | solution.py:398
  128.0 34.1 %collective-permute-start.1 = (bf16[128,2176]{1,0:T(8,128)(2,1)S(1)}, bf16[128,2176]{1,0:T(8,128)(2,1)S(1)}, u32[]{:S(2)}, u32[]{:S(2)}) collective-permute-start(bf16[128,2176]{1,0:T(8,128)(2,1)S(1)} %bitcast.17), channel_id=1, source_target_pairs={{0,1},{1,0},{2,3},{3,2},{4,5},{5,4},{6,7},{7,6},{8,9},{9,8},{10,11... | collective-permute-start | bytes 1671176 | tf_op jit(solution)/shard_map/ppermute | solution.py:406
  128.0 43.5 %collective-permute-start.2 = (bf16[128,2176]{1,0:T(8,128)(2,1)S(1)}, bf16[128,2176]{1,0:T(8,128)(2,1)S(1)}, u32[]{:S(2)}, u32[]{:S(2)}) collective-permute-start(bf16[128,2176]{1,0:T(8,128)(2,1)S(1)} %collective-permute-done.refs_1_), channel_id=1, source_target_pairs={{0,1},{1,0},{2,3},{3,2},{4,5},{5,4},{6,7},{7,6},{8,9},{9,8},{10,11... | collective-permute-start | bytes 1671176 | tf_op jit(solution)/shard_map/ppermute | solution.py:406
  134.8 23.7 %collective-permute-start.21 = (bf16[8,256,128]{2,1,0:T(8,128)(2,1)S(1)}, bf16[8,256,128]{2,1,0:T(8,128)(2,1)S(1)}, u32[]{:S(2)}, u32[]{:S(2)}) collective-permute-start(bf16[8,256,128]{2,1,0:T(8,128)(2,1)S(1)} %get-tuple-element.84), channel_id=1, source_target_pairs={{0,2},{1,3},{2,0},{3,1},{4,6},{5,7},{6,4},{7,5},{8,10},{9,11},{10,... | collective-permute-start | bytes 1572872 | tf_op jit(solution)/shard_map/ppermute | solution.py:398
  135.8 26.3 %collective-permute-start.22 = (bf16[8,256,128]{2,1,0:T(8,128)(2,1)S(1)}, bf16[8,256,128]{2,1,0:T(8,128)(2,1)S(1)}, u32[]{:S(2)}, u32[]{:S(2)}) collective-permute-start(bf16[8,256,128]{2,1,0:T(8,128)(2,1)S(1)} %get-tuple-element.85), channel_id=1, source_target_pairs={{0,3},{1,0},{2,1},{3,2},{4,7},{5,4},{6,5},{7,6},{8,11},{9,8},{10,9... | collective-permute-start | bytes 1572872 | tf_op jit(solution)/shard_map/ppermute | solution.py:398
  145.5 32.0 %collective-permute-start.28 = (bf16[64,1280]{1,0:T(8,128)(2,1)S(1)}, bf16[64,1280]{1,0:T(8,128)(2,1)S(1)}, u32[]{:S(2)}, u32[]{:S(2)}) collective-permute-start(bf16[64,1280]{1,0:T(8,128)(2,1)S(1)} %copy-done.24), channel_id=1, source_target_pairs={{0,12},{4,16},{8,20},{12,24},{16,28},{20,0},{24,4},{28,8},{1,13},{... | collective-permute-start | bytes 491528 | tf_op jit(solution)/shard_map/ppermute | solution.py:398
  158.5 19.0 %collective-permute-start.29 = (bf16[64,1280]{1,0:T(8,128)(2,1)S(1)}, bf16[64,1280]{1,0:T(8,128)(2,1)S(1)}, u32[]{:S(2)}, u32[]{:S(2)}) collective-permute-start(bf16[64,1280]{1,0:T(8,128)(2,1)S(1)} %copy-done.22), channel_id=1, source_target_pairs={{0,16},{4,20},{8,24},{12,28},{16,0},{20,4},{24,8},{28,12},{1,17},{... | collective-permute-start | bytes 491528 | tf_op jit(solution)/shard_map/ppermute | solution.py:398
  162.1 15.4 %collective-permute-start.30 = (bf16[64,1280]{1,0:T(8,128)(2,1)S(1)}, bf16[64,1280]{1,0:T(8,128)(2,1)S(1)}, u32[]{:S(2)}, u32[]{:S(2)}) collective-permute-start(bf16[64,1280]{1,0:T(8,128)(2,1)S(1)} %copy-done.20), channel_id=1, source_target_pairs={{0,20},{4,24},{8,28},{12,0},{16,4},{20,8},{24,12},{28,16},{1,21},{... | collective-permute-start | bytes 491528 | tf_op jit(solution)/shard_map/ppermute | solution.py:398
  162.2 15.4 %collective-permute-start.31 = (bf16[64,1280]{1,0:T(8,128)(2,1)S(1)}, bf16[64,1280]{1,0:T(8,128)(2,1)S(1)}, u32[]{:S(2)}, u32[]{:S(2)}) collective-permute-start(bf16[64,1280]{1,0:T(8,128)(2,1)S(1)} %copy-done.18), channel_id=1, source_target_pairs={{0,24},{4,28},{8,0},{12,4},{16,8},{20,12},{24,16},{28,20},{1,25},{... | collective-permute-start | bytes 491528 | tf_op jit(solution)/shard_map/ppermute | solution.py:398
  179.5 30.3 %collective-permute-start.33 = (bf16[256,1280]{1,0:T(8,128)(2,1)S(1)}, bf16[256,1280]{1,0:T(8,128)(2,1)S(1)}, u32[]{:S(2)}, u32[]{:S(2)}) collective-permute-start(bf16[256,1280]{1,0:T(8,128)(2,1)S(1)} %get-tuple-element.101), channel_id=1, source_target_pairs={{0,1},{1,0},{2,3},{3,2},{4,5},{5,4},{6,7},{7,6},{8,9},{9,8},{10,11... | collective-permute-start | bytes 1966088 | tf_op jit(solution)/shard_map/ppermute | solution.py:406
  189.4 16.5 %collective-permute-start.38 = (bf16[64,768]{1,0:T(8,128)(2,1)S(1)}, bf16[64,768]{1,0:T(8,128)(2,1)S(1)}, u32[]{:S(2)}, u32[]{:S(2)}) collective-permute-start(bf16[64,768]{1,0:T(8,128)(2,1)S(1)} %copy-done.34), channel_id=1, source_target_pairs={{0,16},{4,20},{8,24},{12,28},{16,0},{20,4},{24,8},{28,12},{1,17},{... | collective-permute-start | bytes 294920 | tf_op jit(solution)/shard_map/ppermute | solution.py:398
  (54 other events, 598.2 us)
